TPU v7x, 128 devices: a whole 4x4x4 slice. The times are simulated.
128 devices in a mesh: sp: 16 (over z, y), dp: 8 (over x, core).
Axes of the slice: x: 4, y: 4, z: 4, core: 2. Of those that a mesh axis runs over, the one named last changes fastest.
Arguments:
- tokens: bfloat16 [8, 5120, 2048], P('dp', 'sp'), may hold values from -6 to 6
- w_query: bfloat16 [2048, 1024], P('dp', 'sp'), may hold values from -0.125 to 0.125
- w_key: bfloat16 [2048, 1024], P('dp', 'sp'), may hold values from -0.125 to 0.125
- w_value: bfloat16 [2048, 1024], P('dp', 'sp'), may hold values from -0.125 to 0.125
- w_output: bfloat16 [1024, 2048], P('sp', 'dp'), may hold values from -0.1875 to 0.1875
- qk_gain: float32 [2, 64], replicated, may hold values from 0.4 to 7
- decay_sums: float32 [8, 16, 5120], P('dp', 'sp'), may hold values from -1024 to 0, as said below
Outputs:
- layer_out: bfloat16 [8, 5120, 2048], P('dp', 'sp')
Inputs may be any that keep to these rules, and one draw needn't show every extreme that they name: `decay_sums`: each row is non-increasing along positions.
All inputs are finite; a program needn't handle non-finite values.
Results may differ from a plain program's by a relative error of at most 0.0075.
The roundings to bfloat16 on the way count: a program that leaves them out, or rounds other values in their place, can miss the bound.
Values may be sent and summed in bfloat16 or wider, within the bound.
No kernel may reach another device: no remote copies, remote signals or barrier semaphores. Data moves between devices by JAX's collectives and lax.ppermute only.
A program may use at most 128 MiB of HBM per device.

v0:
```python
import functools

import jax
import jax.numpy as jnp
from jax import lax
from jax.experimental import pallas as pl
from jax.experimental.pallas import tpu as pltpu
from jax.sharding import Mesh
from jax.sharding import PartitionSpec as P


DP = ("dp_0", "dp_1")
SP = ("sp_0", "sp_1")
Z, Y, X, C = "sp_0", "sp_1", "dp_0", "dp_1"
LOG2E = 1.4426950408889634
T = 5120
BLK = 320
BQ = 512
W = 1024
NT = (((1,), (1,)), ((), ()))
NN = (((1,), (0,)), ((), ()))
f32 = jnp.float32
bf16 = jnp.bfloat16
SMEM = pl.BlockSpec(memory_space=pltpu.SMEM)
VMEM = pl.BlockSpec(memory_space=pltpu.VMEM)


def attn_kernel(pos_ref, fast_ref, d_ref, *refs, nblk):
    nin=len(nblk)
    ins=refs[:nin]; out_ref=refs[nin]; ka,qa,vs,vt,ot=refs[nin+1:]
    lane=lax.broadcasted_iota(jnp.int32,(BLK,128),1)
    lo=lane<64
    lanev=lax.broadcasted_iota(jnp.int32,(BLK//2,128),1)
    tail=jnp.where(lanev==64,1.0,0.0)
    n=0
    for a,nb in zip(ins,nblk):
        for b in range(nb):
            base=pl.multiple_of(pos_ref[n]*BLK,64); n+=1
            qk=a[b*480:b*480+320,:].astype(f32)
            rolled=pltpu.roll(qk,64,1)
            ka[pl.ds(base,BLK),0:128]=jnp.where(lo,rolled,qk).astype(bf16)
            qs=jnp.where(lo,qk,rolled)*LOG2E
            hi=qs.astype(bf16).astype(f32)
            qa[pl.ds(base,BLK),0:128]=jnp.where(lo,hi,qs-hi).astype(bf16)
            v=a[b*480+320:b*480+480,:].astype(f32)
            vs[pl.ds(base,BLK//2),:]=jnp.where(lanev<64,v,tail)
            vs[pl.ds(base+BLK//2,BLK//2),:]=jnp.where(lanev<64,pltpu.roll(v,64,1),tail)
    dt=d_ref[...].T
    dl=lax.broadcasted_iota(jnp.int32,(256,128),1)
    key_one=jnp.where((dl>=60)&(dl<120),1.0,0.0)
    query_one=jnp.where(dl<60,1.0,0.0)
    for i in range(T//256):
        s=slice(i*256,(i+1)*256)
        km=(dl==i)|(dl==20+i)|(dl==40+i)
        qm=(dl==60+i)|(dl==80+i)|(dl==100+i)
        ka[s,128:256]=jnp.where(km,dt,key_one).astype(bf16)
        qa[s,128:256]=jnp.where(qm,dt,query_one).astype(bf16)
    for i in range(T//256):
        vt[:,i*256:(i+1)*256]=vs[i*256:(i+1)*256,:].T[0:80].astype(bf16)

    def finish(acc):
        o=acc[0:64]/acc[64:65]
        return o*lax.rsqrt(jnp.mean(o*o,axis=0,keepdims=True)+1e-6)

    def fast():
        kio=lax.broadcasted_iota(jnp.int32,(BQ,BQ),0); qio=lax.broadcasted_iota(jnp.int32,(BQ,BQ),1)
        keep=kio<=qio
        for qi in range(T//BQ):
            q0=qi*BQ
            qb=qa[q0:q0+BQ,:]
            def tile(k0,w,mask):
                s=lax.dot_general(ka[k0:k0+w,:],qb,NT,preferred_element_type=f32)
                p=jnp.exp2(s)
                if mask:
                    p=jnp.where(keep,p,0.0)
                return lax.dot_general(vt[:,k0:k0+w],p.astype(bf16),NN,preferred_element_type=f32)
            acc=tile(q0,BQ,True)
            for k0 in range(0,q0,W):
                acc=acc+tile(k0,min(W,q0-k0),False)
            ot[:,q0:q0+BQ]=finish(acc)

    def slow():
        kio=lax.broadcasted_iota(jnp.int32,(BQ,BQ),0); qio=lax.broadcasted_iota(jnp.int32,(BQ,BQ),1)
        def per_q(qi,_):
            q0=pl.multiple_of(qi*BQ,BQ)
            qb=qa[pl.ds(q0,BQ),:]
            def body(j,c):
                m,acc=c
                k0=pl.multiple_of(j*BQ,BQ)
                s=lax.dot_general(ka[pl.ds(k0,BQ),:],qb,NT,preferred_element_type=f32)
                s=jnp.where(kio+k0<=qio+q0,s,-jnp.inf)
                m2=jnp.maximum(m,jnp.max(s,axis=0,keepdims=True))
                p=jnp.exp2(s-m2).astype(bf16)
                acc=acc*jnp.exp2(m-m2)+lax.dot_general(vt[:,pl.ds(k0,BQ)],p,NN,preferred_element_type=f32)
                return m2,acc
            m0=jnp.full((1,BQ),-jnp.inf,f32)
            c=body(qi,(m0,jnp.zeros((80,BQ),f32)))
            _,acc=lax.fori_loop(0,qi,body,c)
            ot[:,pl.ds(q0,BQ)]=finish(acc)
            return 0
        lax.fori_loop(0,T//BQ,per_q,0)
    isfast=fast_ref[0]>0
    pl.when(isfast)(fast)
    pl.when(jnp.logical_not(isfast))(slow)
    for i in range(T//256):
        s=slice(i*256,(i+1)*256)
        vs[s,0:64]=ot[:,s].T
    for j in range(T//BLK):
        a=vs[j*BLK:j*BLK+160,:]; b=vs[j*BLK+160:(j+1)*BLK,:]
        out_ref[j]=jnp.where(lanev<64,a,pltpu.roll(b,64,1)).astype(bf16)


def decay_pieces(d):
    x = d * LOG2E
    h = lax.reduce_precision(x, 8, 7)
    m = lax.reduce_precision(x - h, 8, 7)
    l = lax.reduce_precision(x - h - m, 8, 7)
    return jnp.concatenate([-h, -m, -l, h, m, l, jnp.zeros((8, 256), f32)], 0)


def attention(pos,fast,dp,ins,nblk):
    V=pltpu.VMEM
    return pl.pallas_call(functools.partial(attn_kernel,nblk=nblk),
        out_shape=jax.ShapeDtypeStruct((16,160,128),bf16),
        in_specs=[pl.BlockSpec(memory_space=pltpu.SMEM)]*2+[pl.BlockSpec(memory_space=pltpu.VMEM)]*(1+len(ins)),
        out_specs=pl.BlockSpec(memory_space=pltpu.VMEM),
        scratch_shapes=[V((T,256),bf16),V((T,256),bf16),V((T,128),f32),V((80,T),bf16),V((64,T),f32)],
        compiler_params=pltpu.CompilerParams(vmem_limit_bytes=24*1024*1024),
        name="attention")(pos,fast,dp,*ins)


def pack_kernel(*refs):
    ins, w, wo = refs[:4], refs[4], refs[5]
    for h in range(4):
        w[h * 192 : h * 192 + 192, :] = ins[h][0:192, :]
        wo[h * 64 : h * 64 + 64, :] = ins[h][192:256, :]


def pack(pieces):
    return pl.pallas_call(
        pack_kernel,
        out_shape=[jax.ShapeDtypeStruct((768, 256), bf16), jax.ShapeDtypeStruct((256, 256), bf16)],
        in_specs=[VMEM] * 4,
        out_specs=[VMEM] * 2,
        compiler_params=pltpu.CompilerParams(vmem_limit_bytes=4 * 1024 * 1024),
        name="pack",
    )(*pieces)


def proj_kernel(idx_ref, gain_ref, *refs, pieces):
    ntok = sum(len(p) for p in pieces)
    toks = refs[:ntok]
    ws = refs[ntok : ntok + 8]
    outs = refs[ntok + 8 : ntok + 12]
    lo = lax.broadcasted_iota(jnp.int32, (BLK, 128), 1) < 64
    half = lax.broadcasted_iota(jnp.int32, (BLK // 2, 128), 1) < 64
    pad = jnp.zeros((64, 256), bf16)

    def head(h, _):
        rows = pl.ds(pl.multiple_of(h * 192, 64), 192)
        at = 0
        for b, piece in enumerate(pieces):
            acc = None
            for j in range(8):
                cols = pl.ds(pl.multiple_of(idx_ref[j] * 256, 256), 256)
                parts = [toks[at + n][:, cols] for n in range(len(piece))]
                tok = parts[0] if len(parts) == 1 else jnp.concatenate(parts, 0)
                rhs = jnp.concatenate([ws[j][rows, :], pad], 0)
                part = lax.dot_general(tok, rhs, NT, preferred_element_type=f32)
                acc = part if acc is None else acc + part
            at += len(piece)
            qk = acc[:, :128].astype(bf16).astype(f32)
            sq = qk * qk
            s_lo = jnp.sum(jnp.where(lo, sq, 0.0), axis=1, keepdims=True)
            s_hi = jnp.sum(jnp.where(lo, 0.0, sq), axis=1, keepdims=True)
            inv = lax.rsqrt(jnp.where(lo, s_lo, s_hi) * (1 / 64) + 1e-6)
            unit = (qk * inv * gain_ref[...]).astype(bf16)
            v = acc[:, 128:]
            v = jnp.where(half, v[:160], pltpu.roll(v[160:], 64, 1)).astype(bf16)
            for k in range(4):

                @pl.when(h == k)
                def _(k=k, b=b, unit=unit, v=v):
                    outs[k][b * 480 : b * 480 + 320, :] = unit
                    outs[k][b * 480 + 320 : b * 480 + 480, :] = v

        return 0

    lax.fori_loop(0, 4, head, 0)


def project(cols, gains, pieces, ws):
    sizes = tuple(tuple(p.shape[0] for p in ps) for ps in pieces)
    toks = [p for ps in pieces for p in ps]
    return pl.pallas_call(
        functools.partial(proj_kernel, pieces=sizes),
        out_shape=[jax.ShapeDtypeStruct((len(pieces) * 480, 128), bf16)] * 4,
        in_specs=[SMEM] + [VMEM] * (1 + len(toks) + 8),
        out_specs=[VMEM] * 4,
        compiler_params=pltpu.CompilerParams(vmem_limit_bytes=12 * 1024 * 1024),
        name="project",
    )(cols, gains, *toks, *ws)


def out_kernel(head_ref, col_ref, heads_ref, *refs):
    ws, o_ref, lhs = refs[:8], refs[8], refs[9]
    half = lax.broadcasted_iota(jnp.int32, (BLK // 2, 128), 1) < 64
    for p in range(8):
        a = heads_ref[head_ref[2 * p]].astype(f32)
        b = heads_ref[head_ref[2 * p + 1]].astype(f32)
        s = slice(p * 128, p * 128 + 128)
        lhs[0:160, s] = jnp.where(half, a, pltpu.roll(b, 64, 1)).astype(bf16)
        lhs[160:320, s] = jnp.where(half, pltpu.roll(a, 64, 1), b).astype(bf16)
    for par in range(2):
        for dx in range(4):
            acc = None
            for dy in range(4):
                rhs = ws[par * 4 + dy][dx * 256 : dx * 256 + 256, :]
                part = lax.dot_general(
                    lhs[:, dy * 256 : dy * 256 + 256], rhs, NN, preferred_element_type=f32
                )
                acc = part if acc is None else acc + part
            cols = pl.ds(pl.multiple_of(col_ref[par * 4 + dx] * 256, 256), 256)
            o_ref[:, cols] = acc.astype(bf16)


def output(order, cols, heads, ws):
    return pl.pallas_call(
        out_kernel,
        out_shape=jax.ShapeDtypeStruct((BLK, 2048), bf16),
        in_specs=[SMEM, SMEM] + [VMEM] * 9,
        out_specs=VMEM,
        scratch_shapes=[pltpu.VMEM((BLK, 1024), bf16)],
        compiler_params=pltpu.CompilerParams(vmem_limit_bytes=12 * 1024 * 1024),
        name="output",
    )(order, cols, heads, *ws)


def turn(step):
    return [(i, (i + step) % 4) for i in range(4)]


def move(value, axis, step):
    pairs = [(0, 1), (1, 0)] if axis == C else turn(step)
    return lax.ppermute(value, axis, pairs)


def around(value, axis):
    return [value] + [move(value, axis, -d) for d in (1, 2, 3)]


def on_device(tokens, w_query, w_key, w_value, w_output, qk_gain, decay_sums):
    own = tokens[0]
    z, y, x, c = (lax.axis_index(a) for a in (Z, Y, X, C))
    t1 = move(own, Y, -1)
    t3 = move(own, Y, 1)
    t2 = [move(t1[:160], Y, -1), move(t3[160:], Y, 1)]
    piece = jnp.concatenate([w_query.T, w_key.T, w_value.T, w_output], 0)
    w4, wo4 = pack(around(piece, Z))
    ws = around(w4, X)
    ws = ws + [move(w, C, 0) for w in ws]

    cols = jnp.stack(
        [2 * ((x + d) % 4) + e for e in (c, 1 - c) for d in range(4)]
    ).astype(jnp.int32)
    gains = jnp.concatenate([qk_gain[0] * 0.125, qk_gain[1]])[None]
    dp = decay_pieces(decay_sums[0, 0].reshape(20, 256))
    bound = jnp.max(jnp.abs(qk_gain[0])) * jnp.max(jnp.abs(qk_gain[1]))
    fast = (bound <= 7.7).astype(jnp.int32)[None]
    gains, dp, fast = lax.optimization_barrier((gains, dp, fast))
    part1 = project(cols, gains, [[own], [t1], [t3]], ws)
    *part1, wo4 = lax.optimization_barrier((*part1, wo4))
    part2 = project(cols, gains, [t2], ws)
    recv = []
    for part in (part1, part2):
        recv += [part[0]] + [move(part[d], Z, d) for d in (1, 2, 3)]
    wo16 = jnp.concatenate(around(wo4, X), 0)
    wo = around(wo16, Y)
    pos = [4 * ((z - d) % 4) + (y + e) % 4 for d in range(4) for e in (0, 1, 3)]
    pos += [4 * ((z - d) % 4) + (y + 2) % 4 for d in range(4)]
    pos = jnp.stack(pos).astype(jnp.int32)
    heads = attention(pos, fast, dp, recv, (3, 3, 3, 3, 1, 1, 1, 1))
    heads, *wo = lax.optimization_barrier((heads, *wo))
    wo = wo + [move(w, C, 0) for w in wo]
    merged = lax.all_to_all(heads, SP, 0, 0, tiled=True)
    order = jnp.stack(
        [4 * ((z + d) % 4) + (y + e) % 4 for e in range(4) for d in range(4)]
    ).astype(jnp.int32)
    return output(order, cols, merged, wo)[None]


def solution(mesh):
    torus = Mesh(mesh.devices.reshape(4, 4, 4, 2), ("sp_0", "sp_1", "dp_0", "dp_1"))
    in_specs = (P(DP, SP, None), P(DP, SP), P(DP, SP), P(DP, SP), P(SP, DP), P(), P(DP, SP, None))
    out_specs = P(DP, SP, None)
    return jax.shard_map(
        on_device, mesh=torus, in_specs=in_specs, out_specs=out_specs, check_vma=False
    )
```

profile of v0, /device:TPU:0, one launch (start us, length us, event | category | flops | bytes accessed | tf_op | source)
XLA Modules:
  0.0 173.7 jit_solution(16437231595526586669)
XLA Ops:
  0.0 3.1 %collective-permute-start = (bf16[320,2048]{1,0:T(8,128)(2,1)}, bf16[320,2048]{1,0:T(8,128)(2,1)S(1)}, u32[]{:S(2)}, u32[]{:S(2)}) collective-permute-start(bf16[320,2048]{1,0:T(8,128)(2,1)} %bitcast.50), channel_id=1, source_target_pairs={{0,24},{8,0},{16,8},{24,16},{1,25},{9,1},{17,9},{25,17},{2,26},{10... | collective-permute-start | bytes 3932168 | tf_op jit(solution)/shard_map/ppermute | solution.py:245
  4.0 4.1 %collective-permute-start.2 = (bf16[256,256]{1,0:T(8,128)(2,1)S(1)}, bf16[256,256]{1,0:T(8,128)(2,1)S(1)}, u32[]{:S(2)}, u32[]{:S(2)}) collective-permute-start(bf16[256,256]{1,0:T(8,128)(2,1)S(1)} %pad_maximum_fusion.refs_0_), channel_id=1, source_target_pairs={{0,96},{32,0},{64,32},{96,64},{1,97},{33,1},{65,33},{97,65},{2,98}... | collective-permute-start | bytes 393224 | tf_op jit(solution)/shard_map/ppermute | solution.py:245
  8.1 1.3 collective-permute-start.4
  9.3 4.0 %collective-permute-done.2.refs_1_ = bf16[256,256]{1,0:T(8,128)(2,1)S(1)} collective-permute-done((bf16[256,256]{1,0:T(8,128)(2,1)S(1)}, bf16[256,256]{1,0:T(8,128)(2,1)S(1)}, u32[]{:S(2)}, u32[]{:S(2)}) %collective-permute-start.2) | collective-permute-done | bytes 131104 | tf_op jit(solution)/shard_map/ppermute | solution.py:245
  13.3 2.3 %collective-permute-done.3.refs_2_ = bf16[256,256]{1,0:T(8,128)(2,1)S(1)} collective-permute-done((bf16[256,256]{1,0:T(8,128)(2,1)S(1)}, bf16[256,256]{1,0:T(8,128)(2,1)S(1)}, u32[]{:S(2)}, u32[]{:S(2)}) %collective-permute-start.3) | collective-permute-done | bytes 131104 | tf_op jit(solution)/shard_map/ppermute | solution.py:245
  15.7 1.1 collective-permute-done.4.refs_3_
  17.4 2.8 %collective-permute-start.5 = (bf16[768,256]{1,0:T(8,128)(2,1)S(1)}, bf16[768,256]{1,0:T(8,128)(2,1)S(1)}, u32[]{:S(2)}, u32[]{:S(2)}) collective-permute-start(bf16[768,256]{1,0:T(8,128)(2,1)S(1)} %get-tuple-element.31.refs_3_.refs_2_), channel_id=1, source_target_pairs={{0,6},{2,0},{4,2},{6,4},{1,7},{3,1},{5,3},{7,5},{8,14},{10,8},{12,... | collective-permute-start | bytes 1179656 | tf_op jit(solution)/shard_map/ppermute | solution.py:245
  21.9 15.0 %collective-permute-done.5.refs_4_.refs_3_ = bf16[768,256]{1,0:T(8,128)(2,1)S(1)} collective-permute-done((bf16[768,256]{1,0:T(8,128)(2,1)S(1)}, bf16[768,256]{1,0:T(8,128)(2,1)S(1)}, u32[]{:S(2)}, u32[]{:S(2)}) %collective-permute-start.5) | collective-permute-done | bytes 393248 | tf_op jit(solution)/shard_map/ppermute | solution.py:245
  38.3 2.4 %collective-permute-done.7.refs_6_.refs_5_ = bf16[768,256]{1,0:T(8,128)(2,1)} collective-permute-done((bf16[768,256]{1,0:T(8,128)(2,1)S(1)}, bf16[768,256]{1,0:T(8,128)(2,1)}, u32[]{:S(2)}, u32[]{:S(2)}) %collective-permute-start.7) | collective-permute-done | bytes 393248 | tf_op jit(solution)/shard_map/ppermute | solution.py:245
  41.9 1.4 abs_reduce_fusion.1
  44.2 2.8 %collective-permute-start.15 = (bf16[160,2048]{1,0:T(8,128)(2,1)}, bf16[160,2048]{1,0:T(8,128)(2,1)}, u32[]{:S(2)}, u32[]{:S(2)}) collective-permute-start(bf16[160,2048]{1,0:T(8,128)(2,1)} %slice.18), channel_id=1, source_target_pairs={{0,24},{8,0},{16,8},{24,16},{1,25},{9,1},{17,9},{25,17},{2,26},{10... | collective-permute-start | bytes 1966088 | tf_op jit(solution)/shard_map/ppermute | solution.py:245
  49.6 4.6 %concatenate.13.d_ref = f32[128,256]{1,0:T(8,128)S(1)} concatenate(f32[20,256]{1,0:T(8,128)} %get-tuple-element.54, f32[20,256]{1,0:T(8,128)} %get-tuple-element.53, f32[20,256]{1,0:T(8,128)} %get-tuple-element.52, f32[20,256]{1,0:T(8,128)} %get-tuple-element.56, f32[20,256]{1,0:T(8,128)} %get-tuple-element.55, f32[20,256]{1,0:T(8,128)} %get-tuple-element.51, ...), dimensions={0} | concatenate | bytes 262144 | tf_op jit(solution)/shard_map/concatenate | solution.py:118
  54.4 1.3 copy-done
  55.7 13.3 %project.2 = (bf16[1440,128]{1,0:T(8,128)(2,1)S(1)}, bf16[1440,128]{1,0:T(8,128)(2,1)S(1)}, bf16[1440,128]{1,0:T(8,128)(2,1)S(1)}, bf16[1440,128]{1,0:T(8,128)(2,1)S(1)}) custom-call(s32[8]{0:T(128)S(1)} %stack.146.idx_ref.col_ref, f32[1,128]{1,0:T(1,128)S(1)} %maximum_bitcast_fusion.gain_ref, bf16[320,2048]{1,0:T(8,128)(2,1)S(1)} %bitcast.52, ...), custom_call_target="tpu_custom_call" | custom-call | tf_op jit(solution)/shard_map/project/pallas_call | solution.py:195
  69.1 1.3 collective-permute-start.20
  70.5 5.0 %collective-permute-done.20 = bf16[256,256]{1,0:T(8,128)(2,1)S(1)} collective-permute-done((bf16[256,256]{1,0:T(8,128)(2,1)S(1)}, bf16[256,256]{1,0:T(8,128)(2,1)S(1)}, u32[]{:S(2)}, u32[]{:S(2)}) %collective-permute-start.20) | collective-permute-done | bytes 131104 | tf_op jit(solution)/shard_map/ppermute | solution.py:245
  75.5 1.4 collective-permute-done.21
  76.9 4.8 %collective-permute-done.22 = bf16[256,256]{1,0:T(8,128)(2,1)S(1)} collective-permute-done((bf16[256,256]{1,0:T(8,128)(2,1)S(1)}, bf16[256,256]{1,0:T(8,128)(2,1)S(1)}, u32[]{:S(2)}, u32[]{:S(2)}) %collective-permute-start.22) | collective-permute-done | bytes 131104 | tf_op jit(solution)/shard_map/ppermute | solution.py:245
  81.7 3.2 %collective-permute-start.23 = (bf16[1024,256]{1,0:T(8,128)(2,1)S(1)}, bf16[1024,256]{1,0:T(8,128)(2,1)S(1)}, u32[]{:S(2)}, u32[]{:S(2)}) collective-permute-start(bf16[1024,256]{1,0:T(8,128)(2,1)S(1)} %constant_dynamic-update-slice_fusion.refs_0_), channel_id=1, source_target_pairs={{0,24},{8,0},{16,8},{24,16},{1,25},{9,1},{17,9},{25,17},{2,26},{10... | collective-permute-start | bytes 1572872 | tf_op jit(solution)/shard_map/ppermute | solution.py:245
  84.9 4.7 %collective-permute-done.12.refs_1_ = bf16[1440,128]{1,0:T(8,128)(2,1)S(1)} collective-permute-done((bf16[1440,128]{1,0:T(8,128)(2,1)S(1)}, bf16[1440,128]{1,0:T(8,128)(2,1)S(1)}, u32[]{:S(2)}, u32[]{:S(2)}) %collective-permute-start.12) | collective-permute-done | bytes 368672 | tf_op jit(solution)/shard_map/ppermute | solution.py:245
  89.5 1.5 collective-permute-start.24
  91.0 2.3 %collective-permute-start.25 = (bf16[1024,256]{1,0:T(8,128)(2,1)S(1)}, bf16[1024,256]{1,0:T(8,128)(2,1)}, u32[]{:S(2)}, u32[]{:S(2)}) collective-permute-start(bf16[1024,256]{1,0:T(8,128)(2,1)S(1)} %constant_dynamic-update-slice_fusion.refs_0_), channel_id=1, source_target_pairs={{0,8},{8,16},{16,24},{24,0},{1,9},{9,17},{17,25},{25,1},{2,10},{10... | collective-permute-start | bytes 1572872 | tf_op jit(solution)/shard_map/ppermute | solution.py:245
  93.4 5.8 %project.3 = (bf16[480,128]{1,0:T(8,128)(2,1)S(1)}, bf16[480,128]{1,0:T(8,128)(2,1)S(1)}, bf16[480,128]{1,0:T(8,128)(2,1)}, bf16[480,128]{1,0:T(8,128)(2,1)}) custom-call(s32[8]{0:T(128)S(1)} %stack.146.idx_ref.col_ref, f32[1,128]{1,0:T(1,128)S(1)} %maximum_bitcast_fusion.gain_ref, bf16[160,2048]{1,0:T(8,128)(2,1)} %collective-permute-done.15.refs_0_, ...), custom_call_target="tpu_custom_call" | custom-call | tf_op jit(solution)/shard_map/project/pallas_call | solution.py:195
  99.1 2.1 %collective-permute-start.17 = (bf16[480,128]{1,0:T(8,128)(2,1)S(1)}, bf16[480,128]{1,0:T(8,128)(2,1)S(1)}, u32[]{:S(2)}, u32[]{:S(2)}) collective-permute-start(bf16[480,128]{1,0:T(8,128)(2,1)S(1)} %get-tuple-element.42), channel_id=1, source_target_pairs={{0,32},{32,64},{64,96},{96,0},{1,33},{33,65},{65,97},{97,1},{2,34}... | collective-permute-start | bytes 368648 | tf_op jit(solution)/shard_map/ppermute | solution.py:245
  103.2 2.1 %collective-permute-done.17.refs_5_ = bf16[480,128]{1,0:T(8,128)(2,1)S(1)} collective-permute-done((bf16[480,128]{1,0:T(8,128)(2,1)S(1)}, bf16[480,128]{1,0:T(8,128)(2,1)S(1)}, u32[]{:S(2)}, u32[]{:S(2)}) %collective-permute-start.17) | collective-permute-done | bytes 122912 | tf_op jit(solution)/shard_map/ppermute | solution.py:245
  105.4 4.1 %collective-permute-done.18.refs_6_ = bf16[480,128]{1,0:T(8,128)(2,1)S(1)} collective-permute-done((bf16[480,128]{1,0:T(8,128)(2,1)}, bf16[480,128]{1,0:T(8,128)(2,1)S(1)}, u32[]{:S(2)}, u32[]{:S(2)}) %collective-permute-start.18) | collective-permute-done | bytes 122912 | tf_op jit(solution)/shard_map/ppermute | solution.py:245
  110.4 1.0 copy-done.2
  111.4 1.0 copy-done.4
  112.4 41.9 %attention.1 = bf16[16,160,128]{2,1,0:T(8,128)(2,1)} custom-call(s32[16]{0:T(128)S(1)} %stack.159.pos_ref, s32[1]{0:T(128)} %bitcast.39.fast_ref, f32[128,256]{1,0:T(8,128)S(1)} %concatenate.13.d_ref, bf16[1440,128]{1,0:T(8,128)(2,1)S(1)} %copy-done.2, bf16[1440,128]{1,0:T(8,128)(2,1)S(1)} %collective-permute-done.12.refs_1_, ...), custom_call_target="tpu_custom_call" | custom-call | tf_op jit(solution)/shard_map/attention/pallas_call | solution.py:123
  154.3 4.5 %all-to-all-start = ((bf16[16,160,128]{2,1,0:T(8,128)(2,1)}), bf16[16,160,128]{2,1,0:T(8,128)(2,1)S(1)}, u32[]{:S(2)}, u32[]{:S(2)}) async-start(bf16[16,160,128]{2,1,0:T(8,128)(2,1)} %attention.1), calls=%async_computation | async-start | bytes 1310720 | tf_op jit(solution)/shard_map/all_to_all | solution.py:285
  163.1 6.5 %all-to-all-done.heads_ref = bf16[16,160,128]{2,1,0:T(8,128)(2,1)S(1)} async-done(((bf16[16,160,128]{2,1,0:T(8,128)(2,1)}), bf16[16,160,128]{2,1,0:T(8,128)(2,1)S(1)}, u32[]{:S(2)}, u32[]{:S(2)}) %all-to-all-start) | async-done | bytes 655392 | tf_op jit(solution)/shard_map/all_to_all | solution.py:285
  169.6 4.1 %output.1 = bf16[320,2048]{1,0:T(8,128)(2,1)} custom-call(s32[16]{0:T(128)S(1)} %stack.137.head_ref, s32[8]{0:T(128)S(1)} %stack.146.idx_ref.col_ref, bf16[16,160,128]{2,1,0:T(8,128)(2,1)S(1)} %all-to-all-done.heads_ref, bf16[1024,256]{1,0:T(8,128)(2,1)S(1)} %constant_dynamic-update-slice_fusion.refs_0_, ...), custom_call_target="tpu_custom_call" | custom-call | tf_op jit(solution)/shard_map/output/pallas_call | solution.py:228
  (69 shorter events, 15.8 us)
Async XLA Ops:
  0.0 40.7 %collective-permute-start = (bf16[320,2048]{1,0:T(8,128)(2,1)}, bf16[320,2048]{1,0:T(8,128)(2,1)S(1)}, u32[]{:S(2)}, u32[]{:S(2)}) collective-permute-start(bf16[320,2048]{1,0:T(8,128)(2,1)} %bitcast.50), channel_id=1, source_target_pairs={{0,24},{8,0},{16,8},{24,16},{1,25},{9,1},{17,9},{25,17},{2,26},{10... | collective-permute-start | bytes 3932168 | tf_op jit(solution)/shard_map/ppermute | solution.py:245
  3.1 41.0 %collective-permute-start.1 = (bf16[320,2048]{1,0:T(8,128)(2,1)}, bf16[320,2048]{1,0:T(8,128)(2,1)S(1)}, u32[]{:S(2)}, u32[]{:S(2)}) collective-permute-start(bf16[320,2048]{1,0:T(8,128)(2,1)} %bitcast.51), channel_id=1, source_target_pairs={{0,8},{8,16},{16,24},{24,0},{1,9},{9,17},{17,25},{25,1},{2,10},{10... | collective-permute-start | bytes 3932168 | tf_op jit(solution)/shard_map/ppermute | solution.py:245
  4.0 9.4 %collective-permute-start.2 = (bf16[256,256]{1,0:T(8,128)(2,1)S(1)}, bf16[256,256]{1,0:T(8,128)(2,1)S(1)}, u32[]{:S(2)}, u32[]{:S(2)}) collective-permute-start(bf16[256,256]{1,0:T(8,128)(2,1)S(1)} %pad_maximum_fusion.refs_0_), channel_id=1, source_target_pairs={{0,96},{32,0},{64,32},{96,64},{1,97},{33,1},{65,33},{97,65},{2,98}... | collective-permute-start | bytes 393224 | tf_op jit(solution)/shard_map/ppermute | solution.py:245
  8.1 7.6 %collective-permute-start.3 = (bf16[256,256]{1,0:T(8,128)(2,1)S(1)}, bf16[256,256]{1,0:T(8,128)(2,1)S(1)}, u32[]{:S(2)}, u32[]{:S(2)}) collective-permute-start(bf16[256,256]{1,0:T(8,128)(2,1)S(1)} %pad_maximum_fusion.refs_0_), channel_id=1, source_target_pairs={{0,64},{32,96},{64,0},{96,32},{1,65},{33,97},{65,1},{97,33},{2,66}... | collective-permute-start | bytes 393224 | tf_op jit(solution)/shard_map/ppermute | solution.py:245
  8.1 8.7 %collective-permute-start.4 = (bf16[256,256]{1,0:T(8,128)(2,1)S(1)}, bf16[256,256]{1,0:T(8,128)(2,1)S(1)}, u32[]{:S(2)}, u32[]{:S(2)}) collective-permute-start(bf16[256,256]{1,0:T(8,128)(2,1)S(1)} %pad_maximum_fusion.refs_0_), channel_id=1, source_target_pairs={{0,32},{32,64},{64,96},{96,0},{1,33},{33,65},{65,97},{97,1},{2,34}... | collective-permute-start | bytes 393224 | tf_op jit(solution)/shard_map/ppermute | solution.py:245
  17.4 19.5 %collective-permute-start.5 = (bf16[768,256]{1,0:T(8,128)(2,1)S(1)}, bf16[768,256]{1,0:T(8,128)(2,1)S(1)}, u32[]{:S(2)}, u32[]{:S(2)}) collective-permute-start(bf16[768,256]{1,0:T(8,128)(2,1)S(1)} %get-tuple-element.31.refs_3_.refs_2_), channel_id=1, source_target_pairs={{0,6},{2,0},{4,2},{6,4},{1,7},{3,1},{5,3},{7,5},{8,14},{10,8},{12,... | collective-permute-start | bytes 1179656 | tf_op jit(solution)/shard_map/ppermute | solution.py:245
  20.2 17.5 %collective-permute-start.6 = (bf16[768,256]{1,0:T(8,128)(2,1)S(1)}, bf16[768,256]{1,0:T(8,128)(2,1)}, u32[]{:S(2)}, u32[]{:S(2)}) collective-permute-start(bf16[768,256]{1,0:T(8,128)(2,1)S(1)} %get-tuple-element.31.refs_3_.refs_2_), channel_id=1, source_target_pairs={{0,4},{2,6},{4,0},{6,2},{1,5},{3,7},{5,1},{7,3},{8,12},{10,14},{12... | collective-permute-start | bytes 1179656 | tf_op jit(solution)/shard_map/ppermute | solution.py:245
  21.0 19.7 %collective-permute-start.7 = (bf16[768,256]{1,0:T(8,128)(2,1)S(1)}, bf16[768,256]{1,0:T(8,128)(2,1)}, u32[]{:S(2)}, u32[]{:S(2)}) collective-permute-start(bf16[768,256]{1,0:T(8,128)(2,1)S(1)} %get-tuple-element.31.refs_3_.refs_2_), channel_id=1, source_target_pairs={{0,2},{2,4},{4,6},{6,0},{1,3},{3,5},{5,7},{7,1},{8,10},{10,12},{12... | collective-permute-start | bytes 1179656 | tf_op jit(solution)/shard_map/ppermute | solution.py:245
  36.9 10.9 %collective-permute-start.8 = (bf16[768,256]{1,0:T(8,128)(2,1)S(1)}, bf16[768,256]{1,0:T(8,128)(2,1)}, u32[]{:S(2)}, u32[]{:S(2)}) collective-permute-start(bf16[768,256]{1,0:T(8,128)(2,1)S(1)} %get-tuple-element.31.refs_3_.refs_2_), channel_id=1, source_target_pairs={{0,1},{1,0},{2,3},{3,2},{4,5},{5,4},{6,7},{7,6},{8,9},{9,8},{10,11... | collective-permute-start | bytes 1179656 | tf_op jit(solution)/shard_map/ppermute | solution.py:245
  37.7 16.7 %collective-permute-start.9 = (bf16[768,256]{1,0:T(8,128)(2,1)S(1)}, bf16[768,256]{1,0:T(8,128)(2,1)}, u32[]{:S(2)}, u32[]{:S(2)}) collective-permute-start(bf16[768,256]{1,0:T(8,128)(2,1)S(1)} %collective-permute-done.5.refs_4_.refs_3_), channel_id=1, source_target_pairs={{0,1},{1,0},{2,3},{3,2},{4,5},{5,4},{6,7},{7,6},{8,9},{9,8},{10,11... | collective-permute-start | bytes 1179656 | tf_op jit(solution)/shard_map/ppermute | solution.py:245
  40.7 13.7 %collective-permute-start.10 = (bf16[768,256]{1,0:T(8,128)(2,1)}, bf16[768,256]{1,0:T(8,128)(2,1)}, u32[]{:S(2)}, u32[]{:S(2)}) collective-permute-start(bf16[768,256]{1,0:T(8,128)(2,1)} %collective-permute-done.6.refs_5_.refs_4_), channel_id=1, source_target_pairs={{0,1},{1,0},{2,3},{3,2},{4,5},{5,4},{6,7},{7,6},{8,9},{9,8},{10,11... | collective-permute-start | bytes 1179656 | tf_op jit(solution)/shard_map/ppermute | solution.py:245
  40.7 13.7 %collective-permute-start.11 = (bf16[768,256]{1,0:T(8,128)(2,1)}, bf16[768,256]{1,0:T(8,128)(2,1)}, u32[]{:S(2)}, u32[]{:S(2)}) collective-permute-start(bf16[768,256]{1,0:T(8,128)(2,1)} %collective-permute-done.7.refs_6_.refs_5_), channel_id=1, source_target_pairs={{0,1},{1,0},{2,3},{3,2},{4,5},{5,4},{6,7},{7,6},{8,9},{9,8},{10,11... | collective-permute-start | bytes 1179656 | tf_op jit(solution)/shard_map/ppermute | solution.py:245
  44.2 46.9 %collective-permute-start.15 = (bf16[160,2048]{1,0:T(8,128)(2,1)}, bf16[160,2048]{1,0:T(8,128)(2,1)}, u32[]{:S(2)}, u32[]{:S(2)}) collective-permute-start(bf16[160,2048]{1,0:T(8,128)(2,1)} %slice.18), channel_id=1, source_target_pairs={{0,24},{8,0},{16,8},{24,16},{1,25},{9,1},{17,9},{25,17},{2,26},{10... | collective-permute-start | bytes 1966088 | tf_op jit(solution)/shard_map/ppermute | solution.py:245
  47.8 45.6 %collective-permute-start.16 = (bf16[160,2048]{1,0:T(8,128)(2,1)}, bf16[160,2048]{1,0:T(8,128)(2,1)}, u32[]{:S(2)}, u32[]{:S(2)}) collective-permute-start(bf16[160,2048]{1,0:T(8,128)(2,1)} %slice.19), channel_id=1, source_target_pairs={{0,8},{8,16},{16,24},{24,0},{1,9},{9,17},{17,25},{25,1},{2,10},{10... | collective-permute-start | bytes 1966088 | tf_op jit(solution)/shard_map/ppermute | solution.py:245
  69.0 30.1 %copy-start.1 = (bf16[1440,128]{1,0:T(8,128)(2,1)}, bf16[1440,128]{1,0:T(8,128)(2,1)S(1)}, u32[]{:S(2)}) copy-start(bf16[1440,128]{1,0:T(8,128)(2,1)S(1)} %get-tuple-element.37.refs_0_) | copy-start | bytes 1105924
  69.1 6.4 %collective-permute-start.20 = (bf16[256,256]{1,0:T(8,128)(2,1)S(1)}, bf16[256,256]{1,0:T(8,128)(2,1)S(1)}, u32[]{:S(2)}, u32[]{:S(2)}) collective-permute-start(bf16[256,256]{1,0:T(8,128)(2,1)S(1)} %copy-done.6), channel_id=1, source_target_pairs={{0,6},{2,0},{4,2},{6,4},{1,7},{3,1},{5,3},{7,5},{8,14},{10,8},{12,... | collective-permute-start | bytes 393224 | tf_op jit(solution)/shard_map/ppermute | solution.py:245
  70.4 6.5 %collective-permute-start.21 = (bf16[256,256]{1,0:T(8,128)(2,1)S(1)}, bf16[256,256]{1,0:T(8,128)(2,1)S(1)}, u32[]{:S(2)}, u32[]{:S(2)}) collective-permute-start(bf16[256,256]{1,0:T(8,128)(2,1)S(1)} %copy-done.6), channel_id=1, source_target_pairs={{0,4},{2,6},{4,0},{6,2},{1,5},{3,7},{5,1},{7,3},{8,12},{10,14},{12... | collective-permute-start | bytes 393224 | tf_op jit(solution)/shard_map/ppermute | solution.py:245
  70.5 19.0 %collective-permute-start.12 = (bf16[1440,128]{1,0:T(8,128)(2,1)S(1)}, bf16[1440,128]{1,0:T(8,128)(2,1)S(1)}, u32[]{:S(2)}, u32[]{:S(2)}) collective-permute-start(bf16[1440,128]{1,0:T(8,128)(2,1)S(1)} %get-tuple-element.38), channel_id=1, source_target_pairs={{0,32},{32,64},{64,96},{96,0},{1,33},{33,65},{65,97},{97,1},{2,34}... | collective-permute-start | bytes 1105928 | tf_op jit(solution)/shard_map/ppermute | solution.py:245
  75.5 6.2 %collective-permute-start.22 = (bf16[256,256]{1,0:T(8,128)(2,1)S(1)}, bf16[256,256]{1,0:T(8,128)(2,1)S(1)}, u32[]{:S(2)}, u32[]{:S(2)}) collective-permute-start(bf16[256,256]{1,0:T(8,128)(2,1)S(1)} %copy-done.6), channel_id=1, source_target_pairs={{0,2},{2,4},{4,6},{6,0},{1,3},{3,5},{5,7},{7,1},{8,10},{10,12},{12... | collective-permute-start | bytes 393224 | tf_op jit(solution)/shard_map/ppermute | solution.py:245
  76.9 22.3 %collective-permute-start.13 = (bf16[1440,128]{1,0:T(8,128)(2,1)S(1)}, bf16[1440,128]{1,0:T(8,128)(2,1)S(1)}, u32[]{:S(2)}, u32[]{:S(2)}) collective-permute-start(bf16[1440,128]{1,0:T(8,128)(2,1)S(1)} %get-tuple-element.39), channel_id=1, source_target_pairs={{0,64},{32,96},{64,0},{96,32},{1,65},{33,97},{65,1},{97,33},{2,66}... | collective-permute-start | bytes 1105928 | tf_op jit(solution)/shard_map/ppermute | solution.py:245
  81.7 72.6 %collective-permute-start.23 = (bf16[1024,256]{1,0:T(8,128)(2,1)S(1)}, bf16[1024,256]{1,0:T(8,128)(2,1)S(1)}, u32[]{:S(2)}, u32[]{:S(2)}) collective-permute-start(bf16[1024,256]{1,0:T(8,128)(2,1)S(1)} %constant_dynamic-update-slice_fusion.refs_0_), channel_id=1, source_target_pairs={{0,24},{8,0},{16,8},{24,16},{1,25},{9,1},{17,9},{25,17},{2,26},{10... | collective-permute-start | bytes 1572872 | tf_op jit(solution)/shard_map/ppermute | solution.py:245
  89.5 64.7 %collective-permute-start.24 = (bf16[1024,256]{1,0:T(8,128)(2,1)S(1)}, bf16[1024,256]{1,0:T(8,128)(2,1)S(1)}, u32[]{:S(2)}, u32[]{:S(2)}) collective-permute-start(bf16[1024,256]{1,0:T(8,128)(2,1)S(1)} %constant_dynamic-update-slice_fusion.refs_0_), channel_id=1, source_target_pairs={{0,16},{8,24},{16,0},{24,8},{1,17},{9,25},{17,1},{25,9},{2,18},{10... | collective-permute-start | bytes 1572872 | tf_op jit(solution)/shard_map/ppermute | solution.py:245
  91.0 63.2 %collective-permute-start.25 = (bf16[1024,256]{1,0:T(8,128)(2,1)S(1)}, bf16[1024,256]{1,0:T(8,128)(2,1)}, u32[]{:S(2)}, u32[]{:S(2)}) collective-permute-start(bf16[1024,256]{1,0:T(8,128)(2,1)S(1)} %constant_dynamic-update-slice_fusion.refs_0_), channel_id=1, source_target_pairs={{0,8},{8,16},{16,24},{24,0},{1,9},{9,17},{17,25},{25,1},{2,10},{10... | collective-permute-start | bytes 1572872 | tf_op jit(solution)/shard_map/ppermute | solution.py:245
  93.4 8.8 %collective-permute-start.14 = (bf16[1440,128]{1,0:T(8,128)(2,1)S(1)}, bf16[1440,128]{1,0:T(8,128)(2,1)S(1)}, u32[]{:S(2)}, u32[]{:S(2)}) collective-permute-start(bf16[1440,128]{1,0:T(8,128)(2,1)S(1)} %get-tuple-element.40), channel_id=1, source_target_pairs={{0,96},{32,0},{64,32},{96,64},{1,97},{33,1},{65,33},{97,65},{2,98}... | collective-permute-start | bytes 1105928 | tf_op jit(solution)/shard_map/ppermute | solution.py:245
  99.1 6.2 %collective-permute-start.17 = (bf16[480,128]{1,0:T(8,128)(2,1)S(1)}, bf16[480,128]{1,0:T(8,128)(2,1)S(1)}, u32[]{:S(2)}, u32[]{:S(2)}) collective-permute-start(bf16[480,128]{1,0:T(8,128)(2,1)S(1)} %get-tuple-element.42), channel_id=1, source_target_pairs={{0,32},{32,64},{64,96},{96,0},{1,33},{33,65},{65,97},{97,1},{2,34}... | collective-permute-start | bytes 368648 | tf_op jit(solution)/shard_map/ppermute | solution.py:245
  102.9 6.6 %collective-permute-start.18 = (bf16[480,128]{1,0:T(8,128)(2,1)}, bf16[480,128]{1,0:T(8,128)(2,1)S(1)}, u32[]{:S(2)}, u32[]{:S(2)}) collective-permute-start(bf16[480,128]{1,0:T(8,128)(2,1)} %get-tuple-element.43), channel_id=1, source_target_pairs={{0,64},{32,96},{64,0},{96,32},{1,65},{33,97},{65,1},{97,33},{2,66}... | collective-permute-start | bytes 368648 | tf_op jit(solution)/shard_map/ppermute | solution.py:245
  105.3 5.1 %collective-permute-start.19 = (bf16[480,128]{1,0:T(8,128)(2,1)}, bf16[480,128]{1,0:T(8,128)(2,1)S(1)}, u32[]{:S(2)}, u32[]{:S(2)}) collective-permute-start(bf16[480,128]{1,0:T(8,128)(2,1)} %get-tuple-element.44), channel_id=1, source_target_pairs={{0,96},{32,0},{64,32},{96,64},{1,97},{33,1},{65,33},{97,65},{2,98}... | collective-permute-start | bytes 368648 | tf_op jit(solution)/shard_map/ppermute | solution.py:245
  154.3 15.3 %all-to-all-start = ((bf16[16,160,128]{2,1,0:T(8,128)(2,1)}), bf16[16,160,128]{2,1,0:T(8,128)(2,1)S(1)}, u32[]{:S(2)}, u32[]{:S(2)}) async-start(bf16[16,160,128]{2,1,0:T(8,128)(2,1)} %attention.1), calls=%async_computation | async-start | bytes 1310720 | tf_op jit(solution)/shard_map/all_to_all | solution.py:285
  158.8 2.0 %collective-permute-start.26 = (bf16[1024,256]{1,0:T(8,128)(2,1)S(1)}, bf16[1024,256]{1,0:T(8,128)(2,1)S(1)}, u32[]{:S(2)}, u32[]{:S(2)}) collective-permute-start(bf16[1024,256]{1,0:T(8,128)(2,1)S(1)} %constant_dynamic-update-slice_fusion.refs_0_), channel_id=1, source_target_pairs={{0,1},{1,0},{2,3},{3,2},{4,5},{5,4},{6,7},{7,6},{8,9},{9,8},{10,11... | collective-permute-start | bytes 1572872 | tf_op jit(solution)/shard_map/ppermute | solution.py:245
  158.9 2.6 %collective-permute-start.27 = (bf16[1024,256]{1,0:T(8,128)(2,1)S(1)}, bf16[1024,256]{1,0:T(8,128)(2,1)S(1)}, u32[]{:S(2)}, u32[]{:S(2)}) collective-permute-start(bf16[1024,256]{1,0:T(8,128)(2,1)S(1)} %collective-permute-done.23.refs_1_), channel_id=1, source_target_pairs={{0,1},{1,0},{2,3},{3,2},{4,5},{5,4},{6,7},{7,6},{8,9},{9,8},{10,11... | collective-permute-start | bytes 1572872 | tf_op jit(solution)/shard_map/ppermute | solution.py:245
  159.4 3.0 %collective-permute-start.28 = (bf16[1024,256]{1,0:T(8,128)(2,1)S(1)}, bf16[1024,256]{1,0:T(8,128)(2,1)}, u32[]{:S(2)}, u32[]{:S(2)}) collective-permute-start(bf16[1024,256]{1,0:T(8,128)(2,1)S(1)} %collective-permute-done.24.refs_2_), channel_id=1, source_target_pairs={{0,1},{1,0},{2,3},{3,2},{4,5},{5,4},{6,7},{7,6},{8,9},{9,8},{10,11... | collective-permute-start | bytes 1572872 | tf_op jit(solution)/shard_map/ppermute | solution.py:245
  159.4 3.7 %collective-permute-start.29 = (bf16[1024,256]{1,0:T(8,128)(2,1)}, bf16[1024,256]{1,0:T(8,128)(2,1)}, u32[]{:S(2)}, u32[]{:S(2)}) collective-permute-start(bf16[1024,256]{1,0:T(8,128)(2,1)} %collective-permute-done.25.refs_3_), channel_id=1, source_target_pairs={{0,1},{1,0},{2,3},{3,2},{4,5},{5,4},{6,7},{7,6},{8,9},{9,8},{10,11... | collective-permute-start | bytes 1572872 | tf_op jit(solution)/shard_map/ppermute | solution.py:245
  (7 other events, 22.5 us)
where the time goes:
time: 175 us; the launch traced here: 174 us
  Pallas kernels  65.1 us (37%)
  waiting for transfers between devices  58.3 us (33%)
  starting transfers between devices  33.3 us (19%)
  local copies, waits for them, and re-layouts  11.4 us (7%)
  other arithmetic  4.32 us (2%)
    ppermute x30, waiting for transfers between devices, move(): return lax.ppermute(value, axis, pairs)  51.8 us
    pallas_call x1, Pallas kernels, attention(): pl.pallas_call(functools.partial(attn_kernel, nblk=nblk), out_shape=jax.S...  41.9 us
    ppermute x30, starting transfers between devices, move(): return lax.ppermute(value, axis, pairs)  28.8 us
    pallas_call x2, Pallas kernels, project(): pl.pallas_call(functools.partial(proj_kernel, pieces=sizes), out_shape=[j...  19.1 us
    all_to_all x1, waiting for transfers between devices, on_device(): merged = lax.all_to_all(heads, SP, 0, 0, tiled=True)  6.47 us
    unnamed x19, local copies, waits for them, and re-layouts  4.7 us
    concatenate x1, local copies, waits for them, and re-layouts, decay_pieces(): return jnp.concatenate([-h, -m, -l, h, m, l, jnp.zeros((8, 256), f32)], 0)  4.64 us
    all_to_all x1, starting transfers between devices, on_device(): merged = lax.all_to_all(heads, SP, 0, 0, tiled=True)  4.49 us
  transfers between devices with their start and end apart: 31, of which 18 were waited for; matrix products, arithmetic and copies ran while one was open for 6% of the time, Pallas kernels for 35%

commit v1 on v0

--- a/solution.py
+++ b/solution.py
@@ -25,7 +25,7 @@
 VMEM = pl.BlockSpec(memory_space=pltpu.VMEM)
 
 
-def attn_kernel(pos_ref, fast_ref, d_ref, *refs, nblk):
+def attn_kernel(pos_ref, gain_ref, d_ref, *refs, nblk):
     nin=len(nblk)
     ins=refs[:nin]; out_ref=refs[nin]; ka,qa,vs,vt,ot=refs[nin+1:]
     lane=lax.broadcasted_iota(jnp.int32,(BLK,128),1)
@@ -45,16 +45,18 @@
             v=a[b*480+320:b*480+480,:].astype(f32)
             vs[pl.ds(base,BLK//2),:]=jnp.where(lanev<64,v,tail)
             vs[pl.ds(base+BLK//2,BLK//2),:]=jnp.where(lanev<64,pltpu.roll(v,64,1),tail)
-    dt=d_ref[...].T
-    dl=lax.broadcasted_iota(jnp.int32,(256,128),1)
-    key_one=jnp.where((dl>=60)&(dl<120),1.0,0.0)
-    query_one=jnp.where(dl<60,1.0,0.0)
-    for i in range(T//256):
-        s=slice(i*256,(i+1)*256)
-        km=(dl==i)|(dl==20+i)|(dl==40+i)
-        qm=(dl==60+i)|(dl==80+i)|(dl==100+i)
-        ka[s,128:256]=jnp.where(km,dt,key_one).astype(bf16)
-        qa[s,128:256]=jnp.where(qm,dt,query_one).astype(bf16)
+    x=d_ref[...]*LOG2E
+    h=x.astype(bf16).astype(f32)
+    m=(x-h).astype(bf16).astype(f32)
+    l=x-h-m
+    dt=jnp.concatenate([-h,-m,-l,h,m,l,jnp.zeros((80,640),f32)],0).T
+    dl=lax.broadcasted_iota(jnp.int32,(640,128),1)
+    key_one=jnp.where((dl>=24)&(dl<48),1.0,0.0)
+    query_one=jnp.where(dl<24,1.0,0.0)
+    for i in range(T//640):
+        s=slice(i*640,(i+1)*640)
+        ka[s,128:256]=jnp.where((dl==i)|(dl==8+i)|(dl==16+i),dt,key_one).astype(bf16)
+        qa[s,128:256]=jnp.where((dl==24+i)|(dl==32+i)|(dl==40+i),dt,query_one).astype(bf16)
     for i in range(T//256):
         vt[:,i*256:(i+1)*256]=vs[i*256:(i+1)*256,:].T[0:80].astype(bf16)
 
@@ -99,7 +101,8 @@
             ot[:,pl.ds(q0,BQ)]=finish(acc)
             return 0
         lax.fori_loop(0,T//BQ,per_q,0)
-    isfast=fast_ref[0]>0
+    g=jnp.abs(gain_ref[...])
+    isfast=jnp.max(g[0:1])*jnp.max(g[1:2])<=7.7
     pl.when(isfast)(fast)
     pl.when(jnp.logical_not(isfast))(slow)
     for i in range(T//256):
@@ -110,23 +113,15 @@
         out_ref[j]=jnp.where(lanev<64,a,pltpu.roll(b,64,1)).astype(bf16)
 
 
-def decay_pieces(d):
-    x = d * LOG2E
-    h = lax.reduce_precision(x, 8, 7)
-    m = lax.reduce_precision(x - h, 8, 7)
-    l = lax.reduce_precision(x - h - m, 8, 7)
-    return jnp.concatenate([-h, -m, -l, h, m, l, jnp.zeros((8, 256), f32)], 0)
-
-
-def attention(pos,fast,dp,ins,nblk):
+def attention(pos,gain,d,ins,nblk):
     V=pltpu.VMEM
     return pl.pallas_call(functools.partial(attn_kernel,nblk=nblk),
         out_shape=jax.ShapeDtypeStruct((16,160,128),bf16),
-        in_specs=[pl.BlockSpec(memory_space=pltpu.SMEM)]*2+[pl.BlockSpec(memory_space=pltpu.VMEM)]*(1+len(ins)),
-        out_specs=pl.BlockSpec(memory_space=pltpu.VMEM),
+        in_specs=[SMEM]+[VMEM]*(2+len(ins)),
+        out_specs=VMEM,
         scratch_shapes=[V((T,256),bf16),V((T,256),bf16),V((T,128),f32),V((80,T),bf16),V((64,T),f32)],
         compiler_params=pltpu.CompilerParams(vmem_limit_bytes=24*1024*1024),
-        name="attention")(pos,fast,dp,*ins)
+        name="attention")(pos,gain,d,*ins)
 
 
 def pack_kernel(*refs):
@@ -147,59 +142,69 @@
     )(*pieces)
 
 
-def proj_kernel(idx_ref, gain_ref, *refs, pieces):
-    ntok = sum(len(p) for p in pieces)
-    toks = refs[:ntok]
-    ws = refs[ntok : ntok + 8]
-    outs = refs[ntok + 8 : ntok + 12]
+def join_kernel(*refs):
+    for i in range(4):
+        refs[4][i * 256 : i * 256 + 256, :] = refs[i][...]
+
+
+def join(pieces):
+    return pl.pallas_call(
+        join_kernel,
+        out_shape=jax.ShapeDtypeStruct((1024, 256), bf16),
+        in_specs=[VMEM] * 4,
+        out_specs=VMEM,
+        compiler_params=pltpu.CompilerParams(vmem_limit_bytes=4 * 1024 * 1024),
+        name="join",
+    )(*pieces)
+
+
+def proj_block(tok, w, gains, out, at):
     lo = lax.broadcasted_iota(jnp.int32, (BLK, 128), 1) < 64
     half = lax.broadcasted_iota(jnp.int32, (BLK // 2, 128), 1) < 64
-    pad = jnp.zeros((64, 256), bf16)
-
-    def head(h, _):
-        rows = pl.ds(pl.multiple_of(h * 192, 64), 192)
-        at = 0
-        for b, piece in enumerate(pieces):
-            acc = None
-            for j in range(8):
-                cols = pl.ds(pl.multiple_of(idx_ref[j] * 256, 256), 256)
-                parts = [toks[at + n][:, cols] for n in range(len(piece))]
-                tok = parts[0] if len(parts) == 1 else jnp.concatenate(parts, 0)
-                rhs = jnp.concatenate([ws[j][rows, :], pad], 0)
-                part = lax.dot_general(tok, rhs, NT, preferred_element_type=f32)
-                acc = part if acc is None else acc + part
-            at += len(piece)
-            qk = acc[:, :128].astype(bf16).astype(f32)
-            sq = qk * qk
-            s_lo = jnp.sum(jnp.where(lo, sq, 0.0), axis=1, keepdims=True)
-            s_hi = jnp.sum(jnp.where(lo, 0.0, sq), axis=1, keepdims=True)
-            inv = lax.rsqrt(jnp.where(lo, s_lo, s_hi) * (1 / 64) + 1e-6)
-            unit = (qk * inv * gain_ref[...]).astype(bf16)
-            v = acc[:, 128:]
-            v = jnp.where(half, v[:160], pltpu.roll(v[160:], 64, 1)).astype(bf16)
-            for k in range(4):
-
-                @pl.when(h == k)
-                def _(k=k, b=b, unit=unit, v=v):
-                    outs[k][b * 480 : b * 480 + 320, :] = unit
-                    outs[k][b * 480 + 320 : b * 480 + 480, :] = v
-
-        return 0
-
-    lax.fori_loop(0, 4, head, 0)
-
-
-def project(cols, gains, pieces, ws):
-    sizes = tuple(tuple(p.shape[0] for p in ps) for ps in pieces)
-    toks = [p for ps in pieces for p in ps]
-    return pl.pallas_call(
-        functools.partial(proj_kernel, pieces=sizes),
-        out_shape=[jax.ShapeDtypeStruct((len(pieces) * 480, 128), bf16)] * 4,
-        in_specs=[SMEM] + [VMEM] * (1 + len(toks) + 8),
+    acc = lax.dot_general(tok, w, NT, preferred_element_type=f32)
+    for h in range(4):
+        qk = acc[:, h * 128 : h * 128 + 128].astype(bf16).astype(f32)
+        sq = qk * qk
+        s_lo = jnp.sum(jnp.where(lo, sq, 0.0), axis=1, keepdims=True)
+        s_hi = jnp.sum(jnp.where(lo, 0.0, sq), axis=1, keepdims=True)
+        inv = lax.rsqrt(jnp.where(lo, s_lo, s_hi) * (1 / 64) + 1e-6)
+        out[h][at : at + 320, :] = (qk * inv * gains).astype(bf16)
+        c = 512 + (h // 2) * 128
+        top, bot = acc[:160, c : c + 128], acc[160:, c : c + 128]
+        if h % 2:
+            top = pltpu.roll(top, 64, 1)
+        else:
+            bot = pltpu.roll(bot, 64, 1)
+        out[h][at + 320 : at + 480, :] = jnp.where(half, top, bot).astype(bf16)
+
+
+def gain_row(gain_ref):
+    return jnp.concatenate([gain_ref[0:1, :] * 0.125, gain_ref[1:2, :]], 1)
+
+
+def proj_kernel(idx_ref, gain_ref, *refs, count):
+    toks, ws, outs, w = refs[:count], refs[count : count + 8], refs[count + 8 : count + 12], refs[-1]
+    for j in range(8):
+        cols = pl.ds(pl.multiple_of(idx_ref[j] * 256, 256), 256)
+        for h in range(4):
+            w[h * 128 : h * 128 + 128, cols] = ws[j][h * 192 : h * 192 + 128, :]
+            w[512 + h * 64 : 576 + h * 64, cols] = ws[j][h * 192 + 128 : h * 192 + 192, :]
+    gains = gain_row(gain_ref)
+    for b in range(count):
+        proj_block(toks[b][...], w[...], gains, outs, b * 480)
+
+
+def project(cols, gain, toks, ws):
+    count = len(toks)
+    return pl.pallas_call(
+        functools.partial(proj_kernel, count=count),
+        out_shape=[jax.ShapeDtypeStruct((count * 480, 128), bf16)] * 4,
+        in_specs=[SMEM] + [VMEM] * (1 + count + 8),
         out_specs=[VMEM] * 4,
-        compiler_params=pltpu.CompilerParams(vmem_limit_bytes=12 * 1024 * 1024),
+        scratch_shapes=[pltpu.VMEM((768, 2048), bf16)],
+        compiler_params=pltpu.CompilerParams(vmem_limit_bytes=20 * 1024 * 1024),
         name="project",
-    )(cols, gains, *toks, *ws)
+    )(cols, gain, *toks, *ws)
 
 
 def out_kernel(head_ref, col_ref, heads_ref, *refs):
@@ -254,7 +259,7 @@
     z, y, x, c = (lax.axis_index(a) for a in (Z, Y, X, C))
     t1 = move(own, Y, -1)
     t3 = move(own, Y, 1)
-    t2 = [move(t1[:160], Y, -1), move(t3[160:], Y, 1)]
+    t2 = move(own, Y, 2)
     piece = jnp.concatenate([w_query.T, w_key.T, w_value.T, w_output], 0)
     w4, wo4 = pack(around(piece, Z))
     ws = around(w4, X)
@@ -263,23 +268,19 @@
     cols = jnp.stack(
         [2 * ((x + d) % 4) + e for e in (c, 1 - c) for d in range(4)]
     ).astype(jnp.int32)
-    gains = jnp.concatenate([qk_gain[0] * 0.125, qk_gain[1]])[None]
-    dp = decay_pieces(decay_sums[0, 0].reshape(20, 256))
-    bound = jnp.max(jnp.abs(qk_gain[0])) * jnp.max(jnp.abs(qk_gain[1]))
-    fast = (bound <= 7.7).astype(jnp.int32)[None]
-    gains, dp, fast = lax.optimization_barrier((gains, dp, fast))
-    part1 = project(cols, gains, [[own], [t1], [t3]], ws)
+    gain, decay = lax.optimization_barrier((qk_gain, decay_sums.reshape(8, 640)))
+    part1 = project(cols, gain, [own, t1, t3], ws)
     *part1, wo4 = lax.optimization_barrier((*part1, wo4))
-    part2 = project(cols, gains, [t2], ws)
+    part2 = project(cols, gain, [t2], ws)
     recv = []
     for part in (part1, part2):
         recv += [part[0]] + [move(part[d], Z, d) for d in (1, 2, 3)]
-    wo16 = jnp.concatenate(around(wo4, X), 0)
+    wo16 = join(around(wo4, X))
     wo = around(wo16, Y)
     pos = [4 * ((z - d) % 4) + (y + e) % 4 for d in range(4) for e in (0, 1, 3)]
     pos += [4 * ((z - d) % 4) + (y + 2) % 4 for d in range(4)]
     pos = jnp.stack(pos).astype(jnp.int32)
-    heads = attention(pos, fast, dp, recv, (3, 3, 3, 3, 1, 1, 1, 1))
+    heads = attention(pos, gain, decay, recv, (3, 3, 3, 3, 1, 1, 1, 1))
     heads, *wo = lax.optimization_barrier((heads, *wo))
     wo = wo + [move(w, C, 0) for w in wo]
     merged = lax.all_to_all(heads, SP, 0, 0, tiled=True)

time: 175 us -> 189 us (1.080)
  waiting for transfers between devices: 58.3 us -> 89.7 us
  Pallas kernels: 65.1 us -> 56.5 us
  local copies, waits for them, and re-layouts: 11.4 us -> 7.69 us
  other arithmetic: 4.32 us -> 2.26 us
    ppermute x30 -> x29, waiting for transfers between devices: 51.8 us -> 83.2 us  [move(): return lax.ppermute(value, axis, pairs)]
    pallas_call x2 -> x3, Pallas kernels: 19.1 us -> 10.6 us  [the longest x2 10.6 us: project(): pl.pallas_call(functools.partial(proj_kernel, count=count), out_shape=[ja...]
    concatenate x2 -> x0, local copies, waits for them, and re-layouts: 4.65 us -> none  [the longest x1 4.64 us: decay_pieces(): return jnp.concatenate([-h, -m, -l, h, m, l, jnp.zeros((8, 256), f32)], 0)]
    unnamed x19 -> x23, local copies, waits for them, and re-layouts: 4.7 us -> 7.41 us
    ppermute x30 -> x29, starting transfers between devices: 28.8 us -> 26.7 us  [move(): return lax.ppermute(value, axis, pairs)]
    reduce_max x2 -> x0, other arithmetic: 1.97 us -> none  [on_device(): bound = jnp.max(jnp.abs(qk_gain[0])) * jnp.max(jnp.abs(qk_gain[1]))]
  transfers between devices with their start and end apart: 31 -> 30, of which waited for: 18 -> 18; matrix products, arithmetic and copies ran while one was open for 6% -> 1% of each run, Pallas kernels for 35% -> 28%
where the time goes in v1:
time: 189 us
  waiting for transfers between devices  89.7 us (47%)
  Pallas kernels  56.5 us (30%)
  starting transfers between devices  32.3 us (17%)
  local copies, waits for them, and re-layouts  7.69 us (4%)
  other arithmetic  2.26 us (1%)
    ppermute x29, waiting for transfers between devices, move(): return lax.ppermute(value, axis, pairs)  83.2 us
    pallas_call x1, Pallas kernels, attention(): pl.pallas_call(functools.partial(attn_kernel, nblk=nblk), out_shape=jax.S...  41.7 us
    ppermute x29, starting transfers between devices, move(): return lax.ppermute(value, axis, pairs)  26.7 us
    pallas_call x2, Pallas kernels, project(): pl.pallas_call(functools.partial(proj_kernel, count=count), out_shape=[ja...  10.6 us
    unnamed x23, local copies, waits for them, and re-layouts  7.41 us
    all_to_all x1, waiting for transfers between devices, on_device(): merged = lax.all_to_all(heads, SP, 0, 0, tiled=True)  6.47 us
    all_to_all x1, starting transfers between devices, on_device(): merged = lax.all_to_all(heads, SP, 0, 0, tiled=True)  5.66 us
    pallas_call x1, Pallas kernels, output(): pl.pallas_call(out_kernel, out_shape=jax.ShapeDtypeStruct((BLK, 2048), bf...  4.15 us
  transfers between devices with their start and end apart: 30, of which 18 were waited for; matrix products, arithmetic and copies ran while one was open for 1% of the time, Pallas kernels for 28%

profile of v1, /device:TPU:0, one launch (start us, length us, event | category | flops | bytes accessed | tf_op | source)
XLA Modules:
  0.0 188.6 jit_solution(17924560375432313589)
XLA Ops:
  0.8 4.2 %collective-permute-start.2 = (bf16[256,256]{1,0:T(8,128)(2,1)S(1)}, bf16[256,256]{1,0:T(8,128)(2,1)S(1)}, u32[]{:S(2)}, u32[]{:S(2)}) collective-permute-start(bf16[256,256]{1,0:T(8,128)(2,1)S(1)} %pad_maximum_fusion.refs_0_), channel_id=1, source_target_pairs={{0,96},{32,0},{64,32},{96,64},{1,97},{33,1},{65,33},{97,65},{2,98}... | collective-permute-start | bytes 393224 | tf_op jit(solution)/shard_map/ppermute | solution.py:250
  5.0 1.3 collective-permute-start.4
  6.3 4.3 %collective-permute-done.2.refs_1_ = bf16[256,256]{1,0:T(8,128)(2,1)S(1)} collective-permute-done((bf16[256,256]{1,0:T(8,128)(2,1)S(1)}, bf16[256,256]{1,0:T(8,128)(2,1)S(1)}, u32[]{:S(2)}, u32[]{:S(2)}) %collective-permute-start.2) | collective-permute-done | bytes 131104 | tf_op jit(solution)/shard_map/ppermute | solution.py:250
  10.6 2.3 %collective-permute-done.3.refs_2_ = bf16[256,256]{1,0:T(8,128)(2,1)S(1)} collective-permute-done((bf16[256,256]{1,0:T(8,128)(2,1)S(1)}, bf16[256,256]{1,0:T(8,128)(2,1)S(1)}, u32[]{:S(2)}, u32[]{:S(2)}) %collective-permute-start.3) | collective-permute-done | bytes 131104 | tf_op jit(solution)/shard_map/ppermute | solution.py:250
  12.9 1.1 collective-permute-done.4.refs_3_
  14.7 2.8 %collective-permute-start.5 = (bf16[768,256]{1,0:T(8,128)(2,1)S(1)}, bf16[768,256]{1,0:T(8,128)(2,1)S(1)}, u32[]{:S(2)}, u32[]{:S(2)}) collective-permute-start(bf16[768,256]{1,0:T(8,128)(2,1)S(1)} %get-tuple-element.29.refs_3_.refs_1_), channel_id=1, source_target_pairs={{0,6},{2,0},{4,2},{6,4},{1,7},{3,1},{5,3},{7,5},{8,14},{10,8},{12,... | collective-permute-start | bytes 1179656 | tf_op jit(solution)/shard_map/ppermute | solution.py:250
  17.5 3.0 %collective-permute-start = (bf16[320,2048]{1,0:T(8,128)(2,1)}, bf16[320,2048]{1,0:T(8,128)(2,1)}, u32[]{:S(2)}, u32[]{:S(2)}) collective-permute-start(bf16[320,2048]{1,0:T(8,128)(2,1)} %bitcast.41), channel_id=1, source_target_pairs={{0,24},{8,0},{16,8},{24,16},{1,25},{9,1},{17,9},{25,17},{2,26},{10... | collective-permute-start | bytes 3932168 | tf_op jit(solution)/shard_map/ppermute | solution.py:250
  20.5 2.2 %collective-permute-start.15 = (bf16[320,2048]{1,0:T(8,128)(2,1)}, bf16[320,2048]{1,0:T(8,128)(2,1)}, u32[]{:S(2)}, u32[]{:S(2)}) collective-permute-start(bf16[320,2048]{1,0:T(8,128)(2,1)} %bitcast.43), channel_id=1, source_target_pairs={{0,16},{8,24},{16,0},{24,8},{1,17},{9,25},{17,1},{25,9},{2,18},{10... | collective-permute-start | bytes 3932168 | tf_op jit(solution)/shard_map/ppermute | solution.py:250
  23.5 10.7 %collective-permute-done.5.refs_4_.refs_2_ = bf16[768,256]{1,0:T(8,128)(2,1)S(1)} collective-permute-done((bf16[768,256]{1,0:T(8,128)(2,1)S(1)}, bf16[768,256]{1,0:T(8,128)(2,1)S(1)}, u32[]{:S(2)}, u32[]{:S(2)}) %collective-permute-start.5) | collective-permute-done | bytes 393248 | tf_op jit(solution)/shard_map/ppermute | solution.py:250
  34.2 1.8 collective-permute-done.6.refs_5_.refs_3_
  36.0 7.6 %collective-permute-done.7.refs_6_.refs_4_ = bf16[768,256]{1,0:T(8,128)(2,1)S(1)} collective-permute-done((bf16[768,256]{1,0:T(8,128)(2,1)S(1)}, bf16[768,256]{1,0:T(8,128)(2,1)S(1)}, u32[]{:S(2)}, u32[]{:S(2)}) %collective-permute-start.7) | collective-permute-done | bytes 393248 | tf_op jit(solution)/shard_map/ppermute | solution.py:250
  44.1 1.2 collective-permute-done.9.refs_8_.refs_6_
  46.0 1.4 reduce.3
  47.6 28.9 %collective-permute-done.refs_1_ = bf16[320,2048]{1,0:T(8,128)(2,1)} collective-permute-done((bf16[320,2048]{1,0:T(8,128)(2,1)}, bf16[320,2048]{1,0:T(8,128)(2,1)}, u32[]{:S(2)}, u32[]{:S(2)}) %collective-permute-start) | collective-permute-done | bytes 1310752 | tf_op jit(solution)/shard_map/ppermute | solution.py:250
  76.5 3.4 %collective-permute-done.1.refs_2_ = bf16[320,2048]{1,0:T(8,128)(2,1)} collective-permute-done((bf16[320,2048]{1,0:T(8,128)(2,1)}, bf16[320,2048]{1,0:T(8,128)(2,1)}, u32[]{:S(2)}, u32[]{:S(2)}) %collective-permute-start.1) | collective-permute-done | bytes 1310752 | tf_op jit(solution)/shard_map/ppermute | solution.py:250
  79.9 1.3 copy-done
  81.9 7.0 %project.2 = (bf16[1440,128]{1,0:T(8,128)(2,1)S(1)}, bf16[1440,128]{1,0:T(8,128)(2,1)S(1)}, bf16[1440,128]{1,0:T(8,128)(2,1)}, bf16[1440,128]{1,0:T(8,128)(2,1)}) custom-call(s32[8]{0:T(128)S(1)} %stack.146.idx_ref.col_ref, f32[2,64]{1,0:T(2,128)S(1)} %copy-done.9, bf16[320,2048]{1,0:T(8,128)(2,1)S(1)} %bitcast.44, ...), custom_call_target="tpu_custom_call" | custom-call | tf_op jit(solution)/shard_map/project/pallas_call | solution.py:199
  91.2 3.6 %project.3 = (bf16[480,128]{1,0:T(8,128)(2,1)S(1)}, bf16[480,128]{1,0:T(8,128)(2,1)S(1)}, bf16[480,128]{1,0:T(8,128)(2,1)S(1)}, bf16[480,128]{1,0:T(8,128)(2,1)S(1)}) custom-call(s32[8]{0:T(128)S(1)} %stack.146.idx_ref.col_ref, f32[2,64]{1,0:T(2,128)S(1)} %copy-done.9, bf16[320,2048]{1,0:T(8,128)(2,1)} %collective-permute-done.15.refs_0_, ...), custom_call_target="tpu_custom_call" | custom-call | tf_op jit(solution)/shard_map/project/pallas_call | solution.py:199
  95.1 4.5 %collective-permute-start.17 = (bf16[480,128]{1,0:T(8,128)(2,1)S(1)}, bf16[480,128]{1,0:T(8,128)(2,1)S(1)}, u32[]{:S(2)}, u32[]{:S(2)}) collective-permute-start(bf16[480,128]{1,0:T(8,128)(2,1)S(1)} %get-tuple-element.41), channel_id=1, source_target_pairs={{0,64},{32,96},{64,0},{96,32},{1,65},{33,97},{65,1},{97,33},{2,66}... | collective-permute-start | bytes 368648 | tf_op jit(solution)/shard_map/ppermute | solution.py:250
  100.0 5.1 %collective-permute-done.16.refs_5_ = bf16[480,128]{1,0:T(8,128)(2,1)S(1)} collective-permute-done((bf16[480,128]{1,0:T(8,128)(2,1)S(1)}, bf16[480,128]{1,0:T(8,128)(2,1)S(1)}, u32[]{:S(2)}, u32[]{:S(2)}) %collective-permute-start.16) | collective-permute-done | bytes 122912 | tf_op jit(solution)/shard_map/ppermute | solution.py:250
  105.1 1.0 collective-permute-start.18
  106.1 3.8 %collective-permute-done.18.refs_7_ = bf16[480,128]{1,0:T(8,128)(2,1)S(1)} collective-permute-done((bf16[480,128]{1,0:T(8,128)(2,1)S(1)}, bf16[480,128]{1,0:T(8,128)(2,1)S(1)}, u32[]{:S(2)}, u32[]{:S(2)}) %collective-permute-start.18) | collective-permute-done | bytes 122912 | tf_op jit(solution)/shard_map/ppermute | solution.py:250
  110.6 0.9 collective-permute-start.13
  112.3 1.4 collective-permute-start.14
  113.7 6.1 %collective-permute-done.13.refs_2_ = bf16[1440,128]{1,0:T(8,128)(2,1)S(1)} collective-permute-done((bf16[1440,128]{1,0:T(8,128)(2,1)}, bf16[1440,128]{1,0:T(8,128)(2,1)S(1)}, u32[]{:S(2)}, u32[]{:S(2)}) %collective-permute-start.13) | collective-permute-done | bytes 368672 | tf_op jit(solution)/shard_map/ppermute | solution.py:250
  119.8 3.6 %collective-permute-done.14.refs_3_ = bf16[1440,128]{1,0:T(8,128)(2,1)S(1)} collective-permute-done((bf16[1440,128]{1,0:T(8,128)(2,1)}, bf16[1440,128]{1,0:T(8,128)(2,1)S(1)}, u32[]{:S(2)}, u32[]{:S(2)}) %collective-permute-start.14) | collective-permute-done | bytes 368672 | tf_op jit(solution)/shard_map/ppermute | solution.py:250
  123.4 1.0 copy-done.2
  124.4 0.9 copy-done.6
  126.2 41.7 %attention.1 = bf16[16,160,128]{2,1,0:T(8,128)(2,1)} custom-call(s32[16]{0:T(128)S(1)} %stack.159.pos_ref, f32[2,64]{1,0:T(2,128)S(1)} %copy-done.10, f32[8,640]{1,0:T(8,128)S(1)} %reshape.3.d_ref, bf16[1440,128]{1,0:T(8,128)(2,1)S(1)} %get-tuple-element.35.refs_0_, bf16[1440,128]{1,0:T(8,128)(2,1)S(1)} %copy-done.2, ...), custom_call_target="tpu_custom_call" | custom-call | tf_op jit(solution)/shard_map/attention/pallas_call | solution.py:118
  167.9 5.7 %all-to-all-start = ((bf16[16,160,128]{2,1,0:T(8,128)(2,1)}), bf16[16,160,128]{2,1,0:T(8,128)(2,1)S(1)}, u32[]{:S(2)}, u32[]{:S(2)}) async-start(bf16[16,160,128]{2,1,0:T(8,128)(2,1)} %attention.1), calls=%async_computation | async-start | bytes 1310720 | tf_op jit(solution)/shard_map/all_to_all | solution.py:286
  178.0 6.5 %all-to-all-done.heads_ref = bf16[16,160,128]{2,1,0:T(8,128)(2,1)S(1)} async-done(((bf16[16,160,128]{2,1,0:T(8,128)(2,1)}), bf16[16,160,128]{2,1,0:T(8,128)(2,1)S(1)}, u32[]{:S(2)}, u32[]{:S(2)}) %all-to-all-start) | async-done | bytes 655392 | tf_op jit(solution)/shard_map/all_to_all | solution.py:286
  184.4 4.2 %output.1 = bf16[320,2048]{1,0:T(8,128)(2,1)} custom-call(s32[16]{0:T(128)S(1)} %stack.137.head_ref, s32[8]{0:T(128)S(1)} %stack.146.idx_ref.col_ref, bf16[16,160,128]{2,1,0:T(8,128)(2,1)S(1)} %all-to-all-done.heads_ref, bf16[1024,256]{1,0:T(8,128)(2,1)S(1)} %join.1.refs_0_, bf16[1024,256]{1,0:T(8,128)(2,1)S(1)} %collective-permute-done.22.refs_1_, ...), custom_call_target="tpu_custom_call" | custom-call | tf_op jit(solution)/shard_map/output/pallas_call | solution.py:233
  (63 shorter events, 14.0 us)
Async XLA Ops:
  0.8 9.8 %collective-permute-start.2 = (bf16[256,256]{1,0:T(8,128)(2,1)S(1)}, bf16[256,256]{1,0:T(8,128)(2,1)S(1)}, u32[]{:S(2)}, u32[]{:S(2)}) collective-permute-start(bf16[256,256]{1,0:T(8,128)(2,1)S(1)} %pad_maximum_fusion.refs_0_), channel_id=1, source_target_pairs={{0,96},{32,0},{64,32},{96,64},{1,97},{33,1},{65,33},{97,65},{2,98}... | collective-permute-start | bytes 393224 | tf_op jit(solution)/shard_map/ppermute | solution.py:250
  5.0 7.9 %collective-permute-start.3 = (bf16[256,256]{1,0:T(8,128)(2,1)S(1)}, bf16[256,256]{1,0:T(8,128)(2,1)S(1)}, u32[]{:S(2)}, u32[]{:S(2)}) collective-permute-start(bf16[256,256]{1,0:T(8,128)(2,1)S(1)} %pad_maximum_fusion.refs_0_), channel_id=1, source_target_pairs={{0,64},{32,96},{64,0},{96,32},{1,65},{33,97},{65,1},{97,33},{2,66}... | collective-permute-start | bytes 393224 | tf_op jit(solution)/shard_map/ppermute | solution.py:250
  5.0 9.0 %collective-permute-start.4 = (bf16[256,256]{1,0:T(8,128)(2,1)S(1)}, bf16[256,256]{1,0:T(8,128)(2,1)S(1)}, u32[]{:S(2)}, u32[]{:S(2)}) collective-permute-start(bf16[256,256]{1,0:T(8,128)(2,1)S(1)} %pad_maximum_fusion.refs_0_), channel_id=1, source_target_pairs={{0,32},{32,64},{64,96},{96,0},{1,33},{33,65},{65,97},{97,1},{2,34}... | collective-permute-start | bytes 393224 | tf_op jit(solution)/shard_map/ppermute | solution.py:250
  14.7 19.5 %collective-permute-start.5 = (bf16[768,256]{1,0:T(8,128)(2,1)S(1)}, bf16[768,256]{1,0:T(8,128)(2,1)S(1)}, u32[]{:S(2)}, u32[]{:S(2)}) collective-permute-start(bf16[768,256]{1,0:T(8,128)(2,1)S(1)} %get-tuple-element.29.refs_3_.refs_1_), channel_id=1, source_target_pairs={{0,6},{2,0},{4,2},{6,4},{1,7},{3,1},{5,3},{7,5},{8,14},{10,8},{12,... | collective-permute-start | bytes 1179656 | tf_op jit(solution)/shard_map/ppermute | solution.py:250
  17.5 59.1 %collective-permute-start = (bf16[320,2048]{1,0:T(8,128)(2,1)}, bf16[320,2048]{1,0:T(8,128)(2,1)}, u32[]{:S(2)}, u32[]{:S(2)}) collective-permute-start(bf16[320,2048]{1,0:T(8,128)(2,1)} %bitcast.41), channel_id=1, source_target_pairs={{0,24},{8,0},{16,8},{24,16},{1,25},{9,1},{17,9},{25,17},{2,26},{10... | collective-permute-start | bytes 3932168 | tf_op jit(solution)/shard_map/ppermute | solution.py:250
  20.5 59.5 %collective-permute-start.1 = (bf16[320,2048]{1,0:T(8,128)(2,1)}, bf16[320,2048]{1,0:T(8,128)(2,1)}, u32[]{:S(2)}, u32[]{:S(2)}) collective-permute-start(bf16[320,2048]{1,0:T(8,128)(2,1)} %bitcast.42), channel_id=1, source_target_pairs={{0,8},{8,16},{16,24},{24,0},{1,9},{9,17},{17,25},{25,1},{2,10},{10... | collective-permute-start | bytes 3932168 | tf_op jit(solution)/shard_map/ppermute | solution.py:250
  20.5 70.7 %collective-permute-start.15 = (bf16[320,2048]{1,0:T(8,128)(2,1)}, bf16[320,2048]{1,0:T(8,128)(2,1)}, u32[]{:S(2)}, u32[]{:S(2)}) collective-permute-start(bf16[320,2048]{1,0:T(8,128)(2,1)} %bitcast.43), channel_id=1, source_target_pairs={{0,16},{8,24},{16,0},{24,8},{1,17},{9,25},{17,1},{25,9},{2,18},{10... | collective-permute-start | bytes 3932168 | tf_op jit(solution)/shard_map/ppermute | solution.py:250
  22.7 13.3 %collective-permute-start.6 = (bf16[768,256]{1,0:T(8,128)(2,1)S(1)}, bf16[768,256]{1,0:T(8,128)(2,1)S(1)}, u32[]{:S(2)}, u32[]{:S(2)}) collective-permute-start(bf16[768,256]{1,0:T(8,128)(2,1)S(1)} %get-tuple-element.29.refs_3_.refs_1_), channel_id=1, source_target_pairs={{0,4},{2,6},{4,0},{6,2},{1,5},{3,7},{5,1},{7,3},{8,12},{10,14},{12... | collective-permute-start | bytes 1179656 | tf_op jit(solution)/shard_map/ppermute | solution.py:250
  34.2 9.4 %collective-permute-start.7 = (bf16[768,256]{1,0:T(8,128)(2,1)S(1)}, bf16[768,256]{1,0:T(8,128)(2,1)S(1)}, u32[]{:S(2)}, u32[]{:S(2)}) collective-permute-start(bf16[768,256]{1,0:T(8,128)(2,1)S(1)} %get-tuple-element.29.refs_3_.refs_1_), channel_id=1, source_target_pairs={{0,2},{2,4},{4,6},{6,0},{1,3},{3,5},{5,7},{7,1},{8,10},{10,12},{12... | collective-permute-start | bytes 1179656 | tf_op jit(solution)/shard_map/ppermute | solution.py:250
  36.0 7.7 %collective-permute-start.8 = (bf16[768,256]{1,0:T(8,128)(2,1)S(1)}, bf16[768,256]{1,0:T(8,128)(2,1)S(1)}, u32[]{:S(2)}, u32[]{:S(2)}) collective-permute-start(bf16[768,256]{1,0:T(8,128)(2,1)S(1)} %get-tuple-element.29.refs_3_.refs_1_), channel_id=1, source_target_pairs={{0,1},{1,0},{2,3},{3,2},{4,5},{5,4},{6,7},{7,6},{8,9},{9,8},{10,11... | collective-permute-start | bytes 1179656 | tf_op jit(solution)/shard_map/ppermute | solution.py:250
  43.6 1.7 collective-permute-start.9
  43.6 4.0 %collective-permute-start.10 = (bf16[768,256]{1,0:T(8,128)(2,1)S(1)}, bf16[768,256]{1,0:T(8,128)(2,1)S(1)}, u32[]{:S(2)}, u32[]{:S(2)}) collective-permute-start(bf16[768,256]{1,0:T(8,128)(2,1)S(1)} %collective-permute-done.6.refs_5_.refs_3_), channel_id=1, source_target_pairs={{0,1},{1,0},{2,3},{3,2},{4,5},{5,4},{6,7},{7,6},{8,9},{9,8},{10,11... | collective-permute-start | bytes 1179656 | tf_op jit(solution)/shard_map/ppermute | solution.py:250
  45.3 2.3 %collective-permute-start.11 = (bf16[768,256]{1,0:T(8,128)(2,1)S(1)}, bf16[768,256]{1,0:T(8,128)(2,1)S(1)}, u32[]{:S(2)}, u32[]{:S(2)}) collective-permute-start(bf16[768,256]{1,0:T(8,128)(2,1)S(1)} %collective-permute-done.7.refs_6_.refs_4_), channel_id=1, source_target_pairs={{0,1},{1,0},{2,3},{3,2},{4,5},{5,4},{6,7},{7,6},{8,9},{9,8},{10,11... | collective-permute-start | bytes 1179656 | tf_op jit(solution)/shard_map/ppermute | solution.py:250
  88.9 6.2 %collective-permute-start.19 = (bf16[256,256]{1,0:T(8,128)(2,1)S(1)}, bf16[256,256]{1,0:T(8,128)(2,1)S(1)}, u32[]{:S(2)}, u32[]{:S(2)}) collective-permute-start(bf16[256,256]{1,0:T(8,128)(2,1)S(1)} %copy-done.4), channel_id=1, source_target_pairs={{0,6},{2,0},{4,2},{6,4},{1,7},{3,1},{5,3},{7,5},{8,14},{10,8},{12,... | collective-permute-start | bytes 393224 | tf_op jit(solution)/shard_map/ppermute | solution.py:250
  89.8 21.8 %collective-permute-start.12 = (bf16[1440,128]{1,0:T(8,128)(2,1)S(1)}, bf16[1440,128]{1,0:T(8,128)(2,1)S(1)}, u32[]{:S(2)}, u32[]{:S(2)}) collective-permute-start(bf16[1440,128]{1,0:T(8,128)(2,1)S(1)} %get-tuple-element.36), channel_id=1, source_target_pairs={{0,32},{32,64},{64,96},{96,0},{1,33},{33,65},{65,97},{97,1},{2,34}... | collective-permute-start | bytes 1105928 | tf_op jit(solution)/shard_map/ppermute | solution.py:250
  89.8 9.8 %collective-permute-start.20 = (bf16[256,256]{1,0:T(8,128)(2,1)S(1)}, bf16[256,256]{1,0:T(8,128)(2,1)S(1)}, u32[]{:S(2)}, u32[]{:S(2)}) collective-permute-start(bf16[256,256]{1,0:T(8,128)(2,1)S(1)} %copy-done.4), channel_id=1, source_target_pairs={{0,4},{2,6},{4,0},{6,2},{1,5},{3,7},{5,1},{7,3},{8,12},{10,14},{12... | collective-permute-start | bytes 393224 | tf_op jit(solution)/shard_map/ppermute | solution.py:250
  90.3 9.3 %collective-permute-start.21 = (bf16[256,256]{1,0:T(8,128)(2,1)S(1)}, bf16[256,256]{1,0:T(8,128)(2,1)S(1)}, u32[]{:S(2)}, u32[]{:S(2)}) collective-permute-start(bf16[256,256]{1,0:T(8,128)(2,1)S(1)} %copy-done.4), channel_id=1, source_target_pairs={{0,2},{2,4},{4,6},{6,0},{1,3},{3,5},{5,7},{7,1},{8,10},{10,12},{12... | collective-permute-start | bytes 393224 | tf_op jit(solution)/shard_map/ppermute | solution.py:250
  94.8 16.7 %copy-start.5 = (bf16[480,128]{1,0:T(8,128)(2,1)}, bf16[480,128]{1,0:T(8,128)(2,1)S(1)}, u32[]{:S(2)}) copy-start(bf16[480,128]{1,0:T(8,128)(2,1)S(1)} %get-tuple-element.39.refs_4_) | copy-start | bytes 368644
  94.8 28.6 %copy-start.10 = (f32[2,64]{1,0:T(2,128)S(1)}, f32[2,64]{1,0:T(2,128)}, u32[]{:S(2)}) copy-start(f32[2,64]{1,0:T(2,128)} %gain_ref.2) | copy-start | bytes 1540
  94.8 10.2 %collective-permute-start.16 = (bf16[480,128]{1,0:T(8,128)(2,1)S(1)}, bf16[480,128]{1,0:T(8,128)(2,1)S(1)}, u32[]{:S(2)}, u32[]{:S(2)}) collective-permute-start(bf16[480,128]{1,0:T(8,128)(2,1)S(1)} %get-tuple-element.40), channel_id=1, source_target_pairs={{0,32},{32,64},{64,96},{96,0},{1,33},{33,65},{65,97},{97,1},{2,34}... | collective-permute-start | bytes 368648 | tf_op jit(solution)/shard_map/ppermute | solution.py:250
  95.1 10.0 %collective-permute-start.17 = (bf16[480,128]{1,0:T(8,128)(2,1)S(1)}, bf16[480,128]{1,0:T(8,128)(2,1)S(1)}, u32[]{:S(2)}, u32[]{:S(2)}) collective-permute-start(bf16[480,128]{1,0:T(8,128)(2,1)S(1)} %get-tuple-element.41), channel_id=1, source_target_pairs={{0,64},{32,96},{64,0},{96,32},{1,65},{33,97},{65,1},{97,33},{2,66}... | collective-permute-start | bytes 368648 | tf_op jit(solution)/shard_map/ppermute | solution.py:250
  99.6 68.3 %collective-permute-start.22 = (bf16[1024,256]{1,0:T(8,128)(2,1)S(1)}, bf16[1024,256]{1,0:T(8,128)(2,1)S(1)}, u32[]{:S(2)}, u32[]{:S(2)}) collective-permute-start(bf16[1024,256]{1,0:T(8,128)(2,1)S(1)} %join.1.refs_0_), channel_id=1, source_target_pairs={{0,24},{8,0},{16,8},{24,16},{1,25},{9,1},{17,9},{25,17},{2,26},{10... | collective-permute-start | bytes 1572872 | tf_op jit(solution)/shard_map/ppermute | solution.py:250
  100.0 67.9 %collective-permute-start.23 = (bf16[1024,256]{1,0:T(8,128)(2,1)S(1)}, bf16[1024,256]{1,0:T(8,128)(2,1)S(1)}, u32[]{:S(2)}, u32[]{:S(2)}) collective-permute-start(bf16[1024,256]{1,0:T(8,128)(2,1)S(1)} %join.1.refs_0_), channel_id=1, source_target_pairs={{0,16},{8,24},{16,0},{24,8},{1,17},{9,25},{17,1},{25,9},{2,18},{10... | collective-permute-start | bytes 1572872 | tf_op jit(solution)/shard_map/ppermute | solution.py:250
  105.1 62.8 %collective-permute-start.24 = (bf16[1024,256]{1,0:T(8,128)(2,1)S(1)}, bf16[1024,256]{1,0:T(8,128)(2,1)S(1)}, u32[]{:S(2)}, u32[]{:S(2)}) collective-permute-start(bf16[1024,256]{1,0:T(8,128)(2,1)S(1)} %join.1.refs_0_), channel_id=1, source_target_pairs={{0,8},{8,16},{16,24},{24,0},{1,9},{9,17},{17,25},{25,1},{2,10},{10... | collective-permute-start | bytes 1572872 | tf_op jit(solution)/shard_map/ppermute | solution.py:250
  105.1 4.9 %collective-permute-start.18 = (bf16[480,128]{1,0:T(8,128)(2,1)S(1)}, bf16[480,128]{1,0:T(8,128)(2,1)S(1)}, u32[]{:S(2)}, u32[]{:S(2)}) collective-permute-start(bf16[480,128]{1,0:T(8,128)(2,1)S(1)} %get-tuple-element.42), channel_id=1, source_target_pairs={{0,96},{32,0},{64,32},{96,64},{1,97},{33,1},{65,33},{97,65},{2,98}... | collective-permute-start | bytes 368648 | tf_op jit(solution)/shard_map/ppermute | solution.py:250
  110.6 9.2 %collective-permute-start.13 = (bf16[1440,128]{1,0:T(8,128)(2,1)}, bf16[1440,128]{1,0:T(8,128)(2,1)S(1)}, u32[]{:S(2)}, u32[]{:S(2)}) collective-permute-start(bf16[1440,128]{1,0:T(8,128)(2,1)} %get-tuple-element.37), channel_id=1, source_target_pairs={{0,64},{32,96},{64,0},{96,32},{1,65},{33,97},{65,1},{97,33},{2,66}... | collective-permute-start | bytes 1105928 | tf_op jit(solution)/shard_map/ppermute | solution.py:250
  112.3 11.1 %collective-permute-start.14 = (bf16[1440,128]{1,0:T(8,128)(2,1)}, bf16[1440,128]{1,0:T(8,128)(2,1)S(1)}, u32[]{:S(2)}, u32[]{:S(2)}) collective-permute-start(bf16[1440,128]{1,0:T(8,128)(2,1)} %get-tuple-element.38), channel_id=1, source_target_pairs={{0,96},{32,0},{64,32},{96,64},{1,97},{33,1},{65,33},{97,65},{2,98}... | collective-permute-start | bytes 1105928 | tf_op jit(solution)/shard_map/ppermute | solution.py:250
  167.9 16.5 %all-to-all-start = ((bf16[16,160,128]{2,1,0:T(8,128)(2,1)}), bf16[16,160,128]{2,1,0:T(8,128)(2,1)S(1)}, u32[]{:S(2)}, u32[]{:S(2)}) async-start(bf16[16,160,128]{2,1,0:T(8,128)(2,1)} %attention.1), calls=%async_computation | async-start | bytes 1310720 | tf_op jit(solution)/shard_map/all_to_all | solution.py:286
  173.6 2.0 %collective-permute-start.25 = (bf16[1024,256]{1,0:T(8,128)(2,1)S(1)}, bf16[1024,256]{1,0:T(8,128)(2,1)S(1)}, u32[]{:S(2)}, u32[]{:S(2)}) collective-permute-start(bf16[1024,256]{1,0:T(8,128)(2,1)S(1)} %join.1.refs_0_), channel_id=1, source_target_pairs={{0,1},{1,0},{2,3},{3,2},{4,5},{5,4},{6,7},{7,6},{8,9},{9,8},{10,11... | collective-permute-start | bytes 1572872 | tf_op jit(solution)/shard_map/ppermute | solution.py:250
  173.7 2.8 %collective-permute-start.26 = (bf16[1024,256]{1,0:T(8,128)(2,1)S(1)}, bf16[1024,256]{1,0:T(8,128)(2,1)}, u32[]{:S(2)}, u32[]{:S(2)}) collective-permute-start(bf16[1024,256]{1,0:T(8,128)(2,1)S(1)} %collective-permute-done.22.refs_1_), channel_id=1, source_target_pairs={{0,1},{1,0},{2,3},{3,2},{4,5},{5,4},{6,7},{7,6},{8,9},{9,8},{10,11... | collective-permute-start | bytes 1572872 | tf_op jit(solution)/shard_map/ppermute | solution.py:250
  174.2 3.0 %collective-permute-start.27 = (bf16[1024,256]{1,0:T(8,128)(2,1)S(1)}, bf16[1024,256]{1,0:T(8,128)(2,1)}, u32[]{:S(2)}, u32[]{:S(2)}) collective-permute-start(bf16[1024,256]{1,0:T(8,128)(2,1)S(1)} %collective-permute-done.23.refs_2_), channel_id=1, source_target_pairs={{0,1},{1,0},{2,3},{3,2},{4,5},{5,4},{6,7},{7,6},{8,9},{9,8},{10,11... | collective-permute-start | bytes 1572872 | tf_op jit(solution)/shard_map/ppermute | solution.py:250
  174.3 3.7 %collective-permute-start.28 = (bf16[1024,256]{1,0:T(8,128)(2,1)S(1)}, bf16[1024,256]{1,0:T(8,128)(2,1)}, u32[]{:S(2)}, u32[]{:S(2)}) collective-permute-start(bf16[1024,256]{1,0:T(8,128)(2,1)S(1)} %collective-permute-done.24.refs_3_), channel_id=1, source_target_pairs={{0,1},{1,0},{2,3},{3,2},{4,5},{5,4},{6,7},{7,6},{8,9},{9,8},{10,11... | collective-permute-start | bytes 1572872 | tf_op jit(solution)/shard_map/ppermute | solution.py:250
  (9 other events, 13.8 us)

commit v2 on v1

--- a/solution.py
+++ b/solution.py
@@ -182,24 +182,29 @@
     return jnp.concatenate([gain_ref[0:1, :] * 0.125, gain_ref[1:2, :]], 1)
 
 
-def proj_kernel(idx_ref, gain_ref, *refs, count):
-    toks, ws, outs, w = refs[:count], refs[count : count + 8], refs[count + 8 : count + 12], refs[-1]
+def proj_kernel(idx_ref, gain_ref, *refs, sizes):
+    n = sum(sizes)
+    toks, ws, outs, w = refs[:n], refs[n : n + 8], refs[n + 8 : n + 12], refs[-1]
     for j in range(8):
         cols = pl.ds(pl.multiple_of(idx_ref[j] * 256, 256), 256)
         for h in range(4):
             w[h * 128 : h * 128 + 128, cols] = ws[j][h * 192 : h * 192 + 128, :]
             w[512 + h * 64 : 576 + h * 64, cols] = ws[j][h * 192 + 128 : h * 192 + 192, :]
     gains = gain_row(gain_ref)
-    for b in range(count):
-        proj_block(toks[b][...], w[...], gains, outs, b * 480)
-
-
-def project(cols, gain, toks, ws):
-    count = len(toks)
+    at = 0
+    for b, size in enumerate(sizes):
+        parts = [t[...] for t in toks[at : at + size]]
+        at += size
+        tok = parts[0] if size == 1 else jnp.concatenate(parts, 0)
+        proj_block(tok, w[...], gains, outs, b * 480)
+
+
+def project(cols, gain, blocks, ws):
+    toks = [p for block in blocks for p in block]
     return pl.pallas_call(
-        functools.partial(proj_kernel, count=count),
-        out_shape=[jax.ShapeDtypeStruct((count * 480, 128), bf16)] * 4,
-        in_specs=[SMEM] + [VMEM] * (1 + count + 8),
+        functools.partial(proj_kernel, sizes=tuple(len(b) for b in blocks)),
+        out_shape=[jax.ShapeDtypeStruct((len(blocks) * 480, 128), bf16)] * 4,
+        in_specs=[SMEM] + [VMEM] * (1 + len(toks) + 8),
         out_specs=[VMEM] * 4,
         scratch_shapes=[pltpu.VMEM((768, 2048), bf16)],
         compiler_params=pltpu.CompilerParams(vmem_limit_bytes=20 * 1024 * 1024),
@@ -257,9 +262,10 @@
 def on_device(tokens, w_query, w_key, w_value, w_output, qk_gain, decay_sums):
     own = tokens[0]
     z, y, x, c = (lax.axis_index(a) for a in (Z, Y, X, C))
-    t1 = move(own, Y, -1)
-    t3 = move(own, Y, 1)
-    t2 = move(own, Y, 2)
+    top, bot = own[:160], own[160:]
+    t1 = [move(top, Y, -1), move(bot, Y, -1)]
+    t3 = [move(top, Y, 1), move(bot, Y, 1)]
+    t2 = [move(t1[0], Y, -1), move(t3[1], Y, 1)]
     piece = jnp.concatenate([w_query.T, w_key.T, w_value.T, w_output], 0)
     w4, wo4 = pack(around(piece, Z))
     ws = around(w4, X)
@@ -269,7 +275,7 @@
         [2 * ((x + d) % 4) + e for e in (c, 1 - c) for d in range(4)]
     ).astype(jnp.int32)
     gain, decay = lax.optimization_barrier((qk_gain, decay_sums.reshape(8, 640)))
-    part1 = project(cols, gain, [own, t1, t3], ws)
+    part1 = project(cols, gain, [[own], t1, t3], ws)
     *part1, wo4 = lax.optimization_barrier((*part1, wo4))
     part2 = project(cols, gain, [t2], ws)
     recv = []

time: 189 us -> 175 us (0.926)
  waiting for transfers between devices: 89.7 us -> 59.5 us
  starting transfers between devices: 32.3 us -> 45.7 us
  local copies, waits for them, and re-layouts: 7.69 us -> 10.6 us
    ppermute x29 -> x32, waiting for transfers between devices: 83.2 us -> 52.9 us  [move(): return lax.ppermute(value, axis, pairs)]
    ppermute x29 -> x32, starting transfers between devices: 26.7 us -> 38.8 us  [move(): return lax.ppermute(value, axis, pairs)]
    unnamed x23 -> x27, local copies, waits for them, and re-layouts: 7.41 us -> 8.87 us
  transfers between devices with their start and end apart: 30 -> 33, of which waited for: 18 -> 19; matrix products, arithmetic and copies ran while one was open for 1% -> 2% of each run, Pallas kernels for 28% -> 30%
where the time goes in v2:
time: 175 us; the launch traced here: 174 us
  waiting for transfers between devices  59.5 us (34%)
  Pallas kernels  56.5 us (32%)
  starting transfers between devices  45.7 us (26%)
  local copies, waits for them, and re-layouts  10.6 us (6%)
    ppermute x32, waiting for transfers between devices, move(): return lax.ppermute(value, axis, pairs)  52.9 us
    pallas_call x1, Pallas kernels, attention(): pl.pallas_call(functools.partial(attn_kernel, nblk=nblk), out_shape=jax.S...  41.7 us
    ppermute x32, starting transfers between devices, move(): return lax.ppermute(value, axis, pairs)  38.8 us
    pallas_call x2, Pallas kernels, project(): pl.pallas_call(functools.partial(proj_kernel, sizes=tuple((len(b) for b i...  10.6 us
    unnamed x27, local copies, waits for them, and re-layouts  8.87 us
    all_to_all x1, starting transfers between devices, on_device(): merged = lax.all_to_all(heads, SP, 0, 0, tiled=True)  6.93 us
    all_to_all x1, waiting for transfers between devices, on_device(): merged = lax.all_to_all(heads, SP, 0, 0, tiled=True)  6.6 us
    pallas_call x1, Pallas kernels, output(): pl.pallas_call(out_kernel, out_shape=jax.ShapeDtypeStruct((BLK, 2048), bf...  4.12 us
  transfers between devices with their start and end apart: 33, of which 19 were waited for; matrix products, arithmetic and copies ran while one was open for 2% of the time, Pallas kernels for 30%

profile of v2, /device:TPU:0, one launch (start us, length us, event | category | flops | bytes accessed | tf_op | source)
XLA Modules:
  0.0 174.0 jit_solution(13002443262135897694)
XLA Ops:
  0.8 4.2 %collective-permute-start.4 = (bf16[256,256]{1,0:T(8,128)(2,1)S(1)}, bf16[256,256]{1,0:T(8,128)(2,1)S(1)}, u32[]{:S(2)}, u32[]{:S(2)}) collective-permute-start(bf16[256,256]{1,0:T(8,128)(2,1)S(1)} %pad_maximum_fusion.refs_0_), channel_id=1, source_target_pairs={{0,96},{32,0},{64,32},{96,64},{1,97},{33,1},{65,33},{97,65},{2,98}... | collective-permute-start | bytes 393224 | tf_op jit(solution)/shard_map/ppermute | solution.py:255
  5.0 1.3 collective-permute-start.6
  6.3 4.3 %collective-permute-done.4.refs_1_ = bf16[256,256]{1,0:T(8,128)(2,1)S(1)} collective-permute-done((bf16[256,256]{1,0:T(8,128)(2,1)S(1)}, bf16[256,256]{1,0:T(8,128)(2,1)S(1)}, u32[]{:S(2)}, u32[]{:S(2)}) %collective-permute-start.4) | collective-permute-done | bytes 131104 | tf_op jit(solution)/shard_map/ppermute | solution.py:255
  10.6 2.3 %collective-permute-done.5.refs_2_ = bf16[256,256]{1,0:T(8,128)(2,1)S(1)} collective-permute-done((bf16[256,256]{1,0:T(8,128)(2,1)S(1)}, bf16[256,256]{1,0:T(8,128)(2,1)S(1)}, u32[]{:S(2)}, u32[]{:S(2)}) %collective-permute-start.5) | collective-permute-done | bytes 131104 | tf_op jit(solution)/shard_map/ppermute | solution.py:255
  12.9 1.1 collective-permute-done.6.refs_3_
  14.1 2.8 %collective-permute-start.7 = (bf16[768,256]{1,0:T(8,128)(2,1)S(1)}, bf16[768,256]{1,0:T(8,128)(2,1)S(1)}, u32[]{:S(2)}, u32[]{:S(2)}) collective-permute-start(bf16[768,256]{1,0:T(8,128)(2,1)S(1)} %get-tuple-element.29.refs_5_.refs_2_), channel_id=1, source_target_pairs={{0,6},{2,0},{4,2},{6,4},{1,7},{3,1},{5,3},{7,5},{8,14},{10,8},{12,... | collective-permute-start | bytes 1179656 | tf_op jit(solution)/shard_map/ppermute | solution.py:255
  18.6 1.4 slice_bitcast_fusion
  20.0 3.1 %collective-permute-start = (bf16[160,2048]{1,0:T(8,128)(2,1)S(1)}, bf16[160,2048]{1,0:T(8,128)(2,1)}, u32[]{:S(2)}, u32[]{:S(2)}) collective-permute-start(bf16[160,2048]{1,0:T(8,128)(2,1)S(1)} %get-tuple-element.50), channel_id=1, source_target_pairs={{0,24},{8,0},{16,8},{24,16},{1,25},{9,1},{17,9},{25,17},{2,26},{10... | collective-permute-start | bytes 1966088 | tf_op jit(solution)/shard_map/ppermute | solution.py:255
  23.9 9.8 %collective-permute-done.7.refs_6_.refs_3_ = bf16[768,256]{1,0:T(8,128)(2,1)S(1)} collective-permute-done((bf16[768,256]{1,0:T(8,128)(2,1)S(1)}, bf16[768,256]{1,0:T(8,128)(2,1)S(1)}, u32[]{:S(2)}, u32[]{:S(2)}) %collective-permute-start.7) | collective-permute-done | bytes 393248 | tf_op jit(solution)/shard_map/ppermute | solution.py:255
  33.6 1.6 collective-permute-start.2
  35.2 1.6 collective-permute-start.3
  37.3 1.7 collective-permute-done.10.refs_9_.refs_6_
  39.6 10.6 %collective-permute-done.1.refs_2_ = bf16[160,2048]{1,0:T(8,128)(2,1)S(1)} collective-permute-done((bf16[160,2048]{1,0:T(8,128)(2,1)S(1)}, bf16[160,2048]{1,0:T(8,128)(2,1)S(1)}, u32[]{:S(2)}, u32[]{:S(2)}) %collective-permute-start.1) | collective-permute-done | bytes 655392 | tf_op jit(solution)/shard_map/ppermute | solution.py:255
  51.9 3.7 %collective-permute-start.17 = (bf16[160,2048]{1,0:T(8,128)(2,1)}, bf16[160,2048]{1,0:T(8,128)(2,1)}, u32[]{:S(2)}, u32[]{:S(2)}) collective-permute-start(bf16[160,2048]{1,0:T(8,128)(2,1)} %collective-permute-done.refs_1_), channel_id=1, source_target_pairs={{0,24},{8,0},{16,8},{24,16},{1,25},{9,1},{17,9},{25,17},{2,26},{10... | collective-permute-start | bytes 1966088 | tf_op jit(solution)/shard_map/ppermute | solution.py:255
  55.6 1.3 collective-permute-done.3.refs_4_
  60.7 6.0 %project.2 = (bf16[1440,128]{1,0:T(8,128)(2,1)S(1)}, bf16[1440,128]{1,0:T(8,128)(2,1)S(1)}, bf16[1440,128]{1,0:T(8,128)(2,1)S(1)}, bf16[1440,128]{1,0:T(8,128)(2,1)S(1)}) custom-call(s32[8]{0:T(128)S(1)} %stack.146.idx_ref.col_ref, f32[2,64]{1,0:T(2,128)S(1)} %copy-done.11, bf16[320,2048]{1,0:T(8,128)(2,1)S(1)} %bitcast.45, ...), custom_call_target="tpu_custom_call" | custom-call | tf_op jit(solution)/shard_map/project/pallas_call | solution.py:204
  66.9 5.7 %collective-permute-start.22 = (bf16[256,256]{1,0:T(8,128)(2,1)S(1)}, bf16[256,256]{1,0:T(8,128)(2,1)S(1)}, u32[]{:S(2)}, u32[]{:S(2)}) collective-permute-start(bf16[256,256]{1,0:T(8,128)(2,1)S(1)} %get-tuple-element.43.refs_0_), channel_id=1, source_target_pairs={{0,6},{2,0},{4,2},{6,4},{1,7},{3,1},{5,3},{7,5},{8,14},{10,8},{12,... | collective-permute-start | bytes 393224 | tf_op jit(solution)/shard_map/ppermute | solution.py:255
  72.5 3.9 %collective-permute-done.22.refs_1_ = bf16[256,256]{1,0:T(8,128)(2,1)S(1)} collective-permute-done((bf16[256,256]{1,0:T(8,128)(2,1)S(1)}, bf16[256,256]{1,0:T(8,128)(2,1)S(1)}, u32[]{:S(2)}, u32[]{:S(2)}) %collective-permute-start.22) | collective-permute-done | bytes 131104 | tf_op jit(solution)/shard_map/ppermute | solution.py:255
  76.5 3.1 %collective-permute-done.23.refs_2_ = bf16[256,256]{1,0:T(8,128)(2,1)S(1)} collective-permute-done((bf16[256,256]{1,0:T(8,128)(2,1)S(1)}, bf16[256,256]{1,0:T(8,128)(2,1)S(1)}, u32[]{:S(2)}, u32[]{:S(2)}) %collective-permute-start.23) | collective-permute-done | bytes 131104 | tf_op jit(solution)/shard_map/ppermute | solution.py:255
  80.4 2.6 %collective-permute-done.24.refs_3_ = bf16[256,256]{1,0:T(8,128)(2,1)S(1)} collective-permute-done((bf16[256,256]{1,0:T(8,128)(2,1)S(1)}, bf16[256,256]{1,0:T(8,128)(2,1)S(1)}, u32[]{:S(2)}, u32[]{:S(2)}) %collective-permute-start.24) | collective-permute-done | bytes 131104 | tf_op jit(solution)/shard_map/ppermute | solution.py:255
  83.1 1.7 collective-permute-start.25
  84.8 3.0 %collective-permute-start.26 = (bf16[1024,256]{1,0:T(8,128)(2,1)S(1)}, bf16[1024,256]{1,0:T(8,128)(2,1)}, u32[]{:S(2)}, u32[]{:S(2)}) collective-permute-start(bf16[1024,256]{1,0:T(8,128)(2,1)S(1)} %join.1.refs_0_), channel_id=1, source_target_pairs={{0,16},{8,24},{16,0},{24,8},{1,17},{9,25},{17,1},{25,9},{2,18},{10... | collective-permute-start | bytes 1572872 | tf_op jit(solution)/shard_map/ppermute | solution.py:255
  87.8 3.2 %collective-permute-start.16 = (bf16[1440,128]{1,0:T(8,128)(2,1)S(1)}, bf16[1440,128]{1,0:T(8,128)(2,1)S(1)}, u32[]{:S(2)}, u32[]{:S(2)}) collective-permute-start(bf16[1440,128]{1,0:T(8,128)(2,1)S(1)} %get-tuple-element.38), channel_id=1, source_target_pairs={{0,96},{32,0},{64,32},{96,64},{1,97},{33,1},{65,33},{97,65},{2,98}... | collective-permute-start | bytes 1105928 | tf_op jit(solution)/shard_map/ppermute | solution.py:255
  91.1 4.6 %project.3 = (bf16[480,128]{1,0:T(8,128)(2,1)S(1)}, bf16[480,128]{1,0:T(8,128)(2,1)S(1)}, bf16[480,128]{1,0:T(8,128)(2,1)}, bf16[480,128]{1,0:T(8,128)(2,1)S(1)}) custom-call(s32[8]{0:T(128)S(1)} %stack.146.idx_ref.col_ref, f32[2,64]{1,0:T(2,128)S(1)} %copy-done.11, bf16[160,2048]{1,0:T(8,128)(2,1)} %collective-permute-done.17.refs_0_, ...), custom_call_target="tpu_custom_call" | custom-call | tf_op jit(solution)/shard_map/project/pallas_call | solution.py:204
  97.2 1.6 collective-permute-start.20
  98.8 3.7 %collective-permute-done.19.refs_5_ = bf16[480,128]{1,0:T(8,128)(2,1)S(1)} collective-permute-done((bf16[480,128]{1,0:T(8,128)(2,1)S(1)}, bf16[480,128]{1,0:T(8,128)(2,1)S(1)}, u32[]{:S(2)}, u32[]{:S(2)}) %collective-permute-start.19) | collective-permute-done | bytes 122912 | tf_op jit(solution)/shard_map/ppermute | solution.py:255
  102.6 1.2 collective-permute-done.20.refs_6_
  103.8 3.6 %collective-permute-done.21.refs_7_ = bf16[480,128]{1,0:T(8,128)(2,1)S(1)} collective-permute-done((bf16[480,128]{1,0:T(8,128)(2,1)S(1)}, bf16[480,128]{1,0:T(8,128)(2,1)S(1)}, u32[]{:S(2)}, u32[]{:S(2)}) %collective-permute-start.21) | collective-permute-done | bytes 122912 | tf_op jit(solution)/shard_map/ppermute | solution.py:255
  110.4 41.7 %attention.1 = bf16[16,160,128]{2,1,0:T(8,128)(2,1)} custom-call(s32[16]{0:T(128)S(1)} %stack.159.pos_ref, f32[2,64]{1,0:T(2,128)S(1)} %copy-done.11, f32[8,640]{1,0:T(8,128)S(1)} %reshape.5.d_ref, bf16[1440,128]{1,0:T(8,128)(2,1)S(1)} %copy-done.6, bf16[1440,128]{1,0:T(8,128)(2,1)S(1)} %collective-permute-done.14.refs_1_, bf16[1440,128]{1,0:T(8,128)(2,1)S(1)} %copy-done.8, ...), custom_call_target="tpu_custom_call" | custom-call | tf_op jit(solution)/shard_map/attention/pallas_call | solution.py:118
  152.1 6.9 %all-to-all-start = ((bf16[16,160,128]{2,1,0:T(8,128)(2,1)}), bf16[16,160,128]{2,1,0:T(8,128)(2,1)S(1)}, u32[]{:S(2)}, u32[]{:S(2)}) async-start(bf16[16,160,128]{2,1,0:T(8,128)(2,1)} %attention.1), calls=%async_computation | async-start | bytes 1310720 | tf_op jit(solution)/shard_map/all_to_all | solution.py:292
  163.2 6.6 %all-to-all-done.heads_ref = bf16[16,160,128]{2,1,0:T(8,128)(2,1)S(1)} async-done(((bf16[16,160,128]{2,1,0:T(8,128)(2,1)}), bf16[16,160,128]{2,1,0:T(8,128)(2,1)S(1)}, u32[]{:S(2)}, u32[]{:S(2)}) %all-to-all-start) | async-done | bytes 655392 | tf_op jit(solution)/shard_map/all_to_all | solution.py:292
  169.8 4.1 %output.1 = bf16[320,2048]{1,0:T(8,128)(2,1)} custom-call(s32[16]{0:T(128)S(1)} %stack.137.head_ref, s32[8]{0:T(128)S(1)} %stack.146.idx_ref.col_ref, bf16[16,160,128]{2,1,0:T(8,128)(2,1)S(1)} %all-to-all-done.heads_ref, bf16[1024,256]{1,0:T(8,128)(2,1)S(1)} %join.1.refs_0_, bf16[1024,256]{1,0:T(8,128)(2,1)} %collective-permute-done.25.refs_1_, ...), custom_call_target="tpu_custom_call" | custom-call | tf_op jit(solution)/shard_map/output/pallas_call | solution.py:238
  (74 shorter events, 19.6 us)
Async XLA Ops:
  0.8 9.8 %collective-permute-start.4 = (bf16[256,256]{1,0:T(8,128)(2,1)S(1)}, bf16[256,256]{1,0:T(8,128)(2,1)S(1)}, u32[]{:S(2)}, u32[]{:S(2)}) collective-permute-start(bf16[256,256]{1,0:T(8,128)(2,1)S(1)} %pad_maximum_fusion.refs_0_), channel_id=1, source_target_pairs={{0,96},{32,0},{64,32},{96,64},{1,97},{33,1},{65,33},{97,65},{2,98}... | collective-permute-start | bytes 393224 | tf_op jit(solution)/shard_map/ppermute | solution.py:255
  5.0 7.9 %collective-permute-start.5 = (bf16[256,256]{1,0:T(8,128)(2,1)S(1)}, bf16[256,256]{1,0:T(8,128)(2,1)S(1)}, u32[]{:S(2)}, u32[]{:S(2)}) collective-permute-start(bf16[256,256]{1,0:T(8,128)(2,1)S(1)} %pad_maximum_fusion.refs_0_), channel_id=1, source_target_pairs={{0,64},{32,96},{64,0},{96,32},{1,65},{33,97},{65,1},{97,33},{2,66}... | collective-permute-start | bytes 393224 | tf_op jit(solution)/shard_map/ppermute | solution.py:255
  5.0 9.0 %collective-permute-start.6 = (bf16[256,256]{1,0:T(8,128)(2,1)S(1)}, bf16[256,256]{1,0:T(8,128)(2,1)S(1)}, u32[]{:S(2)}, u32[]{:S(2)}) collective-permute-start(bf16[256,256]{1,0:T(8,128)(2,1)S(1)} %pad_maximum_fusion.refs_0_), channel_id=1, source_target_pairs={{0,32},{32,64},{64,96},{96,0},{1,33},{33,65},{65,97},{97,1},{2,34}... | collective-permute-start | bytes 393224 | tf_op jit(solution)/shard_map/ppermute | solution.py:255
  14.1 19.6 %collective-permute-start.7 = (bf16[768,256]{1,0:T(8,128)(2,1)S(1)}, bf16[768,256]{1,0:T(8,128)(2,1)S(1)}, u32[]{:S(2)}, u32[]{:S(2)}) collective-permute-start(bf16[768,256]{1,0:T(8,128)(2,1)S(1)} %get-tuple-element.29.refs_5_.refs_2_), channel_id=1, source_target_pairs={{0,6},{2,0},{4,2},{6,4},{1,7},{3,1},{5,3},{7,5},{8,14},{10,8},{12,... | collective-permute-start | bytes 1179656 | tf_op jit(solution)/shard_map/ppermute | solution.py:255
  16.9 18.3 %collective-permute-start.8 = (bf16[768,256]{1,0:T(8,128)(2,1)S(1)}, bf16[768,256]{1,0:T(8,128)(2,1)S(1)}, u32[]{:S(2)}, u32[]{:S(2)}) collective-permute-start(bf16[768,256]{1,0:T(8,128)(2,1)S(1)} %get-tuple-element.29.refs_5_.refs_2_), channel_id=1, source_target_pairs={{0,4},{2,6},{4,0},{6,2},{1,5},{3,7},{5,1},{7,3},{8,12},{10,14},{12... | collective-permute-start | bytes 1179656 | tf_op jit(solution)/shard_map/ppermute | solution.py:255
  17.7 19.6 %collective-permute-start.9 = (bf16[768,256]{1,0:T(8,128)(2,1)S(1)}, bf16[768,256]{1,0:T(8,128)(2,1)S(1)}, u32[]{:S(2)}, u32[]{:S(2)}) collective-permute-start(bf16[768,256]{1,0:T(8,128)(2,1)S(1)} %get-tuple-element.29.refs_5_.refs_2_), channel_id=1, source_target_pairs={{0,2},{2,4},{4,6},{6,0},{1,3},{3,5},{5,7},{7,1},{8,10},{10,12},{12... | collective-permute-start | bytes 1179656 | tf_op jit(solution)/shard_map/ppermute | solution.py:255
  20.0 19.1 %collective-permute-start = (bf16[160,2048]{1,0:T(8,128)(2,1)S(1)}, bf16[160,2048]{1,0:T(8,128)(2,1)}, u32[]{:S(2)}, u32[]{:S(2)}) collective-permute-start(bf16[160,2048]{1,0:T(8,128)(2,1)S(1)} %get-tuple-element.50), channel_id=1, source_target_pairs={{0,24},{8,0},{16,8},{24,16},{1,25},{9,1},{17,9},{25,17},{2,26},{10... | collective-permute-start | bytes 1966088 | tf_op jit(solution)/shard_map/ppermute | solution.py:255
  23.1 27.1 %collective-permute-start.1 = (bf16[160,2048]{1,0:T(8,128)(2,1)S(1)}, bf16[160,2048]{1,0:T(8,128)(2,1)S(1)}, u32[]{:S(2)}, u32[]{:S(2)}) collective-permute-start(bf16[160,2048]{1,0:T(8,128)(2,1)S(1)} %get-tuple-element.49), channel_id=1, source_target_pairs={{0,24},{8,0},{16,8},{24,16},{1,25},{9,1},{17,9},{25,17},{2,26},{10... | collective-permute-start | bytes 1966088 | tf_op jit(solution)/shard_map/ppermute | solution.py:255
  33.6 17.4 %collective-permute-start.2 = (bf16[160,2048]{1,0:T(8,128)(2,1)S(1)}, bf16[160,2048]{1,0:T(8,128)(2,1)S(1)}, u32[]{:S(2)}, u32[]{:S(2)}) collective-permute-start(bf16[160,2048]{1,0:T(8,128)(2,1)S(1)} %get-tuple-element.50), channel_id=1, source_target_pairs={{0,8},{8,16},{16,24},{24,0},{1,9},{9,17},{17,25},{25,1},{2,10},{10... | collective-permute-start | bytes 1966088 | tf_op jit(solution)/shard_map/ppermute | solution.py:255
  35.2 21.7 %collective-permute-start.3 = (bf16[160,2048]{1,0:T(8,128)(2,1)S(1)}, bf16[160,2048]{1,0:T(8,128)(2,1)}, u32[]{:S(2)}, u32[]{:S(2)}) collective-permute-start(bf16[160,2048]{1,0:T(8,128)(2,1)S(1)} %get-tuple-element.49), channel_id=1, source_target_pairs={{0,8},{8,16},{16,24},{24,0},{1,9},{9,17},{17,25},{25,1},{2,10},{10... | collective-permute-start | bytes 1966088 | tf_op jit(solution)/shard_map/ppermute | solution.py:255
  39.0 19.5 %collective-permute-start.11 = (bf16[768,256]{1,0:T(8,128)(2,1)S(1)}, bf16[768,256]{1,0:T(8,128)(2,1)}, u32[]{:S(2)}, u32[]{:S(2)}) collective-permute-start(bf16[768,256]{1,0:T(8,128)(2,1)S(1)} %collective-permute-done.7.refs_6_.refs_3_), channel_id=1, source_target_pairs={{0,1},{1,0},{2,3},{3,2},{4,5},{5,4},{6,7},{7,6},{8,9},{9,8},{10,11... | collective-permute-start | bytes 1179656 | tf_op jit(solution)/shard_map/ppermute | solution.py:255
  39.2 19.3 %collective-permute-start.12 = (bf16[768,256]{1,0:T(8,128)(2,1)S(1)}, bf16[768,256]{1,0:T(8,128)(2,1)}, u32[]{:S(2)}, u32[]{:S(2)}) collective-permute-start(bf16[768,256]{1,0:T(8,128)(2,1)S(1)} %collective-permute-done.8.refs_7_.refs_4_), channel_id=1, source_target_pairs={{0,1},{1,0},{2,3},{3,2},{4,5},{5,4},{6,7},{7,6},{8,9},{9,8},{10,11... | collective-permute-start | bytes 1179656 | tf_op jit(solution)/shard_map/ppermute | solution.py:255
  51.0 7.5 %collective-permute-start.13 = (bf16[768,256]{1,0:T(8,128)(2,1)S(1)}, bf16[768,256]{1,0:T(8,128)(2,1)}, u32[]{:S(2)}, u32[]{:S(2)}) collective-permute-start(bf16[768,256]{1,0:T(8,128)(2,1)S(1)} %collective-permute-done.9.refs_8_.refs_5_), channel_id=1, source_target_pairs={{0,1},{1,0},{2,3},{3,2},{4,5},{5,4},{6,7},{7,6},{8,9},{9,8},{10,11... | collective-permute-start | bytes 1179656 | tf_op jit(solution)/shard_map/ppermute | solution.py:255
  51.9 35.9 %collective-permute-start.17 = (bf16[160,2048]{1,0:T(8,128)(2,1)}, bf16[160,2048]{1,0:T(8,128)(2,1)}, u32[]{:S(2)}, u32[]{:S(2)}) collective-permute-start(bf16[160,2048]{1,0:T(8,128)(2,1)} %collective-permute-done.refs_1_), channel_id=1, source_target_pairs={{0,24},{8,0},{16,8},{24,16},{1,25},{9,1},{17,9},{25,17},{2,26},{10... | collective-permute-start | bytes 1966088 | tf_op jit(solution)/shard_map/ppermute | solution.py:255
  56.9 30.9 %collective-permute-start.18 = (bf16[160,2048]{1,0:T(8,128)(2,1)}, bf16[160,2048]{1,0:T(8,128)(2,1)}, u32[]{:S(2)}, u32[]{:S(2)}) collective-permute-start(bf16[160,2048]{1,0:T(8,128)(2,1)} %collective-permute-done.3.refs_4_), channel_id=1, source_target_pairs={{0,8},{8,16},{16,24},{24,0},{1,9},{9,17},{17,25},{25,1},{2,10},{10... | collective-permute-start | bytes 1966088 | tf_op jit(solution)/shard_map/ppermute | solution.py:255
  66.8 18.0 %collective-permute-start.14 = (bf16[1440,128]{1,0:T(8,128)(2,1)S(1)}, bf16[1440,128]{1,0:T(8,128)(2,1)S(1)}, u32[]{:S(2)}, u32[]{:S(2)}) collective-permute-start(bf16[1440,128]{1,0:T(8,128)(2,1)S(1)} %get-tuple-element.36), channel_id=1, source_target_pairs={{0,32},{32,64},{64,96},{96,0},{1,33},{33,65},{65,97},{97,1},{2,34}... | collective-permute-start | bytes 1105928 | tf_op jit(solution)/shard_map/ppermute | solution.py:255
  66.9 9.6 %collective-permute-start.22 = (bf16[256,256]{1,0:T(8,128)(2,1)S(1)}, bf16[256,256]{1,0:T(8,128)(2,1)S(1)}, u32[]{:S(2)}, u32[]{:S(2)}) collective-permute-start(bf16[256,256]{1,0:T(8,128)(2,1)S(1)} %get-tuple-element.43.refs_0_), channel_id=1, source_target_pairs={{0,6},{2,0},{4,2},{6,4},{1,7},{3,1},{5,3},{7,5},{8,14},{10,8},{12,... | collective-permute-start | bytes 393224 | tf_op jit(solution)/shard_map/ppermute | solution.py:255
  72.5 7.0 %collective-permute-start.23 = (bf16[256,256]{1,0:T(8,128)(2,1)S(1)}, bf16[256,256]{1,0:T(8,128)(2,1)S(1)}, u32[]{:S(2)}, u32[]{:S(2)}) collective-permute-start(bf16[256,256]{1,0:T(8,128)(2,1)S(1)} %get-tuple-element.43.refs_0_), channel_id=1, source_target_pairs={{0,4},{2,6},{4,0},{6,2},{1,5},{3,7},{5,1},{7,3},{8,12},{10,14},{12... | collective-permute-start | bytes 393224 | tf_op jit(solution)/shard_map/ppermute | solution.py:255
  76.5 6.6 %collective-permute-start.24 = (bf16[256,256]{1,0:T(8,128)(2,1)S(1)}, bf16[256,256]{1,0:T(8,128)(2,1)S(1)}, u32[]{:S(2)}, u32[]{:S(2)}) collective-permute-start(bf16[256,256]{1,0:T(8,128)(2,1)S(1)} %get-tuple-element.43.refs_0_), channel_id=1, source_target_pairs={{0,2},{2,4},{4,6},{6,0},{1,3},{3,5},{5,7},{7,1},{8,10},{10,12},{12... | collective-permute-start | bytes 393224 | tf_op jit(solution)/shard_map/ppermute | solution.py:255
  79.6 16.1 %collective-permute-start.15 = (bf16[1440,128]{1,0:T(8,128)(2,1)S(1)}, bf16[1440,128]{1,0:T(8,128)(2,1)S(1)}, u32[]{:S(2)}, u32[]{:S(2)}) collective-permute-start(bf16[1440,128]{1,0:T(8,128)(2,1)S(1)} %get-tuple-element.37), channel_id=1, source_target_pairs={{0,64},{32,96},{64,0},{96,32},{1,65},{33,97},{65,1},{97,33},{2,66}... | collective-permute-start | bytes 1105928 | tf_op jit(solution)/shard_map/ppermute | solution.py:255
  83.1 69.0 %collective-permute-start.25 = (bf16[1024,256]{1,0:T(8,128)(2,1)S(1)}, bf16[1024,256]{1,0:T(8,128)(2,1)}, u32[]{:S(2)}, u32[]{:S(2)}) collective-permute-start(bf16[1024,256]{1,0:T(8,128)(2,1)S(1)} %join.1.refs_0_), channel_id=1, source_target_pairs={{0,24},{8,0},{16,8},{24,16},{1,25},{9,1},{17,9},{25,17},{2,26},{10... | collective-permute-start | bytes 1572872 | tf_op jit(solution)/shard_map/ppermute | solution.py:255
  84.8 67.3 %collective-permute-start.26 = (bf16[1024,256]{1,0:T(8,128)(2,1)S(1)}, bf16[1024,256]{1,0:T(8,128)(2,1)}, u32[]{:S(2)}, u32[]{:S(2)}) collective-permute-start(bf16[1024,256]{1,0:T(8,128)(2,1)S(1)} %join.1.refs_0_), channel_id=1, source_target_pairs={{0,16},{8,24},{16,0},{24,8},{1,17},{9,25},{17,1},{25,9},{2,18},{10... | collective-permute-start | bytes 1572872 | tf_op jit(solution)/shard_map/ppermute | solution.py:255
  87.8 64.2 %collective-permute-start.27 = (bf16[1024,256]{1,0:T(8,128)(2,1)S(1)}, bf16[1024,256]{1,0:T(8,128)(2,1)}, u32[]{:S(2)}, u32[]{:S(2)}) collective-permute-start(bf16[1024,256]{1,0:T(8,128)(2,1)S(1)} %join.1.refs_0_), channel_id=1, source_target_pairs={{0,8},{8,16},{16,24},{24,0},{1,9},{9,17},{17,25},{25,1},{2,10},{10... | collective-permute-start | bytes 1572872 | tf_op jit(solution)/shard_map/ppermute | solution.py:255
  87.8 8.6 %collective-permute-start.16 = (bf16[1440,128]{1,0:T(8,128)(2,1)S(1)}, bf16[1440,128]{1,0:T(8,128)(2,1)S(1)}, u32[]{:S(2)}, u32[]{:S(2)}) collective-permute-start(bf16[1440,128]{1,0:T(8,128)(2,1)S(1)} %get-tuple-element.38), channel_id=1, source_target_pairs={{0,96},{32,0},{64,32},{96,64},{1,97},{33,1},{65,33},{97,65},{2,98}... | collective-permute-start | bytes 1105928 | tf_op jit(solution)/shard_map/ppermute | solution.py:255
  96.4 6.1 %collective-permute-start.19 = (bf16[480,128]{1,0:T(8,128)(2,1)S(1)}, bf16[480,128]{1,0:T(8,128)(2,1)S(1)}, u32[]{:S(2)}, u32[]{:S(2)}) collective-permute-start(bf16[480,128]{1,0:T(8,128)(2,1)S(1)} %get-tuple-element.40), channel_id=1, source_target_pairs={{0,32},{32,64},{64,96},{96,0},{1,33},{33,65},{65,97},{97,1},{2,34}... | collective-permute-start | bytes 368648 | tf_op jit(solution)/shard_map/ppermute | solution.py:255
  97.2 6.6 %collective-permute-start.20 = (bf16[480,128]{1,0:T(8,128)(2,1)}, bf16[480,128]{1,0:T(8,128)(2,1)S(1)}, u32[]{:S(2)}, u32[]{:S(2)}) collective-permute-start(bf16[480,128]{1,0:T(8,128)(2,1)} %get-tuple-element.41), channel_id=1, source_target_pairs={{0,64},{32,96},{64,0},{96,32},{1,65},{33,97},{65,1},{97,33},{2,66}... | collective-permute-start | bytes 368648 | tf_op jit(solution)/shard_map/ppermute | solution.py:255
  102.5 4.9 %collective-permute-start.21 = (bf16[480,128]{1,0:T(8,128)(2,1)S(1)}, bf16[480,128]{1,0:T(8,128)(2,1)S(1)}, u32[]{:S(2)}, u32[]{:S(2)}) collective-permute-start(bf16[480,128]{1,0:T(8,128)(2,1)S(1)} %get-tuple-element.42), channel_id=1, source_target_pairs={{0,96},{32,0},{64,32},{96,64},{1,97},{33,1},{65,33},{97,65},{2,98}... | collective-permute-start | bytes 368648 | tf_op jit(solution)/shard_map/ppermute | solution.py:255
  152.1 17.8 %all-to-all-start = ((bf16[16,160,128]{2,1,0:T(8,128)(2,1)}), bf16[16,160,128]{2,1,0:T(8,128)(2,1)S(1)}, u32[]{:S(2)}, u32[]{:S(2)}) async-start(bf16[16,160,128]{2,1,0:T(8,128)(2,1)} %attention.1), calls=%async_computation | async-start | bytes 1310720 | tf_op jit(solution)/shard_map/all_to_all | solution.py:292
  159.0 2.0 %collective-permute-start.28 = (bf16[1024,256]{1,0:T(8,128)(2,1)S(1)}, bf16[1024,256]{1,0:T(8,128)(2,1)S(1)}, u32[]{:S(2)}, u32[]{:S(2)}) collective-permute-start(bf16[1024,256]{1,0:T(8,128)(2,1)S(1)} %join.1.refs_0_), channel_id=1, source_target_pairs={{0,1},{1,0},{2,3},{3,2},{4,5},{5,4},{6,7},{7,6},{8,9},{9,8},{10,11... | collective-permute-start | bytes 1572872 | tf_op jit(solution)/shard_map/ppermute | solution.py:255
  159.1 2.6 %collective-permute-start.29 = (bf16[1024,256]{1,0:T(8,128)(2,1)}, bf16[1024,256]{1,0:T(8,128)(2,1)S(1)}, u32[]{:S(2)}, u32[]{:S(2)}) collective-permute-start(bf16[1024,256]{1,0:T(8,128)(2,1)} %collective-permute-done.25.refs_1_), channel_id=1, source_target_pairs={{0,1},{1,0},{2,3},{3,2},{4,5},{5,4},{6,7},{7,6},{8,9},{9,8},{10,11... | collective-permute-start | bytes 1572872 | tf_op jit(solution)/shard_map/ppermute | solution.py:255
  159.6 2.9 %collective-permute-start.30 = (bf16[1024,256]{1,0:T(8,128)(2,1)}, bf16[1024,256]{1,0:T(8,128)(2,1)S(1)}, u32[]{:S(2)}, u32[]{:S(2)}) collective-permute-start(bf16[1024,256]{1,0:T(8,128)(2,1)} %collective-permute-done.26.refs_2_), channel_id=1, source_target_pairs={{0,1},{1,0},{2,3},{3,2},{4,5},{5,4},{6,7},{7,6},{8,9},{9,8},{10,11... | collective-permute-start | bytes 1572872 | tf_op jit(solution)/shard_map/ppermute | solution.py:255
  159.7 3.6 %collective-permute-start.31 = (bf16[1024,256]{1,0:T(8,128)(2,1)}, bf16[1024,256]{1,0:T(8,128)(2,1)S(1)}, u32[]{:S(2)}, u32[]{:S(2)}) collective-permute-start(bf16[1024,256]{1,0:T(8,128)(2,1)} %collective-permute-done.27.refs_3_), channel_id=1, source_target_pairs={{0,1},{1,0},{2,3},{3,2},{4,5},{5,4},{6,7},{7,6},{8,9},{9,8},{10,11... | collective-permute-start | bytes 1572872 | tf_op jit(solution)/shard_map/ppermute | solution.py:255
  (14 other events, 171.6 us)

commit v3 on v2

--- a/solution.py
+++ b/solution.py
@@ -255,6 +255,11 @@
     return lax.ppermute(value, axis, pairs)
 
 
+def spread(value, step):
+    pairs = [(2 * i + k, 2 * ((i + (step, -step)[k]) % 4) + k) for i in range(4) for k in (0, 1)]
+    return lax.ppermute(value, (Y, C), pairs)
+
+
 def around(value, axis):
     return [value] + [move(value, axis, -d) for d in (1, 2, 3)]
 
@@ -262,10 +267,10 @@
 def on_device(tokens, w_query, w_key, w_value, w_output, qk_gain, decay_sums):
     own = tokens[0]
     z, y, x, c = (lax.axis_index(a) for a in (Z, Y, X, C))
-    top, bot = own[:160], own[160:]
-    t1 = [move(top, Y, -1), move(bot, Y, -1)]
-    t3 = [move(top, Y, 1), move(bot, Y, 1)]
-    t2 = [move(t1[0], Y, -1), move(t3[1], Y, 1)]
+    t1 = spread(own, -1)
+    t3 = spread(own, 1)
+    t2 = spread(t1, -1)
+    near = jnp.where(c == 0, 1, 3)
     piece = jnp.concatenate([w_query.T, w_key.T, w_value.T, w_output], 0)
     w4, wo4 = pack(around(piece, Z))
     ws = around(w4, X)
@@ -275,15 +280,15 @@
         [2 * ((x + d) % 4) + e for e in (c, 1 - c) for d in range(4)]
     ).astype(jnp.int32)
     gain, decay = lax.optimization_barrier((qk_gain, decay_sums.reshape(8, 640)))
-    part1 = project(cols, gain, [[own], t1, t3], ws)
+    part1 = project(cols, gain, [[own], [t1], [t3]], ws)
     *part1, wo4 = lax.optimization_barrier((*part1, wo4))
-    part2 = project(cols, gain, [t2], ws)
+    part2 = project(cols, gain, [[t2]], ws)
     recv = []
     for part in (part1, part2):
         recv += [part[0]] + [move(part[d], Z, d) for d in (1, 2, 3)]
     wo16 = join(around(wo4, X))
     wo = around(wo16, Y)
-    pos = [4 * ((z - d) % 4) + (y + e) % 4 for d in range(4) for e in (0, 1, 3)]
+    pos = [4 * ((z - d) % 4) + (y + e) % 4 for d in range(4) for e in (0, near, 4 - near)]
     pos += [4 * ((z - d) % 4) + (y + 2) % 4 for d in range(4)]
     pos = jnp.stack(pos).astype(jnp.int32)
     heads = attention(pos, gain, decay, recv, (3, 3, 3, 3, 1, 1, 1, 1))

time: 175 us -> 165 us (0.943)
  waiting for transfers between devices: 59.5 us -> 41.9 us
  starting transfers between devices: 45.7 us -> 51.7 us
    ppermute x32 -> x26, waiting for transfers between devices: 52.9 us -> 25.4 us  [move(): return lax.ppermute(value, axis, pairs)]
    ppermute x0 -> x3, waiting for transfers between devices: none -> 9.88 us  [spread(): return lax.ppermute(value, (Y, C), pairs)]
    ppermute x0 -> x3, starting transfers between devices: none -> 6.82 us  [spread(): return lax.ppermute(value, (Y, C), pairs)]
    unnamed x27 -> x33, local copies, waits for them, and re-layouts: 8.87 us -> 11.3 us
    ppermute x32 -> x26, starting transfers between devices: 38.8 us -> 39.4 us  [move(): return lax.ppermute(value, axis, pairs)]
  transfers between devices with their start and end apart: 33 -> 30, of which waited for: 19 -> 15; matrix products, arithmetic and copies ran while one was open for 2% -> 2% of each run, Pallas kernels for 30% -> 32%
where the time goes in v3:
time: 165 us; the launch traced here: 164 us
  Pallas kernels  56.3 us (34%)
  starting transfers between devices  51.7 us (31%)
  waiting for transfers between devices  41.9 us (25%)
  local copies, waits for them, and re-layouts  12.1 us (7%)
  other arithmetic  2.23 us (1%)
    pallas_call x1, Pallas kernels, attention(): pl.pallas_call(functools.partial(attn_kernel, nblk=nblk), out_shape=jax.S...  41.7 us
    ppermute x26, starting transfers between devices, move(): return lax.ppermute(value, axis, pairs)  39.4 us
    ppermute x26, waiting for transfers between devices, move(): return lax.ppermute(value, axis, pairs)  25.4 us
    unnamed x33, local copies, waits for them, and re-layouts  11.3 us
    pallas_call x2, Pallas kernels, project(): pl.pallas_call(functools.partial(proj_kernel, sizes=tuple((len(b) for b i...  10.4 us
    ppermute x3, waiting for transfers between devices, spread(): return lax.ppermute(value, (Y, C), pairs)  9.88 us
    ppermute x3, starting transfers between devices, spread(): return lax.ppermute(value, (Y, C), pairs)  6.82 us
    all_to_all x1, waiting for transfers between devices, on_device(): merged = lax.all_to_all(heads, SP, 0, 0, tiled=True)  6.6 us
  transfers between devices with their start and end apart: 30, of which 15 were waited for; matrix products, arithmetic and copies ran while one was open for 2% of the time, Pallas kernels for 32%

profile of v3, /device:TPU:0, one launch (start us, length us, event | category | flops | bytes accessed | tf_op | source)
XLA Modules:
  0.0 164.4 jit_solution(6084621794967159694)
XLA Ops:
  0.0 3.1 %collective-permute-start = (bf16[320,2048]{1,0:T(8,128)(2,1)}, bf16[320,2048]{1,0:T(8,128)(2,1)}, u32[]{:S(2)}, u32[]{:S(2)}) collective-permute-start(bf16[320,2048]{1,0:T(8,128)(2,1)} %bitcast.43), channel_id=1, source_target_pairs={{0,24},{1,9},{8,0},{9,17},{16,8},{17,25},{24,16},{25,1},{2,26},{3,... | collective-permute-start | bytes 3932168 | tf_op jit(solution)/shard_map/ppermute | solution.py:260
  3.9 4.1 %collective-permute-start.2 = (bf16[256,256]{1,0:T(8,128)(2,1)S(1)}, bf16[256,256]{1,0:T(8,128)(2,1)S(1)}, u32[]{:S(2)}, u32[]{:S(2)}) collective-permute-start(bf16[256,256]{1,0:T(8,128)(2,1)S(1)} %pad_maximum_fusion.refs_0_), channel_id=1, source_target_pairs={{0,96},{32,0},{64,32},{96,64},{1,97},{33,1},{65,33},{97,65},{2,98}... | collective-permute-start | bytes 393224 | tf_op jit(solution)/shard_map/ppermute | solution.py:255
  8.1 1.3 collective-permute-start.4
  9.3 2.8 %collective-permute-done.2.refs_1_ = bf16[256,256]{1,0:T(8,128)(2,1)S(1)} collective-permute-done((bf16[256,256]{1,0:T(8,128)(2,1)S(1)}, bf16[256,256]{1,0:T(8,128)(2,1)S(1)}, u32[]{:S(2)}, u32[]{:S(2)}) %collective-permute-start.2) | collective-permute-done | bytes 131104 | tf_op jit(solution)/shard_map/ppermute | solution.py:255
  12.2 2.5 %collective-permute-done.3.refs_2_ = bf16[256,256]{1,0:T(8,128)(2,1)S(1)} collective-permute-done((bf16[256,256]{1,0:T(8,128)(2,1)S(1)}, bf16[256,256]{1,0:T(8,128)(2,1)S(1)}, u32[]{:S(2)}, u32[]{:S(2)}) %collective-permute-start.3) | collective-permute-done | bytes 131104 | tf_op jit(solution)/shard_map/ppermute | solution.py:255
  14.6 1.0 collective-permute-done.4.refs_3_
  15.7 2.8 %collective-permute-start.5 = (bf16[768,256]{1,0:T(8,128)(2,1)S(1)}, bf16[768,256]{1,0:T(8,128)(2,1)S(1)}, u32[]{:S(2)}, u32[]{:S(2)}) collective-permute-start(bf16[768,256]{1,0:T(8,128)(2,1)S(1)} %get-tuple-element.29.refs_3_.refs_1_), channel_id=1, source_target_pairs={{0,6},{2,0},{4,2},{6,4},{1,7},{3,1},{5,3},{7,5},{8,14},{10,8},{12,... | collective-permute-start | bytes 1179656 | tf_op jit(solution)/shard_map/ppermute | solution.py:255
  18.5 9.9 %collective-permute-done.refs_1_ = bf16[320,2048]{1,0:T(8,128)(2,1)} collective-permute-done((bf16[320,2048]{1,0:T(8,128)(2,1)}, bf16[320,2048]{1,0:T(8,128)(2,1)}, u32[]{:S(2)}, u32[]{:S(2)}) %collective-permute-start) | collective-permute-done | bytes 1310752 | tf_op jit(solution)/shard_map/ppermute | solution.py:260
  28.4 3.7 %collective-permute-start.15 = (bf16[320,2048]{1,0:T(8,128)(2,1)}, bf16[320,2048]{1,0:T(8,128)(2,1)}, u32[]{:S(2)}, u32[]{:S(2)}) collective-permute-start(bf16[320,2048]{1,0:T(8,128)(2,1)} %collective-permute-done.refs_1_), channel_id=1, source_target_pairs={{0,24},{1,9},{8,0},{9,17},{16,8},{17,25},{24,16},{25,1},{2,26},{3,... | collective-permute-start | bytes 3932168 | tf_op jit(solution)/shard_map/ppermute | solution.py:260
  32.1 3.0 %collective-permute-start.6 = (bf16[768,256]{1,0:T(8,128)(2,1)S(1)}, bf16[768,256]{1,0:T(8,128)(2,1)S(1)}, u32[]{:S(2)}, u32[]{:S(2)}) collective-permute-start(bf16[768,256]{1,0:T(8,128)(2,1)S(1)} %get-tuple-element.29.refs_3_.refs_1_), channel_id=1, source_target_pairs={{0,4},{2,6},{4,0},{6,2},{1,5},{3,7},{5,1},{7,3},{8,12},{10,14},{12... | collective-permute-start | bytes 1179656 | tf_op jit(solution)/shard_map/ppermute | solution.py:255
  35.7 5.8 %collective-permute-done.6.refs_5_.refs_3_ = bf16[768,256]{1,0:T(8,128)(2,1)S(1)} collective-permute-done((bf16[768,256]{1,0:T(8,128)(2,1)S(1)}, bf16[768,256]{1,0:T(8,128)(2,1)S(1)}, u32[]{:S(2)}, u32[]{:S(2)}) %collective-permute-start.6) | collective-permute-done | bytes 393248 | tf_op jit(solution)/shard_map/ppermute | solution.py:255
  41.5 4.1 %collective-permute-done.7.refs_6_.refs_4_ = bf16[768,256]{1,0:T(8,128)(2,1)S(1)} collective-permute-done((bf16[768,256]{1,0:T(8,128)(2,1)S(1)}, bf16[768,256]{1,0:T(8,128)(2,1)S(1)}, u32[]{:S(2)}, u32[]{:S(2)}) %collective-permute-start.7) | collective-permute-done | bytes 393248 | tf_op jit(solution)/shard_map/ppermute | solution.py:255
  46.7 1.4 reduce.3
  48.8 1.4 copy-done.2
  51.0 6.1 %project.2 = (bf16[1440,128]{1,0:T(8,128)(2,1)S(1)}, bf16[1440,128]{1,0:T(8,128)(2,1)S(1)}, bf16[1440,128]{1,0:T(8,128)(2,1)S(1)}, bf16[1440,128]{1,0:T(8,128)(2,1)S(1)}) custom-call(s32[8]{0:T(128)S(1)} %stack.150.idx_ref.col_ref, f32[2,64]{1,0:T(2,128)S(1)} %copy-done.14, bf16[320,2048]{1,0:T(8,128)(2,1)S(1)} %bitcast.45, ...), custom_call_target="tpu_custom_call" | custom-call | tf_op jit(solution)/shard_map/project/pallas_call | solution.py:204
  57.8 1.6 collective-permute-start.12
  60.0 3.1 %collective-permute-start.20 = (bf16[256,256]{1,0:T(8,128)(2,1)S(1)}, bf16[256,256]{1,0:T(8,128)(2,1)S(1)}, u32[]{:S(2)}, u32[]{:S(2)}) collective-permute-start(bf16[256,256]{1,0:T(8,128)(2,1)S(1)} %get-tuple-element.43.refs_0_), channel_id=1, source_target_pairs={{0,4},{2,6},{4,0},{6,2},{1,5},{3,7},{5,1},{7,3},{8,12},{10,14},{12... | collective-permute-start | bytes 393224 | tf_op jit(solution)/shard_map/ppermute | solution.py:255
  63.1 2.7 %collective-permute-done.19.refs_1_ = bf16[256,256]{1,0:T(8,128)(2,1)S(1)} collective-permute-done((bf16[256,256]{1,0:T(8,128)(2,1)S(1)}, bf16[256,256]{1,0:T(8,128)(2,1)S(1)}, u32[]{:S(2)}, u32[]{:S(2)}) %collective-permute-start.19) | collective-permute-done | bytes 131104 | tf_op jit(solution)/shard_map/ppermute | solution.py:255
  65.8 5.7 %collective-permute-start.13 = (bf16[1440,128]{1,0:T(8,128)(2,1)S(1)}, bf16[1440,128]{1,0:T(8,128)(2,1)S(1)}, u32[]{:S(2)}, u32[]{:S(2)}) collective-permute-start(bf16[1440,128]{1,0:T(8,128)(2,1)S(1)} %get-tuple-element.37), channel_id=1, source_target_pairs={{0,64},{32,96},{64,0},{96,32},{1,65},{33,97},{65,1},{97,33},{2,66}... | collective-permute-start | bytes 1105928 | tf_op jit(solution)/shard_map/ppermute | solution.py:255
  72.4 1.7 %collective-permute-start.22 = (bf16[1024,256]{1,0:T(8,128)(2,1)S(1)}, bf16[1024,256]{1,0:T(8,128)(2,1)}, u32[]{:S(2)}, u32[]{:S(2)}) collective-permute-start(bf16[1024,256]{1,0:T(8,128)(2,1)S(1)} %join.1.refs_0_), channel_id=1, source_target_pairs={{0,24},{8,0},{16,8},{24,16},{1,25},{9,1},{17,9},{25,17},{2,26},{10... | collective-permute-start | bytes 1572872 | tf_op jit(solution)/shard_map/ppermute | solution.py:255
  74.1 2.2 %collective-permute-start.23 = (bf16[1024,256]{1,0:T(8,128)(2,1)S(1)}, bf16[1024,256]{1,0:T(8,128)(2,1)}, u32[]{:S(2)}, u32[]{:S(2)}) collective-permute-start(bf16[1024,256]{1,0:T(8,128)(2,1)S(1)} %join.1.refs_0_), channel_id=1, source_target_pairs={{0,16},{8,24},{16,0},{24,8},{1,17},{9,25},{17,1},{25,9},{2,18},{10... | collective-permute-start | bytes 1572872 | tf_op jit(solution)/shard_map/ppermute | solution.py:255
  77.5 2.6 %collective-permute-start.14 = (bf16[1440,128]{1,0:T(8,128)(2,1)S(1)}, bf16[1440,128]{1,0:T(8,128)(2,1)S(1)}, u32[]{:S(2)}, u32[]{:S(2)}) collective-permute-start(bf16[1440,128]{1,0:T(8,128)(2,1)S(1)} %get-tuple-element.38), channel_id=1, source_target_pairs={{0,96},{32,0},{64,32},{96,64},{1,97},{33,1},{65,33},{97,65},{2,98}... | collective-permute-start | bytes 1105928 | tf_op jit(solution)/shard_map/ppermute | solution.py:255
  80.1 4.3 %project.3 = (bf16[480,128]{1,0:T(8,128)(2,1)S(1)}, bf16[480,128]{1,0:T(8,128)(2,1)S(1)}, bf16[480,128]{1,0:T(8,128)(2,1)}, bf16[480,128]{1,0:T(8,128)(2,1)}) custom-call(s32[8]{0:T(128)S(1)} %stack.150.idx_ref.col_ref, f32[2,64]{1,0:T(2,128)S(1)} %copy-done.14, bf16[320,2048]{1,0:T(8,128)(2,1)} %collective-permute-done.15.refs_0_, ...), custom_call_target="tpu_custom_call" | custom-call | tf_op jit(solution)/shard_map/project/pallas_call | solution.py:204
  85.1 1.4 collective-permute-start.16
  87.7 4.8 %collective-permute-start.17 = (bf16[480,128]{1,0:T(8,128)(2,1)}, bf16[480,128]{1,0:T(8,128)(2,1)S(1)}, u32[]{:S(2)}, u32[]{:S(2)}) collective-permute-start(bf16[480,128]{1,0:T(8,128)(2,1)} %get-tuple-element.41), channel_id=1, source_target_pairs={{0,64},{32,96},{64,0},{96,32},{1,65},{33,97},{65,1},{97,33},{2,66}... | collective-permute-start | bytes 368648 | tf_op jit(solution)/shard_map/ppermute | solution.py:255
  92.5 2.0 %collective-permute-start.18 = (bf16[480,128]{1,0:T(8,128)(2,1)}, bf16[480,128]{1,0:T(8,128)(2,1)S(1)}, u32[]{:S(2)}, u32[]{:S(2)}) collective-permute-start(bf16[480,128]{1,0:T(8,128)(2,1)} %get-tuple-element.42), channel_id=1, source_target_pairs={{0,96},{32,0},{64,32},{96,64},{1,97},{33,1},{65,33},{97,65},{2,98}... | collective-permute-start | bytes 368648 | tf_op jit(solution)/shard_map/ppermute | solution.py:255
  94.6 1.0 collective-permute-done.17.refs_6_
  95.6 2.0 %collective-permute-done.18.refs_7_ = bf16[480,128]{1,0:T(8,128)(2,1)S(1)} collective-permute-done((bf16[480,128]{1,0:T(8,128)(2,1)}, bf16[480,128]{1,0:T(8,128)(2,1)S(1)}, u32[]{:S(2)}, u32[]{:S(2)}) %collective-permute-start.18) | collective-permute-done | bytes 122912 | tf_op jit(solution)/shard_map/ppermute | solution.py:255
  102.3 41.7 %attention.1 = bf16[16,160,128]{2,1,0:T(8,128)(2,1)} custom-call(s32[16]{0:T(128)S(1)} %stack.165.pos_ref, f32[2,64]{1,0:T(2,128)S(1)} %copy-done.15, f32[8,640]{1,0:T(8,128)S(1)} %copy-done.13, bf16[1440,128]{1,0:T(8,128)(2,1)S(1)} %copy-done.4, bf16[1440,128]{1,0:T(8,128)(2,1)S(1)} %copy-done.6, bf16[1440,128]{1,0:T(8,128)(2,1)S(1)} %copy-done.8, ...), custom_call_target="tpu_custom_call" | custom-call | tf_op jit(solution)/shard_map/attention/pallas_call | solution.py:118
  144.0 5.4 %all-to-all-start = ((bf16[16,160,128]{2,1,0:T(8,128)(2,1)}), bf16[16,160,128]{2,1,0:T(8,128)(2,1)S(1)}, u32[]{:S(2)}, u32[]{:S(2)}) async-start(bf16[16,160,128]{2,1,0:T(8,128)(2,1)} %attention.1), calls=%async_computation | async-start | bytes 1310720 | tf_op jit(solution)/shard_map/all_to_all | solution.py:297
  153.7 6.6 %all-to-all-done.heads_ref = bf16[16,160,128]{2,1,0:T(8,128)(2,1)S(1)} async-done(((bf16[16,160,128]{2,1,0:T(8,128)(2,1)}), bf16[16,160,128]{2,1,0:T(8,128)(2,1)S(1)}, u32[]{:S(2)}, u32[]{:S(2)}) %all-to-all-start) | async-done | bytes 655392 | tf_op jit(solution)/shard_map/all_to_all | solution.py:297
  160.3 4.1 %output.1 = bf16[320,2048]{1,0:T(8,128)(2,1)} custom-call(s32[16]{0:T(128)S(1)} %stack.141.head_ref, s32[8]{0:T(128)S(1)} %stack.150.idx_ref.col_ref, bf16[16,160,128]{2,1,0:T(8,128)(2,1)S(1)} %all-to-all-done.heads_ref, bf16[1024,256]{1,0:T(8,128)(2,1)S(1)} %join.1.refs_0_, bf16[1024,256]{1,0:T(8,128)(2,1)} %collective-permute-done.22.refs_1_, ...), custom_call_target="tpu_custom_call" | custom-call | tf_op jit(solution)/shard_map/output/pallas_call | solution.py:238
  (73 shorter events, 18.2 us)
Async XLA Ops:
  0.0 28.4 %collective-permute-start = (bf16[320,2048]{1,0:T(8,128)(2,1)}, bf16[320,2048]{1,0:T(8,128)(2,1)}, u32[]{:S(2)}, u32[]{:S(2)}) collective-permute-start(bf16[320,2048]{1,0:T(8,128)(2,1)} %bitcast.43), channel_id=1, source_target_pairs={{0,24},{1,9},{8,0},{9,17},{16,8},{17,25},{24,16},{25,1},{2,26},{3,... | collective-permute-start | bytes 3932168 | tf_op jit(solution)/shard_map/ppermute | solution.py:260
  3.9 8.2 %collective-permute-start.2 = (bf16[256,256]{1,0:T(8,128)(2,1)S(1)}, bf16[256,256]{1,0:T(8,128)(2,1)S(1)}, u32[]{:S(2)}, u32[]{:S(2)}) collective-permute-start(bf16[256,256]{1,0:T(8,128)(2,1)S(1)} %pad_maximum_fusion.refs_0_), channel_id=1, source_target_pairs={{0,96},{32,0},{64,32},{96,64},{1,97},{33,1},{65,33},{97,65},{2,98}... | collective-permute-start | bytes 393224 | tf_op jit(solution)/shard_map/ppermute | solution.py:255
  8.1 6.6 %collective-permute-start.3 = (bf16[256,256]{1,0:T(8,128)(2,1)S(1)}, bf16[256,256]{1,0:T(8,128)(2,1)S(1)}, u32[]{:S(2)}, u32[]{:S(2)}) collective-permute-start(bf16[256,256]{1,0:T(8,128)(2,1)S(1)} %pad_maximum_fusion.refs_0_), channel_id=1, source_target_pairs={{0,64},{32,96},{64,0},{96,32},{1,65},{33,97},{65,1},{97,33},{2,66}... | collective-permute-start | bytes 393224 | tf_op jit(solution)/shard_map/ppermute | solution.py:255
  8.1 7.6 %collective-permute-start.4 = (bf16[256,256]{1,0:T(8,128)(2,1)S(1)}, bf16[256,256]{1,0:T(8,128)(2,1)S(1)}, u32[]{:S(2)}, u32[]{:S(2)}) collective-permute-start(bf16[256,256]{1,0:T(8,128)(2,1)S(1)} %pad_maximum_fusion.refs_0_), channel_id=1, source_target_pairs={{0,32},{32,64},{64,96},{96,0},{1,33},{33,65},{65,97},{97,1},{2,34}... | collective-permute-start | bytes 393224 | tf_op jit(solution)/shard_map/ppermute | solution.py:255
  9.3 39.5 %collective-permute-start.1 = (bf16[320,2048]{1,0:T(8,128)(2,1)}, bf16[320,2048]{1,0:T(8,128)(2,1)}, u32[]{:S(2)}, u32[]{:S(2)}) collective-permute-start(bf16[320,2048]{1,0:T(8,128)(2,1)} %bitcast.44), channel_id=1, source_target_pairs={{0,8},{1,25},{8,16},{9,1},{16,24},{17,9},{24,0},{25,17},{2,10},{3,... | collective-permute-start | bytes 3932168 | tf_op jit(solution)/shard_map/ppermute | solution.py:260
  15.7 47.4 %copy-start.11 = (bf16[256,256]{1,0:T(8,128)(2,1)}, bf16[256,256]{1,0:T(8,128)(2,1)S(1)}, u32[]{:S(2)}) copy-start(bf16[256,256]{1,0:T(8,128)(2,1)S(1)} %get-tuple-element.43.refs_0_) | copy-start | bytes 393220
  15.7 20.0 %collective-permute-start.5 = (bf16[768,256]{1,0:T(8,128)(2,1)S(1)}, bf16[768,256]{1,0:T(8,128)(2,1)S(1)}, u32[]{:S(2)}, u32[]{:S(2)}) collective-permute-start(bf16[768,256]{1,0:T(8,128)(2,1)S(1)} %get-tuple-element.29.refs_3_.refs_1_), channel_id=1, source_target_pairs={{0,6},{2,0},{4,2},{6,4},{1,7},{3,1},{5,3},{7,5},{8,14},{10,8},{12,... | collective-permute-start | bytes 1179656 | tf_op jit(solution)/shard_map/ppermute | solution.py:255
  28.4 49.1 %collective-permute-start.15 = (bf16[320,2048]{1,0:T(8,128)(2,1)}, bf16[320,2048]{1,0:T(8,128)(2,1)}, u32[]{:S(2)}, u32[]{:S(2)}) collective-permute-start(bf16[320,2048]{1,0:T(8,128)(2,1)} %collective-permute-done.refs_1_), channel_id=1, source_target_pairs={{0,24},{1,9},{8,0},{9,17},{16,8},{17,25},{24,16},{25,1},{2,26},{3,... | collective-permute-start | bytes 3932168 | tf_op jit(solution)/shard_map/ppermute | solution.py:260
  32.1 9.4 %collective-permute-start.6 = (bf16[768,256]{1,0:T(8,128)(2,1)S(1)}, bf16[768,256]{1,0:T(8,128)(2,1)S(1)}, u32[]{:S(2)}, u32[]{:S(2)}) collective-permute-start(bf16[768,256]{1,0:T(8,128)(2,1)S(1)} %get-tuple-element.29.refs_3_.refs_1_), channel_id=1, source_target_pairs={{0,4},{2,6},{4,0},{6,2},{1,5},{3,7},{5,1},{7,3},{8,12},{10,14},{12... | collective-permute-start | bytes 1179656 | tf_op jit(solution)/shard_map/ppermute | solution.py:255
  35.1 10.5 %collective-permute-start.7 = (bf16[768,256]{1,0:T(8,128)(2,1)S(1)}, bf16[768,256]{1,0:T(8,128)(2,1)S(1)}, u32[]{:S(2)}, u32[]{:S(2)}) collective-permute-start(bf16[768,256]{1,0:T(8,128)(2,1)S(1)} %get-tuple-element.29.refs_3_.refs_1_), channel_id=1, source_target_pairs={{0,2},{2,4},{4,6},{6,0},{1,3},{3,5},{5,7},{7,1},{8,10},{10,12},{12... | collective-permute-start | bytes 1179656 | tf_op jit(solution)/shard_map/ppermute | solution.py:255
  35.7 9.9 %collective-permute-start.8 = (bf16[768,256]{1,0:T(8,128)(2,1)S(1)}, bf16[768,256]{1,0:T(8,128)(2,1)S(1)}, u32[]{:S(2)}, u32[]{:S(2)}) collective-permute-start(bf16[768,256]{1,0:T(8,128)(2,1)S(1)} %get-tuple-element.29.refs_3_.refs_1_), channel_id=1, source_target_pairs={{0,1},{1,0},{2,3},{3,2},{4,5},{5,4},{6,7},{7,6},{8,9},{9,8},{10,11... | collective-permute-start | bytes 1179656 | tf_op jit(solution)/shard_map/ppermute | solution.py:255
  41.5 7.3 %collective-permute-start.9 = (bf16[768,256]{1,0:T(8,128)(2,1)S(1)}, bf16[768,256]{1,0:T(8,128)(2,1)S(1)}, u32[]{:S(2)}, u32[]{:S(2)}) collective-permute-start(bf16[768,256]{1,0:T(8,128)(2,1)S(1)} %collective-permute-done.5.refs_4_.refs_2_), channel_id=1, source_target_pairs={{0,1},{1,0},{2,3},{3,2},{4,5},{5,4},{6,7},{7,6},{8,9},{9,8},{10,11... | collective-permute-start | bytes 1179656 | tf_op jit(solution)/shard_map/ppermute | solution.py:255
  45.6 3.2 %collective-permute-start.10 = (bf16[768,256]{1,0:T(8,128)(2,1)S(1)}, bf16[768,256]{1,0:T(8,128)(2,1)S(1)}, u32[]{:S(2)}, u32[]{:S(2)}) collective-permute-start(bf16[768,256]{1,0:T(8,128)(2,1)S(1)} %collective-permute-done.6.refs_5_.refs_3_), channel_id=1, source_target_pairs={{0,1},{1,0},{2,3},{3,2},{4,5},{5,4},{6,7},{7,6},{8,9},{9,8},{10,11... | collective-permute-start | bytes 1179656 | tf_op jit(solution)/shard_map/ppermute | solution.py:255
  45.6 3.2 %collective-permute-start.11 = (bf16[768,256]{1,0:T(8,128)(2,1)S(1)}, bf16[768,256]{1,0:T(8,128)(2,1)S(1)}, u32[]{:S(2)}, u32[]{:S(2)}) collective-permute-start(bf16[768,256]{1,0:T(8,128)(2,1)S(1)} %collective-permute-done.7.refs_6_.refs_4_), channel_id=1, source_target_pairs={{0,1},{1,0},{2,3},{3,2},{4,5},{5,4},{6,7},{7,6},{8,9},{9,8},{10,11... | collective-permute-start | bytes 1179656 | tf_op jit(solution)/shard_map/ppermute | solution.py:255
  57.8 18.6 %collective-permute-start.12 = (bf16[1440,128]{1,0:T(8,128)(2,1)S(1)}, bf16[1440,128]{1,0:T(8,128)(2,1)S(1)}, u32[]{:S(2)}, u32[]{:S(2)}) collective-permute-start(bf16[1440,128]{1,0:T(8,128)(2,1)S(1)} %get-tuple-element.36), channel_id=1, source_target_pairs={{0,32},{32,64},{64,96},{96,0},{1,33},{33,65},{65,97},{97,1},{2,34}... | collective-permute-start | bytes 1105928 | tf_op jit(solution)/shard_map/ppermute | solution.py:255
  59.4 6.4 %collective-permute-start.19 = (bf16[256,256]{1,0:T(8,128)(2,1)S(1)}, bf16[256,256]{1,0:T(8,128)(2,1)S(1)}, u32[]{:S(2)}, u32[]{:S(2)}) collective-permute-start(bf16[256,256]{1,0:T(8,128)(2,1)S(1)} %get-tuple-element.43.refs_0_), channel_id=1, source_target_pairs={{0,6},{2,0},{4,2},{6,4},{1,7},{3,1},{5,3},{7,5},{8,14},{10,8},{12,... | collective-permute-start | bytes 393224 | tf_op jit(solution)/shard_map/ppermute | solution.py:255
  60.0 11.5 %collective-permute-start.20 = (bf16[256,256]{1,0:T(8,128)(2,1)S(1)}, bf16[256,256]{1,0:T(8,128)(2,1)S(1)}, u32[]{:S(2)}, u32[]{:S(2)}) collective-permute-start(bf16[256,256]{1,0:T(8,128)(2,1)S(1)} %get-tuple-element.43.refs_0_), channel_id=1, source_target_pairs={{0,4},{2,6},{4,0},{6,2},{1,5},{3,7},{5,1},{7,3},{8,12},{10,14},{12... | collective-permute-start | bytes 393224 | tf_op jit(solution)/shard_map/ppermute | solution.py:255
  63.1 8.4 %collective-permute-start.21 = (bf16[256,256]{1,0:T(8,128)(2,1)S(1)}, bf16[256,256]{1,0:T(8,128)(2,1)S(1)}, u32[]{:S(2)}, u32[]{:S(2)}) collective-permute-start(bf16[256,256]{1,0:T(8,128)(2,1)S(1)} %get-tuple-element.43.refs_0_), channel_id=1, source_target_pairs={{0,2},{2,4},{4,6},{6,0},{1,3},{3,5},{5,7},{7,1},{8,10},{10,12},{12... | collective-permute-start | bytes 393224 | tf_op jit(solution)/shard_map/ppermute | solution.py:255
  65.8 18.6 %collective-permute-start.13 = (bf16[1440,128]{1,0:T(8,128)(2,1)S(1)}, bf16[1440,128]{1,0:T(8,128)(2,1)S(1)}, u32[]{:S(2)}, u32[]{:S(2)}) collective-permute-start(bf16[1440,128]{1,0:T(8,128)(2,1)S(1)} %get-tuple-element.37), channel_id=1, source_target_pairs={{0,64},{32,96},{64,0},{96,32},{1,65},{33,97},{65,1},{97,33},{2,66}... | collective-permute-start | bytes 1105928 | tf_op jit(solution)/shard_map/ppermute | solution.py:255
  72.4 25.2 %copy-start.15 = (f32[2,64]{1,0:T(2,128)S(1)}, f32[2,64]{1,0:T(2,128)}, u32[]{:S(2)}) copy-start(f32[2,64]{1,0:T(2,128)} %gain_ref.2) | copy-start | bytes 1540
  72.4 71.6 %collective-permute-start.22 = (bf16[1024,256]{1,0:T(8,128)(2,1)S(1)}, bf16[1024,256]{1,0:T(8,128)(2,1)}, u32[]{:S(2)}, u32[]{:S(2)}) collective-permute-start(bf16[1024,256]{1,0:T(8,128)(2,1)S(1)} %join.1.refs_0_), channel_id=1, source_target_pairs={{0,24},{8,0},{16,8},{24,16},{1,25},{9,1},{17,9},{25,17},{2,26},{10... | collective-permute-start | bytes 1572872 | tf_op jit(solution)/shard_map/ppermute | solution.py:255
  74.1 69.9 %collective-permute-start.23 = (bf16[1024,256]{1,0:T(8,128)(2,1)S(1)}, bf16[1024,256]{1,0:T(8,128)(2,1)}, u32[]{:S(2)}, u32[]{:S(2)}) collective-permute-start(bf16[1024,256]{1,0:T(8,128)(2,1)S(1)} %join.1.refs_0_), channel_id=1, source_target_pairs={{0,16},{8,24},{16,0},{24,8},{1,17},{9,25},{17,1},{25,9},{2,18},{10... | collective-permute-start | bytes 1572872 | tf_op jit(solution)/shard_map/ppermute | solution.py:255
  77.1 66.9 %collective-permute-start.24 = (bf16[1024,256]{1,0:T(8,128)(2,1)S(1)}, bf16[1024,256]{1,0:T(8,128)(2,1)}, u32[]{:S(2)}, u32[]{:S(2)}) collective-permute-start(bf16[1024,256]{1,0:T(8,128)(2,1)S(1)} %join.1.refs_0_), channel_id=1, source_target_pairs={{0,8},{8,16},{16,24},{24,0},{1,9},{9,17},{17,25},{25,1},{2,10},{10... | collective-permute-start | bytes 1572872 | tf_op jit(solution)/shard_map/ppermute | solution.py:255
  77.5 9.5 %collective-permute-start.14 = (bf16[1440,128]{1,0:T(8,128)(2,1)S(1)}, bf16[1440,128]{1,0:T(8,128)(2,1)S(1)}, u32[]{:S(2)}, u32[]{:S(2)}) collective-permute-start(bf16[1440,128]{1,0:T(8,128)(2,1)S(1)} %get-tuple-element.38), channel_id=1, source_target_pairs={{0,96},{32,0},{64,32},{96,64},{1,97},{33,1},{65,33},{97,65},{2,98}... | collective-permute-start | bytes 1105928 | tf_op jit(solution)/shard_map/ppermute | solution.py:255
  85.1 7.4 %collective-permute-start.16 = (bf16[480,128]{1,0:T(8,128)(2,1)S(1)}, bf16[480,128]{1,0:T(8,128)(2,1)S(1)}, u32[]{:S(2)}, u32[]{:S(2)}) collective-permute-start(bf16[480,128]{1,0:T(8,128)(2,1)S(1)} %get-tuple-element.40), channel_id=1, source_target_pairs={{0,32},{32,64},{64,96},{96,0},{1,33},{33,65},{65,97},{97,1},{2,34}... | collective-permute-start | bytes 368648 | tf_op jit(solution)/shard_map/ppermute | solution.py:255
  87.7 7.9 %collective-permute-start.17 = (bf16[480,128]{1,0:T(8,128)(2,1)}, bf16[480,128]{1,0:T(8,128)(2,1)S(1)}, u32[]{:S(2)}, u32[]{:S(2)}) collective-permute-start(bf16[480,128]{1,0:T(8,128)(2,1)} %get-tuple-element.41), channel_id=1, source_target_pairs={{0,64},{32,96},{64,0},{96,32},{1,65},{33,97},{65,1},{97,33},{2,66}... | collective-permute-start | bytes 368648 | tf_op jit(solution)/shard_map/ppermute | solution.py:255
  92.5 5.1 %collective-permute-start.18 = (bf16[480,128]{1,0:T(8,128)(2,1)}, bf16[480,128]{1,0:T(8,128)(2,1)S(1)}, u32[]{:S(2)}, u32[]{:S(2)}) collective-permute-start(bf16[480,128]{1,0:T(8,128)(2,1)} %get-tuple-element.42), channel_id=1, source_target_pairs={{0,96},{32,0},{64,32},{96,64},{1,97},{33,1},{65,33},{97,65},{2,98}... | collective-permute-start | bytes 368648 | tf_op jit(solution)/shard_map/ppermute | solution.py:255
  144.0 16.3 %all-to-all-start = ((bf16[16,160,128]{2,1,0:T(8,128)(2,1)}), bf16[16,160,128]{2,1,0:T(8,128)(2,1)S(1)}, u32[]{:S(2)}, u32[]{:S(2)}) async-start(bf16[16,160,128]{2,1,0:T(8,128)(2,1)} %attention.1), calls=%async_computation | async-start | bytes 1310720 | tf_op jit(solution)/shard_map/all_to_all | solution.py:297
  149.5 2.0 %collective-permute-start.25 = (bf16[1024,256]{1,0:T(8,128)(2,1)S(1)}, bf16[1024,256]{1,0:T(8,128)(2,1)S(1)}, u32[]{:S(2)}, u32[]{:S(2)}) collective-permute-start(bf16[1024,256]{1,0:T(8,128)(2,1)S(1)} %join.1.refs_0_), channel_id=1, source_target_pairs={{0,1},{1,0},{2,3},{3,2},{4,5},{5,4},{6,7},{7,6},{8,9},{9,8},{10,11... | collective-permute-start | bytes 1572872 | tf_op jit(solution)/shard_map/ppermute | solution.py:255
  149.6 2.6 %collective-permute-start.26 = (bf16[1024,256]{1,0:T(8,128)(2,1)}, bf16[1024,256]{1,0:T(8,128)(2,1)S(1)}, u32[]{:S(2)}, u32[]{:S(2)}) collective-permute-start(bf16[1024,256]{1,0:T(8,128)(2,1)} %collective-permute-done.22.refs_1_), channel_id=1, source_target_pairs={{0,1},{1,0},{2,3},{3,2},{4,5},{5,4},{6,7},{7,6},{8,9},{9,8},{10,11... | collective-permute-start | bytes 1572872 | tf_op jit(solution)/shard_map/ppermute | solution.py:255
  150.0 2.9 %collective-permute-start.27 = (bf16[1024,256]{1,0:T(8,128)(2,1)}, bf16[1024,256]{1,0:T(8,128)(2,1)S(1)}, u32[]{:S(2)}, u32[]{:S(2)}) collective-permute-start(bf16[1024,256]{1,0:T(8,128)(2,1)} %collective-permute-done.23.refs_2_), channel_id=1, source_target_pairs={{0,1},{1,0},{2,3},{3,2},{4,5},{5,4},{6,7},{7,6},{8,9},{9,8},{10,11... | collective-permute-start | bytes 1572872 | tf_op jit(solution)/shard_map/ppermute | solution.py:255
  150.1 3.6 %collective-permute-start.28 = (bf16[1024,256]{1,0:T(8,128)(2,1)}, bf16[1024,256]{1,0:T(8,128)(2,1)S(1)}, u32[]{:S(2)}, u32[]{:S(2)}) collective-permute-start(bf16[1024,256]{1,0:T(8,128)(2,1)} %collective-permute-done.24.refs_3_), channel_id=1, source_target_pairs={{0,1},{1,0},{2,3},{3,2},{4,5},{5,4},{6,7},{7,6},{8,9},{9,8},{10,11... | collective-permute-start | bytes 1572872 | tf_op jit(solution)/shard_map/ppermute | solution.py:255
  (14 other events, 41.2 us)

commit v4 on v1

--- a/solution.py
+++ b/solution.py
@@ -23,6 +23,7 @@
 bf16 = jnp.bfloat16
 SMEM = pl.BlockSpec(memory_space=pltpu.SMEM)
 VMEM = pl.BlockSpec(memory_space=pltpu.VMEM)
+HBM = pl.BlockSpec(memory_space=pltpu.HBM)
 
 
 def attn_kernel(pos_ref, gain_ref, d_ref, *refs, nblk):
@@ -45,7 +46,7 @@
             v=a[b*480+320:b*480+480,:].astype(f32)
             vs[pl.ds(base,BLK//2),:]=jnp.where(lanev<64,v,tail)
             vs[pl.ds(base+BLK//2,BLK//2),:]=jnp.where(lanev<64,pltpu.roll(v,64,1),tail)
-    x=d_ref[...]*LOG2E
+    x=jnp.concatenate([d_ref[0:1,i*640:(i+1)*640] for i in range(8)],0)*LOG2E
     h=x.astype(bf16).astype(f32)
     m=(x-h).astype(bf16).astype(f32)
     l=x-h-m
@@ -183,15 +184,22 @@
 
 
 def proj_kernel(idx_ref, gain_ref, *refs, count):
-    toks, ws, outs, w = refs[:count], refs[count : count + 8], refs[count + 8 : count + 12], refs[-1]
+    toks, ws, outs = refs[:count], refs[count : count + 8], refs[count + 8 : count + 12]
+    tv, wv, w, sem_t, sem_w = refs[count + 12 :]
+    loads = [pltpu.make_async_copy(ws[j], wv.at[j], sem_w.at[j]) for j in range(8)]
+    fetch = [pltpu.make_async_copy(toks[b], tv.at[b], sem_t.at[b]) for b in range(count)]
+    for copy in loads + fetch:
+        copy.start()
     for j in range(8):
+        loads[j].wait()
         cols = pl.ds(pl.multiple_of(idx_ref[j] * 256, 256), 256)
         for h in range(4):
-            w[h * 128 : h * 128 + 128, cols] = ws[j][h * 192 : h * 192 + 128, :]
-            w[512 + h * 64 : 576 + h * 64, cols] = ws[j][h * 192 + 128 : h * 192 + 192, :]
+            w[h * 128 : h * 128 + 128, cols] = wv[j, h * 192 : h * 192 + 128, :]
+            w[512 + h * 64 : 576 + h * 64, cols] = wv[j, h * 192 + 128 : h * 192 + 192, :]
     gains = gain_row(gain_ref)
     for b in range(count):
-        proj_block(toks[b][...], w[...], gains, outs, b * 480)
+        fetch[b].wait()
+        proj_block(tv[b], w[...], gains, outs, b * 480)
 
 
 def project(cols, gain, toks, ws):
@@ -199,10 +207,16 @@
     return pl.pallas_call(
         functools.partial(proj_kernel, count=count),
         out_shape=[jax.ShapeDtypeStruct((count * 480, 128), bf16)] * 4,
-        in_specs=[SMEM] + [VMEM] * (1 + count + 8),
+        in_specs=[SMEM, VMEM] + [HBM] * (count + 8),
         out_specs=[VMEM] * 4,
-        scratch_shapes=[pltpu.VMEM((768, 2048), bf16)],
-        compiler_params=pltpu.CompilerParams(vmem_limit_bytes=20 * 1024 * 1024),
+        scratch_shapes=[
+            pltpu.VMEM((count, BLK, 2048), bf16),
+            pltpu.VMEM((8, 768, 256), bf16),
+            pltpu.VMEM((768, 2048), bf16),
+            pltpu.SemaphoreType.DMA((count,)),
+            pltpu.SemaphoreType.DMA((8,)),
+        ],
+        compiler_params=pltpu.CompilerParams(vmem_limit_bytes=24 * 1024 * 1024),
         name="project",
     )(cols, gain, *toks, *ws)
 
@@ -250,6 +264,11 @@
     return lax.ppermute(value, axis, pairs)
 
 
+def spread(value, step):
+    pairs = [(2 * i + k, 2 * ((i + (step, -step)[k]) % 4) + k) for i in range(4) for k in (0, 1)]
+    return lax.ppermute(value, (Y, C), pairs)
+
+
 def around(value, axis):
     return [value] + [move(value, axis, -d) for d in (1, 2, 3)]
 
@@ -257,9 +276,10 @@
 def on_device(tokens, w_query, w_key, w_value, w_output, qk_gain, decay_sums):
     own = tokens[0]
     z, y, x, c = (lax.axis_index(a) for a in (Z, Y, X, C))
-    t1 = move(own, Y, -1)
-    t3 = move(own, Y, 1)
-    t2 = move(own, Y, 2)
+    t1 = spread(own, -1)
+    t3 = spread(own, 1)
+    t2 = spread(t1, -1)
+    near = jnp.where(c == 0, 1, 3)
     piece = jnp.concatenate([w_query.T, w_key.T, w_value.T, w_output], 0)
     w4, wo4 = pack(around(piece, Z))
     ws = around(w4, X)
@@ -268,19 +288,18 @@
     cols = jnp.stack(
         [2 * ((x + d) % 4) + e for e in (c, 1 - c) for d in range(4)]
     ).astype(jnp.int32)
-    gain, decay = lax.optimization_barrier((qk_gain, decay_sums.reshape(8, 640)))
-    part1 = project(cols, gain, [own, t1, t3], ws)
+    part1 = project(cols, qk_gain, [own, t1, t3], ws)
     *part1, wo4 = lax.optimization_barrier((*part1, wo4))
-    part2 = project(cols, gain, [t2], ws)
+    part2 = project(cols, qk_gain, [t2], ws)
     recv = []
     for part in (part1, part2):
         recv += [part[0]] + [move(part[d], Z, d) for d in (1, 2, 3)]
     wo16 = join(around(wo4, X))
     wo = around(wo16, Y)
-    pos = [4 * ((z - d) % 4) + (y + e) % 4 for d in range(4) for e in (0, 1, 3)]
+    pos = [4 * ((z - d) % 4) + (y + e) % 4 for d in range(4) for e in (0, near, 4 - near)]
     pos += [4 * ((z - d) % 4) + (y + 2) % 4 for d in range(4)]
     pos = jnp.stack(pos).astype(jnp.int32)
-    heads = attention(pos, gain, decay, recv, (3, 3, 3, 3, 1, 1, 1, 1))
+    heads = attention(pos, qk_gain, decay_sums[0], recv, (3, 3, 3, 3, 1, 1, 1, 1))
     heads, *wo = lax.optimization_barrier((heads, *wo))
     wo = wo + [move(w, C, 0) for w in wo]
     merged = lax.all_to_all(heads, SP, 0, 0, tiled=True)

time: 189 us -> 168 us (0.89)
  waiting for transfers between devices: 89.7 us -> 43.8 us
  starting transfers between devices: 32.3 us -> 51.6 us
  Pallas kernels: 56.5 us -> 60.2 us
  local copies, waits for them, and re-layouts: 7.69 us -> 11 us
    ppermute x29 -> x26, waiting for transfers between devices: 83.2 us -> 27.3 us  [move(): return lax.ppermute(value, axis, pairs)]
    ppermute x29 -> x26, starting transfers between devices: 26.7 us -> 39.3 us  [move(): return lax.ppermute(value, axis, pairs)]
    ppermute x0 -> x3, waiting for transfers between devices: none -> 9.88 us  [spread(): return lax.ppermute(value, (Y, C), pairs)]
    ppermute x0 -> x3, starting transfers between devices: none -> 6.82 us  [spread(): return lax.ppermute(value, (Y, C), pairs)]
    pallas_call x2, Pallas kernels: 10.6 us -> 14.1 us  [project(): pl.pallas_call(functools.partial(proj_kernel, count=count), out_shape=[ja...]
    unnamed x23 -> x32, local copies, waits for them, and re-layouts: 7.41 us -> 10.7 us
  transfers between devices with their start and end apart: 30 -> 30, of which waited for: 18 -> 17; matrix products, arithmetic and copies ran while one was open for 1% -> 1% of each run, Pallas kernels for 28% -> 33%
where the time goes in v4:
time: 168 us
  Pallas kernels  60.2 us (36%)
  starting transfers between devices  51.6 us (31%)
  waiting for transfers between devices  43.8 us (26%)
  local copies, waits for them, and re-layouts  11 us (7%)
    pallas_call x1, Pallas kernels, attention(): pl.pallas_call(functools.partial(attn_kernel, nblk=nblk), out_shape=jax.S...  41.9 us
    ppermute x26, starting transfers between devices, move(): return lax.ppermute(value, axis, pairs)  39.3 us
    ppermute x26, waiting for transfers between devices, move(): return lax.ppermute(value, axis, pairs)  27.3 us
    pallas_call x2, Pallas kernels, project(): pl.pallas_call(functools.partial(proj_kernel, count=count), out_shape=[ja...  14.1 us
    unnamed x32, local copies, waits for them, and re-layouts  10.7 us
    ppermute x3, waiting for transfers between devices, spread(): return lax.ppermute(value, (Y, C), pairs)  9.88 us
    ppermute x3, starting transfers between devices, spread(): return lax.ppermute(value, (Y, C), pairs)  6.82 us
    all_to_all x1, waiting for transfers between devices, on_device(): merged = lax.all_to_all(heads, SP, 0, 0, tiled=True)  6.6 us
  transfers between devices with their start and end apart: 30, of which 17 were waited for; matrix products, arithmetic and copies ran while one was open for 1% of the time, Pallas kernels for 33%

profile of v4, /device:TPU:0, one launch (start us, length us, event | category | flops | bytes accessed | tf_op | source)
XLA Modules:
  0.0 167.5 jit_solution(8714208093606573353)
XLA Ops:
  0.0 3.1 %collective-permute-start = (bf16[320,2048]{1,0:T(8,128)(2,1)}, bf16[320,2048]{1,0:T(8,128)(2,1)}, u32[]{:S(2)}, u32[]{:S(2)}) collective-permute-start(bf16[320,2048]{1,0:T(8,128)(2,1)} %bitcast.44), channel_id=1, source_target_pairs={{0,24},{1,9},{8,0},{9,17},{16,8},{17,25},{24,16},{25,1},{2,26},{3,... | collective-permute-start | bytes 3932168 | tf_op jit(solution)/shard_map/ppermute | solution.py:269
  3.9 4.1 %collective-permute-start.2 = (bf16[256,256]{1,0:T(8,128)(2,1)S(1)}, bf16[256,256]{1,0:T(8,128)(2,1)S(1)}, u32[]{:S(2)}, u32[]{:S(2)}) collective-permute-start(bf16[256,256]{1,0:T(8,128)(2,1)S(1)} %pad_maximum_fusion.refs_0_), channel_id=1, source_target_pairs={{0,96},{32,0},{64,32},{96,64},{1,97},{33,1},{65,33},{97,65},{2,98}... | collective-permute-start | bytes 393224 | tf_op jit(solution)/shard_map/ppermute | solution.py:264
  8.1 1.3 collective-permute-start.4
  9.3 2.8 %collective-permute-done.2.refs_1_ = bf16[256,256]{1,0:T(8,128)(2,1)S(1)} collective-permute-done((bf16[256,256]{1,0:T(8,128)(2,1)S(1)}, bf16[256,256]{1,0:T(8,128)(2,1)S(1)}, u32[]{:S(2)}, u32[]{:S(2)}) %collective-permute-start.2) | collective-permute-done | bytes 131104 | tf_op jit(solution)/shard_map/ppermute | solution.py:264
  12.2 2.5 %collective-permute-done.3.refs_2_ = bf16[256,256]{1,0:T(8,128)(2,1)S(1)} collective-permute-done((bf16[256,256]{1,0:T(8,128)(2,1)S(1)}, bf16[256,256]{1,0:T(8,128)(2,1)S(1)}, u32[]{:S(2)}, u32[]{:S(2)}) %collective-permute-start.3) | collective-permute-done | bytes 131104 | tf_op jit(solution)/shard_map/ppermute | solution.py:264
  14.6 1.0 collective-permute-done.4.refs_3_
  15.7 2.8 %collective-permute-start.5 = (bf16[768,256]{1,0:T(8,128)(2,1)S(1)}, bf16[768,256]{1,0:T(8,128)(2,1)S(1)}, u32[]{:S(2)}, u32[]{:S(2)}) collective-permute-start(bf16[768,256]{1,0:T(8,128)(2,1)S(1)} %get-tuple-element.25.refs_3_.refs_1_), channel_id=1, source_target_pairs={{0,6},{2,0},{4,2},{6,4},{1,7},{3,1},{5,3},{7,5},{8,14},{10,8},{12,... | collective-permute-start | bytes 1179656 | tf_op jit(solution)/shard_map/ppermute | solution.py:264
  18.5 9.9 %collective-permute-done.refs_1_ = bf16[320,2048]{1,0:T(8,128)(2,1)} collective-permute-done((bf16[320,2048]{1,0:T(8,128)(2,1)}, bf16[320,2048]{1,0:T(8,128)(2,1)}, u32[]{:S(2)}, u32[]{:S(2)}) %collective-permute-start) | collective-permute-done | bytes 1310752 | tf_op jit(solution)/shard_map/ppermute | solution.py:269
  28.4 3.7 %collective-permute-start.15 = (bf16[320,2048]{1,0:T(8,128)(2,1)}, bf16[320,2048]{1,0:T(8,128)(2,1)}, u32[]{:S(2)}, u32[]{:S(2)}) collective-permute-start(bf16[320,2048]{1,0:T(8,128)(2,1)} %collective-permute-done.refs_1_), channel_id=1, source_target_pairs={{0,24},{1,9},{8,0},{9,17},{16,8},{17,25},{24,16},{25,1},{2,26},{3,... | collective-permute-start | bytes 3932168 | tf_op jit(solution)/shard_map/ppermute | solution.py:269
  32.1 3.0 %collective-permute-start.6 = (bf16[768,256]{1,0:T(8,128)(2,1)S(1)}, bf16[768,256]{1,0:T(8,128)(2,1)S(1)}, u32[]{:S(2)}, u32[]{:S(2)}) collective-permute-start(bf16[768,256]{1,0:T(8,128)(2,1)S(1)} %get-tuple-element.25.refs_3_.refs_1_), channel_id=1, source_target_pairs={{0,4},{2,6},{4,0},{6,2},{1,5},{3,7},{5,1},{7,3},{8,12},{10,14},{12... | collective-permute-start | bytes 1179656 | tf_op jit(solution)/shard_map/ppermute | solution.py:264
  35.7 5.8 %collective-permute-done.6.refs_5_.refs_3_ = bf16[768,256]{1,0:T(8,128)(2,1)S(1)} collective-permute-done((bf16[768,256]{1,0:T(8,128)(2,1)S(1)}, bf16[768,256]{1,0:T(8,128)(2,1)S(1)}, u32[]{:S(2)}, u32[]{:S(2)}) %collective-permute-start.6) | collective-permute-done | bytes 393248 | tf_op jit(solution)/shard_map/ppermute | solution.py:264
  41.5 4.1 %collective-permute-done.7.refs_6_.refs_4_ = bf16[768,256]{1,0:T(8,128)(2,1)S(1)} collective-permute-done((bf16[768,256]{1,0:T(8,128)(2,1)S(1)}, bf16[768,256]{1,0:T(8,128)(2,1)S(1)}, u32[]{:S(2)}, u32[]{:S(2)}) %collective-permute-start.7) | collective-permute-done | bytes 393248 | tf_op jit(solution)/shard_map/ppermute | solution.py:264
  46.2 1.1 collective-permute-done.10.refs_9_.refs_7_
  47.9 1.5 copy-done.2
  50.0 8.0 %project.2 = (bf16[1440,128]{1,0:T(8,128)(2,1)S(1)}, bf16[1440,128]{1,0:T(8,128)(2,1)S(1)}, bf16[1440,128]{1,0:T(8,128)(2,1)S(1)}, bf16[1440,128]{1,0:T(8,128)(2,1)S(1)}) custom-call(s32[8]{0:T(128)S(1)} %stack.150.idx_ref.col_ref, f32[2,64]{1,0:T(2,128)S(1)} %copy-done.14, bf16[320,2048]{1,0:T(8,128)(2,1)S(1)} %bitcast.46, ...), custom_call_target="tpu_custom_call" | custom-call | tf_op jit(solution)/shard_map/project/pallas_call | solution.py:207
  58.7 1.6 collective-permute-start.12
  60.9 3.1 %collective-permute-start.20 = (bf16[256,256]{1,0:T(8,128)(2,1)S(1)}, bf16[256,256]{1,0:T(8,128)(2,1)S(1)}, u32[]{:S(2)}, u32[]{:S(2)}) collective-permute-start(bf16[256,256]{1,0:T(8,128)(2,1)S(1)} %get-tuple-element.39.refs_0_), channel_id=1, source_target_pairs={{0,4},{2,6},{4,0},{6,2},{1,5},{3,7},{5,1},{7,3},{8,12},{10,14},{12... | collective-permute-start | bytes 393224 | tf_op jit(solution)/shard_map/ppermute | solution.py:264
  64.0 2.7 %collective-permute-done.19.refs_1_ = bf16[256,256]{1,0:T(8,128)(2,1)S(1)} collective-permute-done((bf16[256,256]{1,0:T(8,128)(2,1)S(1)}, bf16[256,256]{1,0:T(8,128)(2,1)S(1)}, u32[]{:S(2)}, u32[]{:S(2)}) %collective-permute-start.19) | collective-permute-done | bytes 131104 | tf_op jit(solution)/shard_map/ppermute | solution.py:264
  66.7 5.7 %collective-permute-start.13 = (bf16[1440,128]{1,0:T(8,128)(2,1)S(1)}, bf16[1440,128]{1,0:T(8,128)(2,1)S(1)}, u32[]{:S(2)}, u32[]{:S(2)}) collective-permute-start(bf16[1440,128]{1,0:T(8,128)(2,1)S(1)} %get-tuple-element.33), channel_id=1, source_target_pairs={{0,64},{32,96},{64,0},{96,32},{1,65},{33,97},{65,1},{97,33},{2,66}... | collective-permute-start | bytes 1105928 | tf_op jit(solution)/shard_map/ppermute | solution.py:264
  73.4 1.7 %collective-permute-start.22 = (bf16[1024,256]{1,0:T(8,128)(2,1)S(1)}, bf16[1024,256]{1,0:T(8,128)(2,1)}, u32[]{:S(2)}, u32[]{:S(2)}) collective-permute-start(bf16[1024,256]{1,0:T(8,128)(2,1)S(1)} %join.1.refs_0_), channel_id=1, source_target_pairs={{0,24},{8,0},{16,8},{24,16},{1,25},{9,1},{17,9},{25,17},{2,26},{10... | collective-permute-start | bytes 1572872 | tf_op jit(solution)/shard_map/ppermute | solution.py:264
  75.1 2.2 %collective-permute-start.23 = (bf16[1024,256]{1,0:T(8,128)(2,1)S(1)}, bf16[1024,256]{1,0:T(8,128)(2,1)}, u32[]{:S(2)}, u32[]{:S(2)}) collective-permute-start(bf16[1024,256]{1,0:T(8,128)(2,1)S(1)} %join.1.refs_0_), channel_id=1, source_target_pairs={{0,16},{8,24},{16,0},{24,8},{1,17},{9,25},{17,1},{25,9},{2,18},{10... | collective-permute-start | bytes 1572872 | tf_op jit(solution)/shard_map/ppermute | solution.py:264
  78.5 2.7 %collective-permute-start.14 = (bf16[1440,128]{1,0:T(8,128)(2,1)S(1)}, bf16[1440,128]{1,0:T(8,128)(2,1)S(1)}, u32[]{:S(2)}, u32[]{:S(2)}) collective-permute-start(bf16[1440,128]{1,0:T(8,128)(2,1)S(1)} %get-tuple-element.34), channel_id=1, source_target_pairs={{0,96},{32,0},{64,32},{96,64},{1,97},{33,1},{65,33},{97,65},{2,98}... | collective-permute-start | bytes 1105928 | tf_op jit(solution)/shard_map/ppermute | solution.py:264
  81.2 6.1 %project.3 = (bf16[480,128]{1,0:T(8,128)(2,1)S(1)}, bf16[480,128]{1,0:T(8,128)(2,1)S(1)}, bf16[480,128]{1,0:T(8,128)(2,1)}, bf16[480,128]{1,0:T(8,128)(2,1)}) custom-call(s32[8]{0:T(128)S(1)} %stack.150.idx_ref.col_ref, f32[2,64]{1,0:T(2,128)S(1)} %copy-done.14, bf16[320,2048]{1,0:T(8,128)(2,1)} %collective-permute-done.15.refs_0_, ...), custom_call_target="tpu_custom_call" | custom-call | tf_op jit(solution)/shard_map/project/pallas_call | solution.py:207
  88.8 5.9 %collective-permute-start.17 = (bf16[480,128]{1,0:T(8,128)(2,1)}, bf16[480,128]{1,0:T(8,128)(2,1)S(1)}, u32[]{:S(2)}, u32[]{:S(2)}) collective-permute-start(bf16[480,128]{1,0:T(8,128)(2,1)} %get-tuple-element.37), channel_id=1, source_target_pairs={{0,64},{32,96},{64,0},{96,32},{1,65},{33,97},{65,1},{97,33},{2,66}... | collective-permute-start | bytes 368648 | tf_op jit(solution)/shard_map/ppermute | solution.py:264
  95.3 2.0 %collective-permute-start.18 = (bf16[480,128]{1,0:T(8,128)(2,1)}, bf16[480,128]{1,0:T(8,128)(2,1)S(1)}, u32[]{:S(2)}, u32[]{:S(2)}) collective-permute-start(bf16[480,128]{1,0:T(8,128)(2,1)} %get-tuple-element.38), channel_id=1, source_target_pairs={{0,96},{32,0},{64,32},{96,64},{1,97},{33,1},{65,33},{97,65},{2,98}... | collective-permute-start | bytes 368648 | tf_op jit(solution)/shard_map/ppermute | solution.py:264
  98.1 2.3 %collective-permute-done.18.refs_7_ = bf16[480,128]{1,0:T(8,128)(2,1)S(1)} collective-permute-done((bf16[480,128]{1,0:T(8,128)(2,1)}, bf16[480,128]{1,0:T(8,128)(2,1)S(1)}, u32[]{:S(2)}, u32[]{:S(2)}) %collective-permute-start.18) | collective-permute-done | bytes 122912 | tf_op jit(solution)/shard_map/ppermute | solution.py:264
  100.4 1.0 copy-done.4
  101.4 1.0 copy-done.6
  105.1 41.9 %attention.1 = bf16[16,160,128]{2,1,0:T(8,128)(2,1)} custom-call(s32[16]{0:T(128)S(1)} %stack.165.pos_ref, f32[2,64]{1,0:T(2,128)S(1)} %copy-done.15, f32[1,5120]{1,0:T(1,128)S(1)} %bitcast.47, bf16[1440,128]{1,0:T(8,128)(2,1)S(1)} %copy-done.4, bf16[1440,128]{1,0:T(8,128)(2,1)S(1)} %copy-done.6, bf16[1440,128]{1,0:T(8,128)(2,1)S(1)} %copy-done.8, ...), custom_call_target="tpu_custom_call" | custom-call | tf_op jit(solution)/shard_map/attention/pallas_call | solution.py:119
  147.0 5.5 %all-to-all-start = ((bf16[16,160,128]{2,1,0:T(8,128)(2,1)}), bf16[16,160,128]{2,1,0:T(8,128)(2,1)S(1)}, u32[]{:S(2)}, u32[]{:S(2)}) async-start(bf16[16,160,128]{2,1,0:T(8,128)(2,1)} %attention.1), calls=%async_computation | async-start | bytes 1310720 | tf_op jit(solution)/shard_map/all_to_all | solution.py:305
  156.8 6.6 %all-to-all-done.heads_ref = bf16[16,160,128]{2,1,0:T(8,128)(2,1)S(1)} async-done(((bf16[16,160,128]{2,1,0:T(8,128)(2,1)}), bf16[16,160,128]{2,1,0:T(8,128)(2,1)S(1)}, u32[]{:S(2)}, u32[]{:S(2)}) %all-to-all-start) | async-done | bytes 655392 | tf_op jit(solution)/shard_map/all_to_all | solution.py:305
  163.4 4.1 %output.1 = bf16[320,2048]{1,0:T(8,128)(2,1)} custom-call(s32[16]{0:T(128)S(1)} %stack.141.head_ref, s32[8]{0:T(128)S(1)} %stack.150.idx_ref.col_ref, bf16[16,160,128]{2,1,0:T(8,128)(2,1)S(1)} %all-to-all-done.heads_ref, bf16[1024,256]{1,0:T(8,128)(2,1)S(1)} %join.1.refs_0_, bf16[1024,256]{1,0:T(8,128)(2,1)} %collective-permute-done.22.refs_1_, ...), custom_call_target="tpu_custom_call" | custom-call | tf_op jit(solution)/shard_map/output/pallas_call | solution.py:247
  (70 shorter events, 16.5 us)
Async XLA Ops:
  0.0 28.4 %collective-permute-start = (bf16[320,2048]{1,0:T(8,128)(2,1)}, bf16[320,2048]{1,0:T(8,128)(2,1)}, u32[]{:S(2)}, u32[]{:S(2)}) collective-permute-start(bf16[320,2048]{1,0:T(8,128)(2,1)} %bitcast.44), channel_id=1, source_target_pairs={{0,24},{1,9},{8,0},{9,17},{16,8},{17,25},{24,16},{25,1},{2,26},{3,... | collective-permute-start | bytes 3932168 | tf_op jit(solution)/shard_map/ppermute | solution.py:269
  3.9 8.2 %collective-permute-start.2 = (bf16[256,256]{1,0:T(8,128)(2,1)S(1)}, bf16[256,256]{1,0:T(8,128)(2,1)S(1)}, u32[]{:S(2)}, u32[]{:S(2)}) collective-permute-start(bf16[256,256]{1,0:T(8,128)(2,1)S(1)} %pad_maximum_fusion.refs_0_), channel_id=1, source_target_pairs={{0,96},{32,0},{64,32},{96,64},{1,97},{33,1},{65,33},{97,65},{2,98}... | collective-permute-start | bytes 393224 | tf_op jit(solution)/shard_map/ppermute | solution.py:264
  8.1 6.6 %collective-permute-start.3 = (bf16[256,256]{1,0:T(8,128)(2,1)S(1)}, bf16[256,256]{1,0:T(8,128)(2,1)S(1)}, u32[]{:S(2)}, u32[]{:S(2)}) collective-permute-start(bf16[256,256]{1,0:T(8,128)(2,1)S(1)} %pad_maximum_fusion.refs_0_), channel_id=1, source_target_pairs={{0,64},{32,96},{64,0},{96,32},{1,65},{33,97},{65,1},{97,33},{2,66}... | collective-permute-start | bytes 393224 | tf_op jit(solution)/shard_map/ppermute | solution.py:264
  8.1 7.6 %collective-permute-start.4 = (bf16[256,256]{1,0:T(8,128)(2,1)S(1)}, bf16[256,256]{1,0:T(8,128)(2,1)S(1)}, u32[]{:S(2)}, u32[]{:S(2)}) collective-permute-start(bf16[256,256]{1,0:T(8,128)(2,1)S(1)} %pad_maximum_fusion.refs_0_), channel_id=1, source_target_pairs={{0,32},{32,64},{64,96},{96,0},{1,33},{33,65},{65,97},{97,1},{2,34}... | collective-permute-start | bytes 393224 | tf_op jit(solution)/shard_map/ppermute | solution.py:264
  9.3 38.6 %collective-permute-start.1 = (bf16[320,2048]{1,0:T(8,128)(2,1)}, bf16[320,2048]{1,0:T(8,128)(2,1)}, u32[]{:S(2)}, u32[]{:S(2)}) collective-permute-start(bf16[320,2048]{1,0:T(8,128)(2,1)} %bitcast.45), channel_id=1, source_target_pairs={{0,8},{1,25},{8,16},{9,1},{16,24},{17,9},{24,0},{25,17},{2,10},{3,... | collective-permute-start | bytes 3932168 | tf_op jit(solution)/shard_map/ppermute | solution.py:269
  15.7 48.3 %copy-start.11 = (bf16[256,256]{1,0:T(8,128)(2,1)}, bf16[256,256]{1,0:T(8,128)(2,1)S(1)}, u32[]{:S(2)}) copy-start(bf16[256,256]{1,0:T(8,128)(2,1)S(1)} %get-tuple-element.39.refs_0_) | copy-start | bytes 393220
  15.7 20.0 %collective-permute-start.5 = (bf16[768,256]{1,0:T(8,128)(2,1)S(1)}, bf16[768,256]{1,0:T(8,128)(2,1)S(1)}, u32[]{:S(2)}, u32[]{:S(2)}) collective-permute-start(bf16[768,256]{1,0:T(8,128)(2,1)S(1)} %get-tuple-element.25.refs_3_.refs_1_), channel_id=1, source_target_pairs={{0,6},{2,0},{4,2},{6,4},{1,7},{3,1},{5,3},{7,5},{8,14},{10,8},{12,... | collective-permute-start | bytes 1179656 | tf_op jit(solution)/shard_map/ppermute | solution.py:264
  28.4 50.1 %collective-permute-start.15 = (bf16[320,2048]{1,0:T(8,128)(2,1)}, bf16[320,2048]{1,0:T(8,128)(2,1)}, u32[]{:S(2)}, u32[]{:S(2)}) collective-permute-start(bf16[320,2048]{1,0:T(8,128)(2,1)} %collective-permute-done.refs_1_), channel_id=1, source_target_pairs={{0,24},{1,9},{8,0},{9,17},{16,8},{17,25},{24,16},{25,1},{2,26},{3,... | collective-permute-start | bytes 3932168 | tf_op jit(solution)/shard_map/ppermute | solution.py:269
  32.1 9.4 %collective-permute-start.6 = (bf16[768,256]{1,0:T(8,128)(2,1)S(1)}, bf16[768,256]{1,0:T(8,128)(2,1)S(1)}, u32[]{:S(2)}, u32[]{:S(2)}) collective-permute-start(bf16[768,256]{1,0:T(8,128)(2,1)S(1)} %get-tuple-element.25.refs_3_.refs_1_), channel_id=1, source_target_pairs={{0,4},{2,6},{4,0},{6,2},{1,5},{3,7},{5,1},{7,3},{8,12},{10,14},{12... | collective-permute-start | bytes 1179656 | tf_op jit(solution)/shard_map/ppermute | solution.py:264
  35.1 10.5 %collective-permute-start.7 = (bf16[768,256]{1,0:T(8,128)(2,1)S(1)}, bf16[768,256]{1,0:T(8,128)(2,1)S(1)}, u32[]{:S(2)}, u32[]{:S(2)}) collective-permute-start(bf16[768,256]{1,0:T(8,128)(2,1)S(1)} %get-tuple-element.25.refs_3_.refs_1_), channel_id=1, source_target_pairs={{0,2},{2,4},{4,6},{6,0},{1,3},{3,5},{5,7},{7,1},{8,10},{10,12},{12... | collective-permute-start | bytes 1179656 | tf_op jit(solution)/shard_map/ppermute | solution.py:264
  35.7 9.9 %collective-permute-start.8 = (bf16[768,256]{1,0:T(8,128)(2,1)S(1)}, bf16[768,256]{1,0:T(8,128)(2,1)S(1)}, u32[]{:S(2)}, u32[]{:S(2)}) collective-permute-start(bf16[768,256]{1,0:T(8,128)(2,1)S(1)} %get-tuple-element.25.refs_3_.refs_1_), channel_id=1, source_target_pairs={{0,1},{1,0},{2,3},{3,2},{4,5},{5,4},{6,7},{7,6},{8,9},{9,8},{10,11... | collective-permute-start | bytes 1179656 | tf_op jit(solution)/shard_map/ppermute | solution.py:264
  41.5 4.7 %collective-permute-start.9 = (bf16[768,256]{1,0:T(8,128)(2,1)S(1)}, bf16[768,256]{1,0:T(8,128)(2,1)S(1)}, u32[]{:S(2)}, u32[]{:S(2)}) collective-permute-start(bf16[768,256]{1,0:T(8,128)(2,1)S(1)} %collective-permute-done.5.refs_4_.refs_2_), channel_id=1, source_target_pairs={{0,1},{1,0},{2,3},{3,2},{4,5},{5,4},{6,7},{7,6},{8,9},{9,8},{10,11... | collective-permute-start | bytes 1179656 | tf_op jit(solution)/shard_map/ppermute | solution.py:264
  45.6 1.7 %collective-permute-start.10 = (bf16[768,256]{1,0:T(8,128)(2,1)S(1)}, bf16[768,256]{1,0:T(8,128)(2,1)S(1)}, u32[]{:S(2)}, u32[]{:S(2)}) collective-permute-start(bf16[768,256]{1,0:T(8,128)(2,1)S(1)} %collective-permute-done.6.refs_5_.refs_3_), channel_id=1, source_target_pairs={{0,1},{1,0},{2,3},{3,2},{4,5},{5,4},{6,7},{7,6},{8,9},{9,8},{10,11... | collective-permute-start | bytes 1179656 | tf_op jit(solution)/shard_map/ppermute | solution.py:264
  45.6 2.3 %collective-permute-start.11 = (bf16[768,256]{1,0:T(8,128)(2,1)S(1)}, bf16[768,256]{1,0:T(8,128)(2,1)S(1)}, u32[]{:S(2)}, u32[]{:S(2)}) collective-permute-start(bf16[768,256]{1,0:T(8,128)(2,1)S(1)} %collective-permute-done.7.refs_6_.refs_4_), channel_id=1, source_target_pairs={{0,1},{1,0},{2,3},{3,2},{4,5},{5,4},{6,7},{7,6},{8,9},{9,8},{10,11... | collective-permute-start | bytes 1179656 | tf_op jit(solution)/shard_map/ppermute | solution.py:264
  58.7 18.6 %collective-permute-start.12 = (bf16[1440,128]{1,0:T(8,128)(2,1)S(1)}, bf16[1440,128]{1,0:T(8,128)(2,1)S(1)}, u32[]{:S(2)}, u32[]{:S(2)}) collective-permute-start(bf16[1440,128]{1,0:T(8,128)(2,1)S(1)} %get-tuple-element.32), channel_id=1, source_target_pairs={{0,32},{32,64},{64,96},{96,0},{1,33},{33,65},{65,97},{97,1},{2,34}... | collective-permute-start | bytes 1105928 | tf_op jit(solution)/shard_map/ppermute | solution.py:264
  60.3 6.4 %collective-permute-start.19 = (bf16[256,256]{1,0:T(8,128)(2,1)S(1)}, bf16[256,256]{1,0:T(8,128)(2,1)S(1)}, u32[]{:S(2)}, u32[]{:S(2)}) collective-permute-start(bf16[256,256]{1,0:T(8,128)(2,1)S(1)} %get-tuple-element.39.refs_0_), channel_id=1, source_target_pairs={{0,6},{2,0},{4,2},{6,4},{1,7},{3,1},{5,3},{7,5},{8,14},{10,8},{12,... | collective-permute-start | bytes 393224 | tf_op jit(solution)/shard_map/ppermute | solution.py:264
  60.9 11.5 %collective-permute-start.20 = (bf16[256,256]{1,0:T(8,128)(2,1)S(1)}, bf16[256,256]{1,0:T(8,128)(2,1)S(1)}, u32[]{:S(2)}, u32[]{:S(2)}) collective-permute-start(bf16[256,256]{1,0:T(8,128)(2,1)S(1)} %get-tuple-element.39.refs_0_), channel_id=1, source_target_pairs={{0,4},{2,6},{4,0},{6,2},{1,5},{3,7},{5,1},{7,3},{8,12},{10,14},{12... | collective-permute-start | bytes 393224 | tf_op jit(solution)/shard_map/ppermute | solution.py:264
  64.0 8.4 %collective-permute-start.21 = (bf16[256,256]{1,0:T(8,128)(2,1)S(1)}, bf16[256,256]{1,0:T(8,128)(2,1)S(1)}, u32[]{:S(2)}, u32[]{:S(2)}) collective-permute-start(bf16[256,256]{1,0:T(8,128)(2,1)S(1)} %get-tuple-element.39.refs_0_), channel_id=1, source_target_pairs={{0,2},{2,4},{4,6},{6,0},{1,3},{3,5},{5,7},{7,1},{8,10},{10,12},{12... | collective-permute-start | bytes 393224 | tf_op jit(solution)/shard_map/ppermute | solution.py:264
  66.7 20.5 %collective-permute-start.13 = (bf16[1440,128]{1,0:T(8,128)(2,1)S(1)}, bf16[1440,128]{1,0:T(8,128)(2,1)S(1)}, u32[]{:S(2)}, u32[]{:S(2)}) collective-permute-start(bf16[1440,128]{1,0:T(8,128)(2,1)S(1)} %get-tuple-element.33), channel_id=1, source_target_pairs={{0,64},{32,96},{64,0},{96,32},{1,65},{33,97},{65,1},{97,33},{2,66}... | collective-permute-start | bytes 1105928 | tf_op jit(solution)/shard_map/ppermute | solution.py:264
  73.3 27.1 %copy-start.15 = (f32[2,64]{1,0:T(2,128)S(1)}, f32[2,64]{1,0:T(2,128)}, u32[]{:S(2)}) copy-start(f32[2,64]{1,0:T(2,128)} %gain_ref.5) | copy-start | bytes 1540
  73.4 73.7 %collective-permute-start.22 = (bf16[1024,256]{1,0:T(8,128)(2,1)S(1)}, bf16[1024,256]{1,0:T(8,128)(2,1)}, u32[]{:S(2)}, u32[]{:S(2)}) collective-permute-start(bf16[1024,256]{1,0:T(8,128)(2,1)S(1)} %join.1.refs_0_), channel_id=1, source_target_pairs={{0,24},{8,0},{16,8},{24,16},{1,25},{9,1},{17,9},{25,17},{2,26},{10... | collective-permute-start | bytes 1572872 | tf_op jit(solution)/shard_map/ppermute | solution.py:264
  75.1 71.9 %collective-permute-start.23 = (bf16[1024,256]{1,0:T(8,128)(2,1)S(1)}, bf16[1024,256]{1,0:T(8,128)(2,1)}, u32[]{:S(2)}, u32[]{:S(2)}) collective-permute-start(bf16[1024,256]{1,0:T(8,128)(2,1)S(1)} %join.1.refs_0_), channel_id=1, source_target_pairs={{0,16},{8,24},{16,0},{24,8},{1,17},{9,25},{17,1},{25,9},{2,18},{10... | collective-permute-start | bytes 1572872 | tf_op jit(solution)/shard_map/ppermute | solution.py:264
  78.1 69.0 %collective-permute-start.24 = (bf16[1024,256]{1,0:T(8,128)(2,1)S(1)}, bf16[1024,256]{1,0:T(8,128)(2,1)}, u32[]{:S(2)}, u32[]{:S(2)}) collective-permute-start(bf16[1024,256]{1,0:T(8,128)(2,1)S(1)} %join.1.refs_0_), channel_id=1, source_target_pairs={{0,8},{8,16},{16,24},{24,0},{1,9},{9,17},{17,25},{25,1},{2,10},{10... | collective-permute-start | bytes 1572872 | tf_op jit(solution)/shard_map/ppermute | solution.py:264
  78.5 9.6 %collective-permute-start.14 = (bf16[1440,128]{1,0:T(8,128)(2,1)S(1)}, bf16[1440,128]{1,0:T(8,128)(2,1)S(1)}, u32[]{:S(2)}, u32[]{:S(2)}) collective-permute-start(bf16[1440,128]{1,0:T(8,128)(2,1)S(1)} %get-tuple-element.34), channel_id=1, source_target_pairs={{0,96},{32,0},{64,32},{96,64},{1,97},{33,1},{65,33},{97,65},{2,98}... | collective-permute-start | bytes 1105928 | tf_op jit(solution)/shard_map/ppermute | solution.py:264
  88.0 7.3 %collective-permute-start.16 = (bf16[480,128]{1,0:T(8,128)(2,1)S(1)}, bf16[480,128]{1,0:T(8,128)(2,1)S(1)}, u32[]{:S(2)}, u32[]{:S(2)}) collective-permute-start(bf16[480,128]{1,0:T(8,128)(2,1)S(1)} %get-tuple-element.36), channel_id=1, source_target_pairs={{0,32},{32,64},{64,96},{96,0},{1,33},{33,65},{65,97},{97,1},{2,34}... | collective-permute-start | bytes 368648 | tf_op jit(solution)/shard_map/ppermute | solution.py:264
  88.8 9.3 %collective-permute-start.17 = (bf16[480,128]{1,0:T(8,128)(2,1)}, bf16[480,128]{1,0:T(8,128)(2,1)S(1)}, u32[]{:S(2)}, u32[]{:S(2)}) collective-permute-start(bf16[480,128]{1,0:T(8,128)(2,1)} %get-tuple-element.37), channel_id=1, source_target_pairs={{0,64},{32,96},{64,0},{96,32},{1,65},{33,97},{65,1},{97,33},{2,66}... | collective-permute-start | bytes 368648 | tf_op jit(solution)/shard_map/ppermute | solution.py:264
  95.3 5.1 %collective-permute-start.18 = (bf16[480,128]{1,0:T(8,128)(2,1)}, bf16[480,128]{1,0:T(8,128)(2,1)S(1)}, u32[]{:S(2)}, u32[]{:S(2)}) collective-permute-start(bf16[480,128]{1,0:T(8,128)(2,1)} %get-tuple-element.38), channel_id=1, source_target_pairs={{0,96},{32,0},{64,32},{96,64},{1,97},{33,1},{65,33},{97,65},{2,98}... | collective-permute-start | bytes 368648 | tf_op jit(solution)/shard_map/ppermute | solution.py:264
  147.0 16.3 %all-to-all-start = ((bf16[16,160,128]{2,1,0:T(8,128)(2,1)}), bf16[16,160,128]{2,1,0:T(8,128)(2,1)S(1)}, u32[]{:S(2)}, u32[]{:S(2)}) async-start(bf16[16,160,128]{2,1,0:T(8,128)(2,1)} %attention.1), calls=%async_computation | async-start | bytes 1310720 | tf_op jit(solution)/shard_map/all_to_all | solution.py:305
  152.5 2.0 %collective-permute-start.25 = (bf16[1024,256]{1,0:T(8,128)(2,1)S(1)}, bf16[1024,256]{1,0:T(8,128)(2,1)S(1)}, u32[]{:S(2)}, u32[]{:S(2)}) collective-permute-start(bf16[1024,256]{1,0:T(8,128)(2,1)S(1)} %join.1.refs_0_), channel_id=1, source_target_pairs={{0,1},{1,0},{2,3},{3,2},{4,5},{5,4},{6,7},{7,6},{8,9},{9,8},{10,11... | collective-permute-start | bytes 1572872 | tf_op jit(solution)/shard_map/ppermute | solution.py:264
  152.6 2.6 %collective-permute-start.26 = (bf16[1024,256]{1,0:T(8,128)(2,1)}, bf16[1024,256]{1,0:T(8,128)(2,1)S(1)}, u32[]{:S(2)}, u32[]{:S(2)}) collective-permute-start(bf16[1024,256]{1,0:T(8,128)(2,1)} %collective-permute-done.22.refs_1_), channel_id=1, source_target_pairs={{0,1},{1,0},{2,3},{3,2},{4,5},{5,4},{6,7},{7,6},{8,9},{9,8},{10,11... | collective-permute-start | bytes 1572872 | tf_op jit(solution)/shard_map/ppermute | solution.py:264
  153.1 2.9 %collective-permute-start.27 = (bf16[1024,256]{1,0:T(8,128)(2,1)}, bf16[1024,256]{1,0:T(8,128)(2,1)S(1)}, u32[]{:S(2)}, u32[]{:S(2)}) collective-permute-start(bf16[1024,256]{1,0:T(8,128)(2,1)} %collective-permute-done.23.refs_2_), channel_id=1, source_target_pairs={{0,1},{1,0},{2,3},{3,2},{4,5},{5,4},{6,7},{7,6},{8,9},{9,8},{10,11... | collective-permute-start | bytes 1572872 | tf_op jit(solution)/shard_map/ppermute | solution.py:264
  153.2 3.6 %collective-permute-start.28 = (bf16[1024,256]{1,0:T(8,128)(2,1)}, bf16[1024,256]{1,0:T(8,128)(2,1)S(1)}, u32[]{:S(2)}, u32[]{:S(2)}) collective-permute-start(bf16[1024,256]{1,0:T(8,128)(2,1)} %collective-permute-done.24.refs_3_), channel_id=1, source_target_pairs={{0,1},{1,0},{2,3},{3,2},{4,5},{5,4},{6,7},{7,6},{8,9},{9,8},{10,11... | collective-permute-start | bytes 1572872 | tf_op jit(solution)/shard_map/ppermute | solution.py:264
  (14 other events, 43.2 us)

commit v5 on v3

--- a/solution.py
+++ b/solution.py
@@ -16,7 +16,7 @@
 T = 5120
 BLK = 320
 BQ = 512
-W = 1024
+W = 2048
 NT = (((1,), (1,)), ((), ()))
 NN = (((1,), (0,)), ((), ()))
 f32 = jnp.float32
@@ -27,7 +27,7 @@
 
 def attn_kernel(pos_ref, gain_ref, d_ref, *refs, nblk):
     nin=len(nblk)
-    ins=refs[:nin]; out_ref=refs[nin]; ka,qa,vs,vt,ot=refs[nin+1:]
+    ins=refs[:nin]; out_ref=refs[nin]; ka,qa,vs,vt,ot,rows=refs[nin+1:]
     lane=lax.broadcasted_iota(jnp.int32,(BLK,128),1)
     lo=lane<64
     lanev=lax.broadcasted_iota(jnp.int32,(BLK//2,128),1)
@@ -45,20 +45,29 @@
             v=a[b*480+320:b*480+480,:].astype(f32)
             vs[pl.ds(base,BLK//2),:]=jnp.where(lanev<64,v,tail)
             vs[pl.ds(base+BLK//2,BLK//2),:]=jnp.where(lanev<64,pltpu.roll(v,64,1),tail)
-    x=d_ref[...]*LOG2E
+    x=jnp.concatenate([d_ref[0:1,i*BQ:(i+1)*BQ] for i in range(T//BQ)]+[jnp.zeros((16-T//BQ,BQ),f32)],0)*LOG2E
     h=x.astype(bf16).astype(f32)
     m=(x-h).astype(bf16).astype(f32)
     l=x-h-m
-    dt=jnp.concatenate([-h,-m,-l,h,m,l,jnp.zeros((80,640),f32)],0).T
-    dl=lax.broadcasted_iota(jnp.int32,(640,128),1)
-    key_one=jnp.where((dl>=24)&(dl<48),1.0,0.0)
-    query_one=jnp.where(dl<24,1.0,0.0)
-    for i in range(T//640):
-        s=slice(i*640,(i+1)*640)
-        ka[s,128:256]=jnp.where((dl==i)|(dl==8+i)|(dl==16+i),dt,key_one).astype(bf16)
-        qa[s,128:256]=jnp.where((dl==24+i)|(dl==32+i)|(dl==40+i),dt,query_one).astype(bf16)
-    for i in range(T//256):
-        vt[:,i*256:(i+1)*256]=vs[i*256:(i+1)*256,:].T[0:80].astype(bf16)
+    dt=jnp.concatenate([-h,-m,-l,h,m,l,jnp.zeros((32,BQ),f32)],0).T
+    dl=lax.broadcasted_iota(jnp.int32,(BQ,128),1)
+    key_one=jnp.where((dl>=48)&(dl<96),1.0,0.0)
+    query_one=jnp.where(dl<48,1.0,0.0)
+
+    def prepare(i):
+        s=slice(i*BQ,(i+1)*BQ)
+        ka[s,128:256]=jnp.where((dl==i)|(dl==16+i)|(dl==32+i),dt,key_one).astype(bf16)
+        qa[s,128:256]=jnp.where((dl==48+i)|(dl==64+i)|(dl==80+i),dt,query_one).astype(bf16)
+        vt[:,s]=vs[s,:].T[0:80].astype(bf16)
+
+    def emit(i):
+        s=slice(i*BQ,(i+1)*BQ)
+        rows[s,0:64]=ot[:,s].T
+        for j in range(T//BLK):
+            if i*BQ<(j+1)*BLK<=(i+1)*BQ:
+                a=rows[j*BLK:j*BLK+160,:]
+                b=rows[j*BLK+160:(j+1)*BLK,:]
+                out_ref[j]=jnp.where(lanev<64,a,pltpu.roll(b,64,1)).astype(bf16)
 
     def finish(acc):
         o=acc[0:64]/acc[64:65]
@@ -69,6 +78,7 @@
         keep=kio<=qio
         for qi in range(T//BQ):
             q0=qi*BQ
+            prepare(qi)
             qb=qa[q0:q0+BQ,:]
             def tile(k0,w,mask):
                 s=lax.dot_general(ka[k0:k0+w,:],qb,NT,preferred_element_type=f32)
@@ -80,8 +90,11 @@
             for k0 in range(0,q0,W):
                 acc=acc+tile(k0,min(W,q0-k0),False)
             ot[:,q0:q0+BQ]=finish(acc)
+            emit(qi)
 
     def slow():
+        for i in range(T//BQ):
+            prepare(i)
         kio=lax.broadcasted_iota(jnp.int32,(BQ,BQ),0); qio=lax.broadcasted_iota(jnp.int32,(BQ,BQ),1)
         def per_q(qi,_):
             q0=pl.multiple_of(qi*BQ,BQ)
@@ -101,16 +114,12 @@
             ot[:,pl.ds(q0,BQ)]=finish(acc)
             return 0
         lax.fori_loop(0,T//BQ,per_q,0)
+        for i in range(T//BQ):
+            emit(i)
     g=jnp.abs(gain_ref[...])
     isfast=jnp.max(g[0:1])*jnp.max(g[1:2])<=7.7
     pl.when(isfast)(fast)
     pl.when(jnp.logical_not(isfast))(slow)
-    for i in range(T//256):
-        s=slice(i*256,(i+1)*256)
-        vs[s,0:64]=ot[:,s].T
-    for j in range(T//BLK):
-        a=vs[j*BLK:j*BLK+160,:]; b=vs[j*BLK+160:(j+1)*BLK,:]
-        out_ref[j]=jnp.where(lanev<64,a,pltpu.roll(b,64,1)).astype(bf16)
 
 
 def attention(pos,gain,d,ins,nblk):
@@ -119,7 +128,7 @@
         out_shape=jax.ShapeDtypeStruct((16,160,128),bf16),
         in_specs=[SMEM]+[VMEM]*(2+len(ins)),
         out_specs=VMEM,
-        scratch_shapes=[V((T,256),bf16),V((T,256),bf16),V((T,128),f32),V((80,T),bf16),V((64,T),f32)],
+        scratch_shapes=[V((T,256),bf16),V((T,256),bf16),V((T,128),f32),V((80,T),bf16),V((64,T),f32),V((T,128),f32)],
         compiler_params=pltpu.CompilerParams(vmem_limit_bytes=24*1024*1024),
         name="attention")(pos,gain,d,*ins)
 
@@ -279,10 +288,9 @@
     cols = jnp.stack(
         [2 * ((x + d) % 4) + e for e in (c, 1 - c) for d in range(4)]
     ).astype(jnp.int32)
-    gain, decay = lax.optimization_barrier((qk_gain, decay_sums.reshape(8, 640)))
-    part1 = project(cols, gain, [[own], [t1], [t3]], ws)
+    part1 = project(cols, qk_gain, [[own], [t1], [t3]], ws)
     *part1, wo4 = lax.optimization_barrier((*part1, wo4))
-    part2 = project(cols, gain, [[t2]], ws)
+    part2 = project(cols, qk_gain, [[t2]], ws)
     recv = []
     for part in (part1, part2):
         recv += [part[0]] + [move(part[d], Z, d) for d in (1, 2, 3)]
@@ -291,7 +299,7 @@
     pos = [4 * ((z - d) % 4) + (y + e) % 4 for d in range(4) for e in (0, near, 4 - near)]
     pos += [4 * ((z - d) % 4) + (y + 2) % 4 for d in range(4)]
     pos = jnp.stack(pos).astype(jnp.int32)
-    heads = attention(pos, gain, decay, recv, (3, 3, 3, 3, 1, 1, 1, 1))
+    heads = attention(pos, qk_gain, decay_sums[0], recv, (3, 3, 3, 3, 1, 1, 1, 1))
     heads, *wo = lax.optimization_barrier((heads, *wo))
     wo = wo + [move(w, C, 0) for w in wo]
     merged = lax.all_to_all(heads, SP, 0, 0, tiled=True)

time: 165 us -> 164 us (level)
  waiting for transfers between devices: 41.9 us -> 44.8 us
    ppermute x26, waiting for transfers between devices: 25.4 us -> 28.4 us  [move(): return lax.ppermute(value, axis, pairs)]
    unnamed x33 -> x32, local copies, waits for them, and re-layouts: 11.3 us -> 10.7 us
  transfers between devices with their start and end apart: 30 -> 30, of which waited for: 15 -> 18; matrix products, arithmetic and copies ran while one was open for 2% -> 1% of each run, Pallas kernels for 32% -> 32%
where the time goes in v5:
time: 164 us; the launch traced here: 163 us
  Pallas kernels  56 us (34%)
  starting transfers between devices  50.6 us (31%)
  waiting for transfers between devices  44.8 us (27%)
  local copies, waits for them, and re-layouts  11 us (7%)
    pallas_call x1, Pallas kernels, attention(): pl.pallas_call(functools.partial(attn_kernel, nblk=nblk), out_shape=jax.S...  41.3 us
    ppermute x26, starting transfers between devices, move(): return lax.ppermute(value, axis, pairs)  38.3 us
    ppermute x26, waiting for transfers between devices, move(): return lax.ppermute(value, axis, pairs)  28.4 us
    unnamed x32, local copies, waits for them, and re-layouts  10.7 us
    pallas_call x2, Pallas kernels, project(): pl.pallas_call(functools.partial(proj_kernel, sizes=tuple((len(b) for b i...  10.4 us
    ppermute x3, waiting for transfers between devices, spread(): return lax.ppermute(value, (Y, C), pairs)  9.88 us
    ppermute x3, starting transfers between devices, spread(): return lax.ppermute(value, (Y, C), pairs)  6.82 us
    all_to_all x1, waiting for transfers between devices, on_device(): merged = lax.all_to_all(heads, SP, 0, 0, tiled=True)  6.6 us
  transfers between devices with their start and end apart: 30, of which 18 were waited for; matrix products, arithmetic and copies ran while one was open for 1% of the time, Pallas kernels for 32%

profile of v5, /device:TPU:0, one launch (start us, length us, event | category | flops | bytes accessed | tf_op | source)
XLA Modules:
  0.0 163.3 jit_solution(18103076558642477185)
XLA Ops:
  0.0 3.1 %collective-permute-start = (bf16[320,2048]{1,0:T(8,128)(2,1)}, bf16[320,2048]{1,0:T(8,128)(2,1)}, u32[]{:S(2)}, u32[]{:S(2)}) collective-permute-start(bf16[320,2048]{1,0:T(8,128)(2,1)} %bitcast.44), channel_id=1, source_target_pairs={{0,24},{1,9},{8,0},{9,17},{16,8},{17,25},{24,16},{25,1},{2,26},{3,... | collective-permute-start | bytes 3932168 | tf_op jit(solution)/shard_map/ppermute | solution.py:269
  3.9 4.1 %collective-permute-start.2 = (bf16[256,256]{1,0:T(8,128)(2,1)S(1)}, bf16[256,256]{1,0:T(8,128)(2,1)S(1)}, u32[]{:S(2)}, u32[]{:S(2)}) collective-permute-start(bf16[256,256]{1,0:T(8,128)(2,1)S(1)} %pad_maximum_fusion.refs_0_), channel_id=1, source_target_pairs={{0,96},{32,0},{64,32},{96,64},{1,97},{33,1},{65,33},{97,65},{2,98}... | collective-permute-start | bytes 393224 | tf_op jit(solution)/shard_map/ppermute | solution.py:264
  8.1 1.3 collective-permute-start.4
  9.3 2.8 %collective-permute-done.2.refs_1_ = bf16[256,256]{1,0:T(8,128)(2,1)S(1)} collective-permute-done((bf16[256,256]{1,0:T(8,128)(2,1)S(1)}, bf16[256,256]{1,0:T(8,128)(2,1)S(1)}, u32[]{:S(2)}, u32[]{:S(2)}) %collective-permute-start.2) | collective-permute-done | bytes 131104 | tf_op jit(solution)/shard_map/ppermute | solution.py:264
  12.2 2.5 %collective-permute-done.3.refs_2_ = bf16[256,256]{1,0:T(8,128)(2,1)S(1)} collective-permute-done((bf16[256,256]{1,0:T(8,128)(2,1)S(1)}, bf16[256,256]{1,0:T(8,128)(2,1)S(1)}, u32[]{:S(2)}, u32[]{:S(2)}) %collective-permute-start.3) | collective-permute-done | bytes 131104 | tf_op jit(solution)/shard_map/ppermute | solution.py:264
  14.6 1.0 collective-permute-done.4.refs_3_
  15.7 2.8 %collective-permute-start.5 = (bf16[768,256]{1,0:T(8,128)(2,1)S(1)}, bf16[768,256]{1,0:T(8,128)(2,1)S(1)}, u32[]{:S(2)}, u32[]{:S(2)}) collective-permute-start(bf16[768,256]{1,0:T(8,128)(2,1)S(1)} %get-tuple-element.25.refs_3_.refs_1_), channel_id=1, source_target_pairs={{0,6},{2,0},{4,2},{6,4},{1,7},{3,1},{5,3},{7,5},{8,14},{10,8},{12,... | collective-permute-start | bytes 1179656 | tf_op jit(solution)/shard_map/ppermute | solution.py:264
  18.5 9.9 %collective-permute-done.refs_1_ = bf16[320,2048]{1,0:T(8,128)(2,1)} collective-permute-done((bf16[320,2048]{1,0:T(8,128)(2,1)}, bf16[320,2048]{1,0:T(8,128)(2,1)}, u32[]{:S(2)}, u32[]{:S(2)}) %collective-permute-start) | collective-permute-done | bytes 1310752 | tf_op jit(solution)/shard_map/ppermute | solution.py:269
  28.4 3.7 %collective-permute-start.15 = (bf16[320,2048]{1,0:T(8,128)(2,1)}, bf16[320,2048]{1,0:T(8,128)(2,1)}, u32[]{:S(2)}, u32[]{:S(2)}) collective-permute-start(bf16[320,2048]{1,0:T(8,128)(2,1)} %collective-permute-done.refs_1_), channel_id=1, source_target_pairs={{0,24},{1,9},{8,0},{9,17},{16,8},{17,25},{24,16},{25,1},{2,26},{3,... | collective-permute-start | bytes 3932168 | tf_op jit(solution)/shard_map/ppermute | solution.py:269
  32.1 3.0 %collective-permute-start.6 = (bf16[768,256]{1,0:T(8,128)(2,1)S(1)}, bf16[768,256]{1,0:T(8,128)(2,1)S(1)}, u32[]{:S(2)}, u32[]{:S(2)}) collective-permute-start(bf16[768,256]{1,0:T(8,128)(2,1)S(1)} %get-tuple-element.25.refs_3_.refs_1_), channel_id=1, source_target_pairs={{0,4},{2,6},{4,0},{6,2},{1,5},{3,7},{5,1},{7,3},{8,12},{10,14},{12... | collective-permute-start | bytes 1179656 | tf_op jit(solution)/shard_map/ppermute | solution.py:264
  35.7 5.8 %collective-permute-done.6.refs_5_.refs_3_ = bf16[768,256]{1,0:T(8,128)(2,1)S(1)} collective-permute-done((bf16[768,256]{1,0:T(8,128)(2,1)S(1)}, bf16[768,256]{1,0:T(8,128)(2,1)S(1)}, u32[]{:S(2)}, u32[]{:S(2)}) %collective-permute-start.6) | collective-permute-done | bytes 393248 | tf_op jit(solution)/shard_map/ppermute | solution.py:264
  41.5 4.1 %collective-permute-done.7.refs_6_.refs_4_ = bf16[768,256]{1,0:T(8,128)(2,1)S(1)} collective-permute-done((bf16[768,256]{1,0:T(8,128)(2,1)S(1)}, bf16[768,256]{1,0:T(8,128)(2,1)S(1)}, u32[]{:S(2)}, u32[]{:S(2)}) %collective-permute-start.7) | collective-permute-done | bytes 393248 | tf_op jit(solution)/shard_map/ppermute | solution.py:264
  46.2 1.1 collective-permute-done.10.refs_9_.refs_7_
  47.9 1.5 copy-done.2
  50.0 6.1 %project.2 = (bf16[1440,128]{1,0:T(8,128)(2,1)S(1)}, bf16[1440,128]{1,0:T(8,128)(2,1)S(1)}, bf16[1440,128]{1,0:T(8,128)(2,1)S(1)}, bf16[1440,128]{1,0:T(8,128)(2,1)S(1)}) custom-call(s32[8]{0:T(128)S(1)} %stack.150.idx_ref.col_ref, f32[2,64]{1,0:T(2,128)S(1)} %copy-done.14, bf16[320,2048]{1,0:T(8,128)(2,1)S(1)} %bitcast.46, ...), custom_call_target="tpu_custom_call" | custom-call | tf_op jit(solution)/shard_map/project/pallas_call | solution.py:213
  56.9 1.6 collective-permute-start.12
  59.0 3.1 %collective-permute-start.20 = (bf16[256,256]{1,0:T(8,128)(2,1)S(1)}, bf16[256,256]{1,0:T(8,128)(2,1)S(1)}, u32[]{:S(2)}, u32[]{:S(2)}) collective-permute-start(bf16[256,256]{1,0:T(8,128)(2,1)S(1)} %get-tuple-element.39.refs_0_), channel_id=1, source_target_pairs={{0,4},{2,6},{4,0},{6,2},{1,5},{3,7},{5,1},{7,3},{8,12},{10,14},{12... | collective-permute-start | bytes 393224 | tf_op jit(solution)/shard_map/ppermute | solution.py:264
  62.1 2.7 %collective-permute-done.19.refs_1_ = bf16[256,256]{1,0:T(8,128)(2,1)S(1)} collective-permute-done((bf16[256,256]{1,0:T(8,128)(2,1)S(1)}, bf16[256,256]{1,0:T(8,128)(2,1)S(1)}, u32[]{:S(2)}, u32[]{:S(2)}) %collective-permute-start.19) | collective-permute-done | bytes 131104 | tf_op jit(solution)/shard_map/ppermute | solution.py:264
  64.8 5.7 %collective-permute-start.13 = (bf16[1440,128]{1,0:T(8,128)(2,1)S(1)}, bf16[1440,128]{1,0:T(8,128)(2,1)S(1)}, u32[]{:S(2)}, u32[]{:S(2)}) collective-permute-start(bf16[1440,128]{1,0:T(8,128)(2,1)S(1)} %get-tuple-element.33), channel_id=1, source_target_pairs={{0,64},{32,96},{64,0},{96,32},{1,65},{33,97},{65,1},{97,33},{2,66}... | collective-permute-start | bytes 1105928 | tf_op jit(solution)/shard_map/ppermute | solution.py:264
  71.5 1.7 %collective-permute-start.22 = (bf16[1024,256]{1,0:T(8,128)(2,1)S(1)}, bf16[1024,256]{1,0:T(8,128)(2,1)}, u32[]{:S(2)}, u32[]{:S(2)}) collective-permute-start(bf16[1024,256]{1,0:T(8,128)(2,1)S(1)} %join.1.refs_0_), channel_id=1, source_target_pairs={{0,24},{8,0},{16,8},{24,16},{1,25},{9,1},{17,9},{25,17},{2,26},{10... | collective-permute-start | bytes 1572872 | tf_op jit(solution)/shard_map/ppermute | solution.py:264
  73.2 2.2 %collective-permute-start.23 = (bf16[1024,256]{1,0:T(8,128)(2,1)S(1)}, bf16[1024,256]{1,0:T(8,128)(2,1)}, u32[]{:S(2)}, u32[]{:S(2)}) collective-permute-start(bf16[1024,256]{1,0:T(8,128)(2,1)S(1)} %join.1.refs_0_), channel_id=1, source_target_pairs={{0,16},{8,24},{16,0},{24,8},{1,17},{9,25},{17,1},{25,9},{2,18},{10... | collective-permute-start | bytes 1572872 | tf_op jit(solution)/shard_map/ppermute | solution.py:264
  76.6 2.7 %collective-permute-start.14 = (bf16[1440,128]{1,0:T(8,128)(2,1)S(1)}, bf16[1440,128]{1,0:T(8,128)(2,1)S(1)}, u32[]{:S(2)}, u32[]{:S(2)}) collective-permute-start(bf16[1440,128]{1,0:T(8,128)(2,1)S(1)} %get-tuple-element.34), channel_id=1, source_target_pairs={{0,96},{32,0},{64,32},{96,64},{1,97},{33,1},{65,33},{97,65},{2,98}... | collective-permute-start | bytes 1105928 | tf_op jit(solution)/shard_map/ppermute | solution.py:264
  79.3 4.3 %project.3 = (bf16[480,128]{1,0:T(8,128)(2,1)S(1)}, bf16[480,128]{1,0:T(8,128)(2,1)S(1)}, bf16[480,128]{1,0:T(8,128)(2,1)}, bf16[480,128]{1,0:T(8,128)(2,1)}) custom-call(s32[8]{0:T(128)S(1)} %stack.150.idx_ref.col_ref, f32[2,64]{1,0:T(2,128)S(1)} %copy-done.14, bf16[320,2048]{1,0:T(8,128)(2,1)} %collective-permute-done.15.refs_0_, ...), custom_call_target="tpu_custom_call" | custom-call | tf_op jit(solution)/shard_map/project/pallas_call | solution.py:213
  84.3 1.5 collective-permute-done.14.refs_3_
  86.6 4.9 %collective-permute-start.17 = (bf16[480,128]{1,0:T(8,128)(2,1)}, bf16[480,128]{1,0:T(8,128)(2,1)S(1)}, u32[]{:S(2)}, u32[]{:S(2)}) collective-permute-start(bf16[480,128]{1,0:T(8,128)(2,1)} %get-tuple-element.37), channel_id=1, source_target_pairs={{0,64},{32,96},{64,0},{96,32},{1,65},{33,97},{65,1},{97,33},{2,66}... | collective-permute-start | bytes 368648 | tf_op jit(solution)/shard_map/ppermute | solution.py:264
  91.7 2.0 %collective-permute-start.18 = (bf16[480,128]{1,0:T(8,128)(2,1)}, bf16[480,128]{1,0:T(8,128)(2,1)S(1)}, u32[]{:S(2)}, u32[]{:S(2)}) collective-permute-start(bf16[480,128]{1,0:T(8,128)(2,1)} %get-tuple-element.38), channel_id=1, source_target_pairs={{0,96},{32,0},{64,32},{96,64},{1,97},{33,1},{65,33},{97,65},{2,98}... | collective-permute-start | bytes 368648 | tf_op jit(solution)/shard_map/ppermute | solution.py:264
  94.5 2.2 %collective-permute-done.18.refs_7_ = bf16[480,128]{1,0:T(8,128)(2,1)S(1)} collective-permute-done((bf16[480,128]{1,0:T(8,128)(2,1)}, bf16[480,128]{1,0:T(8,128)(2,1)S(1)}, u32[]{:S(2)}, u32[]{:S(2)}) %collective-permute-start.18) | collective-permute-done | bytes 122912 | tf_op jit(solution)/shard_map/ppermute | solution.py:264
  96.8 1.0 copy-done.4
  101.4 41.3 %attention.1 = bf16[16,160,128]{2,1,0:T(8,128)(2,1)} custom-call(s32[16]{0:T(128)S(1)} %stack.165.pos_ref, f32[2,64]{1,0:T(2,128)S(1)} %copy-done.15, f32[1,5120]{1,0:T(1,128)S(1)} %bitcast.47, bf16[1440,128]{1,0:T(8,128)(2,1)S(1)} %copy-done.4, bf16[1440,128]{1,0:T(8,128)(2,1)S(1)} %copy-done.6, bf16[1440,128]{1,0:T(8,128)(2,1)S(1)} %copy-done.8, ...), custom_call_target="tpu_custom_call" | custom-call | tf_op jit(solution)/shard_map/attention/pallas_call | solution.py:127
  142.8 5.5 %all-to-all-start = ((bf16[16,160,128]{2,1,0:T(8,128)(2,1)}), bf16[16,160,128]{2,1,0:T(8,128)(2,1)S(1)}, u32[]{:S(2)}, u32[]{:S(2)}) async-start(bf16[16,160,128]{2,1,0:T(8,128)(2,1)} %attention.1), calls=%async_computation | async-start | bytes 1310720 | tf_op jit(solution)/shard_map/all_to_all | solution.py:305
  152.5 6.6 %all-to-all-done.heads_ref = bf16[16,160,128]{2,1,0:T(8,128)(2,1)S(1)} async-done(((bf16[16,160,128]{2,1,0:T(8,128)(2,1)}), bf16[16,160,128]{2,1,0:T(8,128)(2,1)S(1)}, u32[]{:S(2)}, u32[]{:S(2)}) %all-to-all-start) | async-done | bytes 655392 | tf_op jit(solution)/shard_map/all_to_all | solution.py:305
  159.1 4.1 %output.1 = bf16[320,2048]{1,0:T(8,128)(2,1)} custom-call(s32[16]{0:T(128)S(1)} %stack.141.head_ref, s32[8]{0:T(128)S(1)} %stack.150.idx_ref.col_ref, bf16[16,160,128]{2,1,0:T(8,128)(2,1)S(1)} %all-to-all-done.heads_ref, bf16[1024,256]{1,0:T(8,128)(2,1)S(1)} %join.1.refs_0_, bf16[1024,256]{1,0:T(8,128)(2,1)} %collective-permute-done.22.refs_1_, ...), custom_call_target="tpu_custom_call" | custom-call | tf_op jit(solution)/shard_map/output/pallas_call | solution.py:247
  (70 shorter events, 17.1 us)
Async XLA Ops:
  0.0 28.4 %collective-permute-start = (bf16[320,2048]{1,0:T(8,128)(2,1)}, bf16[320,2048]{1,0:T(8,128)(2,1)}, u32[]{:S(2)}, u32[]{:S(2)}) collective-permute-start(bf16[320,2048]{1,0:T(8,128)(2,1)} %bitcast.44), channel_id=1, source_target_pairs={{0,24},{1,9},{8,0},{9,17},{16,8},{17,25},{24,16},{25,1},{2,26},{3,... | collective-permute-start | bytes 3932168 | tf_op jit(solution)/shard_map/ppermute | solution.py:269
  3.9 8.2 %collective-permute-start.2 = (bf16[256,256]{1,0:T(8,128)(2,1)S(1)}, bf16[256,256]{1,0:T(8,128)(2,1)S(1)}, u32[]{:S(2)}, u32[]{:S(2)}) collective-permute-start(bf16[256,256]{1,0:T(8,128)(2,1)S(1)} %pad_maximum_fusion.refs_0_), channel_id=1, source_target_pairs={{0,96},{32,0},{64,32},{96,64},{1,97},{33,1},{65,33},{97,65},{2,98}... | collective-permute-start | bytes 393224 | tf_op jit(solution)/shard_map/ppermute | solution.py:264
  8.1 6.6 %collective-permute-start.3 = (bf16[256,256]{1,0:T(8,128)(2,1)S(1)}, bf16[256,256]{1,0:T(8,128)(2,1)S(1)}, u32[]{:S(2)}, u32[]{:S(2)}) collective-permute-start(bf16[256,256]{1,0:T(8,128)(2,1)S(1)} %pad_maximum_fusion.refs_0_), channel_id=1, source_target_pairs={{0,64},{32,96},{64,0},{96,32},{1,65},{33,97},{65,1},{97,33},{2,66}... | collective-permute-start | bytes 393224 | tf_op jit(solution)/shard_map/ppermute | solution.py:264
  8.1 7.6 %collective-permute-start.4 = (bf16[256,256]{1,0:T(8,128)(2,1)S(1)}, bf16[256,256]{1,0:T(8,128)(2,1)S(1)}, u32[]{:S(2)}, u32[]{:S(2)}) collective-permute-start(bf16[256,256]{1,0:T(8,128)(2,1)S(1)} %pad_maximum_fusion.refs_0_), channel_id=1, source_target_pairs={{0,32},{32,64},{64,96},{96,0},{1,33},{33,65},{65,97},{97,1},{2,34}... | collective-permute-start | bytes 393224 | tf_op jit(solution)/shard_map/ppermute | solution.py:264
  9.3 38.6 %collective-permute-start.1 = (bf16[320,2048]{1,0:T(8,128)(2,1)}, bf16[320,2048]{1,0:T(8,128)(2,1)}, u32[]{:S(2)}, u32[]{:S(2)}) collective-permute-start(bf16[320,2048]{1,0:T(8,128)(2,1)} %bitcast.45), channel_id=1, source_target_pairs={{0,8},{1,25},{8,16},{9,1},{16,24},{17,9},{24,0},{25,17},{2,10},{3,... | collective-permute-start | bytes 3932168 | tf_op jit(solution)/shard_map/ppermute | solution.py:269
  15.7 46.4 %copy-start.11 = (bf16[256,256]{1,0:T(8,128)(2,1)}, bf16[256,256]{1,0:T(8,128)(2,1)S(1)}, u32[]{:S(2)}) copy-start(bf16[256,256]{1,0:T(8,128)(2,1)S(1)} %get-tuple-element.39.refs_0_) | copy-start | bytes 393220
  15.7 20.0 %collective-permute-start.5 = (bf16[768,256]{1,0:T(8,128)(2,1)S(1)}, bf16[768,256]{1,0:T(8,128)(2,1)S(1)}, u32[]{:S(2)}, u32[]{:S(2)}) collective-permute-start(bf16[768,256]{1,0:T(8,128)(2,1)S(1)} %get-tuple-element.25.refs_3_.refs_1_), channel_id=1, source_target_pairs={{0,6},{2,0},{4,2},{6,4},{1,7},{3,1},{5,3},{7,5},{8,14},{10,8},{12,... | collective-permute-start | bytes 1179656 | tf_op jit(solution)/shard_map/ppermute | solution.py:264
  28.4 48.2 %collective-permute-start.15 = (bf16[320,2048]{1,0:T(8,128)(2,1)}, bf16[320,2048]{1,0:T(8,128)(2,1)}, u32[]{:S(2)}, u32[]{:S(2)}) collective-permute-start(bf16[320,2048]{1,0:T(8,128)(2,1)} %collective-permute-done.refs_1_), channel_id=1, source_target_pairs={{0,24},{1,9},{8,0},{9,17},{16,8},{17,25},{24,16},{25,1},{2,26},{3,... | collective-permute-start | bytes 3932168 | tf_op jit(solution)/shard_map/ppermute | solution.py:269
  32.1 9.4 %collective-permute-start.6 = (bf16[768,256]{1,0:T(8,128)(2,1)S(1)}, bf16[768,256]{1,0:T(8,128)(2,1)S(1)}, u32[]{:S(2)}, u32[]{:S(2)}) collective-permute-start(bf16[768,256]{1,0:T(8,128)(2,1)S(1)} %get-tuple-element.25.refs_3_.refs_1_), channel_id=1, source_target_pairs={{0,4},{2,6},{4,0},{6,2},{1,5},{3,7},{5,1},{7,3},{8,12},{10,14},{12... | collective-permute-start | bytes 1179656 | tf_op jit(solution)/shard_map/ppermute | solution.py:264
  35.1 10.5 %collective-permute-start.7 = (bf16[768,256]{1,0:T(8,128)(2,1)S(1)}, bf16[768,256]{1,0:T(8,128)(2,1)S(1)}, u32[]{:S(2)}, u32[]{:S(2)}) collective-permute-start(bf16[768,256]{1,0:T(8,128)(2,1)S(1)} %get-tuple-element.25.refs_3_.refs_1_), channel_id=1, source_target_pairs={{0,2},{2,4},{4,6},{6,0},{1,3},{3,5},{5,7},{7,1},{8,10},{10,12},{12... | collective-permute-start | bytes 1179656 | tf_op jit(solution)/shard_map/ppermute | solution.py:264
  35.7 9.9 %collective-permute-start.8 = (bf16[768,256]{1,0:T(8,128)(2,1)S(1)}, bf16[768,256]{1,0:T(8,128)(2,1)S(1)}, u32[]{:S(2)}, u32[]{:S(2)}) collective-permute-start(bf16[768,256]{1,0:T(8,128)(2,1)S(1)} %get-tuple-element.25.refs_3_.refs_1_), channel_id=1, source_target_pairs={{0,1},{1,0},{2,3},{3,2},{4,5},{5,4},{6,7},{7,6},{8,9},{9,8},{10,11... | collective-permute-start | bytes 1179656 | tf_op jit(solution)/shard_map/ppermute | solution.py:264
  41.5 4.7 %collective-permute-start.9 = (bf16[768,256]{1,0:T(8,128)(2,1)S(1)}, bf16[768,256]{1,0:T(8,128)(2,1)S(1)}, u32[]{:S(2)}, u32[]{:S(2)}) collective-permute-start(bf16[768,256]{1,0:T(8,128)(2,1)S(1)} %collective-permute-done.5.refs_4_.refs_2_), channel_id=1, source_target_pairs={{0,1},{1,0},{2,3},{3,2},{4,5},{5,4},{6,7},{7,6},{8,9},{9,8},{10,11... | collective-permute-start | bytes 1179656 | tf_op jit(solution)/shard_map/ppermute | solution.py:264
  45.6 1.7 %collective-permute-start.10 = (bf16[768,256]{1,0:T(8,128)(2,1)S(1)}, bf16[768,256]{1,0:T(8,128)(2,1)S(1)}, u32[]{:S(2)}, u32[]{:S(2)}) collective-permute-start(bf16[768,256]{1,0:T(8,128)(2,1)S(1)} %collective-permute-done.6.refs_5_.refs_3_), channel_id=1, source_target_pairs={{0,1},{1,0},{2,3},{3,2},{4,5},{5,4},{6,7},{7,6},{8,9},{9,8},{10,11... | collective-permute-start | bytes 1179656 | tf_op jit(solution)/shard_map/ppermute | solution.py:264
  45.6 2.3 %collective-permute-start.11 = (bf16[768,256]{1,0:T(8,128)(2,1)S(1)}, bf16[768,256]{1,0:T(8,128)(2,1)S(1)}, u32[]{:S(2)}, u32[]{:S(2)}) collective-permute-start(bf16[768,256]{1,0:T(8,128)(2,1)S(1)} %collective-permute-done.7.refs_6_.refs_4_), channel_id=1, source_target_pairs={{0,1},{1,0},{2,3},{3,2},{4,5},{5,4},{6,7},{7,6},{8,9},{9,8},{10,11... | collective-permute-start | bytes 1179656 | tf_op jit(solution)/shard_map/ppermute | solution.py:264
  56.9 18.6 %collective-permute-start.12 = (bf16[1440,128]{1,0:T(8,128)(2,1)S(1)}, bf16[1440,128]{1,0:T(8,128)(2,1)S(1)}, u32[]{:S(2)}, u32[]{:S(2)}) collective-permute-start(bf16[1440,128]{1,0:T(8,128)(2,1)S(1)} %get-tuple-element.32), channel_id=1, source_target_pairs={{0,32},{32,64},{64,96},{96,0},{1,33},{33,65},{65,97},{97,1},{2,34}... | collective-permute-start | bytes 1105928 | tf_op jit(solution)/shard_map/ppermute | solution.py:264
  58.5 6.4 %collective-permute-start.19 = (bf16[256,256]{1,0:T(8,128)(2,1)S(1)}, bf16[256,256]{1,0:T(8,128)(2,1)S(1)}, u32[]{:S(2)}, u32[]{:S(2)}) collective-permute-start(bf16[256,256]{1,0:T(8,128)(2,1)S(1)} %get-tuple-element.39.refs_0_), channel_id=1, source_target_pairs={{0,6},{2,0},{4,2},{6,4},{1,7},{3,1},{5,3},{7,5},{8,14},{10,8},{12,... | collective-permute-start | bytes 393224 | tf_op jit(solution)/shard_map/ppermute | solution.py:264
  59.0 11.5 %collective-permute-start.20 = (bf16[256,256]{1,0:T(8,128)(2,1)S(1)}, bf16[256,256]{1,0:T(8,128)(2,1)S(1)}, u32[]{:S(2)}, u32[]{:S(2)}) collective-permute-start(bf16[256,256]{1,0:T(8,128)(2,1)S(1)} %get-tuple-element.39.refs_0_), channel_id=1, source_target_pairs={{0,4},{2,6},{4,0},{6,2},{1,5},{3,7},{5,1},{7,3},{8,12},{10,14},{12... | collective-permute-start | bytes 393224 | tf_op jit(solution)/shard_map/ppermute | solution.py:264
  62.1 8.4 %collective-permute-start.21 = (bf16[256,256]{1,0:T(8,128)(2,1)S(1)}, bf16[256,256]{1,0:T(8,128)(2,1)S(1)}, u32[]{:S(2)}, u32[]{:S(2)}) collective-permute-start(bf16[256,256]{1,0:T(8,128)(2,1)S(1)} %get-tuple-element.39.refs_0_), channel_id=1, source_target_pairs={{0,2},{2,4},{4,6},{6,0},{1,3},{3,5},{5,7},{7,1},{8,10},{10,12},{12... | collective-permute-start | bytes 393224 | tf_op jit(solution)/shard_map/ppermute | solution.py:264
  64.8 18.8 %collective-permute-start.13 = (bf16[1440,128]{1,0:T(8,128)(2,1)S(1)}, bf16[1440,128]{1,0:T(8,128)(2,1)S(1)}, u32[]{:S(2)}, u32[]{:S(2)}) collective-permute-start(bf16[1440,128]{1,0:T(8,128)(2,1)S(1)} %get-tuple-element.33), channel_id=1, source_target_pairs={{0,64},{32,96},{64,0},{96,32},{1,65},{33,97},{65,1},{97,33},{2,66}... | collective-permute-start | bytes 1105928 | tf_op jit(solution)/shard_map/ppermute | solution.py:264
  71.5 25.3 %copy-start.15 = (f32[2,64]{1,0:T(2,128)S(1)}, f32[2,64]{1,0:T(2,128)}, u32[]{:S(2)}) copy-start(f32[2,64]{1,0:T(2,128)} %gain_ref.5) | copy-start | bytes 1540
  71.5 71.3 %collective-permute-start.22 = (bf16[1024,256]{1,0:T(8,128)(2,1)S(1)}, bf16[1024,256]{1,0:T(8,128)(2,1)}, u32[]{:S(2)}, u32[]{:S(2)}) collective-permute-start(bf16[1024,256]{1,0:T(8,128)(2,1)S(1)} %join.1.refs_0_), channel_id=1, source_target_pairs={{0,24},{8,0},{16,8},{24,16},{1,25},{9,1},{17,9},{25,17},{2,26},{10... | collective-permute-start | bytes 1572872 | tf_op jit(solution)/shard_map/ppermute | solution.py:264
  73.2 69.6 %collective-permute-start.23 = (bf16[1024,256]{1,0:T(8,128)(2,1)S(1)}, bf16[1024,256]{1,0:T(8,128)(2,1)}, u32[]{:S(2)}, u32[]{:S(2)}) collective-permute-start(bf16[1024,256]{1,0:T(8,128)(2,1)S(1)} %join.1.refs_0_), channel_id=1, source_target_pairs={{0,16},{8,24},{16,0},{24,8},{1,17},{9,25},{17,1},{25,9},{2,18},{10... | collective-permute-start | bytes 1572872 | tf_op jit(solution)/shard_map/ppermute | solution.py:264
  76.2 66.6 %collective-permute-start.24 = (bf16[1024,256]{1,0:T(8,128)(2,1)S(1)}, bf16[1024,256]{1,0:T(8,128)(2,1)}, u32[]{:S(2)}, u32[]{:S(2)}) collective-permute-start(bf16[1024,256]{1,0:T(8,128)(2,1)S(1)} %join.1.refs_0_), channel_id=1, source_target_pairs={{0,8},{8,16},{16,24},{24,0},{1,9},{9,17},{17,25},{25,1},{2,10},{10... | collective-permute-start | bytes 1572872 | tf_op jit(solution)/shard_map/ppermute | solution.py:264
  76.6 9.3 %collective-permute-start.14 = (bf16[1440,128]{1,0:T(8,128)(2,1)S(1)}, bf16[1440,128]{1,0:T(8,128)(2,1)S(1)}, u32[]{:S(2)}, u32[]{:S(2)}) collective-permute-start(bf16[1440,128]{1,0:T(8,128)(2,1)S(1)} %get-tuple-element.34), channel_id=1, source_target_pairs={{0,96},{32,0},{64,32},{96,64},{1,97},{33,1},{65,33},{97,65},{2,98}... | collective-permute-start | bytes 1105928 | tf_op jit(solution)/shard_map/ppermute | solution.py:264
  84.3 7.3 %collective-permute-start.16 = (bf16[480,128]{1,0:T(8,128)(2,1)S(1)}, bf16[480,128]{1,0:T(8,128)(2,1)S(1)}, u32[]{:S(2)}, u32[]{:S(2)}) collective-permute-start(bf16[480,128]{1,0:T(8,128)(2,1)S(1)} %get-tuple-element.36), channel_id=1, source_target_pairs={{0,32},{32,64},{64,96},{96,0},{1,33},{33,65},{65,97},{97,1},{2,34}... | collective-permute-start | bytes 368648 | tf_op jit(solution)/shard_map/ppermute | solution.py:264
  86.6 7.9 %collective-permute-start.17 = (bf16[480,128]{1,0:T(8,128)(2,1)}, bf16[480,128]{1,0:T(8,128)(2,1)S(1)}, u32[]{:S(2)}, u32[]{:S(2)}) collective-permute-start(bf16[480,128]{1,0:T(8,128)(2,1)} %get-tuple-element.37), channel_id=1, source_target_pairs={{0,64},{32,96},{64,0},{96,32},{1,65},{33,97},{65,1},{97,33},{2,66}... | collective-permute-start | bytes 368648 | tf_op jit(solution)/shard_map/ppermute | solution.py:264
  91.7 5.1 %collective-permute-start.18 = (bf16[480,128]{1,0:T(8,128)(2,1)}, bf16[480,128]{1,0:T(8,128)(2,1)S(1)}, u32[]{:S(2)}, u32[]{:S(2)}) collective-permute-start(bf16[480,128]{1,0:T(8,128)(2,1)} %get-tuple-element.38), channel_id=1, source_target_pairs={{0,96},{32,0},{64,32},{96,64},{1,97},{33,1},{65,33},{97,65},{2,98}... | collective-permute-start | bytes 368648 | tf_op jit(solution)/shard_map/ppermute | solution.py:264
  142.8 16.3 %all-to-all-start = ((bf16[16,160,128]{2,1,0:T(8,128)(2,1)}), bf16[16,160,128]{2,1,0:T(8,128)(2,1)S(1)}, u32[]{:S(2)}, u32[]{:S(2)}) async-start(bf16[16,160,128]{2,1,0:T(8,128)(2,1)} %attention.1), calls=%async_computation | async-start | bytes 1310720 | tf_op jit(solution)/shard_map/all_to_all | solution.py:305
  148.3 2.0 %collective-permute-start.25 = (bf16[1024,256]{1,0:T(8,128)(2,1)S(1)}, bf16[1024,256]{1,0:T(8,128)(2,1)S(1)}, u32[]{:S(2)}, u32[]{:S(2)}) collective-permute-start(bf16[1024,256]{1,0:T(8,128)(2,1)S(1)} %join.1.refs_0_), channel_id=1, source_target_pairs={{0,1},{1,0},{2,3},{3,2},{4,5},{5,4},{6,7},{7,6},{8,9},{9,8},{10,11... | collective-permute-start | bytes 1572872 | tf_op jit(solution)/shard_map/ppermute | solution.py:264
  148.4 2.6 %collective-permute-start.26 = (bf16[1024,256]{1,0:T(8,128)(2,1)}, bf16[1024,256]{1,0:T(8,128)(2,1)S(1)}, u32[]{:S(2)}, u32[]{:S(2)}) collective-permute-start(bf16[1024,256]{1,0:T(8,128)(2,1)} %collective-permute-done.22.refs_1_), channel_id=1, source_target_pairs={{0,1},{1,0},{2,3},{3,2},{4,5},{5,4},{6,7},{7,6},{8,9},{9,8},{10,11... | collective-permute-start | bytes 1572872 | tf_op jit(solution)/shard_map/ppermute | solution.py:264
  148.9 2.9 %collective-permute-start.27 = (bf16[1024,256]{1,0:T(8,128)(2,1)}, bf16[1024,256]{1,0:T(8,128)(2,1)S(1)}, u32[]{:S(2)}, u32[]{:S(2)}) collective-permute-start(bf16[1024,256]{1,0:T(8,128)(2,1)} %collective-permute-done.23.refs_2_), channel_id=1, source_target_pairs={{0,1},{1,0},{2,3},{3,2},{4,5},{5,4},{6,7},{7,6},{8,9},{9,8},{10,11... | collective-permute-start | bytes 1572872 | tf_op jit(solution)/shard_map/ppermute | solution.py:264
  149.0 3.6 %collective-permute-start.28 = (bf16[1024,256]{1,0:T(8,128)(2,1)}, bf16[1024,256]{1,0:T(8,128)(2,1)S(1)}, u32[]{:S(2)}, u32[]{:S(2)}) collective-permute-start(bf16[1024,256]{1,0:T(8,128)(2,1)} %collective-permute-done.24.refs_3_), channel_id=1, source_target_pairs={{0,1},{1,0},{2,3},{3,2},{4,5},{5,4},{6,7},{7,6},{8,9},{9,8},{10,11... | collective-permute-start | bytes 1572872 | tf_op jit(solution)/shard_map/ppermute | solution.py:264
  (14 other events, 41.3 us)

commit v6 on v5

--- a/solution.py
+++ b/solution.py
@@ -117,7 +117,7 @@
         for i in range(T//BQ):
             emit(i)
     g=jnp.abs(gain_ref[...])
-    isfast=jnp.max(g[0:1])*jnp.max(g[1:2])<=7.7
+    isfast=jnp.max(g[:,0:64])*jnp.max(g[:,64:128])<=7.7/8
     pl.when(isfast)(fast)
     pl.when(jnp.logical_not(isfast))(slow)
 
@@ -152,17 +152,24 @@
 
 
 def join_kernel(*refs):
-    for i in range(4):
-        refs[4][i * 256 : i * 256 + 256, :] = refs[i][...]
+    out, sem = refs[4], refs[5]
+    copies = [
+        pltpu.make_async_copy(refs[i], out.at[pl.ds(i * 256, 256)], sem.at[i]) for i in range(4)
+    ]
+    for copy in copies:
+        copy.start()
+    for copy in copies:
+        copy.wait()
 
 
 def join(pieces):
+    anywhere = pl.BlockSpec(memory_space=pl.ANY)
     return pl.pallas_call(
         join_kernel,
         out_shape=jax.ShapeDtypeStruct((1024, 256), bf16),
-        in_specs=[VMEM] * 4,
-        out_specs=VMEM,
-        compiler_params=pltpu.CompilerParams(vmem_limit_bytes=4 * 1024 * 1024),
+        in_specs=[anywhere] * 4,
+        out_specs=anywhere,
+        scratch_shapes=[pltpu.SemaphoreType.DMA((4,))],
         name="join",
     )(*pieces)
 
@@ -187,10 +194,6 @@
         out[h][at + 320 : at + 480, :] = jnp.where(half, top, bot).astype(bf16)
 
 
-def gain_row(gain_ref):
-    return jnp.concatenate([gain_ref[0:1, :] * 0.125, gain_ref[1:2, :]], 1)
-
-
 def proj_kernel(idx_ref, gain_ref, *refs, sizes):
     n = sum(sizes)
     toks, ws, outs, w = refs[:n], refs[n : n + 8], refs[n + 8 : n + 12], refs[-1]
@@ -199,7 +202,7 @@
         for h in range(4):
             w[h * 128 : h * 128 + 128, cols] = ws[j][h * 192 : h * 192 + 128, :]
             w[512 + h * 64 : 576 + h * 64, cols] = ws[j][h * 192 + 128 : h * 192 + 192, :]
-    gains = gain_row(gain_ref)
+    gains = gain_ref[...]
     at = 0
     for b, size in enumerate(sizes):
         parts = [t[...] for t in toks[at : at + size]]
@@ -288,18 +291,22 @@
     cols = jnp.stack(
         [2 * ((x + d) % 4) + e for e in (c, 1 - c) for d in range(4)]
     ).astype(jnp.int32)
-    part1 = project(cols, qk_gain, [[own], [t1], [t3]], ws)
-    *part1, wo4 = lax.optimization_barrier((*part1, wo4))
-    part2 = project(cols, qk_gain, [[t2]], ws)
+    gains = jnp.concatenate([qk_gain[0] * 0.125, qk_gain[1]])[None]
+    part0 = project(cols, gains, [[own]], ws)
+    part1 = project(cols, gains, [[t1], [t3]], ws)
+    part2 = project(cols, gains, [[t2]], ws)
     recv = []
-    for part in (part1, part2):
+    for part in (part0, part1, part2):
         recv += [part[0]] + [move(part[d], Z, d) for d in (1, 2, 3)]
-    wo16 = join(around(wo4, X))
+    ox = around(wo4, X)
+    wo16 = join(ox)
     wo = around(wo16, Y)
-    pos = [4 * ((z - d) % 4) + (y + e) % 4 for d in range(4) for e in (0, near, 4 - near)]
-    pos += [4 * ((z - d) % 4) + (y + 2) % 4 for d in range(4)]
+    sources = [4 * ((z - d) % 4) for d in range(4)]
+    pos = [r + y for r in sources]
+    pos += [r + (y + e) % 4 for r in sources for e in (near, 4 - near)]
+    pos += [r + (y + 2) % 4 for r in sources]
     pos = jnp.stack(pos).astype(jnp.int32)
-    heads = attention(pos, qk_gain, decay_sums[0], recv, (3, 3, 3, 3, 1, 1, 1, 1))
+    heads = attention(pos, gains, decay_sums[0], recv, (1,) * 4 + (2,) * 4 + (1,) * 4)
     heads, *wo = lax.optimization_barrier((heads, *wo))
     wo = wo + [move(w, C, 0) for w in wo]
     merged = lax.all_to_all(heads, SP, 0, 0, tiled=True)

time: 164 us -> 182 us (1.11)
  Pallas kernels: 56 us -> 77.5 us
  local copies, waits for them, and re-layouts: 11 us -> 7.28 us
    pallas_call x1, Pallas kernels: 0.03 us -> 17 us  [join(): pl.pallas_call(join_kernel, out_shape=jax.ShapeDtypeStruct((1024, 256), b...]
    pallas_call x2 -> x3, Pallas kernels: 10.4 us -> 14.1 us  [project(): pl.pallas_call(functools.partial(proj_kernel, sizes=tuple((len(b) for b i...]
    unnamed x32, local copies, waits for them, and re-layouts: 10.7 us -> 7.02 us
    ppermute x26 -> x29, waiting for transfers between devices: 28.4 us -> 26.4 us  [move(): return lax.ppermute(value, axis, pairs)]
    ppermute x26 -> x29, starting transfers between devices: 38.3 us -> 38.2 us  [move(): return lax.ppermute(value, axis, pairs)]
  transfers between devices with their start and end apart: 30 -> 33, of which waited for: 18 -> 15; matrix products, arithmetic and copies ran while one was open for 1% -> 1% of each run, Pallas kernels for 32% -> 40%
where the time goes in v6:
time: 182 us
  Pallas kernels  77.5 us (43%)
  starting transfers between devices  50.8 us (28%)
  waiting for transfers between devices  44.1 us (24%)
  local copies, waits for them, and re-layouts  7.28 us (4%)
    pallas_call x1, Pallas kernels, attention(): pl.pallas_call(functools.partial(attn_kernel, nblk=nblk), out_shape=jax.S...  42.2 us
    ppermute x29, starting transfers between devices, move(): return lax.ppermute(value, axis, pairs)  38.2 us
    ppermute x29, waiting for transfers between devices, move(): return lax.ppermute(value, axis, pairs)  26.4 us
    pallas_call x1, Pallas kernels, join(): pl.pallas_call(join_kernel, out_shape=jax.ShapeDtypeStruct((1024, 256), b...  17 us
    pallas_call x3, Pallas kernels, project(): pl.pallas_call(functools.partial(proj_kernel, sizes=tuple((len(b) for b i...  14.1 us
    ppermute x3, waiting for transfers between devices, spread(): return lax.ppermute(value, (Y, C), pairs)  9.88 us
    all_to_all x1, waiting for transfers between devices, on_device(): merged = lax.all_to_all(heads, SP, 0, 0, tiled=True)  7.84 us
    unnamed x32, local copies, waits for them, and re-layouts  7.02 us
  transfers between devices with their start and end apart: 33, of which 15 were waited for; matrix products, arithmetic and copies ran while one was open for 1% of the time, Pallas kernels for 40%

profile of v6, /device:TPU:0, one launch (start us, length us, event | category | flops | bytes accessed | tf_op | source)
XLA Modules:
  0.0 181.5 jit_solution(13194811213652834976)
XLA Ops:
  0.0 3.1 %collective-permute-start.13 = (bf16[320,2048]{1,0:T(8,128)(2,1)}, bf16[320,2048]{1,0:T(8,128)(2,1)}, u32[]{:S(2)}, u32[]{:S(2)}) collective-permute-start(bf16[320,2048]{1,0:T(8,128)(2,1)} %bitcast.51), channel_id=1, source_target_pairs={{0,24},{1,9},{8,0},{9,17},{16,8},{17,25},{24,16},{25,1},{2,26},{3,... | collective-permute-start | bytes 3932168 | tf_op jit(solution)/shard_map/ppermute | solution.py:272
  3.9 4.1 %collective-permute-start = (bf16[256,256]{1,0:T(8,128)(2,1)S(1)}, bf16[256,256]{1,0:T(8,128)(2,1)S(1)}, u32[]{:S(2)}, u32[]{:S(2)}) collective-permute-start(bf16[256,256]{1,0:T(8,128)(2,1)S(1)} %pad_maximum_fusion.refs_0_), channel_id=1, source_target_pairs={{0,96},{32,0},{64,32},{96,64},{1,97},{33,1},{65,33},{97,65},{2,98}... | collective-permute-start | bytes 393224 | tf_op jit(solution)/shard_map/ppermute | solution.py:267
  8.1 1.3 collective-permute-start.2
  9.3 2.8 %collective-permute-done.refs_1_ = bf16[256,256]{1,0:T(8,128)(2,1)S(1)} collective-permute-done((bf16[256,256]{1,0:T(8,128)(2,1)S(1)}, bf16[256,256]{1,0:T(8,128)(2,1)S(1)}, u32[]{:S(2)}, u32[]{:S(2)}) %collective-permute-start) | collective-permute-done | bytes 131104 | tf_op jit(solution)/shard_map/ppermute | solution.py:267
  12.2 2.5 %collective-permute-done.1.refs_2_ = bf16[256,256]{1,0:T(8,128)(2,1)S(1)} collective-permute-done((bf16[256,256]{1,0:T(8,128)(2,1)S(1)}, bf16[256,256]{1,0:T(8,128)(2,1)S(1)}, u32[]{:S(2)}, u32[]{:S(2)}) %collective-permute-start.1) | collective-permute-done | bytes 131104 | tf_op jit(solution)/shard_map/ppermute | solution.py:267
  15.7 2.8 %collective-permute-start.3 = (bf16[768,256]{1,0:T(8,128)(2,1)S(1)}, bf16[768,256]{1,0:T(8,128)(2,1)S(1)}, u32[]{:S(2)}, u32[]{:S(2)}) collective-permute-start(bf16[768,256]{1,0:T(8,128)(2,1)S(1)} %get-tuple-element.24.refs_1_.refs_2_), channel_id=1, source_target_pairs={{0,6},{2,0},{4,2},{6,4},{1,7},{3,1},{5,3},{7,5},{8,14},{10,8},{12,... | collective-permute-start | bytes 1179656 | tf_op jit(solution)/shard_map/ppermute | solution.py:267
  18.5 9.9 %collective-permute-done.13.refs_0_ = bf16[320,2048]{1,0:T(8,128)(2,1)} collective-permute-done((bf16[320,2048]{1,0:T(8,128)(2,1)}, bf16[320,2048]{1,0:T(8,128)(2,1)}, u32[]{:S(2)}, u32[]{:S(2)}) %collective-permute-start.13) | collective-permute-done | bytes 1310752 | tf_op jit(solution)/shard_map/ppermute | solution.py:272
  28.4 3.7 %collective-permute-start.18 = (bf16[320,2048]{1,0:T(8,128)(2,1)}, bf16[320,2048]{1,0:T(8,128)(2,1)}, u32[]{:S(2)}, u32[]{:S(2)}) collective-permute-start(bf16[320,2048]{1,0:T(8,128)(2,1)} %collective-permute-done.13.refs_0_), channel_id=1, source_target_pairs={{0,24},{1,9},{8,0},{9,17},{16,8},{17,25},{24,16},{25,1},{2,26},{3,... | collective-permute-start | bytes 3932168 | tf_op jit(solution)/shard_map/ppermute | solution.py:272
  32.1 3.0 %collective-permute-start.4 = (bf16[768,256]{1,0:T(8,128)(2,1)S(1)}, bf16[768,256]{1,0:T(8,128)(2,1)S(1)}, u32[]{:S(2)}, u32[]{:S(2)}) collective-permute-start(bf16[768,256]{1,0:T(8,128)(2,1)S(1)} %get-tuple-element.24.refs_1_.refs_2_), channel_id=1, source_target_pairs={{0,4},{2,6},{4,0},{6,2},{1,5},{3,7},{5,1},{7,3},{8,12},{10,14},{12... | collective-permute-start | bytes 1179656 | tf_op jit(solution)/shard_map/ppermute | solution.py:267
  35.7 5.8 %collective-permute-done.4.refs_3_.refs_4_ = bf16[768,256]{1,0:T(8,128)(2,1)S(1)} collective-permute-done((bf16[768,256]{1,0:T(8,128)(2,1)S(1)}, bf16[768,256]{1,0:T(8,128)(2,1)S(1)}, u32[]{:S(2)}, u32[]{:S(2)}) %collective-permute-start.4) | collective-permute-done | bytes 393248 | tf_op jit(solution)/shard_map/ppermute | solution.py:267
  41.5 4.1 %collective-permute-done.5.refs_4_.refs_5_ = bf16[768,256]{1,0:T(8,128)(2,1)S(1)} collective-permute-done((bf16[768,256]{1,0:T(8,128)(2,1)S(1)}, bf16[768,256]{1,0:T(8,128)(2,1)S(1)}, u32[]{:S(2)}, u32[]{:S(2)}) %collective-permute-start.5) | collective-permute-done | bytes 393248 | tf_op jit(solution)/shard_map/ppermute | solution.py:267
  47.4 3.1 %collective-permute-start.23 = (bf16[256,256]{1,0:T(8,128)(2,1)S(1)}, bf16[256,256]{1,0:T(8,128)(2,1)}, u32[]{:S(2)}, u32[]{:S(2)}) collective-permute-start(bf16[256,256]{1,0:T(8,128)(2,1)S(1)} %get-tuple-element.37.refs_0_), channel_id=1, source_target_pairs={{0,4},{2,6},{4,0},{6,2},{1,5},{3,7},{5,1},{7,3},{8,12},{10,14},{12... | collective-permute-start | bytes 393224 | tf_op jit(solution)/shard_map/ppermute | solution.py:267
  50.7 6.0 %project.4 = (bf16[960,128]{1,0:T(8,128)(2,1)S(1)}, bf16[960,128]{1,0:T(8,128)(2,1)}, bf16[960,128]{1,0:T(8,128)(2,1)S(1)}, bf16[960,128]{1,0:T(8,128)(2,1)S(1)}) custom-call(s32[8]{0:T(128)S(1)} %stack.152.idx_ref.col_ref, f32[1,128]{1,0:T(1,128)S(1)} %maximum_bitcast_fusion.gain_ref, bf16[320,2048]{1,0:T(8,128)(2,1)} %collective-permute-done.13.refs_0_, ...), custom_call_target="tpu_custom_call" | custom-call | tf_op jit(solution)/shard_map/project/pallas_call | solution.py:216
  56.7 1.7 collective-permute-start.15
  58.3 3.7 %project.3 = (bf16[480,128]{1,0:T(8,128)(2,1)S(1)}, bf16[480,128]{1,0:T(8,128)(2,1)}, bf16[480,128]{1,0:T(8,128)(2,1)}, bf16[480,128]{1,0:T(8,128)(2,1)}) custom-call(s32[8]{0:T(128)S(1)} %stack.152.idx_ref.col_ref, f32[1,128]{1,0:T(1,128)S(1)} %maximum_bitcast_fusion.gain_ref, bf16[320,2048]{1,0:T(8,128)(2,1)S(1)} %bitcast.53, ...), custom_call_target="tpu_custom_call" | custom-call | tf_op jit(solution)/shard_map/project/pallas_call | solution.py:216
  62.6 3.6 %collective-permute-start.10 = (bf16[480,128]{1,0:T(8,128)(2,1)}, bf16[480,128]{1,0:T(8,128)(2,1)}, u32[]{:S(2)}, u32[]{:S(2)}) collective-permute-start(bf16[480,128]{1,0:T(8,128)(2,1)} %get-tuple-element.26), channel_id=1, source_target_pairs={{0,32},{32,64},{64,96},{96,0},{1,33},{33,65},{65,97},{97,1},{2,34}... | collective-permute-start | bytes 368648 | tf_op jit(solution)/shard_map/ppermute | solution.py:267
  66.2 2.2 %collective-permute-start.11 = (bf16[480,128]{1,0:T(8,128)(2,1)}, bf16[480,128]{1,0:T(8,128)(2,1)}, u32[]{:S(2)}, u32[]{:S(2)}) collective-permute-start(bf16[480,128]{1,0:T(8,128)(2,1)} %get-tuple-element.27), channel_id=1, source_target_pairs={{0,64},{32,96},{64,0},{96,32},{1,65},{33,97},{65,1},{97,33},{2,66}... | collective-permute-start | bytes 368648 | tf_op jit(solution)/shard_map/ppermute | solution.py:267
  68.4 2.5 %collective-permute-start.12 = (bf16[480,128]{1,0:T(8,128)(2,1)}, bf16[480,128]{1,0:T(8,128)(2,1)S(1)}, u32[]{:S(2)}, u32[]{:S(2)}) collective-permute-start(bf16[480,128]{1,0:T(8,128)(2,1)} %get-tuple-element.28), channel_id=1, source_target_pairs={{0,96},{32,0},{64,32},{96,64},{1,97},{33,1},{65,33},{97,65},{2,98}... | collective-permute-start | bytes 368648 | tf_op jit(solution)/shard_map/ppermute | solution.py:267
  71.0 17.0 %join.1.refs_0_ = bf16[1024,256]{1,0:T(8,128)(2,1)} custom-call(bf16[256,256]{1,0:T(8,128)(2,1)} %copy-done.6, bf16[256,256]{1,0:T(8,128)(2,1)} %collective-permute-done.22.refs_1_, bf16[256,256]{1,0:T(8,128)(2,1)} %collective-permute-done.23.refs_2_, bf16[256,256]{1,0:T(8,128)(2,1)} %collective-permute-done.24.refs_3_), custom_call_target="tpu_custom_call" | custom-call | tf_op jit(solution)/shard_map/join/pallas_call | solution.py:167
  88.0 1.8 collective-permute-start.25
  89.8 2.2 %collective-permute-start.26 = (bf16[1024,256]{1,0:T(8,128)(2,1)}, bf16[1024,256]{1,0:T(8,128)(2,1)}, u32[]{:S(2)}, u32[]{:S(2)}) collective-permute-start(bf16[1024,256]{1,0:T(8,128)(2,1)} %join.1.refs_0_), channel_id=1, source_target_pairs={{0,16},{8,24},{16,0},{24,8},{1,17},{9,25},{17,1},{25,9},{2,18},{10... | collective-permute-start | bytes 1572872 | tf_op jit(solution)/shard_map/ppermute | solution.py:267
  93.0 2.1 %collective-permute-start.17 = (bf16[960,128]{1,0:T(8,128)(2,1)}, bf16[960,128]{1,0:T(8,128)(2,1)S(1)}, u32[]{:S(2)}, u32[]{:S(2)}) collective-permute-start(bf16[960,128]{1,0:T(8,128)(2,1)} %copy-done.14), channel_id=1, source_target_pairs={{0,96},{32,0},{64,32},{96,64},{1,97},{33,1},{65,33},{97,65},{2,98}... | collective-permute-start | bytes 737288 | tf_op jit(solution)/shard_map/ppermute | solution.py:267
  95.1 4.5 %project.5 = (bf16[480,128]{1,0:T(8,128)(2,1)S(1)}, bf16[480,128]{1,0:T(8,128)(2,1)S(1)}, bf16[480,128]{1,0:T(8,128)(2,1)}, bf16[480,128]{1,0:T(8,128)(2,1)}) custom-call(s32[8]{0:T(128)S(1)} %stack.152.idx_ref.col_ref, f32[1,128]{1,0:T(1,128)S(1)} %maximum_bitcast_fusion.gain_ref, bf16[320,2048]{1,0:T(8,128)(2,1)} %collective-permute-done.18.refs_0_, ...), custom_call_target="tpu_custom_call" | custom-call | tf_op jit(solution)/shard_map/project/pallas_call | solution.py:216
  101.6 1.7 collective-permute-start.19
  104.0 2.4 %collective-permute-start.20 = (bf16[480,128]{1,0:T(8,128)(2,1)}, bf16[480,128]{1,0:T(8,128)(2,1)S(1)}, u32[]{:S(2)}, u32[]{:S(2)}) collective-permute-start(bf16[480,128]{1,0:T(8,128)(2,1)} %get-tuple-element.35), channel_id=1, source_target_pairs={{0,64},{32,96},{64,0},{96,32},{1,65},{33,97},{65,1},{97,33},{2,66}... | collective-permute-start | bytes 368648 | tf_op jit(solution)/shard_map/ppermute | solution.py:267
  106.4 2.0 %collective-permute-done.19.refs_9_ = bf16[480,128]{1,0:T(8,128)(2,1)S(1)} collective-permute-done((bf16[480,128]{1,0:T(8,128)(2,1)S(1)}, bf16[480,128]{1,0:T(8,128)(2,1)S(1)}, u32[]{:S(2)}, u32[]{:S(2)}) %collective-permute-start.19) | collective-permute-done | bytes 122912 | tf_op jit(solution)/shard_map/ppermute | solution.py:267
  109.1 1.5 collective-permute-done.20.refs_10_
  110.5 3.0 %collective-permute-done.21.refs_11_ = bf16[480,128]{1,0:T(8,128)(2,1)S(1)} collective-permute-done((bf16[480,128]{1,0:T(8,128)(2,1)}, bf16[480,128]{1,0:T(8,128)(2,1)S(1)}, u32[]{:S(2)}, u32[]{:S(2)}) %collective-permute-start.21) | collective-permute-done | bytes 122912 | tf_op jit(solution)/shard_map/ppermute | solution.py:267
  117.2 42.2 %attention.1 = bf16[16,160,128]{2,1,0:T(8,128)(2,1)} custom-call(s32[16]{0:T(128)S(1)} %stack.168.pos_ref, f32[1,128]{1,0:T(1,128)S(1)} %maximum_bitcast_fusion.gain_ref, f32[1,5120]{1,0:T(1,128)S(1)} %bitcast.54, bf16[480,128]{1,0:T(8,128)(2,1)S(1)} %copy-done.8, bf16[480,128]{1,0:T(8,128)(2,1)} %collective-permute-done.10.refs_1_, ...), custom_call_target="tpu_custom_call" | custom-call | tf_op jit(solution)/shard_map/attention/pallas_call | solution.py:127
  159.5 5.8 %all-to-all-start = ((bf16[16,160,128]{2,1,0:T(8,128)(2,1)}), bf16[16,160,128]{2,1,0:T(8,128)(2,1)S(1)}, u32[]{:S(2)}, u32[]{:S(2)}) async-start(bf16[16,160,128]{2,1,0:T(8,128)(2,1)} %attention.1), calls=%async_computation | async-start | bytes 1310720 | tf_op jit(solution)/shard_map/all_to_all | solution.py:312
  169.5 7.8 %all-to-all-done.heads_ref = bf16[16,160,128]{2,1,0:T(8,128)(2,1)S(1)} async-done(((bf16[16,160,128]{2,1,0:T(8,128)(2,1)}), bf16[16,160,128]{2,1,0:T(8,128)(2,1)S(1)}, u32[]{:S(2)}, u32[]{:S(2)}) %all-to-all-start) | async-done | bytes 655392 | tf_op jit(solution)/shard_map/all_to_all | solution.py:312
  177.4 4.1 %output.1 = bf16[320,2048]{1,0:T(8,128)(2,1)} custom-call(s32[16]{0:T(128)S(1)} %stack.143.head_ref, s32[8]{0:T(128)S(1)} %stack.152.idx_ref.col_ref, bf16[16,160,128]{2,1,0:T(8,128)(2,1)S(1)} %all-to-all-done.heads_ref, bf16[1024,256]{1,0:T(8,128)(2,1)S(1)} %copy-done, bf16[1024,256]{1,0:T(8,128)(2,1)} %collective-permute-done.25.refs_1_, ...), custom_call_target="tpu_custom_call" | custom-call | tf_op jit(solution)/shard_map/output/pallas_call | solution.py:250
  (79 shorter events, 17.4 us)
Async XLA Ops:
  0.0 28.4 %collective-permute-start.13 = (bf16[320,2048]{1,0:T(8,128)(2,1)}, bf16[320,2048]{1,0:T(8,128)(2,1)}, u32[]{:S(2)}, u32[]{:S(2)}) collective-permute-start(bf16[320,2048]{1,0:T(8,128)(2,1)} %bitcast.51), channel_id=1, source_target_pairs={{0,24},{1,9},{8,0},{9,17},{16,8},{17,25},{24,16},{25,1},{2,26},{3,... | collective-permute-start | bytes 3932168 | tf_op jit(solution)/shard_map/ppermute | solution.py:272
  3.9 8.2 %collective-permute-start = (bf16[256,256]{1,0:T(8,128)(2,1)S(1)}, bf16[256,256]{1,0:T(8,128)(2,1)S(1)}, u32[]{:S(2)}, u32[]{:S(2)}) collective-permute-start(bf16[256,256]{1,0:T(8,128)(2,1)S(1)} %pad_maximum_fusion.refs_0_), channel_id=1, source_target_pairs={{0,96},{32,0},{64,32},{96,64},{1,97},{33,1},{65,33},{97,65},{2,98}... | collective-permute-start | bytes 393224 | tf_op jit(solution)/shard_map/ppermute | solution.py:267
  8.1 6.6 %collective-permute-start.1 = (bf16[256,256]{1,0:T(8,128)(2,1)S(1)}, bf16[256,256]{1,0:T(8,128)(2,1)S(1)}, u32[]{:S(2)}, u32[]{:S(2)}) collective-permute-start(bf16[256,256]{1,0:T(8,128)(2,1)S(1)} %pad_maximum_fusion.refs_0_), channel_id=1, source_target_pairs={{0,64},{32,96},{64,0},{96,32},{1,65},{33,97},{65,1},{97,33},{2,66}... | collective-permute-start | bytes 393224 | tf_op jit(solution)/shard_map/ppermute | solution.py:267
  8.1 7.6 %collective-permute-start.2 = (bf16[256,256]{1,0:T(8,128)(2,1)S(1)}, bf16[256,256]{1,0:T(8,128)(2,1)S(1)}, u32[]{:S(2)}, u32[]{:S(2)}) collective-permute-start(bf16[256,256]{1,0:T(8,128)(2,1)S(1)} %pad_maximum_fusion.refs_0_), channel_id=1, source_target_pairs={{0,32},{32,64},{64,96},{96,0},{1,33},{33,65},{65,97},{97,1},{2,34}... | collective-permute-start | bytes 393224 | tf_op jit(solution)/shard_map/ppermute | solution.py:267
  9.3 41.4 %collective-permute-start.14 = (bf16[320,2048]{1,0:T(8,128)(2,1)}, bf16[320,2048]{1,0:T(8,128)(2,1)}, u32[]{:S(2)}, u32[]{:S(2)}) collective-permute-start(bf16[320,2048]{1,0:T(8,128)(2,1)} %bitcast.52), channel_id=1, source_target_pairs={{0,8},{1,25},{8,16},{9,1},{16,24},{17,9},{24,0},{25,17},{2,10},{3,... | collective-permute-start | bytes 3932168 | tf_op jit(solution)/shard_map/ppermute | solution.py:272
  15.7 20.0 %collective-permute-start.3 = (bf16[768,256]{1,0:T(8,128)(2,1)S(1)}, bf16[768,256]{1,0:T(8,128)(2,1)S(1)}, u32[]{:S(2)}, u32[]{:S(2)}) collective-permute-start(bf16[768,256]{1,0:T(8,128)(2,1)S(1)} %get-tuple-element.24.refs_1_.refs_2_), channel_id=1, source_target_pairs={{0,6},{2,0},{4,2},{6,4},{1,7},{3,1},{5,3},{7,5},{8,14},{10,8},{12,... | collective-permute-start | bytes 1179656 | tf_op jit(solution)/shard_map/ppermute | solution.py:267
  28.4 64.6 %collective-permute-start.18 = (bf16[320,2048]{1,0:T(8,128)(2,1)}, bf16[320,2048]{1,0:T(8,128)(2,1)}, u32[]{:S(2)}, u32[]{:S(2)}) collective-permute-start(bf16[320,2048]{1,0:T(8,128)(2,1)} %collective-permute-done.13.refs_0_), channel_id=1, source_target_pairs={{0,24},{1,9},{8,0},{9,17},{16,8},{17,25},{24,16},{25,1},{2,26},{3,... | collective-permute-start | bytes 3932168 | tf_op jit(solution)/shard_map/ppermute | solution.py:272
  32.1 9.4 %collective-permute-start.4 = (bf16[768,256]{1,0:T(8,128)(2,1)S(1)}, bf16[768,256]{1,0:T(8,128)(2,1)S(1)}, u32[]{:S(2)}, u32[]{:S(2)}) collective-permute-start(bf16[768,256]{1,0:T(8,128)(2,1)S(1)} %get-tuple-element.24.refs_1_.refs_2_), channel_id=1, source_target_pairs={{0,4},{2,6},{4,0},{6,2},{1,5},{3,7},{5,1},{7,3},{8,12},{10,14},{12... | collective-permute-start | bytes 1179656 | tf_op jit(solution)/shard_map/ppermute | solution.py:267
  35.1 10.5 %collective-permute-start.5 = (bf16[768,256]{1,0:T(8,128)(2,1)S(1)}, bf16[768,256]{1,0:T(8,128)(2,1)S(1)}, u32[]{:S(2)}, u32[]{:S(2)}) collective-permute-start(bf16[768,256]{1,0:T(8,128)(2,1)S(1)} %get-tuple-element.24.refs_1_.refs_2_), channel_id=1, source_target_pairs={{0,2},{2,4},{4,6},{6,0},{1,3},{3,5},{5,7},{7,1},{8,10},{10,12},{12... | collective-permute-start | bytes 1179656 | tf_op jit(solution)/shard_map/ppermute | solution.py:267
  35.7 9.9 %collective-permute-start.6 = (bf16[768,256]{1,0:T(8,128)(2,1)S(1)}, bf16[768,256]{1,0:T(8,128)(2,1)S(1)}, u32[]{:S(2)}, u32[]{:S(2)}) collective-permute-start(bf16[768,256]{1,0:T(8,128)(2,1)S(1)} %get-tuple-element.24.refs_1_.refs_2_), channel_id=1, source_target_pairs={{0,1},{1,0},{2,3},{3,2},{4,5},{5,4},{6,7},{7,6},{8,9},{9,8},{10,11... | collective-permute-start | bytes 1179656 | tf_op jit(solution)/shard_map/ppermute | solution.py:267
  41.5 5.4 %collective-permute-start.7 = (bf16[768,256]{1,0:T(8,128)(2,1)S(1)}, bf16[768,256]{1,0:T(8,128)(2,1)S(1)}, u32[]{:S(2)}, u32[]{:S(2)}) collective-permute-start(bf16[768,256]{1,0:T(8,128)(2,1)S(1)} %collective-permute-done.3.refs_2_.refs_3_), channel_id=1, source_target_pairs={{0,1},{1,0},{2,3},{3,2},{4,5},{5,4},{6,7},{7,6},{8,9},{9,8},{10,11... | collective-permute-start | bytes 1179656 | tf_op jit(solution)/shard_map/ppermute | solution.py:267
  45.6 4.9 %collective-permute-start.9 = (bf16[768,256]{1,0:T(8,128)(2,1)S(1)}, bf16[768,256]{1,0:T(8,128)(2,1)S(1)}, u32[]{:S(2)}, u32[]{:S(2)}) collective-permute-start(bf16[768,256]{1,0:T(8,128)(2,1)S(1)} %collective-permute-done.5.refs_4_.refs_5_), channel_id=1, source_target_pairs={{0,1},{1,0},{2,3},{3,2},{4,5},{5,4},{6,7},{7,6},{8,9},{9,8},{10,11... | collective-permute-start | bytes 1179656 | tf_op jit(solution)/shard_map/ppermute | solution.py:267
  46.9 15.8 %collective-permute-start.22 = (bf16[256,256]{1,0:T(8,128)(2,1)S(1)}, bf16[256,256]{1,0:T(8,128)(2,1)}, u32[]{:S(2)}, u32[]{:S(2)}) collective-permute-start(bf16[256,256]{1,0:T(8,128)(2,1)S(1)} %get-tuple-element.37.refs_0_), channel_id=1, source_target_pairs={{0,6},{2,0},{4,2},{6,4},{1,7},{3,1},{5,3},{7,5},{8,14},{10,8},{12,... | collective-permute-start | bytes 393224 | tf_op jit(solution)/shard_map/ppermute | solution.py:267
  47.4 18.8 %collective-permute-start.23 = (bf16[256,256]{1,0:T(8,128)(2,1)S(1)}, bf16[256,256]{1,0:T(8,128)(2,1)}, u32[]{:S(2)}, u32[]{:S(2)}) collective-permute-start(bf16[256,256]{1,0:T(8,128)(2,1)S(1)} %get-tuple-element.37.refs_0_), channel_id=1, source_target_pairs={{0,4},{2,6},{4,0},{6,2},{1,5},{3,7},{5,1},{7,3},{8,12},{10,14},{12... | collective-permute-start | bytes 393224 | tf_op jit(solution)/shard_map/ppermute | solution.py:267
  50.5 17.9 %collective-permute-start.24 = (bf16[256,256]{1,0:T(8,128)(2,1)S(1)}, bf16[256,256]{1,0:T(8,128)(2,1)}, u32[]{:S(2)}, u32[]{:S(2)}) collective-permute-start(bf16[256,256]{1,0:T(8,128)(2,1)S(1)} %get-tuple-element.37.refs_0_), channel_id=1, source_target_pairs={{0,2},{2,4},{4,6},{6,0},{1,3},{3,5},{5,7},{7,1},{8,10},{10,12},{12... | collective-permute-start | bytes 393224 | tf_op jit(solution)/shard_map/ppermute | solution.py:267
  56.7 36.3 %collective-permute-start.15 = (bf16[960,128]{1,0:T(8,128)(2,1)}, bf16[960,128]{1,0:T(8,128)(2,1)}, u32[]{:S(2)}, u32[]{:S(2)}) collective-permute-start(bf16[960,128]{1,0:T(8,128)(2,1)} %get-tuple-element.30), channel_id=1, source_target_pairs={{0,32},{32,64},{64,96},{96,0},{1,33},{33,65},{65,97},{97,1},{2,34}... | collective-permute-start | bytes 737288 | tf_op jit(solution)/shard_map/ppermute | solution.py:267
  62.6 25.3 %collective-permute-start.10 = (bf16[480,128]{1,0:T(8,128)(2,1)}, bf16[480,128]{1,0:T(8,128)(2,1)}, u32[]{:S(2)}, u32[]{:S(2)}) collective-permute-start(bf16[480,128]{1,0:T(8,128)(2,1)} %get-tuple-element.26), channel_id=1, source_target_pairs={{0,32},{32,64},{64,96},{96,0},{1,33},{33,65},{65,97},{97,1},{2,34}... | collective-permute-start | bytes 368648 | tf_op jit(solution)/shard_map/ppermute | solution.py:267
  66.2 23.6 %collective-permute-start.11 = (bf16[480,128]{1,0:T(8,128)(2,1)}, bf16[480,128]{1,0:T(8,128)(2,1)}, u32[]{:S(2)}, u32[]{:S(2)}) collective-permute-start(bf16[480,128]{1,0:T(8,128)(2,1)} %get-tuple-element.27), channel_id=1, source_target_pairs={{0,64},{32,96},{64,0},{96,32},{1,65},{33,97},{65,1},{97,33},{2,66}... | collective-permute-start | bytes 368648 | tf_op jit(solution)/shard_map/ppermute | solution.py:267
  68.4 23.5 %collective-permute-start.12 = (bf16[480,128]{1,0:T(8,128)(2,1)}, bf16[480,128]{1,0:T(8,128)(2,1)S(1)}, u32[]{:S(2)}, u32[]{:S(2)}) collective-permute-start(bf16[480,128]{1,0:T(8,128)(2,1)} %get-tuple-element.28), channel_id=1, source_target_pairs={{0,96},{32,0},{64,32},{96,64},{1,97},{33,1},{65,33},{97,65},{2,98}... | collective-permute-start | bytes 368648 | tf_op jit(solution)/shard_map/ppermute | solution.py:267
  88.0 71.5 %collective-permute-start.25 = (bf16[1024,256]{1,0:T(8,128)(2,1)}, bf16[1024,256]{1,0:T(8,128)(2,1)}, u32[]{:S(2)}, u32[]{:S(2)}) collective-permute-start(bf16[1024,256]{1,0:T(8,128)(2,1)} %join.1.refs_0_), channel_id=1, source_target_pairs={{0,24},{8,0},{16,8},{24,16},{1,25},{9,1},{17,9},{25,17},{2,26},{10... | collective-permute-start | bytes 1572872 | tf_op jit(solution)/shard_map/ppermute | solution.py:267
  89.8 69.7 %collective-permute-start.26 = (bf16[1024,256]{1,0:T(8,128)(2,1)}, bf16[1024,256]{1,0:T(8,128)(2,1)}, u32[]{:S(2)}, u32[]{:S(2)}) collective-permute-start(bf16[1024,256]{1,0:T(8,128)(2,1)} %join.1.refs_0_), channel_id=1, source_target_pairs={{0,16},{8,24},{16,0},{24,8},{1,17},{9,25},{17,1},{25,9},{2,18},{10... | collective-permute-start | bytes 1572872 | tf_op jit(solution)/shard_map/ppermute | solution.py:267
  92.6 66.9 %collective-permute-start.27 = (bf16[1024,256]{1,0:T(8,128)(2,1)}, bf16[1024,256]{1,0:T(8,128)(2,1)}, u32[]{:S(2)}, u32[]{:S(2)}) collective-permute-start(bf16[1024,256]{1,0:T(8,128)(2,1)} %join.1.refs_0_), channel_id=1, source_target_pairs={{0,8},{8,16},{16,24},{24,0},{1,9},{9,17},{17,25},{25,1},{2,10},{10... | collective-permute-start | bytes 1572872 | tf_op jit(solution)/shard_map/ppermute | solution.py:267
  93.0 7.9 %collective-permute-start.16 = (bf16[960,128]{1,0:T(8,128)(2,1)}, bf16[960,128]{1,0:T(8,128)(2,1)S(1)}, u32[]{:S(2)}, u32[]{:S(2)}) collective-permute-start(bf16[960,128]{1,0:T(8,128)(2,1)} %copy-done.15), channel_id=1, source_target_pairs={{0,64},{32,96},{64,0},{96,32},{1,65},{33,97},{65,1},{97,33},{2,66}... | collective-permute-start | bytes 737288 | tf_op jit(solution)/shard_map/ppermute | solution.py:267
  93.0 10.3 %collective-permute-start.17 = (bf16[960,128]{1,0:T(8,128)(2,1)}, bf16[960,128]{1,0:T(8,128)(2,1)S(1)}, u32[]{:S(2)}, u32[]{:S(2)}) collective-permute-start(bf16[960,128]{1,0:T(8,128)(2,1)} %copy-done.14), channel_id=1, source_target_pairs={{0,96},{32,0},{64,32},{96,64},{1,97},{33,1},{65,33},{97,65},{2,98}... | collective-permute-start | bytes 737288 | tf_op jit(solution)/shard_map/ppermute | solution.py:267
  101.6 6.8 %collective-permute-start.19 = (bf16[480,128]{1,0:T(8,128)(2,1)S(1)}, bf16[480,128]{1,0:T(8,128)(2,1)S(1)}, u32[]{:S(2)}, u32[]{:S(2)}) collective-permute-start(bf16[480,128]{1,0:T(8,128)(2,1)S(1)} %get-tuple-element.34), channel_id=1, source_target_pairs={{0,32},{32,64},{64,96},{96,0},{1,33},{33,65},{65,97},{97,1},{2,34}... | collective-permute-start | bytes 368648 | tf_op jit(solution)/shard_map/ppermute | solution.py:267
  104.0 6.6 %collective-permute-start.20 = (bf16[480,128]{1,0:T(8,128)(2,1)}, bf16[480,128]{1,0:T(8,128)(2,1)S(1)}, u32[]{:S(2)}, u32[]{:S(2)}) collective-permute-start(bf16[480,128]{1,0:T(8,128)(2,1)} %get-tuple-element.35), channel_id=1, source_target_pairs={{0,64},{32,96},{64,0},{96,32},{1,65},{33,97},{65,1},{97,33},{2,66}... | collective-permute-start | bytes 368648 | tf_op jit(solution)/shard_map/ppermute | solution.py:267
  108.4 5.1 %collective-permute-start.21 = (bf16[480,128]{1,0:T(8,128)(2,1)}, bf16[480,128]{1,0:T(8,128)(2,1)S(1)}, u32[]{:S(2)}, u32[]{:S(2)}) collective-permute-start(bf16[480,128]{1,0:T(8,128)(2,1)} %get-tuple-element.36), channel_id=1, source_target_pairs={{0,96},{32,0},{64,32},{96,64},{1,97},{33,1},{65,33},{97,65},{2,98}... | collective-permute-start | bytes 368648 | tf_op jit(solution)/shard_map/ppermute | solution.py:267
  159.5 17.9 %all-to-all-start = ((bf16[16,160,128]{2,1,0:T(8,128)(2,1)}), bf16[16,160,128]{2,1,0:T(8,128)(2,1)S(1)}, u32[]{:S(2)}, u32[]{:S(2)}) async-start(bf16[16,160,128]{2,1,0:T(8,128)(2,1)} %attention.1), calls=%async_computation | async-start | bytes 1310720 | tf_op jit(solution)/shard_map/all_to_all | solution.py:312
  165.3 2.0 %collective-permute-start.28 = (bf16[1024,256]{1,0:T(8,128)(2,1)S(1)}, bf16[1024,256]{1,0:T(8,128)(2,1)S(1)}, u32[]{:S(2)}, u32[]{:S(2)}) collective-permute-start(bf16[1024,256]{1,0:T(8,128)(2,1)S(1)} %copy-done), channel_id=1, source_target_pairs={{0,1},{1,0},{2,3},{3,2},{4,5},{5,4},{6,7},{7,6},{8,9},{9,8},{10,11... | collective-permute-start | bytes 1572872 | tf_op jit(solution)/shard_map/ppermute | solution.py:267
  165.4 2.6 %collective-permute-start.29 = (bf16[1024,256]{1,0:T(8,128)(2,1)}, bf16[1024,256]{1,0:T(8,128)(2,1)S(1)}, u32[]{:S(2)}, u32[]{:S(2)}) collective-permute-start(bf16[1024,256]{1,0:T(8,128)(2,1)} %collective-permute-done.25.refs_1_), channel_id=1, source_target_pairs={{0,1},{1,0},{2,3},{3,2},{4,5},{5,4},{6,7},{7,6},{8,9},{9,8},{10,11... | collective-permute-start | bytes 1572872 | tf_op jit(solution)/shard_map/ppermute | solution.py:267
  165.9 2.9 %collective-permute-start.30 = (bf16[1024,256]{1,0:T(8,128)(2,1)}, bf16[1024,256]{1,0:T(8,128)(2,1)S(1)}, u32[]{:S(2)}, u32[]{:S(2)}) collective-permute-start(bf16[1024,256]{1,0:T(8,128)(2,1)} %collective-permute-done.26.refs_2_), channel_id=1, source_target_pairs={{0,1},{1,0},{2,3},{3,2},{4,5},{5,4},{6,7},{7,6},{8,9},{9,8},{10,11... | collective-permute-start | bytes 1572872 | tf_op jit(solution)/shard_map/ppermute | solution.py:267
  166.0 3.6 %collective-permute-start.31 = (bf16[1024,256]{1,0:T(8,128)(2,1)}, bf16[1024,256]{1,0:T(8,128)(2,1)S(1)}, u32[]{:S(2)}, u32[]{:S(2)}) collective-permute-start(bf16[1024,256]{1,0:T(8,128)(2,1)} %collective-permute-done.27.refs_3_), channel_id=1, source_target_pairs={{0,1},{1,0},{2,3},{3,2},{4,5},{5,4},{6,7},{7,6},{8,9},{9,8},{10,11... | collective-permute-start | bytes 1572872 | tf_op jit(solution)/shard_map/ppermute | solution.py:267
  (17 other events, 115.1 us)

commit v7 on v5

--- a/solution.py
+++ b/solution.py
@@ -117,7 +117,7 @@
         for i in range(T//BQ):
             emit(i)
     g=jnp.abs(gain_ref[...])
-    isfast=jnp.max(g[0:1])*jnp.max(g[1:2])<=7.7
+    isfast=jnp.max(g[:,0:64])*jnp.max(g[:,64:128])<=7.7/8
     pl.when(isfast)(fast)
     pl.when(jnp.logical_not(isfast))(slow)
 
@@ -167,58 +167,66 @@
     )(*pieces)
 
 
-def proj_block(tok, w, gains, out, at):
+QK_AT = (0, 256, 384, 512)
+V_AT = (128, 192, 640, 704)
+
+
+def proj_block(tok, w, base, heads, gains, out, at):
     lo = lax.broadcasted_iota(jnp.int32, (BLK, 128), 1) < 64
     half = lax.broadcasted_iota(jnp.int32, (BLK // 2, 128), 1) < 64
     acc = lax.dot_general(tok, w, NT, preferred_element_type=f32)
-    for h in range(4):
-        qk = acc[:, h * 128 : h * 128 + 128].astype(bf16).astype(f32)
+    for h, dst in zip(heads, out):
+        c = QK_AT[h] - base
+        qk = acc[:, c : c + 128].astype(bf16).astype(f32)
         sq = qk * qk
         s_lo = jnp.sum(jnp.where(lo, sq, 0.0), axis=1, keepdims=True)
         s_hi = jnp.sum(jnp.where(lo, 0.0, sq), axis=1, keepdims=True)
         inv = lax.rsqrt(jnp.where(lo, s_lo, s_hi) * (1 / 64) + 1e-6)
-        out[h][at : at + 320, :] = (qk * inv * gains).astype(bf16)
-        c = 512 + (h // 2) * 128
+        dst[at : at + 320, :] = (qk * inv * gains).astype(bf16)
+        c = V_AT[h] // 128 * 128 - base
         top, bot = acc[:160, c : c + 128], acc[160:, c : c + 128]
         if h % 2:
             top = pltpu.roll(top, 64, 1)
         else:
             bot = pltpu.roll(bot, 64, 1)
-        out[h][at + 320 : at + 480, :] = jnp.where(half, top, bot).astype(bf16)
-
-
-def gain_row(gain_ref):
-    return jnp.concatenate([gain_ref[0:1, :] * 0.125, gain_ref[1:2, :]], 1)
-
-
-def proj_kernel(idx_ref, gain_ref, *refs, sizes):
-    n = sum(sizes)
-    toks, ws, outs, w = refs[:n], refs[n : n + 8], refs[n + 8 : n + 12], refs[-1]
+        dst[at + 320 : at + 480, :] = jnp.where(half, top, bot).astype(bf16)
+
+
+def weights_in_order(idx_ref, ws, w):
     for j in range(8):
         cols = pl.ds(pl.multiple_of(idx_ref[j] * 256, 256), 256)
         for h in range(4):
-            w[h * 128 : h * 128 + 128, cols] = ws[j][h * 192 : h * 192 + 128, :]
-            w[512 + h * 64 : 576 + h * 64, cols] = ws[j][h * 192 + 128 : h * 192 + 192, :]
-    gains = gain_row(gain_ref)
-    at = 0
-    for b, size in enumerate(sizes):
-        parts = [t[...] for t in toks[at : at + size]]
-        at += size
-        tok = parts[0] if size == 1 else jnp.concatenate(parts, 0)
-        proj_block(tok, w[...], gains, outs, b * 480)
-
-
-def project(cols, gain, blocks, ws):
-    toks = [p for block in blocks for p in block]
+            w[QK_AT[h] : QK_AT[h] + 128, cols] = ws[j][h * 192 : h * 192 + 128, :]
+            w[V_AT[h] : V_AT[h] + 64, cols] = ws[j][h * 192 + 128 : h * 192 + 192, :]
+
+
+def near_kernel(idx_ref, gain_ref, *refs):
+    toks, ws, outs, w = refs[:3], refs[3:11], refs[11:14], refs[14]
+    weights_in_order(idx_ref, ws, w)
+    gains = gain_ref[...]
+    for b in range(3):
+        proj_block(toks[b][...], w[128:768], 128, (1, 2, 3), gains, outs, b * 480)
+
+
+def far_kernel(idx_ref, gain_ref, *refs):
+    toks, ws, outs, w = refs[:4], refs[4:12], refs[12:17], refs[17]
+    weights_in_order(idx_ref, ws, w)
+    gains = gain_ref[...]
+    proj_block(toks[0][...], w[...], 0, (0, 1, 2, 3), gains, outs[:4], 0)
+    for b in range(3):
+        proj_block(toks[b + 1][...], w[0:256], 0, (0,), gains, outs[4:], b * 480)
+
+
+def project(kernel, lengths, cols, gains, toks, ws):
     return pl.pallas_call(
-        functools.partial(proj_kernel, sizes=tuple(len(b) for b in blocks)),
-        out_shape=[jax.ShapeDtypeStruct((len(blocks) * 480, 128), bf16)] * 4,
+        kernel,
+        out_shape=[jax.ShapeDtypeStruct((n, 128), bf16) for n in lengths],
         in_specs=[SMEM] + [VMEM] * (1 + len(toks) + 8),
-        out_specs=[VMEM] * 4,
+        out_specs=[VMEM] * len(lengths),
         scratch_shapes=[pltpu.VMEM((768, 2048), bf16)],
         compiler_params=pltpu.CompilerParams(vmem_limit_bytes=20 * 1024 * 1024),
         name="project",
-    )(cols, gain, *toks, *ws)
+    )(cols, gains, *toks, *ws)
 
 
 def out_kernel(head_ref, col_ref, heads_ref, *refs):
@@ -264,9 +272,9 @@
     return lax.ppermute(value, axis, pairs)
 
 
-def spread(value, step):
+def spread(value, axis, step):
     pairs = [(2 * i + k, 2 * ((i + (step, -step)[k]) % 4) + k) for i in range(4) for k in (0, 1)]
-    return lax.ppermute(value, (Y, C), pairs)
+    return lax.ppermute(value, (axis, C), pairs)
 
 
 def around(value, axis):
@@ -276,37 +284,44 @@
 def on_device(tokens, w_query, w_key, w_value, w_output, qk_gain, decay_sums):
     own = tokens[0]
     z, y, x, c = (lax.axis_index(a) for a in (Z, Y, X, C))
-    t1 = spread(own, -1)
-    t3 = spread(own, 1)
-    t2 = spread(t1, -1)
-    near = jnp.where(c == 0, 1, 3)
+    t1 = spread(own, Y, -1)
+    t3 = spread(own, Y, 1)
+    t2 = spread(t1, Y, -1)
     piece = jnp.concatenate([w_query.T, w_key.T, w_value.T, w_output], 0)
     w4, wo4 = pack(around(piece, Z))
-    ws = around(w4, X)
+    w1 = spread(w4, X, -1)
+    ws = [w4, w1, spread(w4, X, 1), spread(w1, X, -1)]
     ws = ws + [move(w, C, 0) for w in ws]
 
-    cols = jnp.stack(
+    near = jnp.where(c == 0, 1, 3)
+    turns = [(c, (0, near, 4 - near, 2)), (1 - c, (0, 4 - near, near, 2))]
+    cols = jnp.stack([2 * ((x + d) % 4) + e for e, ds in turns for d in ds]).astype(jnp.int32)
+    out_cols = jnp.stack(
         [2 * ((x + d) % 4) + e for e in (c, 1 - c) for d in range(4)]
     ).astype(jnp.int32)
-    part1 = project(cols, qk_gain, [[own], [t1], [t3]], ws)
+    gains = jnp.concatenate([qk_gain[0] * 0.125, qk_gain[1]])[None]
+    near_toks = [own, t1, t3]
+    part1 = project(near_kernel, (1440,) * 3, cols, gains, near_toks, ws)
     *part1, wo4 = lax.optimization_barrier((*part1, wo4))
-    part2 = project(cols, qk_gain, [[t2]], ws)
+    *part2, mine = project(
+        far_kernel, (480,) * 4 + (1440,), cols, gains, [t2] + near_toks, ws
+    )
     recv = []
-    for part in (part1, part2):
+    for part in ([mine] + part1, part2):
         recv += [part[0]] + [move(part[d], Z, d) for d in (1, 2, 3)]
     wo16 = join(around(wo4, X))
     wo = around(wo16, Y)
     pos = [4 * ((z - d) % 4) + (y + e) % 4 for d in range(4) for e in (0, near, 4 - near)]
     pos += [4 * ((z - d) % 4) + (y + 2) % 4 for d in range(4)]
     pos = jnp.stack(pos).astype(jnp.int32)
-    heads = attention(pos, qk_gain, decay_sums[0], recv, (3, 3, 3, 3, 1, 1, 1, 1))
+    heads = attention(pos, gains, decay_sums[0], recv, (3, 3, 3, 3, 1, 1, 1, 1))
     heads, *wo = lax.optimization_barrier((heads, *wo))
     wo = wo + [move(w, C, 0) for w in wo]
     merged = lax.all_to_all(heads, SP, 0, 0, tiled=True)
     order = jnp.stack(
         [4 * ((z + d) % 4) + (y + e) % 4 for e in range(4) for d in range(4)]
     ).astype(jnp.int32)
-    return output(order, cols, merged, wo)[None]
+    return output(order, out_cols, merged, wo)[None]
 
 
 def solution(mesh):

time: 164 us -> 168 us (1.024)
  starting transfers between devices: 50.6 us -> 42.9 us
  waiting for transfers between devices: 44.8 us -> 50.6 us
  local copies, waits for them, and re-layouts: 11 us -> 14.2 us
    ppermute x26 -> x23, starting transfers between devices: 38.3 us -> 23.6 us  [move(): return lax.ppermute(value, axis, pairs)]
    ppermute x3 -> x6, waiting for transfers between devices: 9.88 us -> 18.8 us  [spread(): return lax.ppermute(value, (axis, C), pairs)]
    ppermute x3 -> x6, starting transfers between devices: 6.82 us -> 12.8 us  [spread(): return lax.ppermute(value, (axis, C), pairs)]
    unnamed x32 -> x40, local copies, waits for them, and re-layouts: 10.7 us -> 13.8 us
    ppermute x26 -> x23, waiting for transfers between devices: 28.4 us -> 25.2 us  [move(): return lax.ppermute(value, axis, pairs)]
  transfers between devices with their start and end apart: 30 -> 30, of which waited for: 18 -> 17; matrix products, arithmetic and copies ran while one was open for 1% -> 1% of each run, Pallas kernels for 32% -> 31%
where the time goes in v7:
time: 168 us; the launch traced here: 166 us
  Pallas kernels  56.5 us (34%)
  waiting for transfers between devices  50.6 us (30%)
  starting transfers between devices  42.9 us (26%)
  local copies, waits for them, and re-layouts  14.2 us (8%)
    pallas_call x1, Pallas kernels, attention(): pl.pallas_call(functools.partial(attn_kernel, nblk=nblk), out_shape=jax.S...  41.3 us
    ppermute x23, waiting for transfers between devices, move(): return lax.ppermute(value, axis, pairs)  25.2 us
    ppermute x23, starting transfers between devices, move(): return lax.ppermute(value, axis, pairs)  23.6 us
    ppermute x6, waiting for transfers between devices, spread(): return lax.ppermute(value, (axis, C), pairs)  18.8 us
    unnamed x40, local copies, waits for them, and re-layouts  13.8 us
    ppermute x6, starting transfers between devices, spread(): return lax.ppermute(value, (axis, C), pairs)  12.8 us
    pallas_call x2, Pallas kernels, project(): pl.pallas_call(kernel, out_shape=[jax.ShapeDtypeStruct((n, 128), bf16) fo...  10.8 us
    all_to_all x1, waiting for transfers between devices, on_device(): merged = lax.all_to_all(heads, SP, 0, 0, tiled=True)  6.47 us
  transfers between devices with their start and end apart: 30, of which 17 were waited for; matrix products, arithmetic and copies ran while one was open for 1% of the time, Pallas kernels for 31%

profile of v7, /device:TPU:0, one launch (start us, length us, event | category | flops | bytes accessed | tf_op | source)
XLA Modules:
  0.0 166.0 jit_solution(18287078403041289319)
XLA Ops:
  0.0 3.1 %collective-permute-start = (bf16[320,2048]{1,0:T(8,128)(2,1)}, bf16[320,2048]{1,0:T(8,128)(2,1)S(1)}, u32[]{:S(2)}, u32[]{:S(2)}) collective-permute-start(bf16[320,2048]{1,0:T(8,128)(2,1)} %bitcast.54), channel_id=1, source_target_pairs={{0,24},{1,9},{8,0},{9,17},{16,8},{17,25},{24,16},{25,1},{2,26},{3,... | collective-permute-start | bytes 3932168 | tf_op jit(solution)/shard_map/ppermute | solution.py:277
  3.9 4.1 %collective-permute-start.3 = (bf16[256,256]{1,0:T(8,128)(2,1)S(1)}, bf16[256,256]{1,0:T(8,128)(2,1)S(1)}, u32[]{:S(2)}, u32[]{:S(2)}) collective-permute-start(bf16[256,256]{1,0:T(8,128)(2,1)S(1)} %pad_maximum_fusion.refs_0_), channel_id=1, source_target_pairs={{0,96},{32,0},{64,32},{96,64},{1,97},{33,1},{65,33},{97,65},{2,98}... | collective-permute-start | bytes 393224 | tf_op jit(solution)/shard_map/ppermute | solution.py:272
  8.1 1.3 collective-permute-start.5
  9.3 2.8 %collective-permute-done.3.refs_1_ = bf16[256,256]{1,0:T(8,128)(2,1)S(1)} collective-permute-done((bf16[256,256]{1,0:T(8,128)(2,1)S(1)}, bf16[256,256]{1,0:T(8,128)(2,1)S(1)}, u32[]{:S(2)}, u32[]{:S(2)}) %collective-permute-start.3) | collective-permute-done | bytes 131104 | tf_op jit(solution)/shard_map/ppermute | solution.py:272
  12.2 2.5 %collective-permute-done.4.refs_2_ = bf16[256,256]{1,0:T(8,128)(2,1)S(1)} collective-permute-done((bf16[256,256]{1,0:T(8,128)(2,1)S(1)}, bf16[256,256]{1,0:T(8,128)(2,1)S(1)}, u32[]{:S(2)}, u32[]{:S(2)}) %collective-permute-start.4) | collective-permute-done | bytes 131104 | tf_op jit(solution)/shard_map/ppermute | solution.py:272
  14.6 1.0 collective-permute-done.5.refs_3_
  15.7 2.8 %collective-permute-start.6 = (bf16[768,256]{1,0:T(8,128)(2,1)S(1)}, bf16[768,256]{1,0:T(8,128)(2,1)S(1)}, u32[]{:S(2)}, u32[]{:S(2)}) collective-permute-start(bf16[768,256]{1,0:T(8,128)(2,1)S(1)} %get-tuple-element.24.refs_4_.refs_3_), channel_id=1, source_target_pairs={{0,6},{1,3},{2,0},{3,5},{4,2},{5,7},{6,4},{7,1},{8,14},{9,11},{10,... | collective-permute-start | bytes 1179656 | tf_op jit(solution)/shard_map/ppermute | solution.py:277
  18.5 9.9 %collective-permute-done.refs_2_.refs_1_ = bf16[320,2048]{1,0:T(8,128)(2,1)S(1)} collective-permute-done((bf16[320,2048]{1,0:T(8,128)(2,1)}, bf16[320,2048]{1,0:T(8,128)(2,1)S(1)}, u32[]{:S(2)}, u32[]{:S(2)}) %collective-permute-start) | collective-permute-done | bytes 1310752 | tf_op jit(solution)/shard_map/ppermute | solution.py:277
  28.4 3.6 %collective-permute-start.1 = (bf16[320,2048]{1,0:T(8,128)(2,1)S(1)}, bf16[320,2048]{1,0:T(8,128)(2,1)}, u32[]{:S(2)}, u32[]{:S(2)}) collective-permute-start(bf16[320,2048]{1,0:T(8,128)(2,1)S(1)} %collective-permute-done.refs_2_.refs_1_), channel_id=1, source_target_pairs={{0,24},{1,9},{8,0},{9,17},{16,8},{17,25},{24,16},{25,1},{2,26},{3,... | collective-permute-start | bytes 3932168 | tf_op jit(solution)/shard_map/ppermute | solution.py:277
  32.0 1.5 collective-permute-start.7
  33.5 1.8 %collective-permute-start.8 = (bf16[768,256]{1,0:T(8,128)(2,1)S(1)}, bf16[768,256]{1,0:T(8,128)(2,1)}, u32[]{:S(2)}, u32[]{:S(2)}) collective-permute-start(bf16[768,256]{1,0:T(8,128)(2,1)S(1)} %collective-permute-done.6.refs_5_.refs_4_), channel_id=1, source_target_pairs={{0,6},{1,3},{2,0},{3,5},{4,2},{5,7},{6,4},{7,1},{8,14},{9,11},{10,... | collective-permute-start | bytes 1179656 | tf_op jit(solution)/shard_map/ppermute | solution.py:277
  35.3 8.9 %collective-permute-done.7.refs_6_.refs_5_ = bf16[768,256]{1,0:T(8,128)(2,1)} collective-permute-done((bf16[768,256]{1,0:T(8,128)(2,1)S(1)}, bf16[768,256]{1,0:T(8,128)(2,1)}, u32[]{:S(2)}, u32[]{:S(2)}) %collective-permute-start.7) | collective-permute-done | bytes 393248 | tf_op jit(solution)/shard_map/ppermute | solution.py:277
  47.8 1.3 copy-done
  49.1 1.0 copy-done.5
  50.1 5.7 %project.3 = (bf16[1440,128]{1,0:T(8,128)(2,1)S(1)}, bf16[1440,128]{1,0:T(8,128)(2,1)S(1)}, bf16[1440,128]{1,0:T(8,128)(2,1)S(1)}) custom-call(s32[8]{0:T(128)S(1)} %stack.189.idx_ref, f32[1,128]{1,0:T(1,128)S(1)} %maximum_bitcast_fusion.gain_ref, bf16[320,2048]{1,0:T(8,128)(2,1)S(1)} %bitcast.56, ...), custom_call_target="tpu_custom_call" | custom-call | tf_op jit(solution)/shard_map/project/pallas_call | solution.py:221
  55.8 1.7 %collective-permute-start.13 = (bf16[1440,128]{1,0:T(8,128)(2,1)S(1)}, bf16[1440,128]{1,0:T(8,128)(2,1)S(1)}, u32[]{:S(2)}, u32[]{:S(2)}) collective-permute-start(bf16[1440,128]{1,0:T(8,128)(2,1)S(1)} %get-tuple-element.30), channel_id=1, source_target_pairs={{0,32},{32,64},{64,96},{96,0},{1,33},{33,65},{65,97},{97,1},{2,34}... | collective-permute-start | bytes 1105928 | tf_op jit(solution)/shard_map/ppermute | solution.py:272
  57.5 2.6 %collective-permute-start.19 = (bf16[256,256]{1,0:T(8,128)(2,1)S(1)}, bf16[256,256]{1,0:T(8,128)(2,1)S(1)}, u32[]{:S(2)}, u32[]{:S(2)}) collective-permute-start(bf16[256,256]{1,0:T(8,128)(2,1)S(1)} %get-tuple-element.37.refs_0_), channel_id=1, source_target_pairs={{0,6},{2,0},{4,2},{6,4},{1,7},{3,1},{5,3},{7,5},{8,14},{10,8},{12,... | collective-permute-start | bytes 393224 | tf_op jit(solution)/shard_map/ppermute | solution.py:272
  61.7 4.2 %collective-permute-done.19.refs_1_ = bf16[256,256]{1,0:T(8,128)(2,1)S(1)} collective-permute-done((bf16[256,256]{1,0:T(8,128)(2,1)S(1)}, bf16[256,256]{1,0:T(8,128)(2,1)S(1)}, u32[]{:S(2)}, u32[]{:S(2)}) %collective-permute-start.19) | collective-permute-done | bytes 131104 | tf_op jit(solution)/shard_map/ppermute | solution.py:272
  65.9 5.7 %collective-permute-start.14 = (bf16[1440,128]{1,0:T(8,128)(2,1)S(1)}, bf16[1440,128]{1,0:T(8,128)(2,1)S(1)}, u32[]{:S(2)}, u32[]{:S(2)}) collective-permute-start(bf16[1440,128]{1,0:T(8,128)(2,1)S(1)} %get-tuple-element.31), channel_id=1, source_target_pairs={{0,64},{32,96},{64,0},{96,32},{1,65},{33,97},{65,1},{97,33},{2,66}... | collective-permute-start | bytes 1105928 | tf_op jit(solution)/shard_map/ppermute | solution.py:272
  73.9 1.5 collective-permute-start.24
  75.4 2.3 %collective-permute-start.15 = (bf16[1440,128]{1,0:T(8,128)(2,1)S(1)}, bf16[1440,128]{1,0:T(8,128)(2,1)S(1)}, u32[]{:S(2)}, u32[]{:S(2)}) collective-permute-start(bf16[1440,128]{1,0:T(8,128)(2,1)S(1)} %get-tuple-element.32), channel_id=1, source_target_pairs={{0,96},{32,0},{64,32},{96,64},{1,97},{33,1},{65,33},{97,65},{2,98}... | collective-permute-start | bytes 1105928 | tf_op jit(solution)/shard_map/ppermute | solution.py:272
  77.7 5.1 %project.2 = (bf16[480,128]{1,0:T(8,128)(2,1)S(1)}, bf16[480,128]{1,0:T(8,128)(2,1)S(1)}, bf16[480,128]{1,0:T(8,128)(2,1)}, bf16[480,128]{1,0:T(8,128)(2,1)}, bf16[1440,128]{1,0:T(8,128)(2,1)S(1)}) custom-call(s32[8]{0:T(128)S(1)} %stack.189.idx_ref, f32[1,128]{1,0:T(1,128)S(1)} %maximum_bitcast_fusion.gain_ref, ...), custom_call_target="tpu_custom_call" | custom-call | tf_op jit(solution)/shard_map/project/pallas_call | solution.py:221
  84.9 2.1 %collective-permute-done.15.refs_3_ = bf16[1440,128]{1,0:T(8,128)(2,1)S(1)} collective-permute-done((bf16[1440,128]{1,0:T(8,128)(2,1)S(1)}, bf16[1440,128]{1,0:T(8,128)(2,1)S(1)}, u32[]{:S(2)}, u32[]{:S(2)}) %collective-permute-start.15) | collective-permute-done | bytes 368672 | tf_op jit(solution)/shard_map/ppermute | solution.py:272
  87.8 1.4 collective-permute-start.17
  89.2 3.1 %collective-permute-done.16.refs_5_ = bf16[480,128]{1,0:T(8,128)(2,1)S(1)} collective-permute-done((bf16[480,128]{1,0:T(8,128)(2,1)S(1)}, bf16[480,128]{1,0:T(8,128)(2,1)S(1)}, u32[]{:S(2)}, u32[]{:S(2)}) %collective-permute-start.16) | collective-permute-done | bytes 122912 | tf_op jit(solution)/shard_map/ppermute | solution.py:272
  92.4 2.0 %collective-permute-done.17.refs_6_ = bf16[480,128]{1,0:T(8,128)(2,1)S(1)} collective-permute-done((bf16[480,128]{1,0:T(8,128)(2,1)}, bf16[480,128]{1,0:T(8,128)(2,1)S(1)}, u32[]{:S(2)}, u32[]{:S(2)}) %collective-permute-start.17) | collective-permute-done | bytes 122912 | tf_op jit(solution)/shard_map/ppermute | solution.py:272
  94.4 3.0 %collective-permute-done.18.refs_7_ = bf16[480,128]{1,0:T(8,128)(2,1)S(1)} collective-permute-done((bf16[480,128]{1,0:T(8,128)(2,1)}, bf16[480,128]{1,0:T(8,128)(2,1)S(1)}, u32[]{:S(2)}, u32[]{:S(2)}) %collective-permute-start.18) | collective-permute-done | bytes 122912 | tf_op jit(solution)/shard_map/ppermute | solution.py:272
  97.4 1.0 copy-done.8
  103.0 41.3 %attention.1 = bf16[16,160,128]{2,1,0:T(8,128)(2,1)} custom-call(s32[16]{0:T(128)S(1)} %stack.184.pos_ref, f32[1,128]{1,0:T(1,128)S(1)} %maximum_bitcast_fusion.gain_ref, f32[1,5120]{1,0:T(1,128)S(1)} %bitcast.58, bf16[1440,128]{1,0:T(8,128)(2,1)S(1)} %copy-done.14, bf16[1440,128]{1,0:T(8,128)(2,1)S(1)} %copy-done.8, bf16[1440,128]{1,0:T(8,128)(2,1)S(1)} %copy-done.10, ...), custom_call_target="tpu_custom_call" | custom-call | tf_op jit(solution)/shard_map/attention/pallas_call | solution.py:127
  144.4 6.5 %all-to-all-start = ((bf16[16,160,128]{2,1,0:T(8,128)(2,1)}), bf16[16,160,128]{2,1,0:T(8,128)(2,1)S(1)}, u32[]{:S(2)}, u32[]{:S(2)}) async-start(bf16[16,160,128]{2,1,0:T(8,128)(2,1)} %attention.1), calls=%async_computation | async-start | bytes 1310720 | tf_op jit(solution)/shard_map/all_to_all | solution.py:320
  155.2 6.5 %all-to-all-done.heads_ref = bf16[16,160,128]{2,1,0:T(8,128)(2,1)S(1)} async-done(((bf16[16,160,128]{2,1,0:T(8,128)(2,1)}), bf16[16,160,128]{2,1,0:T(8,128)(2,1)S(1)}, u32[]{:S(2)}, u32[]{:S(2)}) %all-to-all-start) | async-done | bytes 655392 | tf_op jit(solution)/shard_map/all_to_all | solution.py:320
  161.7 4.3 %output.1 = bf16[320,2048]{1,0:T(8,128)(2,1)} custom-call(s32[16]{0:T(128)S(1)} %stack.160.head_ref, s32[8]{0:T(128)S(1)} %stack.169.col_ref, bf16[16,160,128]{2,1,0:T(8,128)(2,1)S(1)} %all-to-all-done.heads_ref, bf16[1024,256]{1,0:T(8,128)(2,1)S(1)} %join.1.refs_0_, bf16[1024,256]{1,0:T(8,128)(2,1)} %collective-permute-done.22.refs_1_, ...), custom_call_target="tpu_custom_call" | custom-call | tf_op jit(solution)/shard_map/output/pallas_call | solution.py:255
  (81 shorter events, 20.2 us)
Async XLA Ops:
  0.0 28.4 %collective-permute-start = (bf16[320,2048]{1,0:T(8,128)(2,1)}, bf16[320,2048]{1,0:T(8,128)(2,1)S(1)}, u32[]{:S(2)}, u32[]{:S(2)}) collective-permute-start(bf16[320,2048]{1,0:T(8,128)(2,1)} %bitcast.54), channel_id=1, source_target_pairs={{0,24},{1,9},{8,0},{9,17},{16,8},{17,25},{24,16},{25,1},{2,26},{3,... | collective-permute-start | bytes 3932168 | tf_op jit(solution)/shard_map/ppermute | solution.py:277
  3.9 8.2 %collective-permute-start.3 = (bf16[256,256]{1,0:T(8,128)(2,1)S(1)}, bf16[256,256]{1,0:T(8,128)(2,1)S(1)}, u32[]{:S(2)}, u32[]{:S(2)}) collective-permute-start(bf16[256,256]{1,0:T(8,128)(2,1)S(1)} %pad_maximum_fusion.refs_0_), channel_id=1, source_target_pairs={{0,96},{32,0},{64,32},{96,64},{1,97},{33,1},{65,33},{97,65},{2,98}... | collective-permute-start | bytes 393224 | tf_op jit(solution)/shard_map/ppermute | solution.py:272
  8.1 6.6 %collective-permute-start.4 = (bf16[256,256]{1,0:T(8,128)(2,1)S(1)}, bf16[256,256]{1,0:T(8,128)(2,1)S(1)}, u32[]{:S(2)}, u32[]{:S(2)}) collective-permute-start(bf16[256,256]{1,0:T(8,128)(2,1)S(1)} %pad_maximum_fusion.refs_0_), channel_id=1, source_target_pairs={{0,64},{32,96},{64,0},{96,32},{1,65},{33,97},{65,1},{97,33},{2,66}... | collective-permute-start | bytes 393224 | tf_op jit(solution)/shard_map/ppermute | solution.py:272
  8.1 7.6 %collective-permute-start.5 = (bf16[256,256]{1,0:T(8,128)(2,1)S(1)}, bf16[256,256]{1,0:T(8,128)(2,1)S(1)}, u32[]{:S(2)}, u32[]{:S(2)}) collective-permute-start(bf16[256,256]{1,0:T(8,128)(2,1)S(1)} %pad_maximum_fusion.refs_0_), channel_id=1, source_target_pairs={{0,32},{32,64},{64,96},{96,0},{1,33},{33,65},{65,97},{97,1},{2,34}... | collective-permute-start | bytes 393224 | tf_op jit(solution)/shard_map/ppermute | solution.py:272
  9.3 37.9 %collective-permute-start.2 = (bf16[320,2048]{1,0:T(8,128)(2,1)}, bf16[320,2048]{1,0:T(8,128)(2,1)S(1)}, u32[]{:S(2)}, u32[]{:S(2)}) collective-permute-start(bf16[320,2048]{1,0:T(8,128)(2,1)} %bitcast.55), channel_id=1, source_target_pairs={{0,8},{1,25},{8,16},{9,1},{16,24},{17,9},{24,0},{25,17},{2,10},{3,... | collective-permute-start | bytes 3932168 | tf_op jit(solution)/shard_map/ppermute | solution.py:277
  15.7 17.8 %collective-permute-start.6 = (bf16[768,256]{1,0:T(8,128)(2,1)S(1)}, bf16[768,256]{1,0:T(8,128)(2,1)S(1)}, u32[]{:S(2)}, u32[]{:S(2)}) collective-permute-start(bf16[768,256]{1,0:T(8,128)(2,1)S(1)} %get-tuple-element.24.refs_4_.refs_3_), channel_id=1, source_target_pairs={{0,6},{1,3},{2,0},{3,5},{4,2},{5,7},{6,4},{7,1},{8,14},{9,11},{10,... | collective-permute-start | bytes 1179656 | tf_op jit(solution)/shard_map/ppermute | solution.py:277
  28.4 47.0 %collective-permute-start.1 = (bf16[320,2048]{1,0:T(8,128)(2,1)S(1)}, bf16[320,2048]{1,0:T(8,128)(2,1)}, u32[]{:S(2)}, u32[]{:S(2)}) collective-permute-start(bf16[320,2048]{1,0:T(8,128)(2,1)S(1)} %collective-permute-done.refs_2_.refs_1_), channel_id=1, source_target_pairs={{0,24},{1,9},{8,0},{9,17},{16,8},{17,25},{24,16},{25,1},{2,26},{3,... | collective-permute-start | bytes 3932168 | tf_op jit(solution)/shard_map/ppermute | solution.py:277
  32.0 12.3 %collective-permute-start.7 = (bf16[768,256]{1,0:T(8,128)(2,1)S(1)}, bf16[768,256]{1,0:T(8,128)(2,1)}, u32[]{:S(2)}, u32[]{:S(2)}) collective-permute-start(bf16[768,256]{1,0:T(8,128)(2,1)S(1)} %get-tuple-element.24.refs_4_.refs_3_), channel_id=1, source_target_pairs={{0,2},{1,7},{2,4},{3,1},{4,6},{5,3},{6,0},{7,5},{8,10},{9,15},{10,... | collective-permute-start | bytes 1179656 | tf_op jit(solution)/shard_map/ppermute | solution.py:277
  33.5 10.8 %collective-permute-start.9 = (bf16[768,256]{1,0:T(8,128)(2,1)S(1)}, bf16[768,256]{1,0:T(8,128)(2,1)S(1)}, u32[]{:S(2)}, u32[]{:S(2)}) collective-permute-start(bf16[768,256]{1,0:T(8,128)(2,1)S(1)} %get-tuple-element.24.refs_4_.refs_3_), channel_id=1, source_target_pairs={{0,1},{1,0},{2,3},{3,2},{4,5},{5,4},{6,7},{7,6},{8,9},{9,8},{10,11... | collective-permute-start | bytes 1179656 | tf_op jit(solution)/shard_map/ppermute | solution.py:272
  33.5 22.3 %copy-start.2 = (bf16[768,256]{1,0:T(8,128)(2,1)}, bf16[768,256]{1,0:T(8,128)(2,1)S(1)}, u32[]{:S(2)}) copy-start(bf16[768,256]{1,0:T(8,128)(2,1)S(1)} %collective-permute-done.6.refs_5_.refs_4_) | copy-start | bytes 1179652
  33.5 12.0 %collective-permute-start.8 = (bf16[768,256]{1,0:T(8,128)(2,1)S(1)}, bf16[768,256]{1,0:T(8,128)(2,1)}, u32[]{:S(2)}, u32[]{:S(2)}) collective-permute-start(bf16[768,256]{1,0:T(8,128)(2,1)S(1)} %collective-permute-done.6.refs_5_.refs_4_), channel_id=1, source_target_pairs={{0,6},{1,3},{2,0},{3,5},{4,2},{5,7},{6,4},{7,1},{8,14},{9,11},{10,... | collective-permute-start | bytes 1179656 | tf_op jit(solution)/shard_map/ppermute | solution.py:277
  44.2 2.2 %collective-permute-start.10 = (bf16[768,256]{1,0:T(8,128)(2,1)S(1)}, bf16[768,256]{1,0:T(8,128)(2,1)}, u32[]{:S(2)}, u32[]{:S(2)}) collective-permute-start(bf16[768,256]{1,0:T(8,128)(2,1)S(1)} %collective-permute-done.6.refs_5_.refs_4_), channel_id=1, source_target_pairs={{0,1},{1,0},{2,3},{3,2},{4,5},{5,4},{6,7},{7,6},{8,9},{9,8},{10,11... | collective-permute-start | bytes 1179656 | tf_op jit(solution)/shard_map/ppermute | solution.py:272
  45.0 2.2 %collective-permute-start.11 = (bf16[768,256]{1,0:T(8,128)(2,1)}, bf16[768,256]{1,0:T(8,128)(2,1)}, u32[]{:S(2)}, u32[]{:S(2)}) collective-permute-start(bf16[768,256]{1,0:T(8,128)(2,1)} %collective-permute-done.7.refs_6_.refs_5_), channel_id=1, source_target_pairs={{0,1},{1,0},{2,3},{3,2},{4,5},{5,4},{6,7},{7,6},{8,9},{9,8},{10,11... | collective-permute-start | bytes 1179656 | tf_op jit(solution)/shard_map/ppermute | solution.py:272
  45.5 2.3 %collective-permute-start.12 = (bf16[768,256]{1,0:T(8,128)(2,1)}, bf16[768,256]{1,0:T(8,128)(2,1)}, u32[]{:S(2)}, u32[]{:S(2)}) collective-permute-start(bf16[768,256]{1,0:T(8,128)(2,1)} %collective-permute-done.8.refs_7_.refs_6_), channel_id=1, source_target_pairs={{0,1},{1,0},{2,3},{3,2},{4,5},{5,4},{6,7},{7,6},{8,9},{9,8},{10,11... | collective-permute-start | bytes 1179656 | tf_op jit(solution)/shard_map/ppermute | solution.py:272
  50.1 27.6 %copy-start.1 = (bf16[1,320,2048]{2,1,0:T(8,128)(2,1)S(1)}, bf16[1,320,2048]{2,1,0:T(8,128)(2,1)}, u32[]{:S(2)}) copy-start(bf16[1,320,2048]{2,1,0:T(8,128)(2,1)} %param.7) | copy-start | bytes 3932164
  55.8 17.3 %collective-permute-start.13 = (bf16[1440,128]{1,0:T(8,128)(2,1)S(1)}, bf16[1440,128]{1,0:T(8,128)(2,1)S(1)}, u32[]{:S(2)}, u32[]{:S(2)}) collective-permute-start(bf16[1440,128]{1,0:T(8,128)(2,1)S(1)} %get-tuple-element.30), channel_id=1, source_target_pairs={{0,32},{32,64},{64,96},{96,0},{1,33},{33,65},{65,97},{97,1},{2,34}... | collective-permute-start | bytes 1105928 | tf_op jit(solution)/shard_map/ppermute | solution.py:272
  57.5 8.4 %collective-permute-start.19 = (bf16[256,256]{1,0:T(8,128)(2,1)S(1)}, bf16[256,256]{1,0:T(8,128)(2,1)S(1)}, u32[]{:S(2)}, u32[]{:S(2)}) collective-permute-start(bf16[256,256]{1,0:T(8,128)(2,1)S(1)} %get-tuple-element.37.refs_0_), channel_id=1, source_target_pairs={{0,6},{2,0},{4,2},{6,4},{1,7},{3,1},{5,3},{7,5},{8,14},{10,8},{12,... | collective-permute-start | bytes 393224 | tf_op jit(solution)/shard_map/ppermute | solution.py:272
  60.1 11.5 %collective-permute-start.20 = (bf16[256,256]{1,0:T(8,128)(2,1)S(1)}, bf16[256,256]{1,0:T(8,128)(2,1)S(1)}, u32[]{:S(2)}, u32[]{:S(2)}) collective-permute-start(bf16[256,256]{1,0:T(8,128)(2,1)S(1)} %get-tuple-element.37.refs_0_), channel_id=1, source_target_pairs={{0,4},{2,6},{4,0},{6,2},{1,5},{3,7},{5,1},{7,3},{8,12},{10,14},{12... | collective-permute-start | bytes 393224 | tf_op jit(solution)/shard_map/ppermute | solution.py:272
  60.1 11.5 %collective-permute-start.21 = (bf16[256,256]{1,0:T(8,128)(2,1)S(1)}, bf16[256,256]{1,0:T(8,128)(2,1)S(1)}, u32[]{:S(2)}, u32[]{:S(2)}) collective-permute-start(bf16[256,256]{1,0:T(8,128)(2,1)S(1)} %get-tuple-element.37.refs_0_), channel_id=1, source_target_pairs={{0,2},{2,4},{4,6},{6,0},{1,3},{3,5},{5,7},{7,1},{8,10},{10,12},{12... | collective-permute-start | bytes 393224 | tf_op jit(solution)/shard_map/ppermute | solution.py:272
  65.9 18.2 %collective-permute-start.14 = (bf16[1440,128]{1,0:T(8,128)(2,1)S(1)}, bf16[1440,128]{1,0:T(8,128)(2,1)S(1)}, u32[]{:S(2)}, u32[]{:S(2)}) collective-permute-start(bf16[1440,128]{1,0:T(8,128)(2,1)S(1)} %get-tuple-element.31), channel_id=1, source_target_pairs={{0,64},{32,96},{64,0},{96,32},{1,65},{33,97},{65,1},{97,33},{2,66}... | collective-permute-start | bytes 1105928 | tf_op jit(solution)/shard_map/ppermute | solution.py:272
  72.6 71.8 %collective-permute-start.22 = (bf16[1024,256]{1,0:T(8,128)(2,1)S(1)}, bf16[1024,256]{1,0:T(8,128)(2,1)}, u32[]{:S(2)}, u32[]{:S(2)}) collective-permute-start(bf16[1024,256]{1,0:T(8,128)(2,1)S(1)} %join.1.refs_0_), channel_id=1, source_target_pairs={{0,24},{8,0},{16,8},{24,16},{1,25},{9,1},{17,9},{25,17},{2,26},{10... | collective-permute-start | bytes 1572872 | tf_op jit(solution)/shard_map/ppermute | solution.py:272
  72.6 71.7 %collective-permute-start.23 = (bf16[1024,256]{1,0:T(8,128)(2,1)S(1)}, bf16[1024,256]{1,0:T(8,128)(2,1)}, u32[]{:S(2)}, u32[]{:S(2)}) collective-permute-start(bf16[1024,256]{1,0:T(8,128)(2,1)S(1)} %join.1.refs_0_), channel_id=1, source_target_pairs={{0,16},{8,24},{16,0},{24,8},{1,17},{9,25},{17,1},{25,9},{2,18},{10... | collective-permute-start | bytes 1572872 | tf_op jit(solution)/shard_map/ppermute | solution.py:272
  73.9 70.5 %collective-permute-start.24 = (bf16[1024,256]{1,0:T(8,128)(2,1)S(1)}, bf16[1024,256]{1,0:T(8,128)(2,1)}, u32[]{:S(2)}, u32[]{:S(2)}) collective-permute-start(bf16[1024,256]{1,0:T(8,128)(2,1)S(1)} %join.1.refs_0_), channel_id=1, source_target_pairs={{0,8},{8,16},{16,24},{24,0},{1,9},{9,17},{17,25},{25,1},{2,10},{10... | collective-permute-start | bytes 1572872 | tf_op jit(solution)/shard_map/ppermute | solution.py:272
  75.4 11.7 %collective-permute-start.15 = (bf16[1440,128]{1,0:T(8,128)(2,1)S(1)}, bf16[1440,128]{1,0:T(8,128)(2,1)S(1)}, u32[]{:S(2)}, u32[]{:S(2)}) collective-permute-start(bf16[1440,128]{1,0:T(8,128)(2,1)S(1)} %get-tuple-element.32), channel_id=1, source_target_pairs={{0,96},{32,0},{64,32},{96,64},{1,97},{33,1},{65,33},{97,65},{2,98}... | collective-permute-start | bytes 1105928 | tf_op jit(solution)/shard_map/ppermute | solution.py:272
  84.9 7.4 %collective-permute-start.16 = (bf16[480,128]{1,0:T(8,128)(2,1)S(1)}, bf16[480,128]{1,0:T(8,128)(2,1)S(1)}, u32[]{:S(2)}, u32[]{:S(2)}) collective-permute-start(bf16[480,128]{1,0:T(8,128)(2,1)S(1)} %get-tuple-element.34), channel_id=1, source_target_pairs={{0,32},{32,64},{64,96},{96,0},{1,33},{33,65},{65,97},{97,1},{2,34}... | collective-permute-start | bytes 368648 | tf_op jit(solution)/shard_map/ppermute | solution.py:272
  87.8 6.6 %collective-permute-start.17 = (bf16[480,128]{1,0:T(8,128)(2,1)}, bf16[480,128]{1,0:T(8,128)(2,1)S(1)}, u32[]{:S(2)}, u32[]{:S(2)}) collective-permute-start(bf16[480,128]{1,0:T(8,128)(2,1)} %get-tuple-element.35), channel_id=1, source_target_pairs={{0,64},{32,96},{64,0},{96,32},{1,65},{33,97},{65,1},{97,33},{2,66}... | collective-permute-start | bytes 368648 | tf_op jit(solution)/shard_map/ppermute | solution.py:272
  92.3 5.1 %collective-permute-start.18 = (bf16[480,128]{1,0:T(8,128)(2,1)}, bf16[480,128]{1,0:T(8,128)(2,1)S(1)}, u32[]{:S(2)}, u32[]{:S(2)}) collective-permute-start(bf16[480,128]{1,0:T(8,128)(2,1)} %get-tuple-element.36), channel_id=1, source_target_pairs={{0,96},{32,0},{64,32},{96,64},{1,97},{33,1},{65,33},{97,65},{2,98}... | collective-permute-start | bytes 368648 | tf_op jit(solution)/shard_map/ppermute | solution.py:272
  144.4 17.3 %all-to-all-start = ((bf16[16,160,128]{2,1,0:T(8,128)(2,1)}), bf16[16,160,128]{2,1,0:T(8,128)(2,1)S(1)}, u32[]{:S(2)}, u32[]{:S(2)}) async-start(bf16[16,160,128]{2,1,0:T(8,128)(2,1)} %attention.1), calls=%async_computation | async-start | bytes 1310720 | tf_op jit(solution)/shard_map/all_to_all | solution.py:320
  150.8 2.0 %collective-permute-start.25 = (bf16[1024,256]{1,0:T(8,128)(2,1)S(1)}, bf16[1024,256]{1,0:T(8,128)(2,1)S(1)}, u32[]{:S(2)}, u32[]{:S(2)}) collective-permute-start(bf16[1024,256]{1,0:T(8,128)(2,1)S(1)} %join.1.refs_0_), channel_id=1, source_target_pairs={{0,1},{1,0},{2,3},{3,2},{4,5},{5,4},{6,7},{7,6},{8,9},{9,8},{10,11... | collective-permute-start | bytes 1572872 | tf_op jit(solution)/shard_map/ppermute | solution.py:272
  150.9 2.6 %collective-permute-start.26 = (bf16[1024,256]{1,0:T(8,128)(2,1)}, bf16[1024,256]{1,0:T(8,128)(2,1)S(1)}, u32[]{:S(2)}, u32[]{:S(2)}) collective-permute-start(bf16[1024,256]{1,0:T(8,128)(2,1)} %collective-permute-done.22.refs_1_), channel_id=1, source_target_pairs={{0,1},{1,0},{2,3},{3,2},{4,5},{5,4},{6,7},{7,6},{8,9},{9,8},{10,11... | collective-permute-start | bytes 1572872 | tf_op jit(solution)/shard_map/ppermute | solution.py:272
  151.4 2.9 %collective-permute-start.27 = (bf16[1024,256]{1,0:T(8,128)(2,1)}, bf16[1024,256]{1,0:T(8,128)(2,1)S(1)}, u32[]{:S(2)}, u32[]{:S(2)}) collective-permute-start(bf16[1024,256]{1,0:T(8,128)(2,1)} %collective-permute-done.23.refs_2_), channel_id=1, source_target_pairs={{0,1},{1,0},{2,3},{3,2},{4,5},{5,4},{6,7},{7,6},{8,9},{9,8},{10,11... | collective-permute-start | bytes 1572872 | tf_op jit(solution)/shard_map/ppermute | solution.py:272
  151.5 3.7 %collective-permute-start.28 = (bf16[1024,256]{1,0:T(8,128)(2,1)}, bf16[1024,256]{1,0:T(8,128)(2,1)}, u32[]{:S(2)}, u32[]{:S(2)}) collective-permute-start(bf16[1024,256]{1,0:T(8,128)(2,1)} %collective-permute-done.24.refs_3_), channel_id=1, source_target_pairs={{0,1},{1,0},{2,3},{3,2},{4,5},{5,4},{6,7},{7,6},{8,9},{9,8},{10,11... | collective-permute-start | bytes 1572872 | tf_op jit(solution)/shard_map/ppermute | solution.py:272
  (18 other events, 57.6 us)

commit v8 on v5

--- a/solution.py
+++ b/solution.py
@@ -80,12 +80,14 @@
             q0=qi*BQ
             prepare(qi)
             qb=qa[q0:q0+BQ,:]
+
             def tile(k0,w,mask):
                 s=lax.dot_general(ka[k0:k0+w,:],qb,NT,preferred_element_type=f32)
                 p=jnp.exp2(s)
                 if mask:
                     p=jnp.where(keep,p,0.0)
                 return lax.dot_general(vt[:,k0:k0+w],p.astype(bf16),NN,preferred_element_type=f32)
+
             acc=tile(q0,BQ,True)
             for k0 in range(0,q0,W):
                 acc=acc+tile(k0,min(W,q0-k0),False)
@@ -96,9 +98,11 @@
         for i in range(T//BQ):
             prepare(i)
         kio=lax.broadcasted_iota(jnp.int32,(BQ,BQ),0); qio=lax.broadcasted_iota(jnp.int32,(BQ,BQ),1)
+
         def per_q(qi,_):
             q0=pl.multiple_of(qi*BQ,BQ)
             qb=qa[pl.ds(q0,BQ),:]
+
             def body(j,c):
                 m,acc=c
                 k0=pl.multiple_of(j*BQ,BQ)
@@ -108,16 +112,19 @@
                 p=jnp.exp2(s-m2).astype(bf16)
                 acc=acc*jnp.exp2(m-m2)+lax.dot_general(vt[:,pl.ds(k0,BQ)],p,NN,preferred_element_type=f32)
                 return m2,acc
+
             m0=jnp.full((1,BQ),-jnp.inf,f32)
             c=body(qi,(m0,jnp.zeros((80,BQ),f32)))
             _,acc=lax.fori_loop(0,qi,body,c)
             ot[:,pl.ds(q0,BQ)]=finish(acc)
             return 0
+
         lax.fori_loop(0,T//BQ,per_q,0)
         for i in range(T//BQ):
             emit(i)
+
     g=jnp.abs(gain_ref[...])
-    isfast=jnp.max(g[0:1])*jnp.max(g[1:2])<=7.7
+    isfast=jnp.max(g[:,0:64])*jnp.max(g[:,64:128])<=7.7/8
     pl.when(isfast)(fast)
     pl.when(jnp.logical_not(isfast))(slow)
 
@@ -187,10 +194,6 @@
         out[h][at + 320 : at + 480, :] = jnp.where(half, top, bot).astype(bf16)
 
 
-def gain_row(gain_ref):
-    return jnp.concatenate([gain_ref[0:1, :] * 0.125, gain_ref[1:2, :]], 1)
-
-
 def proj_kernel(idx_ref, gain_ref, *refs, sizes):
     n = sum(sizes)
     toks, ws, outs, w = refs[:n], refs[n : n + 8], refs[n + 8 : n + 12], refs[-1]
@@ -199,7 +202,7 @@
         for h in range(4):
             w[h * 128 : h * 128 + 128, cols] = ws[j][h * 192 : h * 192 + 128, :]
             w[512 + h * 64 : 576 + h * 64, cols] = ws[j][h * 192 + 128 : h * 192 + 192, :]
-    gains = gain_row(gain_ref)
+    gains = gain_ref[...]
     at = 0
     for b, size in enumerate(sizes):
         parts = [t[...] for t in toks[at : at + size]]
@@ -223,33 +226,41 @@
 
 def out_kernel(head_ref, col_ref, heads_ref, *refs):
     ws, o_ref, lhs = refs[:8], refs[8], refs[9]
-    half = lax.broadcasted_iota(jnp.int32, (BLK // 2, 128), 1) < 64
-    for p in range(8):
-        a = heads_ref[head_ref[2 * p]].astype(f32)
-        b = heads_ref[head_ref[2 * p + 1]].astype(f32)
-        s = slice(p * 128, p * 128 + 128)
-        lhs[0:160, s] = jnp.where(half, a, pltpu.roll(b, 64, 1)).astype(bf16)
-        lhs[160:320, s] = jnp.where(half, pltpu.roll(a, 64, 1), b).astype(bf16)
+    i = pl.program_id(0)
+
+    @pl.when(i == 0)
+    def _():
+        half = lax.broadcasted_iota(jnp.int32, (BLK // 2, 128), 1) < 64
+        for p in range(8):
+            a = heads_ref[head_ref[2 * p]].astype(f32)
+            b = heads_ref[head_ref[2 * p + 1]].astype(f32)
+            s = slice(p * 128, p * 128 + 128)
+            lhs[0:160, s] = jnp.where(half, a, pltpu.roll(b, 64, 1)).astype(bf16)
+            lhs[160:320, s] = jnp.where(half, pltpu.roll(a, 64, 1), b).astype(bf16)
+
     for par in range(2):
-        for dx in range(4):
-            acc = None
-            for dy in range(4):
-                rhs = ws[par * 4 + dy][dx * 256 : dx * 256 + 256, :]
-                part = lax.dot_general(
-                    lhs[:, dy * 256 : dy * 256 + 256], rhs, NN, preferred_element_type=f32
-                )
-                acc = part if acc is None else acc + part
-            cols = pl.ds(pl.multiple_of(col_ref[par * 4 + dx] * 256, 256), 256)
-            o_ref[:, cols] = acc.astype(bf16)
+        acc = None
+        for dy in range(4):
+            part = lax.dot_general(
+                lhs[:, dy * 256 : dy * 256 + 256], ws[par * 4 + dy][...], NN, preferred_element_type=f32
+            )
+            acc = part if acc is None else acc + part
+        side = col_ref[par * 4 + i] % 2
+        o_ref[:, pl.ds(pl.multiple_of(side * 256, 256), 256)] = acc.astype(bf16)
 
 
 def output(order, cols, heads, ws):
     return pl.pallas_call(
         out_kernel,
         out_shape=jax.ShapeDtypeStruct((BLK, 2048), bf16),
-        in_specs=[SMEM, SMEM] + [VMEM] * 9,
-        out_specs=VMEM,
-        scratch_shapes=[pltpu.VMEM((BLK, 1024), bf16)],
+        grid_spec=pltpu.PrefetchScalarGridSpec(
+            num_scalar_prefetch=2,
+            grid=(4,),
+            in_specs=[pl.BlockSpec((16, 160, 128), lambda i, order, cols: (0, 0, 0))]
+            + [pl.BlockSpec((256, 256), lambda i, order, cols: (i, 0))] * 8,
+            out_specs=pl.BlockSpec((BLK, 512), lambda i, order, cols: (0, cols[i] // 2)),
+            scratch_shapes=[pltpu.VMEM((BLK, 1024), bf16)],
+        ),
         compiler_params=pltpu.CompilerParams(vmem_limit_bytes=12 * 1024 * 1024),
         name="output",
     )(order, cols, heads, *ws)
@@ -264,9 +275,9 @@
     return lax.ppermute(value, axis, pairs)
 
 
-def spread(value, step):
+def spread(value, axis, step):
     pairs = [(2 * i + k, 2 * ((i + (step, -step)[k]) % 4) + k) for i in range(4) for k in (0, 1)]
-    return lax.ppermute(value, (Y, C), pairs)
+    return lax.ppermute(value, (axis, C), pairs)
 
 
 def around(value, axis):
@@ -276,21 +287,25 @@
 def on_device(tokens, w_query, w_key, w_value, w_output, qk_gain, decay_sums):
     own = tokens[0]
     z, y, x, c = (lax.axis_index(a) for a in (Z, Y, X, C))
-    t1 = spread(own, -1)
-    t3 = spread(own, 1)
-    t2 = spread(t1, -1)
-    near = jnp.where(c == 0, 1, 3)
+    t1 = spread(own, Y, -1)
+    t3 = spread(own, Y, 1)
+    t2 = spread(t1, Y, -1)
     piece = jnp.concatenate([w_query.T, w_key.T, w_value.T, w_output], 0)
     w4, wo4 = pack(around(piece, Z))
-    ws = around(w4, X)
+    w1 = spread(w4, X, -1)
+    ws = [w4, w1, spread(w4, X, 1), spread(w1, X, -1)]
     ws = ws + [move(w, C, 0) for w in ws]
 
-    cols = jnp.stack(
+    near = jnp.where(c == 0, 1, 3)
+    turns = [(c, (0, near, 4 - near, 2)), (1 - c, (0, 4 - near, near, 2))]
+    cols = jnp.stack([2 * ((x + d) % 4) + e for e, ds in turns for d in ds]).astype(jnp.int32)
+    out_cols = jnp.stack(
         [2 * ((x + d) % 4) + e for e in (c, 1 - c) for d in range(4)]
     ).astype(jnp.int32)
-    part1 = project(cols, qk_gain, [[own], [t1], [t3]], ws)
+    gains = jnp.concatenate([qk_gain[0] * 0.125, qk_gain[1]])[None]
+    part1 = project(cols, gains, [[own], [t1], [t3]], ws)
     *part1, wo4 = lax.optimization_barrier((*part1, wo4))
-    part2 = project(cols, qk_gain, [[t2]], ws)
+    part2 = project(cols, gains, [[t2]], ws)
     recv = []
     for part in (part1, part2):
         recv += [part[0]] + [move(part[d], Z, d) for d in (1, 2, 3)]
@@ -299,14 +314,14 @@
     pos = [4 * ((z - d) % 4) + (y + e) % 4 for d in range(4) for e in (0, near, 4 - near)]
     pos += [4 * ((z - d) % 4) + (y + 2) % 4 for d in range(4)]
     pos = jnp.stack(pos).astype(jnp.int32)
-    heads = attention(pos, qk_gain, decay_sums[0], recv, (3, 3, 3, 3, 1, 1, 1, 1))
+    heads = attention(pos, gains, decay_sums[0], recv, (3, 3, 3, 3, 1, 1, 1, 1))
     heads, *wo = lax.optimization_barrier((heads, *wo))
     wo = wo + [move(w, C, 0) for w in wo]
     merged = lax.all_to_all(heads, SP, 0, 0, tiled=True)
     order = jnp.stack(
         [4 * ((z + d) % 4) + (y + e) % 4 for e in range(4) for d in range(4)]
     ).astype(jnp.int32)
-    return output(order, cols, merged, wo)[None]
+    return output(order, out_cols, merged, wo)[None]
 
 
 def solution(mesh):

time: 164 us -> 166 us (1.012); the launches traced: 163 us -> 164 us
  starting transfers between devices: 50.6 us -> 47.1 us
  waiting for transfers between devices: 44.8 us -> 46.8 us
  Pallas kernels: 56 us -> 57.7 us
    ppermute x26 -> x23, starting transfers between devices: 38.3 us -> 27 us  [move(): return lax.ppermute(value, axis, pairs)]
    ppermute x3 -> x6, waiting for transfers between devices: 9.88 us -> 18.8 us  [spread(): return lax.ppermute(value, (axis, C), pairs)]
    ppermute x26 -> x23, waiting for transfers between devices: 28.4 us -> 21.4 us  [move(): return lax.ppermute(value, axis, pairs)]
    ppermute x3 -> x6, starting transfers between devices: 6.82 us -> 12.9 us  [spread(): return lax.ppermute(value, (axis, C), pairs)]
    all_to_all x1, starting transfers between devices: 5.49 us -> 7.28 us  [on_device(): merged = lax.all_to_all(heads, SP, 0, 0, tiled=True)]
    unnamed x32 -> x28, local copies, waits for them, and re-layouts: 10.7 us -> 9.86 us
  transfers between devices with their start and end apart: 30 -> 30, of which waited for: 18 -> 16; matrix products, arithmetic and copies ran while one was open for 1% -> 1% of each run, Pallas kernels for 32% -> 32%
where the time goes in v8:
time: 166 us; the launch traced here: 164 us
  Pallas kernels  57.7 us (35%)
  starting transfers between devices  47.1 us (28%)
  waiting for transfers between devices  46.8 us (28%)
  local copies, waits for them, and re-layouts  10.2 us (6%)
    pallas_call x1, Pallas kernels, attention(): pl.pallas_call(functools.partial(attn_kernel, nblk=nblk), out_shape=jax.S...  41.3 us
    ppermute x23, starting transfers between devices, move(): return lax.ppermute(value, axis, pairs)  27 us
    ppermute x23, waiting for transfers between devices, move(): return lax.ppermute(value, axis, pairs)  21.4 us
    ppermute x6, waiting for transfers between devices, spread(): return lax.ppermute(value, (axis, C), pairs)  18.8 us
    ppermute x6, starting transfers between devices, spread(): return lax.ppermute(value, (axis, C), pairs)  12.9 us
    pallas_call x2, Pallas kernels, project(): pl.pallas_call(functools.partial(proj_kernel, sizes=tuple((len(b) for b i...  10.9 us
    unnamed x28, local copies, waits for them, and re-layouts  9.86 us
    all_to_all x1, starting transfers between devices, on_device(): merged = lax.all_to_all(heads, SP, 0, 0, tiled=True)  7.28 us
  transfers between devices with their start and end apart: 30, of which 16 were waited for; matrix products, arithmetic and copies ran while one was open for 1% of the time, Pallas kernels for 32%

profile of v8, /device:TPU:0, one launch (start us, length us, event | category | flops | bytes accessed | tf_op | source)
XLA Modules:
  0.0 163.6 jit_solution(13045547481262530305)
XLA Ops:
  0.0 3.1 %collective-permute-start = (bf16[320,2048]{1,0:T(8,128)(2,1)}, bf16[320,2048]{1,0:T(8,128)(2,1)}, u32[]{:S(2)}, u32[]{:S(2)}) collective-permute-start(bf16[320,2048]{1,0:T(8,128)(2,1)} %bitcast.54), channel_id=1, source_target_pairs={{0,24},{1,9},{8,0},{9,17},{16,8},{17,25},{24,16},{25,1},{2,26},{3,... | collective-permute-start | bytes 3932168 | tf_op jit(solution)/shard_map/ppermute | solution.py:280
  3.9 4.1 %collective-permute-start.2 = (bf16[256,256]{1,0:T(8,128)(2,1)S(1)}, bf16[256,256]{1,0:T(8,128)(2,1)S(1)}, u32[]{:S(2)}, u32[]{:S(2)}) collective-permute-start(bf16[256,256]{1,0:T(8,128)(2,1)S(1)} %pad_maximum_fusion.refs_0_), channel_id=1, source_target_pairs={{0,96},{32,0},{64,32},{96,64},{1,97},{33,1},{65,33},{97,65},{2,98}... | collective-permute-start | bytes 393224 | tf_op jit(solution)/shard_map/ppermute | solution.py:275
  8.1 1.3 collective-permute-start.4
  9.3 2.8 %collective-permute-done.2.refs_1_ = bf16[256,256]{1,0:T(8,128)(2,1)S(1)} collective-permute-done((bf16[256,256]{1,0:T(8,128)(2,1)S(1)}, bf16[256,256]{1,0:T(8,128)(2,1)S(1)}, u32[]{:S(2)}, u32[]{:S(2)}) %collective-permute-start.2) | collective-permute-done | bytes 131104 | tf_op jit(solution)/shard_map/ppermute | solution.py:275
  12.2 2.5 %collective-permute-done.3.refs_2_ = bf16[256,256]{1,0:T(8,128)(2,1)S(1)} collective-permute-done((bf16[256,256]{1,0:T(8,128)(2,1)S(1)}, bf16[256,256]{1,0:T(8,128)(2,1)S(1)}, u32[]{:S(2)}, u32[]{:S(2)}) %collective-permute-start.3) | collective-permute-done | bytes 131104 | tf_op jit(solution)/shard_map/ppermute | solution.py:275
  14.6 1.0 collective-permute-done.4.refs_3_
  15.7 2.8 %collective-permute-start.5 = (bf16[768,256]{1,0:T(8,128)(2,1)S(1)}, bf16[768,256]{1,0:T(8,128)(2,1)S(1)}, u32[]{:S(2)}, u32[]{:S(2)}) collective-permute-start(bf16[768,256]{1,0:T(8,128)(2,1)S(1)} %get-tuple-element.25.refs_3_.refs_1_), channel_id=1, source_target_pairs={{0,6},{1,3},{2,0},{3,5},{4,2},{5,7},{6,4},{7,1},{8,14},{9,11},{10,... | collective-permute-start | bytes 1179656 | tf_op jit(solution)/shard_map/ppermute | solution.py:280
  18.5 9.9 %collective-permute-done.refs_1_ = bf16[320,2048]{1,0:T(8,128)(2,1)} collective-permute-done((bf16[320,2048]{1,0:T(8,128)(2,1)}, bf16[320,2048]{1,0:T(8,128)(2,1)}, u32[]{:S(2)}, u32[]{:S(2)}) %collective-permute-start) | collective-permute-done | bytes 1310752 | tf_op jit(solution)/shard_map/ppermute | solution.py:280
  28.4 3.7 %collective-permute-start.15 = (bf16[320,2048]{1,0:T(8,128)(2,1)}, bf16[320,2048]{1,0:T(8,128)(2,1)}, u32[]{:S(2)}, u32[]{:S(2)}) collective-permute-start(bf16[320,2048]{1,0:T(8,128)(2,1)} %collective-permute-done.refs_1_), channel_id=1, source_target_pairs={{0,24},{1,9},{8,0},{9,17},{16,8},{17,25},{24,16},{25,1},{2,26},{3,... | collective-permute-start | bytes 3932168 | tf_op jit(solution)/shard_map/ppermute | solution.py:280
  32.1 1.5 collective-permute-start.6
  33.6 1.7 %collective-permute-start.7 = (bf16[768,256]{1,0:T(8,128)(2,1)S(1)}, bf16[768,256]{1,0:T(8,128)(2,1)S(1)}, u32[]{:S(2)}, u32[]{:S(2)}) collective-permute-start(bf16[768,256]{1,0:T(8,128)(2,1)S(1)} %collective-permute-done.5.refs_4_.refs_2_), channel_id=1, source_target_pairs={{0,6},{1,3},{2,0},{3,5},{4,2},{5,7},{6,4},{7,1},{8,14},{9,11},{10,... | collective-permute-start | bytes 1179656 | tf_op jit(solution)/shard_map/ppermute | solution.py:280
  35.3 8.9 %collective-permute-done.6.refs_5_.refs_3_ = bf16[768,256]{1,0:T(8,128)(2,1)S(1)} collective-permute-done((bf16[768,256]{1,0:T(8,128)(2,1)S(1)}, bf16[768,256]{1,0:T(8,128)(2,1)S(1)}, u32[]{:S(2)}, u32[]{:S(2)}) %collective-permute-start.6) | collective-permute-done | bytes 393248 | tf_op jit(solution)/shard_map/ppermute | solution.py:280
  47.1 1.3 copy-done.2
  48.4 6.4 %project.2 = (bf16[1440,128]{1,0:T(8,128)(2,1)S(1)}, bf16[1440,128]{1,0:T(8,128)(2,1)S(1)}, bf16[1440,128]{1,0:T(8,128)(2,1)S(1)}, bf16[1440,128]{1,0:T(8,128)(2,1)S(1)}) custom-call(s32[8]{0:T(128)S(1)} %stack.189.idx_ref, f32[1,128]{1,0:T(1,128)S(1)} %maximum_bitcast_fusion.gain_ref, bf16[320,2048]{1,0:T(8,128)(2,1)S(1)} %bitcast.56, ...), custom_call_target="tpu_custom_call" | custom-call | tf_op jit(solution)/shard_map/project/pallas_call | solution.py:216
  55.6 1.6 collective-permute-start.12
  57.2 2.6 %collective-permute-start.19 = (bf16[256,256]{1,0:T(8,128)(2,1)S(1)}, bf16[256,256]{1,0:T(8,128)(2,1)S(1)}, u32[]{:S(2)}, u32[]{:S(2)}) collective-permute-start(bf16[256,256]{1,0:T(8,128)(2,1)S(1)} %get-tuple-element.39.refs_0_), channel_id=1, source_target_pairs={{0,6},{2,0},{4,2},{6,4},{1,7},{3,1},{5,3},{7,5},{8,14},{10,8},{12,... | collective-permute-start | bytes 393224 | tf_op jit(solution)/shard_map/ppermute | solution.py:275
  60.7 4.7 %collective-permute-done.19.refs_1_ = bf16[256,256]{1,0:T(8,128)(2,1)S(1)} collective-permute-done((bf16[256,256]{1,0:T(8,128)(2,1)S(1)}, bf16[256,256]{1,0:T(8,128)(2,1)S(1)}, u32[]{:S(2)}, u32[]{:S(2)}) %collective-permute-start.19) | collective-permute-done | bytes 131104 | tf_op jit(solution)/shard_map/ppermute | solution.py:275
  65.4 5.7 %collective-permute-start.13 = (bf16[1440,128]{1,0:T(8,128)(2,1)S(1)}, bf16[1440,128]{1,0:T(8,128)(2,1)S(1)}, u32[]{:S(2)}, u32[]{:S(2)}) collective-permute-start(bf16[1440,128]{1,0:T(8,128)(2,1)S(1)} %get-tuple-element.33), channel_id=1, source_target_pairs={{0,64},{32,96},{64,0},{96,32},{1,65},{33,97},{65,1},{97,33},{2,66}... | collective-permute-start | bytes 1105928 | tf_op jit(solution)/shard_map/ppermute | solution.py:275
  73.2 1.6 collective-permute-start.24
  74.9 2.2 %collective-permute-start.14 = (bf16[1440,128]{1,0:T(8,128)(2,1)S(1)}, bf16[1440,128]{1,0:T(8,128)(2,1)S(1)}, u32[]{:S(2)}, u32[]{:S(2)}) collective-permute-start(bf16[1440,128]{1,0:T(8,128)(2,1)S(1)} %get-tuple-element.34), channel_id=1, source_target_pairs={{0,96},{32,0},{64,32},{96,64},{1,97},{33,1},{65,33},{97,65},{2,98}... | collective-permute-start | bytes 1105928 | tf_op jit(solution)/shard_map/ppermute | solution.py:275
  77.1 4.4 %project.3 = (bf16[480,128]{1,0:T(8,128)(2,1)S(1)}, bf16[480,128]{1,0:T(8,128)(2,1)S(1)}, bf16[480,128]{1,0:T(8,128)(2,1)}, bf16[480,128]{1,0:T(8,128)(2,1)}) custom-call(s32[8]{0:T(128)S(1)} %stack.189.idx_ref, f32[1,128]{1,0:T(1,128)S(1)} %maximum_bitcast_fusion.gain_ref, bf16[320,2048]{1,0:T(8,128)(2,1)} %collective-permute-done.15.refs_0_, ...), custom_call_target="tpu_custom_call" | custom-call | tf_op jit(solution)/shard_map/project/pallas_call | solution.py:216
  82.3 2.0 %collective-permute-done.14.refs_3_ = bf16[1440,128]{1,0:T(8,128)(2,1)S(1)} collective-permute-done((bf16[1440,128]{1,0:T(8,128)(2,1)S(1)}, bf16[1440,128]{1,0:T(8,128)(2,1)S(1)}, u32[]{:S(2)}, u32[]{:S(2)}) %collective-permute-start.14) | collective-permute-done | bytes 368672 | tf_op jit(solution)/shard_map/ppermute | solution.py:275
  85.0 3.7 %collective-permute-start.17 = (bf16[480,128]{1,0:T(8,128)(2,1)}, bf16[480,128]{1,0:T(8,128)(2,1)S(1)}, u32[]{:S(2)}, u32[]{:S(2)}) collective-permute-start(bf16[480,128]{1,0:T(8,128)(2,1)} %get-tuple-element.37), channel_id=1, source_target_pairs={{0,64},{32,96},{64,0},{96,32},{1,65},{33,97},{65,1},{97,33},{2,66}... | collective-permute-start | bytes 368648 | tf_op jit(solution)/shard_map/ppermute | solution.py:275
  89.6 2.1 %collective-permute-done.17.refs_6_ = bf16[480,128]{1,0:T(8,128)(2,1)S(1)} collective-permute-done((bf16[480,128]{1,0:T(8,128)(2,1)}, bf16[480,128]{1,0:T(8,128)(2,1)S(1)}, u32[]{:S(2)}, u32[]{:S(2)}) %collective-permute-start.17) | collective-permute-done | bytes 122912 | tf_op jit(solution)/shard_map/ppermute | solution.py:275
  91.7 2.3 %collective-permute-done.18.refs_7_ = bf16[480,128]{1,0:T(8,128)(2,1)S(1)} collective-permute-done((bf16[480,128]{1,0:T(8,128)(2,1)}, bf16[480,128]{1,0:T(8,128)(2,1)S(1)}, u32[]{:S(2)}, u32[]{:S(2)}) %collective-permute-start.18) | collective-permute-done | bytes 122912 | tf_op jit(solution)/shard_map/ppermute | solution.py:275
  94.0 1.0 copy-done.4
  95.0 1.0 copy-done.6
  96.0 1.0 copy-done.8
  98.7 41.3 %attention.1 = bf16[16,160,128]{2,1,0:T(8,128)(2,1)} custom-call(s32[16]{0:T(128)S(1)} %stack.184.pos_ref, f32[1,128]{1,0:T(1,128)S(1)} %maximum_bitcast_fusion.gain_ref, f32[1,5120]{1,0:T(1,128)S(1)} %bitcast.57, bf16[1440,128]{1,0:T(8,128)(2,1)S(1)} %copy-done.4, bf16[1440,128]{1,0:T(8,128)(2,1)S(1)} %copy-done.6, bf16[1440,128]{1,0:T(8,128)(2,1)S(1)} %copy-done.8, ...), custom_call_target="tpu_custom_call" | custom-call | tf_op jit(solution)/shard_map/attention/pallas_call | solution.py:134
  140.0 7.3 %all-to-all-start = ((bf16[16,160,128]{2,1,0:T(8,128)(2,1)}), bf16[16,160,128]{2,1,0:T(8,128)(2,1)S(1)}, u32[]{:S(2)}, u32[]{:S(2)}) async-start(bf16[16,160,128]{2,1,0:T(8,128)(2,1)} %attention.1), calls=%async_computation | async-start | bytes 1310720 | tf_op jit(solution)/shard_map/all_to_all | solution.py:320
  151.6 6.6 %all-to-all-done.heads_ref = bf16[16,160,128]{2,1,0:T(8,128)(2,1)S(1)} async-done(((bf16[16,160,128]{2,1,0:T(8,128)(2,1)}), bf16[16,160,128]{2,1,0:T(8,128)(2,1)S(1)}, u32[]{:S(2)}, u32[]{:S(2)}) %all-to-all-start) | async-done | bytes 655392 | tf_op jit(solution)/shard_map/all_to_all | solution.py:320
  158.2 5.4 %output.1 = bf16[320,2048]{1,0:T(8,128)(2,1)} custom-call(s32[16]{0:T(128)S(1)} %stack.160.head_ref, s32[8]{0:T(128)S(1)} %stack.169.col_ref, bf16[16,160,128]{2,1,0:T(8,128)(2,1)S(1)} %all-to-all-done.heads_ref, bf16[1024,256]{1,0:T(8,128)(2,1)S(1)} %join.1.refs_0_, bf16[1024,256]{1,0:T(8,128)(2,1)} %collective-permute-done.22.refs_1_, ...), custom_call_target="tpu_custom_call" | custom-call | tf_op jit(solution)/shard_map/output/pallas_call | solution.py:253
  (69 shorter events, 16.0 us)
Async XLA Ops:
  0.0 28.4 %collective-permute-start = (bf16[320,2048]{1,0:T(8,128)(2,1)}, bf16[320,2048]{1,0:T(8,128)(2,1)}, u32[]{:S(2)}, u32[]{:S(2)}) collective-permute-start(bf16[320,2048]{1,0:T(8,128)(2,1)} %bitcast.54), channel_id=1, source_target_pairs={{0,24},{1,9},{8,0},{9,17},{16,8},{17,25},{24,16},{25,1},{2,26},{3,... | collective-permute-start | bytes 3932168 | tf_op jit(solution)/shard_map/ppermute | solution.py:280
  3.9 8.2 %collective-permute-start.2 = (bf16[256,256]{1,0:T(8,128)(2,1)S(1)}, bf16[256,256]{1,0:T(8,128)(2,1)S(1)}, u32[]{:S(2)}, u32[]{:S(2)}) collective-permute-start(bf16[256,256]{1,0:T(8,128)(2,1)S(1)} %pad_maximum_fusion.refs_0_), channel_id=1, source_target_pairs={{0,96},{32,0},{64,32},{96,64},{1,97},{33,1},{65,33},{97,65},{2,98}... | collective-permute-start | bytes 393224 | tf_op jit(solution)/shard_map/ppermute | solution.py:275
  8.1 6.6 %collective-permute-start.3 = (bf16[256,256]{1,0:T(8,128)(2,1)S(1)}, bf16[256,256]{1,0:T(8,128)(2,1)S(1)}, u32[]{:S(2)}, u32[]{:S(2)}) collective-permute-start(bf16[256,256]{1,0:T(8,128)(2,1)S(1)} %pad_maximum_fusion.refs_0_), channel_id=1, source_target_pairs={{0,64},{32,96},{64,0},{96,32},{1,65},{33,97},{65,1},{97,33},{2,66}... | collective-permute-start | bytes 393224 | tf_op jit(solution)/shard_map/ppermute | solution.py:275
  8.1 7.6 %collective-permute-start.4 = (bf16[256,256]{1,0:T(8,128)(2,1)S(1)}, bf16[256,256]{1,0:T(8,128)(2,1)S(1)}, u32[]{:S(2)}, u32[]{:S(2)}) collective-permute-start(bf16[256,256]{1,0:T(8,128)(2,1)S(1)} %pad_maximum_fusion.refs_0_), channel_id=1, source_target_pairs={{0,32},{32,64},{64,96},{96,0},{1,33},{33,65},{65,97},{97,1},{2,34}... | collective-permute-start | bytes 393224 | tf_op jit(solution)/shard_map/ppermute | solution.py:275
  9.3 37.2 %collective-permute-start.1 = (bf16[320,2048]{1,0:T(8,128)(2,1)}, bf16[320,2048]{1,0:T(8,128)(2,1)}, u32[]{:S(2)}, u32[]{:S(2)}) collective-permute-start(bf16[320,2048]{1,0:T(8,128)(2,1)} %bitcast.55), channel_id=1, source_target_pairs={{0,8},{1,25},{8,16},{9,1},{16,24},{17,9},{24,0},{25,17},{2,10},{3,... | collective-permute-start | bytes 3932168 | tf_op jit(solution)/shard_map/ppermute | solution.py:280
  15.7 44.1 %copy-start.11 = (bf16[256,256]{1,0:T(8,128)(2,1)}, bf16[256,256]{1,0:T(8,128)(2,1)S(1)}, u32[]{:S(2)}) copy-start(bf16[256,256]{1,0:T(8,128)(2,1)S(1)} %get-tuple-element.39.refs_0_) | copy-start | bytes 393220
  15.7 17.9 %collective-permute-start.5 = (bf16[768,256]{1,0:T(8,128)(2,1)S(1)}, bf16[768,256]{1,0:T(8,128)(2,1)S(1)}, u32[]{:S(2)}, u32[]{:S(2)}) collective-permute-start(bf16[768,256]{1,0:T(8,128)(2,1)S(1)} %get-tuple-element.25.refs_3_.refs_1_), channel_id=1, source_target_pairs={{0,6},{1,3},{2,0},{3,5},{4,2},{5,7},{6,4},{7,1},{8,14},{9,11},{10,... | collective-permute-start | bytes 1179656 | tf_op jit(solution)/shard_map/ppermute | solution.py:280
  28.4 46.5 %collective-permute-start.15 = (bf16[320,2048]{1,0:T(8,128)(2,1)}, bf16[320,2048]{1,0:T(8,128)(2,1)}, u32[]{:S(2)}, u32[]{:S(2)}) collective-permute-start(bf16[320,2048]{1,0:T(8,128)(2,1)} %collective-permute-done.refs_1_), channel_id=1, source_target_pairs={{0,24},{1,9},{8,0},{9,17},{16,8},{17,25},{24,16},{25,1},{2,26},{3,... | collective-permute-start | bytes 3932168 | tf_op jit(solution)/shard_map/ppermute | solution.py:280
  32.1 12.2 %collective-permute-start.6 = (bf16[768,256]{1,0:T(8,128)(2,1)S(1)}, bf16[768,256]{1,0:T(8,128)(2,1)S(1)}, u32[]{:S(2)}, u32[]{:S(2)}) collective-permute-start(bf16[768,256]{1,0:T(8,128)(2,1)S(1)} %get-tuple-element.25.refs_3_.refs_1_), channel_id=1, source_target_pairs={{0,2},{1,7},{2,4},{3,1},{4,6},{5,3},{6,0},{7,5},{8,10},{9,15},{10,... | collective-permute-start | bytes 1179656 | tf_op jit(solution)/shard_map/ppermute | solution.py:280
  33.6 10.7 %collective-permute-start.8 = (bf16[768,256]{1,0:T(8,128)(2,1)S(1)}, bf16[768,256]{1,0:T(8,128)(2,1)S(1)}, u32[]{:S(2)}, u32[]{:S(2)}) collective-permute-start(bf16[768,256]{1,0:T(8,128)(2,1)S(1)} %get-tuple-element.25.refs_3_.refs_1_), channel_id=1, source_target_pairs={{0,1},{1,0},{2,3},{3,2},{4,5},{5,4},{6,7},{7,6},{8,9},{9,8},{10,11... | collective-permute-start | bytes 1179656 | tf_op jit(solution)/shard_map/ppermute | solution.py:275
  33.6 11.2 %collective-permute-start.7 = (bf16[768,256]{1,0:T(8,128)(2,1)S(1)}, bf16[768,256]{1,0:T(8,128)(2,1)S(1)}, u32[]{:S(2)}, u32[]{:S(2)}) collective-permute-start(bf16[768,256]{1,0:T(8,128)(2,1)S(1)} %collective-permute-done.5.refs_4_.refs_2_), channel_id=1, source_target_pairs={{0,6},{1,3},{2,0},{3,5},{4,2},{5,7},{6,4},{7,1},{8,14},{9,11},{10,... | collective-permute-start | bytes 1179656 | tf_op jit(solution)/shard_map/ppermute | solution.py:280
  44.3 1.8 %collective-permute-start.9 = (bf16[768,256]{1,0:T(8,128)(2,1)S(1)}, bf16[768,256]{1,0:T(8,128)(2,1)S(1)}, u32[]{:S(2)}, u32[]{:S(2)}) collective-permute-start(bf16[768,256]{1,0:T(8,128)(2,1)S(1)} %collective-permute-done.5.refs_4_.refs_2_), channel_id=1, source_target_pairs={{0,1},{1,0},{2,3},{3,2},{4,5},{5,4},{6,7},{7,6},{8,9},{9,8},{10,11... | collective-permute-start | bytes 1179656 | tf_op jit(solution)/shard_map/ppermute | solution.py:275
  44.3 2.3 %collective-permute-start.10 = (bf16[768,256]{1,0:T(8,128)(2,1)S(1)}, bf16[768,256]{1,0:T(8,128)(2,1)S(1)}, u32[]{:S(2)}, u32[]{:S(2)}) collective-permute-start(bf16[768,256]{1,0:T(8,128)(2,1)S(1)} %collective-permute-done.6.refs_5_.refs_3_), channel_id=1, source_target_pairs={{0,1},{1,0},{2,3},{3,2},{4,5},{5,4},{6,7},{7,6},{8,9},{9,8},{10,11... | collective-permute-start | bytes 1179656 | tf_op jit(solution)/shard_map/ppermute | solution.py:275
  44.8 2.3 %collective-permute-start.11 = (bf16[768,256]{1,0:T(8,128)(2,1)S(1)}, bf16[768,256]{1,0:T(8,128)(2,1)S(1)}, u32[]{:S(2)}, u32[]{:S(2)}) collective-permute-start(bf16[768,256]{1,0:T(8,128)(2,1)S(1)} %collective-permute-done.7.refs_6_.refs_4_), channel_id=1, source_target_pairs={{0,1},{1,0},{2,3},{3,2},{4,5},{5,4},{6,7},{7,6},{8,9},{9,8},{10,11... | collective-permute-start | bytes 1179656 | tf_op jit(solution)/shard_map/ppermute | solution.py:275
  55.6 21.5 %copy-start.1 = (bf16[768,256]{1,0:T(8,128)(2,1)S(1)}, bf16[768,256]{1,0:T(8,128)(2,1)}, u32[]{:S(2)}) copy-start(bf16[768,256]{1,0:T(8,128)(2,1)} %copy-done) | copy-start | bytes 1179652
  55.6 16.9 %collective-permute-start.12 = (bf16[1440,128]{1,0:T(8,128)(2,1)S(1)}, bf16[1440,128]{1,0:T(8,128)(2,1)S(1)}, u32[]{:S(2)}, u32[]{:S(2)}) collective-permute-start(bf16[1440,128]{1,0:T(8,128)(2,1)S(1)} %get-tuple-element.32), channel_id=1, source_target_pairs={{0,32},{32,64},{64,96},{96,0},{1,33},{33,65},{65,97},{97,1},{2,34}... | collective-permute-start | bytes 1105928 | tf_op jit(solution)/shard_map/ppermute | solution.py:275
  57.2 8.2 %collective-permute-start.19 = (bf16[256,256]{1,0:T(8,128)(2,1)S(1)}, bf16[256,256]{1,0:T(8,128)(2,1)S(1)}, u32[]{:S(2)}, u32[]{:S(2)}) collective-permute-start(bf16[256,256]{1,0:T(8,128)(2,1)S(1)} %get-tuple-element.39.refs_0_), channel_id=1, source_target_pairs={{0,6},{2,0},{4,2},{6,4},{1,7},{3,1},{5,3},{7,5},{8,14},{10,8},{12,... | collective-permute-start | bytes 393224 | tf_op jit(solution)/shard_map/ppermute | solution.py:275
  59.8 11.3 %collective-permute-start.20 = (bf16[256,256]{1,0:T(8,128)(2,1)S(1)}, bf16[256,256]{1,0:T(8,128)(2,1)S(1)}, u32[]{:S(2)}, u32[]{:S(2)}) collective-permute-start(bf16[256,256]{1,0:T(8,128)(2,1)S(1)} %get-tuple-element.39.refs_0_), channel_id=1, source_target_pairs={{0,4},{2,6},{4,0},{6,2},{1,5},{3,7},{5,1},{7,3},{8,12},{10,14},{12... | collective-permute-start | bytes 393224 | tf_op jit(solution)/shard_map/ppermute | solution.py:275
  59.8 11.3 %collective-permute-start.21 = (bf16[256,256]{1,0:T(8,128)(2,1)S(1)}, bf16[256,256]{1,0:T(8,128)(2,1)S(1)}, u32[]{:S(2)}, u32[]{:S(2)}) collective-permute-start(bf16[256,256]{1,0:T(8,128)(2,1)S(1)} %get-tuple-element.39.refs_0_), channel_id=1, source_target_pairs={{0,2},{2,4},{4,6},{6,0},{1,3},{3,5},{5,7},{7,1},{8,10},{10,12},{12... | collective-permute-start | bytes 393224 | tf_op jit(solution)/shard_map/ppermute | solution.py:275
  65.4 16.1 %collective-permute-start.13 = (bf16[1440,128]{1,0:T(8,128)(2,1)S(1)}, bf16[1440,128]{1,0:T(8,128)(2,1)S(1)}, u32[]{:S(2)}, u32[]{:S(2)}) collective-permute-start(bf16[1440,128]{1,0:T(8,128)(2,1)S(1)} %get-tuple-element.33), channel_id=1, source_target_pairs={{0,64},{32,96},{64,0},{96,32},{1,65},{33,97},{65,1},{97,33},{2,66}... | collective-permute-start | bytes 1105928 | tf_op jit(solution)/shard_map/ppermute | solution.py:275
  72.0 68.0 %collective-permute-start.22 = (bf16[1024,256]{1,0:T(8,128)(2,1)S(1)}, bf16[1024,256]{1,0:T(8,128)(2,1)}, u32[]{:S(2)}, u32[]{:S(2)}) collective-permute-start(bf16[1024,256]{1,0:T(8,128)(2,1)S(1)} %join.1.refs_0_), channel_id=1, source_target_pairs={{0,24},{8,0},{16,8},{24,16},{1,25},{9,1},{17,9},{25,17},{2,26},{10... | collective-permute-start | bytes 1572872 | tf_op jit(solution)/shard_map/ppermute | solution.py:275
  72.1 67.9 %collective-permute-start.23 = (bf16[1024,256]{1,0:T(8,128)(2,1)S(1)}, bf16[1024,256]{1,0:T(8,128)(2,1)}, u32[]{:S(2)}, u32[]{:S(2)}) collective-permute-start(bf16[1024,256]{1,0:T(8,128)(2,1)S(1)} %join.1.refs_0_), channel_id=1, source_target_pairs={{0,16},{8,24},{16,0},{24,8},{1,17},{9,25},{17,1},{25,9},{2,18},{10... | collective-permute-start | bytes 1572872 | tf_op jit(solution)/shard_map/ppermute | solution.py:275
  73.2 66.8 %collective-permute-start.24 = (bf16[1024,256]{1,0:T(8,128)(2,1)S(1)}, bf16[1024,256]{1,0:T(8,128)(2,1)}, u32[]{:S(2)}, u32[]{:S(2)}) collective-permute-start(bf16[1024,256]{1,0:T(8,128)(2,1)S(1)} %join.1.refs_0_), channel_id=1, source_target_pairs={{0,8},{8,16},{16,24},{24,0},{1,9},{9,17},{17,25},{25,1},{2,10},{10... | collective-permute-start | bytes 1572872 | tf_op jit(solution)/shard_map/ppermute | solution.py:275
  74.9 9.4 %collective-permute-start.14 = (bf16[1440,128]{1,0:T(8,128)(2,1)S(1)}, bf16[1440,128]{1,0:T(8,128)(2,1)S(1)}, u32[]{:S(2)}, u32[]{:S(2)}) collective-permute-start(bf16[1440,128]{1,0:T(8,128)(2,1)S(1)} %get-tuple-element.34), channel_id=1, source_target_pairs={{0,96},{32,0},{64,32},{96,64},{1,97},{33,1},{65,33},{97,65},{2,98}... | collective-permute-start | bytes 1105928 | tf_op jit(solution)/shard_map/ppermute | solution.py:275
  82.3 6.4 %collective-permute-start.16 = (bf16[480,128]{1,0:T(8,128)(2,1)S(1)}, bf16[480,128]{1,0:T(8,128)(2,1)S(1)}, u32[]{:S(2)}, u32[]{:S(2)}) collective-permute-start(bf16[480,128]{1,0:T(8,128)(2,1)S(1)} %get-tuple-element.36), channel_id=1, source_target_pairs={{0,32},{32,64},{64,96},{96,0},{1,33},{33,65},{65,97},{97,1},{2,34}... | collective-permute-start | bytes 368648 | tf_op jit(solution)/shard_map/ppermute | solution.py:275
  85.0 6.7 %collective-permute-start.17 = (bf16[480,128]{1,0:T(8,128)(2,1)}, bf16[480,128]{1,0:T(8,128)(2,1)S(1)}, u32[]{:S(2)}, u32[]{:S(2)}) collective-permute-start(bf16[480,128]{1,0:T(8,128)(2,1)} %get-tuple-element.37), channel_id=1, source_target_pairs={{0,64},{32,96},{64,0},{96,32},{1,65},{33,97},{65,1},{97,33},{2,66}... | collective-permute-start | bytes 368648 | tf_op jit(solution)/shard_map/ppermute | solution.py:275
  88.7 5.3 %collective-permute-start.18 = (bf16[480,128]{1,0:T(8,128)(2,1)}, bf16[480,128]{1,0:T(8,128)(2,1)S(1)}, u32[]{:S(2)}, u32[]{:S(2)}) collective-permute-start(bf16[480,128]{1,0:T(8,128)(2,1)} %get-tuple-element.38), channel_id=1, source_target_pairs={{0,96},{32,0},{64,32},{96,64},{1,97},{33,1},{65,33},{97,65},{2,98}... | collective-permute-start | bytes 368648 | tf_op jit(solution)/shard_map/ppermute | solution.py:275
  140.0 18.1 %all-to-all-start = ((bf16[16,160,128]{2,1,0:T(8,128)(2,1)}), bf16[16,160,128]{2,1,0:T(8,128)(2,1)S(1)}, u32[]{:S(2)}, u32[]{:S(2)}) async-start(bf16[16,160,128]{2,1,0:T(8,128)(2,1)} %attention.1), calls=%async_computation | async-start | bytes 1310720 | tf_op jit(solution)/shard_map/all_to_all | solution.py:320
  147.3 2.0 %collective-permute-start.25 = (bf16[1024,256]{1,0:T(8,128)(2,1)S(1)}, bf16[1024,256]{1,0:T(8,128)(2,1)S(1)}, u32[]{:S(2)}, u32[]{:S(2)}) collective-permute-start(bf16[1024,256]{1,0:T(8,128)(2,1)S(1)} %join.1.refs_0_), channel_id=1, source_target_pairs={{0,1},{1,0},{2,3},{3,2},{4,5},{5,4},{6,7},{7,6},{8,9},{9,8},{10,11... | collective-permute-start | bytes 1572872 | tf_op jit(solution)/shard_map/ppermute | solution.py:275
  147.4 2.6 %collective-permute-start.26 = (bf16[1024,256]{1,0:T(8,128)(2,1)}, bf16[1024,256]{1,0:T(8,128)(2,1)S(1)}, u32[]{:S(2)}, u32[]{:S(2)}) collective-permute-start(bf16[1024,256]{1,0:T(8,128)(2,1)} %collective-permute-done.22.refs_1_), channel_id=1, source_target_pairs={{0,1},{1,0},{2,3},{3,2},{4,5},{5,4},{6,7},{7,6},{8,9},{9,8},{10,11... | collective-permute-start | bytes 1572872 | tf_op jit(solution)/shard_map/ppermute | solution.py:275
  147.9 2.9 %collective-permute-start.27 = (bf16[1024,256]{1,0:T(8,128)(2,1)}, bf16[1024,256]{1,0:T(8,128)(2,1)S(1)}, u32[]{:S(2)}, u32[]{:S(2)}) collective-permute-start(bf16[1024,256]{1,0:T(8,128)(2,1)} %collective-permute-done.23.refs_2_), channel_id=1, source_target_pairs={{0,1},{1,0},{2,3},{3,2},{4,5},{5,4},{6,7},{7,6},{8,9},{9,8},{10,11... | collective-permute-start | bytes 1572872 | tf_op jit(solution)/shard_map/ppermute | solution.py:275
  148.0 3.6 %collective-permute-start.28 = (bf16[1024,256]{1,0:T(8,128)(2,1)}, bf16[1024,256]{1,0:T(8,128)(2,1)S(1)}, u32[]{:S(2)}, u32[]{:S(2)}) collective-permute-start(bf16[1024,256]{1,0:T(8,128)(2,1)} %collective-permute-done.24.refs_3_), channel_id=1, source_target_pairs={{0,1},{1,0},{2,3},{3,2},{4,5},{5,4},{6,7},{7,6},{8,9},{9,8},{10,11... | collective-permute-start | bytes 1572872 | tf_op jit(solution)/shard_map/ppermute | solution.py:275
  (12 other events, 16.3 us)

commit v9 on v5

--- a/solution.py
+++ b/solution.py
@@ -16,7 +16,7 @@
 T = 5120
 BLK = 320
 BQ = 512
-W = 2048
+W = 5120
 NT = (((1,), (1,)), ((), ()))
 NN = (((1,), (0,)), ((), ()))
 f32 = jnp.float32
@@ -117,7 +117,7 @@
         for i in range(T//BQ):
             emit(i)
     g=jnp.abs(gain_ref[...])
-    isfast=jnp.max(g[0:1])*jnp.max(g[1:2])<=7.7
+    isfast=jnp.max(g[:,0:64])*jnp.max(g[:,64:128])<=7.7/8
     pl.when(isfast)(fast)
     pl.when(jnp.logical_not(isfast))(slow)
 
@@ -187,10 +187,6 @@
         out[h][at + 320 : at + 480, :] = jnp.where(half, top, bot).astype(bf16)
 
 
-def gain_row(gain_ref):
-    return jnp.concatenate([gain_ref[0:1, :] * 0.125, gain_ref[1:2, :]], 1)
-
-
 def proj_kernel(idx_ref, gain_ref, *refs, sizes):
     n = sum(sizes)
     toks, ws, outs, w = refs[:n], refs[n : n + 8], refs[n + 8 : n + 12], refs[-1]
@@ -199,7 +195,7 @@
         for h in range(4):
             w[h * 128 : h * 128 + 128, cols] = ws[j][h * 192 : h * 192 + 128, :]
             w[512 + h * 64 : 576 + h * 64, cols] = ws[j][h * 192 + 128 : h * 192 + 192, :]
-    gains = gain_row(gain_ref)
+    gains = gain_ref[...]
     at = 0
     for b, size in enumerate(sizes):
         parts = [t[...] for t in toks[at : at + size]]
@@ -264,9 +260,9 @@
     return lax.ppermute(value, axis, pairs)
 
 
-def spread(value, step):
+def spread(value, axis, step):
     pairs = [(2 * i + k, 2 * ((i + (step, -step)[k]) % 4) + k) for i in range(4) for k in (0, 1)]
-    return lax.ppermute(value, (Y, C), pairs)
+    return lax.ppermute(value, (axis, C), pairs)
 
 
 def around(value, axis):
@@ -276,21 +272,25 @@
 def on_device(tokens, w_query, w_key, w_value, w_output, qk_gain, decay_sums):
     own = tokens[0]
     z, y, x, c = (lax.axis_index(a) for a in (Z, Y, X, C))
-    t1 = spread(own, -1)
-    t3 = spread(own, 1)
-    t2 = spread(t1, -1)
-    near = jnp.where(c == 0, 1, 3)
+    t1 = spread(own, Y, -1)
+    t3 = spread(own, Y, 1)
+    t2 = spread(t1, Y, -1)
     piece = jnp.concatenate([w_query.T, w_key.T, w_value.T, w_output], 0)
     w4, wo4 = pack(around(piece, Z))
-    ws = around(w4, X)
+    w1 = spread(w4, X, -1)
+    ws = [w4, w1, spread(w4, X, 1), spread(w1, X, -1)]
     ws = ws + [move(w, C, 0) for w in ws]
 
-    cols = jnp.stack(
+    near = jnp.where(c == 0, 1, 3)
+    turns = [(c, (0, near, 4 - near, 2)), (1 - c, (0, 4 - near, near, 2))]
+    cols = jnp.stack([2 * ((x + d) % 4) + e for e, ds in turns for d in ds]).astype(jnp.int32)
+    out_cols = jnp.stack(
         [2 * ((x + d) % 4) + e for e in (c, 1 - c) for d in range(4)]
     ).astype(jnp.int32)
-    part1 = project(cols, qk_gain, [[own], [t1], [t3]], ws)
+    gains = jnp.concatenate([qk_gain[0] * 0.125, qk_gain[1]])[None]
+    part1 = project(cols, gains, [[own], [t1], [t3]], ws)
     *part1, wo4 = lax.optimization_barrier((*part1, wo4))
-    part2 = project(cols, qk_gain, [[t2]], ws)
+    part2 = project(cols, gains, [[t2]], ws)
     recv = []
     for part in (part1, part2):
         recv += [part[0]] + [move(part[d], Z, d) for d in (1, 2, 3)]
@@ -299,14 +299,14 @@
     pos = [4 * ((z - d) % 4) + (y + e) % 4 for d in range(4) for e in (0, near, 4 - near)]
     pos += [4 * ((z - d) % 4) + (y + 2) % 4 for d in range(4)]
     pos = jnp.stack(pos).astype(jnp.int32)
-    heads = attention(pos, qk_gain, decay_sums[0], recv, (3, 3, 3, 3, 1, 1, 1, 1))
+    heads = attention(pos, gains, decay_sums[0], recv, (3, 3, 3, 3, 1, 1, 1, 1))
     heads, *wo = lax.optimization_barrier((heads, *wo))
     wo = wo + [move(w, C, 0) for w in wo]
     merged = lax.all_to_all(heads, SP, 0, 0, tiled=True)
     order = jnp.stack(
         [4 * ((z + d) % 4) + (y + e) % 4 for e in range(4) for d in range(4)]
     ).astype(jnp.int32)
-    return output(order, cols, merged, wo)[None]
+    return output(order, out_cols, merged, wo)[None]
 
 
 def solution(mesh):

time: 164 us -> 165 us (level); the launches traced: 163 us -> 162 us
  starting transfers between devices: 50.6 us -> 47.1 us
  waiting for transfers between devices: 44.8 us -> 46.8 us
    ppermute x26 -> x23, starting transfers between devices: 38.3 us -> 27 us  [move(): return lax.ppermute(value, axis, pairs)]
    ppermute x3 -> x6, waiting for transfers between devices: 9.88 us -> 18.8 us  [spread(): return lax.ppermute(value, (axis, C), pairs)]
    ppermute x26 -> x23, waiting for transfers between devices: 28.4 us -> 21.4 us  [move(): return lax.ppermute(value, axis, pairs)]
    ppermute x3 -> x6, starting transfers between devices: 6.82 us -> 12.9 us  [spread(): return lax.ppermute(value, (axis, C), pairs)]
    all_to_all x1, starting transfers between devices: 5.49 us -> 7.28 us  [on_device(): merged = lax.all_to_all(heads, SP, 0, 0, tiled=True)]
    unnamed x32 -> x28, local copies, waits for them, and re-layouts: 10.7 us -> 9.86 us
  transfers between devices with their start and end apart: 30 -> 30, of which waited for: 18 -> 16; matrix products, arithmetic and copies ran while one was open for 1% -> 1% of each run, Pallas kernels for 32% -> 32%
where the time goes in v9:
time: 165 us; the launch traced here: 162 us
  Pallas kernels  56.4 us (34%)
  starting transfers between devices  47.1 us (29%)
  waiting for transfers between devices  46.8 us (28%)
  local copies, waits for them, and re-layouts  10.2 us (6%)
    pallas_call x1, Pallas kernels, attention(): pl.pallas_call(functools.partial(attn_kernel, nblk=nblk), out_shape=jax.S...  41.3 us
    ppermute x23, starting transfers between devices, move(): return lax.ppermute(value, axis, pairs)  27 us
    ppermute x23, waiting for transfers between devices, move(): return lax.ppermute(value, axis, pairs)  21.4 us
    ppermute x6, waiting for transfers between devices, spread(): return lax.ppermute(value, (axis, C), pairs)  18.8 us
    ppermute x6, starting transfers between devices, spread(): return lax.ppermute(value, (axis, C), pairs)  12.9 us
    pallas_call x2, Pallas kernels, project(): pl.pallas_call(functools.partial(proj_kernel, sizes=tuple((len(b) for b i...  10.9 us
    unnamed x28, local copies, waits for them, and re-layouts  9.86 us
    all_to_all x1, starting transfers between devices, on_device(): merged = lax.all_to_all(heads, SP, 0, 0, tiled=True)  7.28 us
  transfers between devices with their start and end apart: 30, of which 16 were waited for; matrix products, arithmetic and copies ran while one was open for 1% of the time, Pallas kernels for 32%

profile of v9, /device:TPU:0, one launch (start us, length us, event | category | flops | bytes accessed | tf_op | source)
XLA Modules:
  0.0 162.3 jit_solution(396119439266383688)
XLA Ops:
  0.0 3.1 %collective-permute-start = (bf16[320,2048]{1,0:T(8,128)(2,1)}, bf16[320,2048]{1,0:T(8,128)(2,1)}, u32[]{:S(2)}, u32[]{:S(2)}) collective-permute-start(bf16[320,2048]{1,0:T(8,128)(2,1)} %bitcast.54), channel_id=1, source_target_pairs={{0,24},{1,9},{8,0},{9,17},{16,8},{17,25},{24,16},{25,1},{2,26},{3,... | collective-permute-start | bytes 3932168 | tf_op jit(solution)/shard_map/ppermute | solution.py:265
  3.9 4.1 %collective-permute-start.2 = (bf16[256,256]{1,0:T(8,128)(2,1)S(1)}, bf16[256,256]{1,0:T(8,128)(2,1)S(1)}, u32[]{:S(2)}, u32[]{:S(2)}) collective-permute-start(bf16[256,256]{1,0:T(8,128)(2,1)S(1)} %pad_maximum_fusion.refs_0_), channel_id=1, source_target_pairs={{0,96},{32,0},{64,32},{96,64},{1,97},{33,1},{65,33},{97,65},{2,98}... | collective-permute-start | bytes 393224 | tf_op jit(solution)/shard_map/ppermute | solution.py:260
  8.1 1.3 collective-permute-start.4
  9.3 2.8 %collective-permute-done.2.refs_1_ = bf16[256,256]{1,0:T(8,128)(2,1)S(1)} collective-permute-done((bf16[256,256]{1,0:T(8,128)(2,1)S(1)}, bf16[256,256]{1,0:T(8,128)(2,1)S(1)}, u32[]{:S(2)}, u32[]{:S(2)}) %collective-permute-start.2) | collective-permute-done | bytes 131104 | tf_op jit(solution)/shard_map/ppermute | solution.py:260
  12.2 2.5 %collective-permute-done.3.refs_2_ = bf16[256,256]{1,0:T(8,128)(2,1)S(1)} collective-permute-done((bf16[256,256]{1,0:T(8,128)(2,1)S(1)}, bf16[256,256]{1,0:T(8,128)(2,1)S(1)}, u32[]{:S(2)}, u32[]{:S(2)}) %collective-permute-start.3) | collective-permute-done | bytes 131104 | tf_op jit(solution)/shard_map/ppermute | solution.py:260
  14.6 1.0 collective-permute-done.4.refs_3_
  15.7 2.8 %collective-permute-start.5 = (bf16[768,256]{1,0:T(8,128)(2,1)S(1)}, bf16[768,256]{1,0:T(8,128)(2,1)S(1)}, u32[]{:S(2)}, u32[]{:S(2)}) collective-permute-start(bf16[768,256]{1,0:T(8,128)(2,1)S(1)} %get-tuple-element.25.refs_3_.refs_1_), channel_id=1, source_target_pairs={{0,6},{1,3},{2,0},{3,5},{4,2},{5,7},{6,4},{7,1},{8,14},{9,11},{10,... | collective-permute-start | bytes 1179656 | tf_op jit(solution)/shard_map/ppermute | solution.py:265
  18.5 9.9 %collective-permute-done.refs_1_ = bf16[320,2048]{1,0:T(8,128)(2,1)} collective-permute-done((bf16[320,2048]{1,0:T(8,128)(2,1)}, bf16[320,2048]{1,0:T(8,128)(2,1)}, u32[]{:S(2)}, u32[]{:S(2)}) %collective-permute-start) | collective-permute-done | bytes 1310752 | tf_op jit(solution)/shard_map/ppermute | solution.py:265
  28.4 3.7 %collective-permute-start.15 = (bf16[320,2048]{1,0:T(8,128)(2,1)}, bf16[320,2048]{1,0:T(8,128)(2,1)}, u32[]{:S(2)}, u32[]{:S(2)}) collective-permute-start(bf16[320,2048]{1,0:T(8,128)(2,1)} %collective-permute-done.refs_1_), channel_id=1, source_target_pairs={{0,24},{1,9},{8,0},{9,17},{16,8},{17,25},{24,16},{25,1},{2,26},{3,... | collective-permute-start | bytes 3932168 | tf_op jit(solution)/shard_map/ppermute | solution.py:265
  32.1 1.5 collective-permute-start.6
  33.6 1.7 %collective-permute-start.7 = (bf16[768,256]{1,0:T(8,128)(2,1)S(1)}, bf16[768,256]{1,0:T(8,128)(2,1)S(1)}, u32[]{:S(2)}, u32[]{:S(2)}) collective-permute-start(bf16[768,256]{1,0:T(8,128)(2,1)S(1)} %collective-permute-done.5.refs_4_.refs_2_), channel_id=1, source_target_pairs={{0,6},{1,3},{2,0},{3,5},{4,2},{5,7},{6,4},{7,1},{8,14},{9,11},{10,... | collective-permute-start | bytes 1179656 | tf_op jit(solution)/shard_map/ppermute | solution.py:265
  35.3 8.9 %collective-permute-done.6.refs_5_.refs_3_ = bf16[768,256]{1,0:T(8,128)(2,1)S(1)} collective-permute-done((bf16[768,256]{1,0:T(8,128)(2,1)S(1)}, bf16[768,256]{1,0:T(8,128)(2,1)S(1)}, u32[]{:S(2)}, u32[]{:S(2)}) %collective-permute-start.6) | collective-permute-done | bytes 393248 | tf_op jit(solution)/shard_map/ppermute | solution.py:265
  47.1 1.3 copy-done.2
  48.4 6.4 %project.2 = (bf16[1440,128]{1,0:T(8,128)(2,1)S(1)}, bf16[1440,128]{1,0:T(8,128)(2,1)S(1)}, bf16[1440,128]{1,0:T(8,128)(2,1)S(1)}, bf16[1440,128]{1,0:T(8,128)(2,1)S(1)}) custom-call(s32[8]{0:T(128)S(1)} %stack.189.idx_ref, f32[1,128]{1,0:T(1,128)S(1)} %maximum_bitcast_fusion.gain_ref, bf16[320,2048]{1,0:T(8,128)(2,1)S(1)} %bitcast.56, ...), custom_call_target="tpu_custom_call" | custom-call | tf_op jit(solution)/shard_map/project/pallas_call | solution.py:209
  55.6 1.6 collective-permute-start.12
  57.2 2.6 %collective-permute-start.19 = (bf16[256,256]{1,0:T(8,128)(2,1)S(1)}, bf16[256,256]{1,0:T(8,128)(2,1)S(1)}, u32[]{:S(2)}, u32[]{:S(2)}) collective-permute-start(bf16[256,256]{1,0:T(8,128)(2,1)S(1)} %get-tuple-element.39.refs_0_), channel_id=1, source_target_pairs={{0,6},{2,0},{4,2},{6,4},{1,7},{3,1},{5,3},{7,5},{8,14},{10,8},{12,... | collective-permute-start | bytes 393224 | tf_op jit(solution)/shard_map/ppermute | solution.py:260
  60.7 4.7 %collective-permute-done.19.refs_1_ = bf16[256,256]{1,0:T(8,128)(2,1)S(1)} collective-permute-done((bf16[256,256]{1,0:T(8,128)(2,1)S(1)}, bf16[256,256]{1,0:T(8,128)(2,1)S(1)}, u32[]{:S(2)}, u32[]{:S(2)}) %collective-permute-start.19) | collective-permute-done | bytes 131104 | tf_op jit(solution)/shard_map/ppermute | solution.py:260
  65.4 5.7 %collective-permute-start.13 = (bf16[1440,128]{1,0:T(8,128)(2,1)S(1)}, bf16[1440,128]{1,0:T(8,128)(2,1)S(1)}, u32[]{:S(2)}, u32[]{:S(2)}) collective-permute-start(bf16[1440,128]{1,0:T(8,128)(2,1)S(1)} %get-tuple-element.33), channel_id=1, source_target_pairs={{0,64},{32,96},{64,0},{96,32},{1,65},{33,97},{65,1},{97,33},{2,66}... | collective-permute-start | bytes 1105928 | tf_op jit(solution)/shard_map/ppermute | solution.py:260
  73.2 1.6 %collective-permute-start.24 = (bf16[1024,256]{1,0:T(8,128)(2,1)S(1)}, bf16[1024,256]{1,0:T(8,128)(2,1)}, u32[]{:S(2)}, u32[]{:S(2)}) collective-permute-start(bf16[1024,256]{1,0:T(8,128)(2,1)S(1)} %join.1.refs_0_), channel_id=1, source_target_pairs={{0,8},{8,16},{16,24},{24,0},{1,9},{9,17},{17,25},{25,1},{2,10},{10... | collective-permute-start | bytes 1572872 | tf_op jit(solution)/shard_map/ppermute | solution.py:260
  74.9 2.2 %collective-permute-start.14 = (bf16[1440,128]{1,0:T(8,128)(2,1)S(1)}, bf16[1440,128]{1,0:T(8,128)(2,1)S(1)}, u32[]{:S(2)}, u32[]{:S(2)}) collective-permute-start(bf16[1440,128]{1,0:T(8,128)(2,1)S(1)} %get-tuple-element.34), channel_id=1, source_target_pairs={{0,96},{32,0},{64,32},{96,64},{1,97},{33,1},{65,33},{97,65},{2,98}... | collective-permute-start | bytes 1105928 | tf_op jit(solution)/shard_map/ppermute | solution.py:260
  77.1 4.4 %project.3 = (bf16[480,128]{1,0:T(8,128)(2,1)S(1)}, bf16[480,128]{1,0:T(8,128)(2,1)S(1)}, bf16[480,128]{1,0:T(8,128)(2,1)}, bf16[480,128]{1,0:T(8,128)(2,1)}) custom-call(s32[8]{0:T(128)S(1)} %stack.189.idx_ref, f32[1,128]{1,0:T(1,128)S(1)} %maximum_bitcast_fusion.gain_ref, bf16[320,2048]{1,0:T(8,128)(2,1)} %collective-permute-done.15.refs_0_, ...), custom_call_target="tpu_custom_call" | custom-call | tf_op jit(solution)/shard_map/project/pallas_call | solution.py:209
  82.3 2.0 %collective-permute-done.14.refs_3_ = bf16[1440,128]{1,0:T(8,128)(2,1)S(1)} collective-permute-done((bf16[1440,128]{1,0:T(8,128)(2,1)S(1)}, bf16[1440,128]{1,0:T(8,128)(2,1)S(1)}, u32[]{:S(2)}, u32[]{:S(2)}) %collective-permute-start.14) | collective-permute-done | bytes 368672 | tf_op jit(solution)/shard_map/ppermute | solution.py:260
  85.0 3.7 %collective-permute-start.17 = (bf16[480,128]{1,0:T(8,128)(2,1)}, bf16[480,128]{1,0:T(8,128)(2,1)S(1)}, u32[]{:S(2)}, u32[]{:S(2)}) collective-permute-start(bf16[480,128]{1,0:T(8,128)(2,1)} %get-tuple-element.37), channel_id=1, source_target_pairs={{0,64},{32,96},{64,0},{96,32},{1,65},{33,97},{65,1},{97,33},{2,66}... | collective-permute-start | bytes 368648 | tf_op jit(solution)/shard_map/ppermute | solution.py:260
  89.6 2.1 %collective-permute-done.17.refs_6_ = bf16[480,128]{1,0:T(8,128)(2,1)S(1)} collective-permute-done((bf16[480,128]{1,0:T(8,128)(2,1)}, bf16[480,128]{1,0:T(8,128)(2,1)S(1)}, u32[]{:S(2)}, u32[]{:S(2)}) %collective-permute-start.17) | collective-permute-done | bytes 122912 | tf_op jit(solution)/shard_map/ppermute | solution.py:260
  91.7 2.3 %collective-permute-done.18.refs_7_ = bf16[480,128]{1,0:T(8,128)(2,1)S(1)} collective-permute-done((bf16[480,128]{1,0:T(8,128)(2,1)}, bf16[480,128]{1,0:T(8,128)(2,1)S(1)}, u32[]{:S(2)}, u32[]{:S(2)}) %collective-permute-start.18) | collective-permute-done | bytes 122912 | tf_op jit(solution)/shard_map/ppermute | solution.py:260
  94.0 1.0 copy-done.4
  95.0 1.0 copy-done.6
  96.0 1.0 copy-done.8
  98.7 41.3 %attention.1 = bf16[16,160,128]{2,1,0:T(8,128)(2,1)} custom-call(s32[16]{0:T(128)S(1)} %stack.184.pos_ref, f32[1,128]{1,0:T(1,128)S(1)} %maximum_bitcast_fusion.gain_ref, f32[1,5120]{1,0:T(1,128)S(1)} %bitcast.57, bf16[1440,128]{1,0:T(8,128)(2,1)S(1)} %copy-done.4, bf16[1440,128]{1,0:T(8,128)(2,1)S(1)} %copy-done.6, bf16[1440,128]{1,0:T(8,128)(2,1)S(1)} %copy-done.8, ...), custom_call_target="tpu_custom_call" | custom-call | tf_op jit(solution)/shard_map/attention/pallas_call | solution.py:127
  140.0 7.3 %all-to-all-start = ((bf16[16,160,128]{2,1,0:T(8,128)(2,1)}), bf16[16,160,128]{2,1,0:T(8,128)(2,1)S(1)}, u32[]{:S(2)}, u32[]{:S(2)}) async-start(bf16[16,160,128]{2,1,0:T(8,128)(2,1)} %attention.1), calls=%async_computation | async-start | bytes 1310720 | tf_op jit(solution)/shard_map/all_to_all | solution.py:305
  151.6 6.6 %all-to-all-done.heads_ref = bf16[16,160,128]{2,1,0:T(8,128)(2,1)S(1)} async-done(((bf16[16,160,128]{2,1,0:T(8,128)(2,1)}), bf16[16,160,128]{2,1,0:T(8,128)(2,1)S(1)}, u32[]{:S(2)}, u32[]{:S(2)}) %all-to-all-start) | async-done | bytes 655392 | tf_op jit(solution)/shard_map/all_to_all | solution.py:305
  158.2 4.1 %output.1 = bf16[320,2048]{1,0:T(8,128)(2,1)} custom-call(s32[16]{0:T(128)S(1)} %stack.160.head_ref, s32[8]{0:T(128)S(1)} %stack.169.col_ref, bf16[16,160,128]{2,1,0:T(8,128)(2,1)S(1)} %all-to-all-done.heads_ref, bf16[1024,256]{1,0:T(8,128)(2,1)S(1)} %join.1.refs_0_, bf16[1024,256]{1,0:T(8,128)(2,1)} %collective-permute-done.22.refs_1_, ...), custom_call_target="tpu_custom_call" | custom-call | tf_op jit(solution)/shard_map/output/pallas_call | solution.py:243
  (69 shorter events, 16.0 us)
Async XLA Ops:
  0.0 28.4 %collective-permute-start = (bf16[320,2048]{1,0:T(8,128)(2,1)}, bf16[320,2048]{1,0:T(8,128)(2,1)}, u32[]{:S(2)}, u32[]{:S(2)}) collective-permute-start(bf16[320,2048]{1,0:T(8,128)(2,1)} %bitcast.54), channel_id=1, source_target_pairs={{0,24},{1,9},{8,0},{9,17},{16,8},{17,25},{24,16},{25,1},{2,26},{3,... | collective-permute-start | bytes 3932168 | tf_op jit(solution)/shard_map/ppermute | solution.py:265
  3.9 8.2 %collective-permute-start.2 = (bf16[256,256]{1,0:T(8,128)(2,1)S(1)}, bf16[256,256]{1,0:T(8,128)(2,1)S(1)}, u32[]{:S(2)}, u32[]{:S(2)}) collective-permute-start(bf16[256,256]{1,0:T(8,128)(2,1)S(1)} %pad_maximum_fusion.refs_0_), channel_id=1, source_target_pairs={{0,96},{32,0},{64,32},{96,64},{1,97},{33,1},{65,33},{97,65},{2,98}... | collective-permute-start | bytes 393224 | tf_op jit(solution)/shard_map/ppermute | solution.py:260
  8.1 6.6 %collective-permute-start.3 = (bf16[256,256]{1,0:T(8,128)(2,1)S(1)}, bf16[256,256]{1,0:T(8,128)(2,1)S(1)}, u32[]{:S(2)}, u32[]{:S(2)}) collective-permute-start(bf16[256,256]{1,0:T(8,128)(2,1)S(1)} %pad_maximum_fusion.refs_0_), channel_id=1, source_target_pairs={{0,64},{32,96},{64,0},{96,32},{1,65},{33,97},{65,1},{97,33},{2,66}... | collective-permute-start | bytes 393224 | tf_op jit(solution)/shard_map/ppermute | solution.py:260
  8.1 7.6 %collective-permute-start.4 = (bf16[256,256]{1,0:T(8,128)(2,1)S(1)}, bf16[256,256]{1,0:T(8,128)(2,1)S(1)}, u32[]{:S(2)}, u32[]{:S(2)}) collective-permute-start(bf16[256,256]{1,0:T(8,128)(2,1)S(1)} %pad_maximum_fusion.refs_0_), channel_id=1, source_target_pairs={{0,32},{32,64},{64,96},{96,0},{1,33},{33,65},{65,97},{97,1},{2,34}... | collective-permute-start | bytes 393224 | tf_op jit(solution)/shard_map/ppermute | solution.py:260
  9.3 37.2 %collective-permute-start.1 = (bf16[320,2048]{1,0:T(8,128)(2,1)}, bf16[320,2048]{1,0:T(8,128)(2,1)}, u32[]{:S(2)}, u32[]{:S(2)}) collective-permute-start(bf16[320,2048]{1,0:T(8,128)(2,1)} %bitcast.55), channel_id=1, source_target_pairs={{0,8},{1,25},{8,16},{9,1},{16,24},{17,9},{24,0},{25,17},{2,10},{3,... | collective-permute-start | bytes 3932168 | tf_op jit(solution)/shard_map/ppermute | solution.py:265
  15.7 44.1 %copy-start.11 = (bf16[256,256]{1,0:T(8,128)(2,1)}, bf16[256,256]{1,0:T(8,128)(2,1)S(1)}, u32[]{:S(2)}) copy-start(bf16[256,256]{1,0:T(8,128)(2,1)S(1)} %get-tuple-element.39.refs_0_) | copy-start | bytes 393220
  15.7 17.9 %collective-permute-start.5 = (bf16[768,256]{1,0:T(8,128)(2,1)S(1)}, bf16[768,256]{1,0:T(8,128)(2,1)S(1)}, u32[]{:S(2)}, u32[]{:S(2)}) collective-permute-start(bf16[768,256]{1,0:T(8,128)(2,1)S(1)} %get-tuple-element.25.refs_3_.refs_1_), channel_id=1, source_target_pairs={{0,6},{1,3},{2,0},{3,5},{4,2},{5,7},{6,4},{7,1},{8,14},{9,11},{10,... | collective-permute-start | bytes 1179656 | tf_op jit(solution)/shard_map/ppermute | solution.py:265
  28.4 46.5 %collective-permute-start.15 = (bf16[320,2048]{1,0:T(8,128)(2,1)}, bf16[320,2048]{1,0:T(8,128)(2,1)}, u32[]{:S(2)}, u32[]{:S(2)}) collective-permute-start(bf16[320,2048]{1,0:T(8,128)(2,1)} %collective-permute-done.refs_1_), channel_id=1, source_target_pairs={{0,24},{1,9},{8,0},{9,17},{16,8},{17,25},{24,16},{25,1},{2,26},{3,... | collective-permute-start | bytes 3932168 | tf_op jit(solution)/shard_map/ppermute | solution.py:265
  32.1 12.2 %collective-permute-start.6 = (bf16[768,256]{1,0:T(8,128)(2,1)S(1)}, bf16[768,256]{1,0:T(8,128)(2,1)S(1)}, u32[]{:S(2)}, u32[]{:S(2)}) collective-permute-start(bf16[768,256]{1,0:T(8,128)(2,1)S(1)} %get-tuple-element.25.refs_3_.refs_1_), channel_id=1, source_target_pairs={{0,2},{1,7},{2,4},{3,1},{4,6},{5,3},{6,0},{7,5},{8,10},{9,15},{10,... | collective-permute-start | bytes 1179656 | tf_op jit(solution)/shard_map/ppermute | solution.py:265
  33.6 10.7 %collective-permute-start.8 = (bf16[768,256]{1,0:T(8,128)(2,1)S(1)}, bf16[768,256]{1,0:T(8,128)(2,1)S(1)}, u32[]{:S(2)}, u32[]{:S(2)}) collective-permute-start(bf16[768,256]{1,0:T(8,128)(2,1)S(1)} %get-tuple-element.25.refs_3_.refs_1_), channel_id=1, source_target_pairs={{0,1},{1,0},{2,3},{3,2},{4,5},{5,4},{6,7},{7,6},{8,9},{9,8},{10,11... | collective-permute-start | bytes 1179656 | tf_op jit(solution)/shard_map/ppermute | solution.py:260
  33.6 11.2 %collective-permute-start.7 = (bf16[768,256]{1,0:T(8,128)(2,1)S(1)}, bf16[768,256]{1,0:T(8,128)(2,1)S(1)}, u32[]{:S(2)}, u32[]{:S(2)}) collective-permute-start(bf16[768,256]{1,0:T(8,128)(2,1)S(1)} %collective-permute-done.5.refs_4_.refs_2_), channel_id=1, source_target_pairs={{0,6},{1,3},{2,0},{3,5},{4,2},{5,7},{6,4},{7,1},{8,14},{9,11},{10,... | collective-permute-start | bytes 1179656 | tf_op jit(solution)/shard_map/ppermute | solution.py:265
  44.3 1.8 %collective-permute-start.9 = (bf16[768,256]{1,0:T(8,128)(2,1)S(1)}, bf16[768,256]{1,0:T(8,128)(2,1)S(1)}, u32[]{:S(2)}, u32[]{:S(2)}) collective-permute-start(bf16[768,256]{1,0:T(8,128)(2,1)S(1)} %collective-permute-done.5.refs_4_.refs_2_), channel_id=1, source_target_pairs={{0,1},{1,0},{2,3},{3,2},{4,5},{5,4},{6,7},{7,6},{8,9},{9,8},{10,11... | collective-permute-start | bytes 1179656 | tf_op jit(solution)/shard_map/ppermute | solution.py:260
  44.3 2.3 %collective-permute-start.10 = (bf16[768,256]{1,0:T(8,128)(2,1)S(1)}, bf16[768,256]{1,0:T(8,128)(2,1)S(1)}, u32[]{:S(2)}, u32[]{:S(2)}) collective-permute-start(bf16[768,256]{1,0:T(8,128)(2,1)S(1)} %collective-permute-done.6.refs_5_.refs_3_), channel_id=1, source_target_pairs={{0,1},{1,0},{2,3},{3,2},{4,5},{5,4},{6,7},{7,6},{8,9},{9,8},{10,11... | collective-permute-start | bytes 1179656 | tf_op jit(solution)/shard_map/ppermute | solution.py:260
  44.8 2.3 %collective-permute-start.11 = (bf16[768,256]{1,0:T(8,128)(2,1)S(1)}, bf16[768,256]{1,0:T(8,128)(2,1)S(1)}, u32[]{:S(2)}, u32[]{:S(2)}) collective-permute-start(bf16[768,256]{1,0:T(8,128)(2,1)S(1)} %collective-permute-done.7.refs_6_.refs_4_), channel_id=1, source_target_pairs={{0,1},{1,0},{2,3},{3,2},{4,5},{5,4},{6,7},{7,6},{8,9},{9,8},{10,11... | collective-permute-start | bytes 1179656 | tf_op jit(solution)/shard_map/ppermute | solution.py:260
  55.6 21.5 %copy-start.1 = (bf16[768,256]{1,0:T(8,128)(2,1)S(1)}, bf16[768,256]{1,0:T(8,128)(2,1)}, u32[]{:S(2)}) copy-start(bf16[768,256]{1,0:T(8,128)(2,1)} %copy-done) | copy-start | bytes 1179652
  55.6 16.9 %collective-permute-start.12 = (bf16[1440,128]{1,0:T(8,128)(2,1)S(1)}, bf16[1440,128]{1,0:T(8,128)(2,1)S(1)}, u32[]{:S(2)}, u32[]{:S(2)}) collective-permute-start(bf16[1440,128]{1,0:T(8,128)(2,1)S(1)} %get-tuple-element.32), channel_id=1, source_target_pairs={{0,32},{32,64},{64,96},{96,0},{1,33},{33,65},{65,97},{97,1},{2,34}... | collective-permute-start | bytes 1105928 | tf_op jit(solution)/shard_map/ppermute | solution.py:260
  57.2 8.2 %collective-permute-start.19 = (bf16[256,256]{1,0:T(8,128)(2,1)S(1)}, bf16[256,256]{1,0:T(8,128)(2,1)S(1)}, u32[]{:S(2)}, u32[]{:S(2)}) collective-permute-start(bf16[256,256]{1,0:T(8,128)(2,1)S(1)} %get-tuple-element.39.refs_0_), channel_id=1, source_target_pairs={{0,6},{2,0},{4,2},{6,4},{1,7},{3,1},{5,3},{7,5},{8,14},{10,8},{12,... | collective-permute-start | bytes 393224 | tf_op jit(solution)/shard_map/ppermute | solution.py:260
  59.8 11.3 %collective-permute-start.20 = (bf16[256,256]{1,0:T(8,128)(2,1)S(1)}, bf16[256,256]{1,0:T(8,128)(2,1)S(1)}, u32[]{:S(2)}, u32[]{:S(2)}) collective-permute-start(bf16[256,256]{1,0:T(8,128)(2,1)S(1)} %get-tuple-element.39.refs_0_), channel_id=1, source_target_pairs={{0,4},{2,6},{4,0},{6,2},{1,5},{3,7},{5,1},{7,3},{8,12},{10,14},{12... | collective-permute-start | bytes 393224 | tf_op jit(solution)/shard_map/ppermute | solution.py:260
  59.8 11.3 %collective-permute-start.21 = (bf16[256,256]{1,0:T(8,128)(2,1)S(1)}, bf16[256,256]{1,0:T(8,128)(2,1)S(1)}, u32[]{:S(2)}, u32[]{:S(2)}) collective-permute-start(bf16[256,256]{1,0:T(8,128)(2,1)S(1)} %get-tuple-element.39.refs_0_), channel_id=1, source_target_pairs={{0,2},{2,4},{4,6},{6,0},{1,3},{3,5},{5,7},{7,1},{8,10},{10,12},{12... | collective-permute-start | bytes 393224 | tf_op jit(solution)/shard_map/ppermute | solution.py:260
  65.4 16.1 %collective-permute-start.13 = (bf16[1440,128]{1,0:T(8,128)(2,1)S(1)}, bf16[1440,128]{1,0:T(8,128)(2,1)S(1)}, u32[]{:S(2)}, u32[]{:S(2)}) collective-permute-start(bf16[1440,128]{1,0:T(8,128)(2,1)S(1)} %get-tuple-element.33), channel_id=1, source_target_pairs={{0,64},{32,96},{64,0},{96,32},{1,65},{33,97},{65,1},{97,33},{2,66}... | collective-permute-start | bytes 1105928 | tf_op jit(solution)/shard_map/ppermute | solution.py:260
  72.0 68.0 %collective-permute-start.22 = (bf16[1024,256]{1,0:T(8,128)(2,1)S(1)}, bf16[1024,256]{1,0:T(8,128)(2,1)}, u32[]{:S(2)}, u32[]{:S(2)}) collective-permute-start(bf16[1024,256]{1,0:T(8,128)(2,1)S(1)} %join.1.refs_0_), channel_id=1, source_target_pairs={{0,24},{8,0},{16,8},{24,16},{1,25},{9,1},{17,9},{25,17},{2,26},{10... | collective-permute-start | bytes 1572872 | tf_op jit(solution)/shard_map/ppermute | solution.py:260
  72.1 67.9 %collective-permute-start.23 = (bf16[1024,256]{1,0:T(8,128)(2,1)S(1)}, bf16[1024,256]{1,0:T(8,128)(2,1)}, u32[]{:S(2)}, u32[]{:S(2)}) collective-permute-start(bf16[1024,256]{1,0:T(8,128)(2,1)S(1)} %join.1.refs_0_), channel_id=1, source_target_pairs={{0,16},{8,24},{16,0},{24,8},{1,17},{9,25},{17,1},{25,9},{2,18},{10... | collective-permute-start | bytes 1572872 | tf_op jit(solution)/shard_map/ppermute | solution.py:260
  73.2 66.8 %collective-permute-start.24 = (bf16[1024,256]{1,0:T(8,128)(2,1)S(1)}, bf16[1024,256]{1,0:T(8,128)(2,1)}, u32[]{:S(2)}, u32[]{:S(2)}) collective-permute-start(bf16[1024,256]{1,0:T(8,128)(2,1)S(1)} %join.1.refs_0_), channel_id=1, source_target_pairs={{0,8},{8,16},{16,24},{24,0},{1,9},{9,17},{17,25},{25,1},{2,10},{10... | collective-permute-start | bytes 1572872 | tf_op jit(solution)/shard_map/ppermute | solution.py:260
  74.9 9.4 %collective-permute-start.14 = (bf16[1440,128]{1,0:T(8,128)(2,1)S(1)}, bf16[1440,128]{1,0:T(8,128)(2,1)S(1)}, u32[]{:S(2)}, u32[]{:S(2)}) collective-permute-start(bf16[1440,128]{1,0:T(8,128)(2,1)S(1)} %get-tuple-element.34), channel_id=1, source_target_pairs={{0,96},{32,0},{64,32},{96,64},{1,97},{33,1},{65,33},{97,65},{2,98}... | collective-permute-start | bytes 1105928 | tf_op jit(solution)/shard_map/ppermute | solution.py:260
  82.3 6.4 %collective-permute-start.16 = (bf16[480,128]{1,0:T(8,128)(2,1)S(1)}, bf16[480,128]{1,0:T(8,128)(2,1)S(1)}, u32[]{:S(2)}, u32[]{:S(2)}) collective-permute-start(bf16[480,128]{1,0:T(8,128)(2,1)S(1)} %get-tuple-element.36), channel_id=1, source_target_pairs={{0,32},{32,64},{64,96},{96,0},{1,33},{33,65},{65,97},{97,1},{2,34}... | collective-permute-start | bytes 368648 | tf_op jit(solution)/shard_map/ppermute | solution.py:260
  85.0 6.7 %collective-permute-start.17 = (bf16[480,128]{1,0:T(8,128)(2,1)}, bf16[480,128]{1,0:T(8,128)(2,1)S(1)}, u32[]{:S(2)}, u32[]{:S(2)}) collective-permute-start(bf16[480,128]{1,0:T(8,128)(2,1)} %get-tuple-element.37), channel_id=1, source_target_pairs={{0,64},{32,96},{64,0},{96,32},{1,65},{33,97},{65,1},{97,33},{2,66}... | collective-permute-start | bytes 368648 | tf_op jit(solution)/shard_map/ppermute | solution.py:260
  88.7 5.3 %collective-permute-start.18 = (bf16[480,128]{1,0:T(8,128)(2,1)}, bf16[480,128]{1,0:T(8,128)(2,1)S(1)}, u32[]{:S(2)}, u32[]{:S(2)}) collective-permute-start(bf16[480,128]{1,0:T(8,128)(2,1)} %get-tuple-element.38), channel_id=1, source_target_pairs={{0,96},{32,0},{64,32},{96,64},{1,97},{33,1},{65,33},{97,65},{2,98}... | collective-permute-start | bytes 368648 | tf_op jit(solution)/shard_map/ppermute | solution.py:260
  140.0 18.1 %all-to-all-start = ((bf16[16,160,128]{2,1,0:T(8,128)(2,1)}), bf16[16,160,128]{2,1,0:T(8,128)(2,1)S(1)}, u32[]{:S(2)}, u32[]{:S(2)}) async-start(bf16[16,160,128]{2,1,0:T(8,128)(2,1)} %attention.1), calls=%async_computation | async-start | bytes 1310720 | tf_op jit(solution)/shard_map/all_to_all | solution.py:305
  147.3 2.0 %collective-permute-start.25 = (bf16[1024,256]{1,0:T(8,128)(2,1)S(1)}, bf16[1024,256]{1,0:T(8,128)(2,1)S(1)}, u32[]{:S(2)}, u32[]{:S(2)}) collective-permute-start(bf16[1024,256]{1,0:T(8,128)(2,1)S(1)} %join.1.refs_0_), channel_id=1, source_target_pairs={{0,1},{1,0},{2,3},{3,2},{4,5},{5,4},{6,7},{7,6},{8,9},{9,8},{10,11... | collective-permute-start | bytes 1572872 | tf_op jit(solution)/shard_map/ppermute | solution.py:260
  147.4 2.6 %collective-permute-start.26 = (bf16[1024,256]{1,0:T(8,128)(2,1)}, bf16[1024,256]{1,0:T(8,128)(2,1)S(1)}, u32[]{:S(2)}, u32[]{:S(2)}) collective-permute-start(bf16[1024,256]{1,0:T(8,128)(2,1)} %collective-permute-done.22.refs_1_), channel_id=1, source_target_pairs={{0,1},{1,0},{2,3},{3,2},{4,5},{5,4},{6,7},{7,6},{8,9},{9,8},{10,11... | collective-permute-start | bytes 1572872 | tf_op jit(solution)/shard_map/ppermute | solution.py:260
  147.9 2.9 %collective-permute-start.27 = (bf16[1024,256]{1,0:T(8,128)(2,1)}, bf16[1024,256]{1,0:T(8,128)(2,1)S(1)}, u32[]{:S(2)}, u32[]{:S(2)}) collective-permute-start(bf16[1024,256]{1,0:T(8,128)(2,1)} %collective-permute-done.23.refs_2_), channel_id=1, source_target_pairs={{0,1},{1,0},{2,3},{3,2},{4,5},{5,4},{6,7},{7,6},{8,9},{9,8},{10,11... | collective-permute-start | bytes 1572872 | tf_op jit(solution)/shard_map/ppermute | solution.py:260
  148.0 3.6 %collective-permute-start.28 = (bf16[1024,256]{1,0:T(8,128)(2,1)}, bf16[1024,256]{1,0:T(8,128)(2,1)S(1)}, u32[]{:S(2)}, u32[]{:S(2)}) collective-permute-start(bf16[1024,256]{1,0:T(8,128)(2,1)} %collective-permute-done.24.refs_3_), channel_id=1, source_target_pairs={{0,1},{1,0},{2,3},{3,2},{4,5},{5,4},{6,7},{7,6},{8,9},{9,8},{10,11... | collective-permute-start | bytes 1572872 | tf_op jit(solution)/shard_map/ppermute | solution.py:260
  (12 other events, 16.3 us)
